TPU v7x, 512 devices: a whole 4x8x8 slice. The times are simulated.
512 devices in a mesh: sp: 32 (over z, x), tp: 16 (over y, core).
Axes of the slice: x: 4, y: 8, z: 8, core: 2. Of those that a mesh axis runs over, the one named last changes fastest.
Arguments:
- hidden_in: bfloat16 [2, 49152, 2048], P(None, ('sp', 'tp')), may hold values from -6 to 6
- w_value: bfloat16 [2048, 2048], P(None, 'tp'), may hold values from -0.125 to 0.125
- w_key: bfloat16 [2048, 2048], P(None, 'tp'), may hold values from -0.125 to 0.125
- w_step: bfloat16 [2048, 32], replicated, may hold values from -0.125 to 0.125
- conv_value: bfloat16 [4, 2048], P(None, 'tp'), may hold values from -3 to 3
- conv_key: bfloat16 [4, 2048], P(None, 'tp'), may hold values from -3 to 3
- step_bias: float32 [32], P('tp'), may hold values from -3 to -1
- decay_rate: float32 [32], P('tp'), may hold values from 2.03450521e-06 to 0.25
- decay_jump: float32 [2, 49152, 32], P(None, 'sp', 'tp'), may hold values from -0.75 to 0
- new_value: bfloat16 [2, 2048], P(None, 'tp'), may hold values from -60 to 60
- new_key: bfloat16 [2, 2048], P(None, 'tp'), may hold values from -6 to 6
- new_query: bfloat16 [2, 2048], P(None, 'tp'), may hold values from -6 to 6
- new_gate: bfloat16 [2, 2048], P(None, 'tp'), may hold values from -6 to 6
- new_step: float32 [2, 32], P(None, 'tp'), may hold values from -6 to 6
- read_gain: bfloat16 [2048], P('tp'), may hold values from 0.099609375 to 1.8984375
Outputs:
- prompt_state: bfloat16 [2, 32, 64, 128], P(None, 'tp', 'sp')
- read_out: bfloat16 [2, 32, 64], P(None, 'tp', 'sp')
All inputs are finite; a program needn't handle non-finite values.
Results may differ from a plain program's by a relative error of at most 0.006.
Values may be sent and summed in bfloat16 or wider, within the bound.
No kernel may reach another device: no remote copies, remote signals or barrier semaphores. Data moves between devices by JAX's collectives and lax.ppermute only.
A program may use at most 64 MiB of HBM per device.

v0:
```python
import jax
import jax.numpy as jnp
from jax import lax
from jax.experimental import pallas as pl
from jax.experimental.pallas import tpu as pltpu
from jax.sharding import Mesh
from jax.sharding import PartitionSpec as P

HEAD_DIM = 64
EPSILON = 1e-05
BF = jnp.bfloat16
F32 = jnp.float32


def mm(a, b, dims):
    return lax.dot_general(a, b, (dims, ((), ())), preferred_element_type=F32)


GRANT = pltpu.CompilerParams(vmem_limit_bytes=14 * 1024 * 1024)


def piece_states(xs, halo, places, w, weight, own, other, rows, pair):
    depth, cols = w.shape[0] - 4, w.shape[1]
    many = len(xs)

    def body(place, *refs):
        x_refs = refs[:many]
        h_ref, w_ref, wt_ref, own_ref, other_ref, own_out, other_out, ext = refs[many:]
        taps = w_ref[depth : depth + 4, :].astype(F32)

        def project(ref):
            return mm(ref[...], w_ref[:depth, :], ((1,), (0,))).astype(BF).astype(F32)

        p = [project(r) for r in x_refs]
        h = project(h_ref)
        low = place[2] == 0
        for s in range(2):
            before = [h[4 * s : 4 * s + 4, :]]
            if pair:
                ends = [v[(s + 1) * rows - 4 : (s + 1) * rows, :] for v in p]
                before = [jnp.where(low, before[0], ends[1]), jnp.where(low, ends[0], before[0])]
            for n in range(many):
                ext[2 * n + s, 4:8, :] = before[n]
                ext[2 * n + s, 8 : 8 + rows, :] = p[n][s * rows : (s + 1) * rows, :]
        for s in range(2):
            sums = [own_ref[s], other_ref[s]]
            for n in range(many):
                mixed = ext[2 * n + s, 5 : 5 + rows, :] * taps[0:1, :]
                for k in range(1, 4):
                    mixed = mixed + ext[2 * n + s, 5 + k : 5 + k + rows, :] * taps[k : k + 1, :]
                mixed = mixed / (1.0 + jnp.exp(-mixed))
                lift = wt_ref[place[n], s * rows : (s + 1) * rows, :]
                for g in range(2):
                    parts = [
                        mixed[:, 256 * g + 64 * e : 256 * g + 64 * e + 64] * lift[:, 2 * g + e : 2 * g + e + 1]
                        for e in range(2)
                    ]
                    values = jnp.concatenate(parts, axis=1).astype(BF)
                    keys = mixed[:, 256 * g + 128 : 256 * g + 256].astype(BF)
                    sums[g] = sums[g] + mm(values, keys, ((0,), (0,)))
            own_out[s] = sums[0]
            other_out[s] = sums[1]

    vmem = pl.BlockSpec(memory_space=pltpu.VMEM)
    return pl.pallas_call(
        body,
        out_shape=[jax.ShapeDtypeStruct(own.shape, F32)] * 2,
        in_specs=[pl.BlockSpec(memory_space=pltpu.SMEM)] + [vmem] * (many + 5),
        out_specs=[vmem] * 2,
        scratch_shapes=[pltpu.VMEM((2 * many, rows + 8, cols), F32)],
        cost_estimate=pl.CostEstimate(
            flops=16 * sum(x.shape[0] for x in xs) * w.size,
            transcendentals=0,
            bytes_accessed=2 * w.size,
        ),
        compiler_params=GRANT,
        name="piece_states",
    )(places, *xs, halo, w, weight, own, other)


def packed(own, got, query, total, sp_count):
    share = HEAD_DIM // sp_count

    def body(a_ref, b_ref, q_ref, t_ref, out_ref):
        def put(row, value):
            out_ref[:, row : row + 1, :] = jnp.broadcast_to(value[None], (sp_count, 1, 128))

        left = t_ref[...]
        for k in range(3):
            part = left.astype(BF)
            left = left - part.astype(F32)
            put(12 + k, part)
        put(15, jnp.zeros((1, 128), BF))
        for s in range(2):
            state = a_ref[s] + b_ref[s]
            read = jnp.sum(state * q_ref[s : s + 1, :], axis=1).reshape(1, 128)
            high = read.astype(BF)
            put(8 + s, high)
            put(10 + s, (read - high.astype(F32)).astype(BF))
            for e in range(2):
                cut = state[64 * e : 64 * e + 64, :].astype(BF).reshape(sp_count, share, 128)
                out_ref[:, 4 * s + 2 * e : 4 * s + 2 * e + share, :] = cut

    return pl.pallas_call(
        body,
        out_shape=jax.ShapeDtypeStruct((sp_count, 16, 128), BF),
        in_specs=[pl.BlockSpec(memory_space=pltpu.VMEM)] * 4,
        out_specs=pl.BlockSpec(memory_space=pltpu.VMEM),
        compiler_params=GRANT,
        name="packed",
    )(own, got, query, total)


def finished(got, fixed, back):
    sp_count = got.shape[0]

    def body(back_ref, got_ref, fix_ref, state_out, read_out):
        run = jnp.zeros((1, 128), F32)
        total = jnp.zeros((16, 128), F32)
        for j in reversed(range(sp_count)):
            g = got_ref[j].astype(F32)
            e = jnp.exp(run)
            one = [jnp.broadcast_to(e[:, i : i + 1], (1, 128)) for i in range(4)]
            mixed = [jnp.concatenate([one[2 * s][:, :64], one[2 * s + 1][:, 64:]], axis=1) for s in range(2)]
            scale = jnp.concatenate([one[0], one[0], one[1], one[1], one[2], one[2], one[3], one[3], *mixed, *mixed, *mixed, *mixed], axis=0)
            total = total + g * scale
            run = run + g[12:13] + g[13:14] + g[14:15]
        for s in range(2):
            for h in range(2):
                state_out[s, h] = total[4 * s + 2 * h : 4 * s + 2 * h + 2].astype(BF)
        read = total[8:10] + total[10:12]
        gated = (fix_ref[0:2] * read + fix_ref[2:4]) * fix_ref[4:6]
        mean = jnp.mean(gated * gated, axis=1, keepdims=True)
        out = gated * lax.rsqrt(mean + EPSILON) * fix_ref[6:7]
        out = jnp.concatenate([out, jnp.zeros((6, 128), F32)], axis=0)
        out = pltpu.roll(out, back_ref[0], 1)
        for s in range(2):
            for h in range(2):
                read_out[s, h : h + 1, :] = out[s : s + 1, 64 * h : 64 * h + 2].astype(BF)

    vmem = pl.BlockSpec(memory_space=pltpu.VMEM)
    return pl.pallas_call(
        body,
        out_shape=[jax.ShapeDtypeStruct((2, 2, 2, 128), BF), jax.ShapeDtypeStruct((2, 2, 2), BF)],
        in_specs=[pl.BlockSpec(memory_space=pltpu.SMEM), vmem, vmem],
        out_specs=[vmem] * 2,
        compiler_params=GRANT,
        name="finished",
    )(back, got, fixed)


def per_device(
    hidden_in, w_value, w_key, w_step, conv_value, conv_key, step_bias, decay_rate, decay_jump,
    new_value, new_key, new_query, new_gate, new_step, read_gain,
):
    sp_count, y_count, c_count = (lax.axis_size(a) for a in ("sp", "y", "c"))
    sp, y, c = (lax.axis_index(a) for a in ("sp", "y", "c"))
    tp_count = y_count * c_count
    count = sp_count * tp_count
    rows, width = hidden_in.shape[1:]
    heads = step_bias.shape[0]
    share = HEAD_DIM // sp_count

    def swap(v):
        return lax.ppermute(v, "c", [(0, 1), (1, 0)])

    def onward(v):
        pairs = []
        for i in range(y_count):
            pairs.append((2 * i, 2 * ((i + 1) % y_count)))
            pairs.append((2 * i + 1, 2 * ((i - 1) % y_count) + 1))
        return lax.ppermute(v, ("y", "c"), pairs)

    def last(v):
        return v[: 2 * rows].reshape(2, rows, width)[:, rows - 4 :, :].reshape(8, width)

    a = [hidden_in.reshape(2 * rows, width)]
    a.append(onward(a[0]))
    b = [swap(a[0])]
    b.append(onward(b[0]))
    early, first = lax.optimization_barrier((a[0], b[0]))
    ends = last(early), last(first)
    before = jnp.where(c == 1, *ends)
    before = lax.ppermute(before, ("sp", "y", "c"), [(i, i + 2) for i in range(count - 2)])
    halo = [before, onward(before)]

    steps = mm(early, w_step, ((1,), (0,))).astype(BF)
    steps = steps.reshape(2, rows, tp_count, heads).transpose(2, 0, 3, 1)
    steps = lax.all_to_all(steps, ("y", "c"), 0, 0, tiled=True)
    steps = steps.transpose(1, 2, 0, 3).reshape(2, heads, tp_count * rows).astype(F32)
    size = jax.nn.softplus(steps + step_bias[None, :, None])
    log_decay = decay_jump.transpose(0, 2, 1) - decay_rate[None, :, None] * size
    total = jnp.sum(log_decay, axis=2)
    weight = size * jnp.exp(total[:, :, None] - jnp.cumsum(log_decay, axis=2))
    weight = weight.reshape(2, heads, tp_count, rows).transpose(2, 0, 3, 1)
    weight = weight.reshape(tp_count, 2 * rows, heads)
    weight = jnp.concatenate([weight, swap(weight)], axis=2)

    w_own = jnp.concatenate(
        [jnp.concatenate([w_value, conv_value], axis=0), jnp.concatenate([w_key, conv_key], axis=0)], axis=1
    )
    w_both = jnp.concatenate([w_own, swap(w_own)], axis=1)

    def add(acc, xs, halo, far):
        away = jnp.where(c == 0, y - far, y + far) % y_count
        places = jnp.stack([away * 2 + c, away * 2 + 1 - c, c]).astype(jnp.int32)
        return piece_states(xs, halo, places, w_both, weight, *acc, rows, len(xs) == 2)

    acc = (jnp.zeros((2, 128, 128), F32),) * 2
    half = y_count // 2
    acc = add(acc, [a[0]], jnp.where(c == 0, before, ends[1]), 0)
    for s in range(1, half):
        a.append(onward(a[s]))
        if s + 1 < half:
            b.append(onward(b[s]))
            halo.append(onward(halo[s]))
        acc = add(acc, [a[s], b[s]], halo[s], s)
    last_halo = onward(jnp.where(c == 0, halo[half - 1], last(b[half - 1])))
    query = new_query.astype(F32)
    new_size = jax.nn.softplus(new_step + step_bias)
    keep = jnp.repeat(jnp.exp(-decay_rate * new_size), HEAD_DIM, axis=1)
    match = jnp.sum(new_key.astype(F32) * query, axis=1)
    term = jnp.repeat(new_size * match[:, None], HEAD_DIM, axis=1) * new_value.astype(F32)
    gain = read_gain.astype(F32)[None]
    fixed = jnp.concatenate([keep, term, jax.nn.silu(new_gate.astype(F32)), gain, jnp.zeros_like(gain)], axis=0)
    lanes = jnp.pad(total.reshape(1, 2 * heads), ((0, 0), (0, 128 - 2 * heads)))

    back = jnp.reshape((128 - sp * share) % 128, (1,)).astype(jnp.int32)
    acc, lanes, fixed, query, back = lax.optimization_barrier((acc, lanes, fixed, query, back))
    own, other = add(acc, [a[half]], last_halo, half)
    sent = packed(own, swap(other), query, lanes, sp_count)
    got = lax.all_to_all(sent, "sp", 0, 0, tiled=True)
    return tuple(finished(got, fixed, back))


def solution(mesh):
    tp = ("y", "c")
    chips = Mesh(mesh.devices.reshape(mesh.shape["sp"], mesh.shape["tp"] // 2, 2), ("sp", *tp))

    return jax.shard_map(
        per_device,
        mesh=chips,
        in_specs=(
            P(None, ("sp", *tp), None), P(None, tp), P(None, tp), P(), P(None, tp), P(None, tp), P(tp), P(tp),
            P(None, "sp", tp), P(None, tp), P(None, tp), P(None, tp), P(None, tp), P(None, tp), P(tp),
        ),
        out_specs=(P(None, tp, "sp", None), P(None, tp, "sp")),
        check_vma=False,
    )
```

profile of v0, /device:TPU:1, one launch (start us, length us, event | category | flops | bytes accessed | tf_op | source)
XLA Modules:
  0.0 124.8 jit_solution(1706880863511426480)
XLA Ops:
  0.7 8.9 %collective-permute-start.3 = (bf16[192,2048]{1,0:T(8,128)(2,1)}, bf16[192,2048]{1,0:T(8,128)(2,1)S(1)}, u32[]{:S(2)}, u32[]{:S(2)}) collective-permute-start(bf16[192,2048]{1,0:T(8,128)(2,1)} %bitcast.62), channel_id=1, source_target_pairs={{0,1},{1,0},{2,3},{3,2},{4,5},{5,4},{6,7},{7,6},{8,9},{9,8},{10,11... | collective-permute-start | bytes 2359304 | tf_op jit(solution)/shard_map/ppermute | solution.py:165
  9.6 1.9 %collective-permute-start = (bf16[192,2048]{1,0:T(8,128)(2,1)}, bf16[192,2048]{1,0:T(8,128)(2,1)}, u32[]{:S(2)}, u32[]{:S(2)}) collective-permute-start(bf16[192,2048]{1,0:T(8,128)(2,1)} %bitcast.63), channel_id=1, source_target_pairs={{0,2},{1,15},{2,4},{3,1},{4,6},{5,3},{6,8},{7,5},{8,10},{9,7},{10,... | collective-permute-start | bytes 2359304 | tf_op jit(solution)/shard_map/ppermute | solution.py:172
  11.6 1.1 constant_dynamic-update-slice_fusion.1
  12.6 1.1 constant_dynamic-update-slice_fusion.3
  13.7 0.7 constant_dynamic-update-slice_fusion
  14.4 0.8 copy-done.4
  15.3 0.1 pad_maximum_fusion.1
  15.4 1.9 %collective-permute-start.11 = (bf16[2052,256]{1,0:T(8,128)(2,1)S(1)}, bf16[2052,256]{1,0:T(8,128)(2,1)}, u32[]{:S(2)}, u32[]{:S(2)}) collective-permute-start(bf16[2052,256]{1,0:T(8,128)(2,1)S(1)} %pad_maximum_fusion.1), channel_id=1, source_target_pairs={{0,1},{1,0},{2,3},{3,2},{4,5},{5,4},{6,7},{7,6},{8,9},{9,8},{10,11... | collective-permute-start | bytes 3151880 | tf_op jit(solution)/shard_map/ppermute | solution.py:165
  17.5 0.1 multiply_reduce_fusion
  18.5 0.3 convolution_convert_fusion
  18.8 0.1 reshape.70
  18.9 0.6 copy.40
  19.5 4.6 %all-to-all-start = ((bf16[16,2,2,96]{3,2,1,0:T(2,128)(2,1)}), bf16[16,2,2,96]{3,2,1,0:T(2,128)(2,1)S(1)}, u32[]{:S(2)}, u32[]{:S(2)}) async-start(bf16[16,2,2,96]{3,2,1,0:T(2,128)(2,1)} %bitcast.60), calls=%async_computation | async-start | bytes 32768 | tf_op jit(solution)/shard_map/all_to_all | solution.py:189
  24.3 3.3 %collective-permute-start.7 = (bf16[8,2048]{1,0:T(8,128)(2,1)S(1)}, bf16[8,2048]{1,0:T(8,128)(2,1)S(1)}, u32[]{:S(2)}, u32[]{:S(2)}) collective-permute-start(bf16[8,2048]{1,0:T(8,128)(2,1)S(1)} %broadcast_select_fusion.2), channel_id=1, source_target_pairs={{0,2},{1,3},{2,4},{3,5},{4,6},{5,7},{6,8},{7,9},{8,10},{9,11},{10,... | collective-permute-start | bytes 98312 | tf_op jit(solution)/shard_map/ppermute | solution.py:184
  27.5 3.1 %collective-permute-start.4 = (bf16[192,2048]{1,0:T(8,128)(2,1)S(1)}, bf16[192,2048]{1,0:T(8,128)(2,1)}, u32[]{:S(2)}, u32[]{:S(2)}) collective-permute-start(bf16[192,2048]{1,0:T(8,128)(2,1)S(1)} %collective-permute-done.3), channel_id=1, source_target_pairs={{0,2},{1,15},{2,4},{3,1},{4,6},{5,3},{6,8},{7,5},{8,10},{9,7},{10,... | collective-permute-start | bytes 2359304 | tf_op jit(solution)/shard_map/ppermute | solution.py:172
  30.7 3.4 %collective-permute-start.1 = (bf16[192,2048]{1,0:T(8,128)(2,1)}, bf16[192,2048]{1,0:T(8,128)(2,1)}, u32[]{:S(2)}, u32[]{:S(2)}) collective-permute-start(bf16[192,2048]{1,0:T(8,128)(2,1)} %collective-permute-done.refs_0_), channel_id=1, source_target_pairs={{0,2},{1,15},{2,4},{3,1},{4,6},{5,3},{6,8},{7,5},{8,10},{9,7},{10,... | collective-permute-start | bytes 2359304 | tf_op jit(solution)/shard_map/ppermute | solution.py:172
  34.1 0.1 reshape.80
  34.2 0.2 fusion.13
  34.5 1.2 reduce-window.6
  35.6 0.2 slice_reduce_fusion
  35.8 0.4 reduce-window.9
  36.3 0.1 fusion.8
  36.6 2.8 %collective-permute-start.12 = (f32[16,192,2]{1,0,2:T(8,128)S(1)}, f32[16,192,2]{1,0,2:T(8,128)S(1)}, u32[]{:S(2)}, u32[]{:S(2)}) collective-permute-start(f32[16,192,2]{1,0,2:T(8,128)S(1)} %reshape.73), channel_id=1, source_target_pairs={{0,1},{1,0},{2,3},{3,2},{4,5},{5,4},{6,7},{7,6},{8,9},{9,8},{10,11... | collective-permute-start | bytes 73736 | tf_op jit(solution)/shard_map/ppermute | solution.py:165
  39.5 3.4 %collective-permute-start.8 = (bf16[8,2048]{1,0:T(8,128)(2,1)S(1)}, bf16[8,2048]{1,0:T(8,128)(2,1)S(1)}, u32[]{:S(2)}, u32[]{:S(2)}) collective-permute-start(bf16[8,2048]{1,0:T(8,128)(2,1)S(1)} %collective-permute-done.7), channel_id=1, source_target_pairs={{0,2},{1,15},{2,4},{3,1},{4,6},{5,3},{6,8},{7,5},{8,10},{9,7},{10,... | collective-permute-start | bytes 98312 | tf_op jit(solution)/shard_map/ppermute | solution.py:172
  42.9 6.6 %collective-permute-done.8.refs_2_ = bf16[8,2048]{1,0:T(8,128)(2,1)S(1)} collective-permute-done((bf16[8,2048]{1,0:T(8,128)(2,1)S(1)}, bf16[8,2048]{1,0:T(8,128)(2,1)S(1)}, u32[]{:S(2)}, u32[]{:S(2)}) %collective-permute-start.8) | collective-permute-done | bytes 32800 | tf_op jit(solution)/shard_map/ppermute | solution.py:172
  49.5 3.9 %collective-permute-start.9 = (bf16[8,2048]{1,0:T(8,128)(2,1)S(1)}, bf16[8,2048]{1,0:T(8,128)(2,1)S(1)}, u32[]{:S(2)}, u32[]{:S(2)}) collective-permute-start(bf16[8,2048]{1,0:T(8,128)(2,1)S(1)} %collective-permute-done.8.refs_2_), channel_id=1, source_target_pairs={{0,2},{1,15},{2,4},{3,1},{4,6},{5,3},{6,8},{7,5},{8,10},{9,7},{10,... | collective-permute-start | bytes 98312 | tf_op jit(solution)/shard_map/ppermute | solution.py:172
  53.4 2.6 %collective-permute-start.5 = (bf16[192,2048]{1,0:T(8,128)(2,1)}, bf16[192,2048]{1,0:T(8,128)(2,1)}, u32[]{:S(2)}, u32[]{:S(2)}) collective-permute-start(bf16[192,2048]{1,0:T(8,128)(2,1)} %collective-permute-done.4.refs_1_), channel_id=1, source_target_pairs={{0,2},{1,15},{2,4},{3,1},{4,6},{5,3},{6,8},{7,5},{8,10},{9,7},{10,... | collective-permute-start | bytes 2359304 | tf_op jit(solution)/shard_map/ppermute | solution.py:172
  56.0 1.7 %copy.35.refs_3_.refs_4_ = f32[16,192,4]{2,1,0:T(8,128)} copy(f32[16,192,4]{1,0,2:T(8,128)S(1)} %pad_maximum_fusion.2) | data formatting | bytes 98304 | tf_op jit(solution)/shard_map/concatenate | solution.py:197
  57.7 3.2 %collective-permute-start.10 = (bf16[8,2048]{1,0:T(8,128)(2,1)S(1)}, bf16[8,2048]{1,0:T(8,128)(2,1)S(1)}, u32[]{:S(2)}, u32[]{:S(2)}) collective-permute-start(bf16[8,2048]{1,0:T(8,128)(2,1)S(1)} %collective-permute-done.9.refs_2_), channel_id=1, source_target_pairs={{0,2},{1,15},{2,4},{3,1},{4,6},{5,3},{6,8},{7,5},{8,10},{9,7},{10,... | collective-permute-start | bytes 98312 | tf_op jit(solution)/shard_map/ppermute | solution.py:172
  60.9 1.7 %pad_maximum_fusion.refs_2_.refs_3_ = bf16[2052,512]{1,0:T(8,128)(2,1)S(1)} fusion(bf16[2052,256]{1,0:T(8,128)(2,1)} %collective-permute-done.11, bf16[2052,128]{1,0:T(8,128)(2,1)} %copy-done.5, bf16[2052,128]{1,0:T(8,128)(2,1)} %copy-done.4), kind=kLoop, calls=%fused_computation | loop fusion | flops 6303744 | bytes 4202496 | tf_op jit(solution)/shard_map/concatenate | solution.py:202
  62.7 3.2 %collective-permute-start.2 = (bf16[192,2048]{1,0:T(8,128)(2,1)}, bf16[192,2048]{1,0:T(8,128)(2,1)}, u32[]{:S(2)}, u32[]{:S(2)}) collective-permute-start(bf16[192,2048]{1,0:T(8,128)(2,1)} %collective-permute-done.1.refs_0_), channel_id=1, source_target_pairs={{0,2},{1,15},{2,4},{3,1},{4,6},{5,3},{6,8},{7,5},{8,10},{9,7},{10,... | collective-permute-start | bytes 2359304 | tf_op jit(solution)/shard_map/ppermute | solution.py:172
  65.9 1.7 %piece_states.5 = (f32[2,128,128]{2,1,0:T(8,128)S(1)}, f32[2,128,128]{2,1,0:T(8,128)S(1)}) custom-call(s32[3]{0:T(128)S(1)} %add_add_fusion.3.place, bf16[192,2048]{1,0:T(8,128)(2,1)S(1)} %bitcast.65, bf16[8,2048]{1,0:T(8,128)(2,1)S(1)} %broadcast_select_fusion.1.refs_1_, bf16[2052,512]{1,0:T(8,128)(2,1)S(1)} %pad_maximum_fusion.refs_2_.refs_3_, ...), custom_call_target="tpu_custom_call" | custom-call | flops 3227516928 | bytes 2101248 | tf_op jit(solution)/shard_map/piece_states/pallas_call | solution.py:65
  67.6 5.0 %collective-permute-start.6 = (bf16[192,2048]{1,0:T(8,128)(2,1)}, bf16[192,2048]{1,0:T(8,128)(2,1)S(1)}, u32[]{:S(2)}, u32[]{:S(2)}) collective-permute-start(bf16[192,2048]{1,0:T(8,128)(2,1)} %collective-permute-done.5.refs_1_), channel_id=1, source_target_pairs={{0,2},{1,15},{2,4},{3,1},{4,6},{5,3},{6,8},{7,5},{8,10},{9,7},{10,... | collective-permute-start | bytes 2359304 | tf_op jit(solution)/shard_map/ppermute | solution.py:172
  72.6 3.1 %piece_states.6 = (f32[2,128,128]{2,1,0:T(8,128)S(1)}, f32[2,128,128]{2,1,0:T(8,128)S(1)}) custom-call(s32[3]{0:T(128)S(1)} %add_add_fusion.2.place, bf16[192,2048]{1,0:T(8,128)(2,1)} %collective-permute-done.refs_0_, bf16[192,2048]{1,0:T(8,128)(2,1)} %collective-permute-done.4.refs_1_, bf16[8,2048]{1,0:T(8,128)(2,1)S(1)} %collective-permute-done.8.refs_2_, ...), custom_call_target="tpu_custom_call" | custom-call | flops 6455033856 | bytes 2101248 | tf_op jit(solution)/shard_map/piece_states/pallas_call | solution.py:65
  75.8 0.2 collective-permute-done.2.refs_0_
  76.0 4.1 %collective-permute-start.13 = (bf16[192,2048]{1,0:T(8,128)(2,1)}, bf16[192,2048]{1,0:T(8,128)(2,1)}, u32[]{:S(2)}, u32[]{:S(2)}) collective-permute-start(bf16[192,2048]{1,0:T(8,128)(2,1)} %collective-permute-done.2.refs_0_), channel_id=1, source_target_pairs={{0,2},{1,15},{2,4},{3,1},{4,6},{5,3},{6,8},{7,5},{8,10},{9,7},{10,... | collective-permute-start | bytes 2359304 | tf_op jit(solution)/shard_map/ppermute | solution.py:172
  80.1 3.1 %piece_states.7 = (f32[2,128,128]{2,1,0:T(8,128)S(1)}, f32[2,128,128]{2,1,0:T(8,128)S(1)}) custom-call(s32[3]{0:T(128)S(1)} %add_add_fusion.1.place, bf16[192,2048]{1,0:T(8,128)(2,1)} %collective-permute-done.1.refs_0_, bf16[192,2048]{1,0:T(8,128)(2,1)} %collective-permute-done.5.refs_1_, bf16[8,2048]{1,0:T(8,128)(2,1)S(1)} %collective-permute-done.9.refs_2_, ...), custom_call_target="tpu_custom_call" | custom-call | flops 6455033856 | bytes 2101248 | tf_op jit(solution)/shard_map/piece_states/pallas_call | solution.py:65
  83.2 1.1 collective-permute-done.6.refs_1_
  84.4 4.2 %collective-permute-start.14 = (bf16[8,2048]{1,0:T(8,128)(2,1)S(1)}, bf16[8,2048]{1,0:T(8,128)(2,1)S(1)}, u32[]{:S(2)}, u32[]{:S(2)}) collective-permute-start(bf16[8,2048]{1,0:T(8,128)(2,1)S(1)} %broadcast_select_fusion), channel_id=1, source_target_pairs={{0,2},{1,15},{2,4},{3,1},{4,6},{5,3},{6,8},{7,5},{8,10},{9,7},{10,... | collective-permute-start | bytes 98312 | tf_op jit(solution)/shard_map/ppermute | solution.py:172
  88.6 1.4 %copy-done.2 = f32[16,192,4]{2,1,0:T(8,128)S(1)} copy-done((f32[16,192,4]{2,1,0:T(8,128)S(1)}, f32[16,192,4]{2,1,0:T(8,128)}, u32[]{:S(2)}) %copy-start.2) | copy-done | bytes 49176
  90.0 2.9 %piece_states.8 = (f32[2,128,128]{2,1,0:T(8,128)S(1)}, f32[2,128,128]{2,1,0:T(8,128)S(1)}) custom-call(s32[3]{0:T(128)S(1)} %add_add_fusion.place, bf16[192,2048]{1,0:T(8,128)(2,1)} %collective-permute-done.2.refs_0_, bf16[192,2048]{1,0:T(8,128)(2,1)S(1)} %collective-permute-done.6.refs_1_, bf16[8,2048]{1,0:T(8,128)(2,1)S(1)} %collective-permute-done.10.refs_2_, ...), custom_call_target="tpu_custom_call" | custom-call | flops 6455033856 | bytes 2101248 | tf_op jit(solution)/shard_map/piece_states/pallas_call | solution.py:65
  92.9 0.3 collective-permute-done.14.refs_1_
  93.2 2.3 %piece_states.9 = (f32[2,128,128]{2,1,0:T(8,128)S(1)}, f32[2,128,128]{2,1,0:T(8,128)S(1)}) custom-call(s32[3]{0:T(128)S(1)} %add_add_fusion.4.place, bf16[192,2048]{1,0:T(8,128)(2,1)} %collective-permute-done.13.refs_0_, bf16[8,2048]{1,0:T(8,128)(2,1)S(1)} %collective-permute-done.14.refs_1_, bf16[2052,512]{1,0:T(8,128)(2,1)S(1)} %pad_maximum_fusion.refs_2_.refs_3_, ...), custom_call_target="tpu_custom_call" | custom-call | flops 3227516928 | bytes 2101248 | tf_op jit(solution)/shard_map/piece_states/pallas_call | solution.py:65
  95.5 7.0 %collective-permute-start.15 = (f32[2,128,128]{2,1,0:T(8,128)S(1)}, f32[2,128,128]{2,1,0:T(8,128)S(1)}, u32[]{:S(2)}, u32[]{:S(2)}) collective-permute-start(f32[2,128,128]{2,1,0:T(8,128)S(1)} %get-tuple-element.34), channel_id=1, source_target_pairs={{0,1},{1,0},{2,3},{3,2},{4,5},{5,4},{6,7},{7,6},{8,9},{9,8},{10,11... | collective-permute-start | bytes 393224 | tf_op jit(solution)/shard_map/ppermute | solution.py:165
  102.6 1.0 collective-permute-done.15.b_ref
  103.5 0.2 packed.1
  103.7 20.0 %all_to_all.10.got_ref = bf16[32,16,128]{2,1,0:T(8,128)(2,1)S(1)} all-to-all(bf16[32,16,128]{2,1,0:T(8,128)(2,1)S(1)} %packed.1), channel_id=1, replica_groups=mesh['sp'=32,'y'=8,'c'=2] {'sp'}, dimensions={0} | all-to-all | bytes 262144 | tf_op jit(solution)/shard_map/all_to_all | solution.py:232
  123.7 1.1 finished.1
  (75 shorter events, 1.5 us)
Async XLA Ops:
  0.6 17.8 %copy-start = (bf16[2048,32]{0,1:T(8,128)(2,1)S(1)}, bf16[2048,32]{0,1:T(8,128)(2,1)}, u32[]{:S(2)}) copy-start(bf16[2048,32]{0,1:T(8,128)(2,1)} %param.18) | copy-start | bytes 393220
  0.6 16.8 %copy-start.12 = (bf16[2,128]{1,0:T(2,128)(2,1)S(1)}, bf16[2,128]{1,0:T(2,128)(2,1)}, u32[]{:S(2)}) copy-start(bf16[2,128]{1,0:T(2,128)(2,1)} %param.26) | copy-start | bytes 1540
  0.7 16.8 %copy-start.13 = (bf16[2,128]{1,0:T(2,128)(2,1)S(1)}, bf16[2,128]{1,0:T(2,128)(2,1)}, u32[]{:S(2)}) copy-start(bf16[2,128]{1,0:T(2,128)(2,1)} %param.25) | copy-start | bytes 1540
  0.7 16.9 %copy-start.9 = (f32[2]{0:T(128)S(1)}, f32[2]{0:T(128)}, u32[]{:S(2)}) copy-start(f32[2]{0:T(128)} %param.22) | copy-start | bytes 28
  0.7 16.9 %copy-start.14 = (bf16[128]{0:T(256)(128)(2,1)S(1)}, bf16[128]{0:T(256)(128)(2,1)}, u32[]{:S(2)}) copy-start(bf16[128]{0:T(256)(128)(2,1)} %param.29) | copy-start | bytes 772
  0.7 16.9 %copy-start.7 = (f32[2]{0:T(128)S(1)}, f32[2]{0:T(128)}, u32[]{:S(2)}) copy-start(f32[2]{0:T(128)} %param.21) | copy-start | bytes 28
  0.7 16.9 %copy-start.8 = (f32[2,2]{1,0:T(2,128)S(1)}, f32[2,2]{1,0:T(2,128)}, u32[]{:S(2)}) copy-start(f32[2,2]{1,0:T(2,128)} %param.28) | copy-start | bytes 52
  0.7 17.3 %copy-start.10 = (bf16[2,128]{1,0:T(2,128)(2,1)S(1)}, bf16[2,128]{1,0:T(2,128)(2,1)}, u32[]{:S(2)}) copy-start(bf16[2,128]{1,0:T(2,128)(2,1)} %param.27) | copy-start | bytes 1540
  0.7 17.3 %copy-start.11 = (bf16[2,128]{1,0:T(2,128)(2,1)S(1)}, bf16[2,128]{1,0:T(2,128)(2,1)}, u32[]{:S(2)}) copy-start(bf16[2,128]{1,0:T(2,128)(2,1)} %param.24) | copy-start | bytes 1540
  0.7 17.7 %copy-start.3 = (bf16[2,96,2048]{2,1,0:T(8,128)(2,1)S(1)}, bf16[2,96,2048]{2,1,0:T(8,128)(2,1)}, u32[]{:S(2)}) copy-start(bf16[2,96,2048]{2,1,0:T(8,128)(2,1)} %param.15) | copy-start | bytes 2359300
  0.7 17.7 %collective-permute-start.3 = (bf16[192,2048]{1,0:T(8,128)(2,1)}, bf16[192,2048]{1,0:T(8,128)(2,1)S(1)}, u32[]{:S(2)}, u32[]{:S(2)}) collective-permute-start(bf16[192,2048]{1,0:T(8,128)(2,1)} %bitcast.62), channel_id=1, source_target_pairs={{0,1},{1,0},{2,3},{3,2},{4,5},{5,4},{6,7},{7,6},{8,9},{9,8},{10,11... | collective-permute-start | bytes 2359304 | tf_op jit(solution)/shard_map/ppermute | solution.py:165
  9.6 21.1 %collective-permute-start = (bf16[192,2048]{1,0:T(8,128)(2,1)}, bf16[192,2048]{1,0:T(8,128)(2,1)}, u32[]{:S(2)}, u32[]{:S(2)}) collective-permute-start(bf16[192,2048]{1,0:T(8,128)(2,1)} %bitcast.63), channel_id=1, source_target_pairs={{0,2},{1,15},{2,4},{3,1},{4,6},{5,3},{6,8},{7,5},{8,10},{9,7},{10,... | collective-permute-start | bytes 2359304 | tf_op jit(solution)/shard_map/ppermute | solution.py:172
  13.7 20.5 %copy-start.6 = (f32[2,1536,2]{1,2,0:T(2,128)S(1)}, f32[2,1536,2]{1,2,0:T(2,128)}, u32[]{:S(2)}) copy-start(f32[2,1536,2]{1,2,0:T(2,128)} %param.23) | copy-start | bytes 73732
  14.4 0.8 copy-start.4
  14.4 1.0 copy-start.5
  15.4 45.5 %collective-permute-start.11 = (bf16[2052,256]{1,0:T(8,128)(2,1)S(1)}, bf16[2052,256]{1,0:T(8,128)(2,1)}, u32[]{:S(2)}, u32[]{:S(2)}) collective-permute-start(bf16[2052,256]{1,0:T(8,128)(2,1)S(1)} %pad_maximum_fusion.1), channel_id=1, source_target_pairs={{0,1},{1,0},{2,3},{3,2},{4,5},{5,4},{6,7},{7,6},{8,9},{9,8},{10,11... | collective-permute-start | bytes 3151880 | tf_op jit(solution)/shard_map/ppermute | solution.py:165
  19.5 14.5 %all-to-all-start = ((bf16[16,2,2,96]{3,2,1,0:T(2,128)(2,1)}), bf16[16,2,2,96]{3,2,1,0:T(2,128)(2,1)S(1)}, u32[]{:S(2)}, u32[]{:S(2)}) async-start(bf16[16,2,2,96]{3,2,1,0:T(2,128)(2,1)} %bitcast.60), calls=%async_computation | async-start | bytes 32768 | tf_op jit(solution)/shard_map/all_to_all | solution.py:189
  24.3 15.2 %collective-permute-start.7 = (bf16[8,2048]{1,0:T(8,128)(2,1)S(1)}, bf16[8,2048]{1,0:T(8,128)(2,1)S(1)}, u32[]{:S(2)}, u32[]{:S(2)}) collective-permute-start(bf16[8,2048]{1,0:T(8,128)(2,1)S(1)} %broadcast_select_fusion.2), channel_id=1, source_target_pairs={{0,2},{1,3},{2,4},{3,5},{4,6},{5,7},{6,8},{7,9},{8,10},{9,11},{10,... | collective-permute-start | bytes 98312 | tf_op jit(solution)/shard_map/ppermute | solution.py:184
  27.5 25.9 %collective-permute-start.4 = (bf16[192,2048]{1,0:T(8,128)(2,1)S(1)}, bf16[192,2048]{1,0:T(8,128)(2,1)}, u32[]{:S(2)}, u32[]{:S(2)}) collective-permute-start(bf16[192,2048]{1,0:T(8,128)(2,1)S(1)} %collective-permute-done.3), channel_id=1, source_target_pairs={{0,2},{1,15},{2,4},{3,1},{4,6},{5,3},{6,8},{7,5},{8,10},{9,7},{10,... | collective-permute-start | bytes 2359304 | tf_op jit(solution)/shard_map/ppermute | solution.py:172
  30.7 32.0 %collective-permute-start.1 = (bf16[192,2048]{1,0:T(8,128)(2,1)}, bf16[192,2048]{1,0:T(8,128)(2,1)}, u32[]{:S(2)}, u32[]{:S(2)}) collective-permute-start(bf16[192,2048]{1,0:T(8,128)(2,1)} %collective-permute-done.refs_0_), channel_id=1, source_target_pairs={{0,2},{1,15},{2,4},{3,1},{4,6},{5,3},{6,8},{7,5},{8,10},{9,7},{10,... | collective-permute-start | bytes 2359304 | tf_op jit(solution)/shard_map/ppermute | solution.py:172
  36.6 19.3 %collective-permute-start.12 = (f32[16,192,2]{1,0,2:T(8,128)S(1)}, f32[16,192,2]{1,0,2:T(8,128)S(1)}, u32[]{:S(2)}, u32[]{:S(2)}) collective-permute-start(f32[16,192,2]{1,0,2:T(8,128)S(1)} %reshape.73), channel_id=1, source_target_pairs={{0,1},{1,0},{2,3},{3,2},{4,5},{5,4},{6,7},{7,6},{8,9},{9,8},{10,11... | collective-permute-start | bytes 73736 | tf_op jit(solution)/shard_map/ppermute | solution.py:165
  39.5 10.0 %collective-permute-start.8 = (bf16[8,2048]{1,0:T(8,128)(2,1)S(1)}, bf16[8,2048]{1,0:T(8,128)(2,1)S(1)}, u32[]{:S(2)}, u32[]{:S(2)}) collective-permute-start(bf16[8,2048]{1,0:T(8,128)(2,1)S(1)} %collective-permute-done.7), channel_id=1, source_target_pairs={{0,2},{1,15},{2,4},{3,1},{4,6},{5,3},{6,8},{7,5},{8,10},{9,7},{10,... | collective-permute-start | bytes 98312 | tf_op jit(solution)/shard_map/ppermute | solution.py:172
  49.5 8.3 %collective-permute-start.9 = (bf16[8,2048]{1,0:T(8,128)(2,1)S(1)}, bf16[8,2048]{1,0:T(8,128)(2,1)S(1)}, u32[]{:S(2)}, u32[]{:S(2)}) collective-permute-start(bf16[8,2048]{1,0:T(8,128)(2,1)S(1)} %collective-permute-done.8.refs_2_), channel_id=1, source_target_pairs={{0,2},{1,15},{2,4},{3,1},{4,6},{5,3},{6,8},{7,5},{8,10},{9,7},{10,... | collective-permute-start | bytes 98312 | tf_op jit(solution)/shard_map/ppermute | solution.py:172
  53.4 14.2 %collective-permute-start.5 = (bf16[192,2048]{1,0:T(8,128)(2,1)}, bf16[192,2048]{1,0:T(8,128)(2,1)}, u32[]{:S(2)}, u32[]{:S(2)}) collective-permute-start(bf16[192,2048]{1,0:T(8,128)(2,1)} %collective-permute-done.4.refs_1_), channel_id=1, source_target_pairs={{0,2},{1,15},{2,4},{3,1},{4,6},{5,3},{6,8},{7,5},{8,10},{9,7},{10,... | collective-permute-start | bytes 2359304 | tf_op jit(solution)/shard_map/ppermute | solution.py:172
  57.7 8.2 %copy-start.1 = (f32[16,192,4]{2,1,0:T(8,128)S(1)}, f32[16,192,4]{2,1,0:T(8,128)}, u32[]{:S(2)}) copy-start(f32[16,192,4]{2,1,0:T(8,128)} %copy.35.refs_3_.refs_4_) | copy-start | bytes 147460
  57.7 26.7 %collective-permute-start.10 = (bf16[8,2048]{1,0:T(8,128)(2,1)S(1)}, bf16[8,2048]{1,0:T(8,128)(2,1)S(1)}, u32[]{:S(2)}, u32[]{:S(2)}) collective-permute-start(bf16[8,2048]{1,0:T(8,128)(2,1)S(1)} %collective-permute-done.9.refs_2_), channel_id=1, source_target_pairs={{0,2},{1,15},{2,4},{3,1},{4,6},{5,3},{6,8},{7,5},{8,10},{9,7},{10,... | collective-permute-start | bytes 98312 | tf_op jit(solution)/shard_map/ppermute | solution.py:172
  62.7 13.3 %collective-permute-start.2 = (bf16[192,2048]{1,0:T(8,128)(2,1)}, bf16[192,2048]{1,0:T(8,128)(2,1)}, u32[]{:S(2)}, u32[]{:S(2)}) collective-permute-start(bf16[192,2048]{1,0:T(8,128)(2,1)} %collective-permute-done.1.refs_0_), channel_id=1, source_target_pairs={{0,2},{1,15},{2,4},{3,1},{4,6},{5,3},{6,8},{7,5},{8,10},{9,7},{10,... | collective-permute-start | bytes 2359304 | tf_op jit(solution)/shard_map/ppermute | solution.py:172
  67.6 16.7 %collective-permute-start.6 = (bf16[192,2048]{1,0:T(8,128)(2,1)}, bf16[192,2048]{1,0:T(8,128)(2,1)S(1)}, u32[]{:S(2)}, u32[]{:S(2)}) collective-permute-start(bf16[192,2048]{1,0:T(8,128)(2,1)} %collective-permute-done.5.refs_1_), channel_id=1, source_target_pairs={{0,2},{1,15},{2,4},{3,1},{4,6},{5,3},{6,8},{7,5},{8,10},{9,7},{10,... | collective-permute-start | bytes 2359304 | tf_op jit(solution)/shard_map/ppermute | solution.py:172
  76.0 16.9 %collective-permute-start.13 = (bf16[192,2048]{1,0:T(8,128)(2,1)}, bf16[192,2048]{1,0:T(8,128)(2,1)}, u32[]{:S(2)}, u32[]{:S(2)}) collective-permute-start(bf16[192,2048]{1,0:T(8,128)(2,1)} %collective-permute-done.2.refs_0_), channel_id=1, source_target_pairs={{0,2},{1,15},{2,4},{3,1},{4,6},{5,3},{6,8},{7,5},{8,10},{9,7},{10,... | collective-permute-start | bytes 2359304 | tf_op jit(solution)/shard_map/ppermute | solution.py:172
  84.4 8.8 %collective-permute-start.14 = (bf16[8,2048]{1,0:T(8,128)(2,1)S(1)}, bf16[8,2048]{1,0:T(8,128)(2,1)S(1)}, u32[]{:S(2)}, u32[]{:S(2)}) collective-permute-start(bf16[8,2048]{1,0:T(8,128)(2,1)S(1)} %broadcast_select_fusion), channel_id=1, source_target_pairs={{0,2},{1,15},{2,4},{3,1},{4,6},{5,3},{6,8},{7,5},{8,10},{9,7},{10,... | collective-permute-start | bytes 98312 | tf_op jit(solution)/shard_map/ppermute | solution.py:172
  88.6 1.4 %copy-start.2 = (f32[16,192,4]{2,1,0:T(8,128)S(1)}, f32[16,192,4]{2,1,0:T(8,128)}, u32[]{:S(2)}) copy-start(f32[16,192,4]{2,1,0:T(8,128)} %copy.35.refs_3_.refs_4_) | copy-start | bytes 147460
  95.5 8.0 %collective-permute-start.15 = (f32[2,128,128]{2,1,0:T(8,128)S(1)}, f32[2,128,128]{2,1,0:T(8,128)S(1)}, u32[]{:S(2)}, u32[]{:S(2)}) collective-permute-start(f32[2,128,128]{2,1,0:T(8,128)S(1)} %get-tuple-element.34), channel_id=1, source_target_pairs={{0,1},{1,0},{2,3},{3,2},{4,5},{5,4},{6,7},{7,6},{8,9},{9,8},{10,11... | collective-permute-start | bytes 393224 | tf_op jit(solution)/shard_map/ppermute | solution.py:165
where the time goes:
time: 126 us; the launch traced here: 125 us
  starting transfers between devices  66.5 us (53%)
  blocking collectives  20 us (16%)
  Pallas kernels  14.4 us (11%)
  waiting for transfers between devices  9.16 us (7%)
  local copies, waits for them, and re-layouts  8.62 us (7%)
  other arithmetic  4.41 us (4%)
  between operations  1.31 us (1%)
    ppermute x11, starting transfers between devices, onward(): return lax.ppermute(v, ('y', 'c'), pairs)  38 us
    ppermute x4, starting transfers between devices, swap(): return lax.ppermute(v, 'c', [(0, 1), (1, 0)])  20.6 us
    all_to_all x1, blocking collectives, per_device(): got = lax.all_to_all(sent, 'sp', 0, 0, tiled=True)  20 us
    pallas_call x5, Pallas kernels, piece_states(): pl.pallas_call(body, out_shape=[jax.ShapeDtypeStruct(own.shape, F32)] * 2...  13.2 us
    ppermute x11, waiting for transfers between devices, onward(): return lax.ppermute(v, ('y', 'c'), pairs)  8.18 us
    all_to_all x1, starting transfers between devices, per_device(): steps = lax.all_to_all(steps, ('y', 'c'), 0, 0, tiled=True)  4.63 us
    unnamed x32, local copies, waits for them, and re-layouts  4.46 us
    ppermute x1, starting transfers between devices, per_device(): lax.ppermute(before, ('sp', 'y', 'c'), [(i, i + 2) for i in range(count -...  3.26 us
  transfers between devices with their start and end apart: 17, of which 5 were waited for; matrix products, arithmetic and copies ran while one was open for 9% of the time, Pallas kernels for 9%

commit v1 on v0

--- a/solution.py
+++ b/solution.py
@@ -19,24 +19,25 @@
 GRANT = pltpu.CompilerParams(vmem_limit_bytes=14 * 1024 * 1024)
 
 
-def piece_states(xs, halo, places, w, weight, own, other, rows, pair):
-    depth, cols = w.shape[0] - 4, w.shape[1]
+def piece_states(xs, halo, places, w, weight, own, other, rows):
+    depth = w[0].shape[0] - 4
     many = len(xs)
 
     def body(place, *refs):
         x_refs = refs[:many]
-        h_ref, w_ref, wt_ref, own_ref, other_ref, own_out, other_out, ext = refs[many:]
-        taps = w_ref[depth : depth + 4, :].astype(F32)
+        h_ref, *w_refs, wt_ref, own_ref, other_ref, own_out, other_out, ext = refs[many:]
+        taps = jnp.concatenate([r[depth : depth + 4, :] for r in w_refs], axis=1).astype(F32)
 
         def project(ref):
-            return mm(ref[...], w_ref[:depth, :], ((1,), (0,))).astype(BF).astype(F32)
+            parts = [mm(ref[...], r[:depth, :], ((1,), (0,))).astype(BF).astype(F32) for r in w_refs]
+            return jnp.concatenate(parts, axis=1)
 
         p = [project(r) for r in x_refs]
         h = project(h_ref)
         low = place[2] == 0
         for s in range(2):
             before = [h[4 * s : 4 * s + 4, :]]
-            if pair:
+            if many == 2:
                 ends = [v[(s + 1) * rows - 4 : (s + 1) * rows, :] for v in p]
                 before = [jnp.where(low, before[0], ends[1]), jnp.where(low, ends[0], before[0])]
             for n in range(many):
@@ -65,17 +66,36 @@
     return pl.pallas_call(
         body,
         out_shape=[jax.ShapeDtypeStruct(own.shape, F32)] * 2,
-        in_specs=[pl.BlockSpec(memory_space=pltpu.SMEM)] + [vmem] * (many + 5),
+        in_specs=[pl.BlockSpec(memory_space=pltpu.SMEM)] + [vmem] * (many + 6),
         out_specs=[vmem] * 2,
-        scratch_shapes=[pltpu.VMEM((2 * many, rows + 8, cols), F32)],
+        scratch_shapes=[pltpu.VMEM((2 * many, rows + 8, 512), F32)],
         cost_estimate=pl.CostEstimate(
-            flops=16 * sum(x.shape[0] for x in xs) * w.size,
+            flops=32 * sum(x.shape[0] for x in xs) * w[0].size,
             transcendentals=0,
-            bytes_accessed=2 * w.size,
+            bytes_accessed=4 * w[0].size,
         ),
         compiler_params=GRANT,
         name="piece_states",
-    )(places, *xs, halo, w, weight, own, other)
+    )(places, *xs, halo, *w, weight, own, other)
+
+
+def joined(w_value, w_key, conv_value, conv_key):
+    depth = w_value.shape[0]
+
+    def body(v_ref, k_ref, cv_ref, ck_ref, out_ref):
+        out_ref[:depth, :128] = v_ref[...]
+        out_ref[:depth, 128:] = k_ref[...]
+        out_ref[depth:, :128] = cv_ref[...]
+        out_ref[depth:, 128:] = ck_ref[...]
+
+    return pl.pallas_call(
+        body,
+        out_shape=jax.ShapeDtypeStruct((depth + conv_value.shape[0], 256), BF),
+        in_specs=[pl.BlockSpec(memory_space=pltpu.VMEM)] * 4,
+        out_specs=pl.BlockSpec(memory_space=pltpu.VMEM),
+        compiler_params=GRANT,
+        name="joined",
+    )(w_value, w_key, conv_value, conv_key)
 
 
 def packed(own, got, query, total, sp_count):
@@ -182,7 +202,13 @@
     ends = last(early), last(first)
     before = jnp.where(c == 1, *ends)
     before = lax.ppermute(before, ("sp", "y", "c"), [(i, i + 2) for i in range(count - 2)])
-    halo = [before, onward(before)]
+
+    def straight(v, far):
+        pairs = []
+        for i in range(y_count):
+            pairs.append((2 * i + 1, 2 * ((i + far) % y_count)))
+            pairs.append((2 * i, 2 * ((i - far) % y_count) + 1))
+        return lax.ppermute(v, ("y", "c"), pairs)
 
     steps = mm(early, w_step, ((1,), (0,))).astype(BF)
     steps = steps.reshape(2, rows, tp_count, heads).transpose(2, 0, 3, 1)
@@ -196,15 +222,13 @@
     weight = weight.reshape(tp_count, 2 * rows, heads)
     weight = jnp.concatenate([weight, swap(weight)], axis=2)
 
-    w_own = jnp.concatenate(
-        [jnp.concatenate([w_value, conv_value], axis=0), jnp.concatenate([w_key, conv_key], axis=0)], axis=1
-    )
-    w_both = jnp.concatenate([w_own, swap(w_own)], axis=1)
+    w_own = joined(w_value, w_key, conv_value, conv_key)
+    w_both = w_own, swap(w_own)
 
     def add(acc, xs, halo, far):
         away = jnp.where(c == 0, y - far, y + far) % y_count
         places = jnp.stack([away * 2 + c, away * 2 + 1 - c, c]).astype(jnp.int32)
-        return piece_states(xs, halo, places, w_both, weight, *acc, rows, len(xs) == 2)
+        return piece_states(xs, halo, places, w_both, weight, *acc, rows)
 
     acc = (jnp.zeros((2, 128, 128), F32),) * 2
     half = y_count // 2
@@ -213,9 +237,8 @@
         a.append(onward(a[s]))
         if s + 1 < half:
             b.append(onward(b[s]))
-            halo.append(onward(halo[s]))
-        acc = add(acc, [a[s], b[s]], halo[s], s)
-    last_halo = onward(jnp.where(c == 0, halo[half - 1], last(b[half - 1])))
+        acc = add(acc, [a[s], b[s]], straight(before, s), s)
+    last_halo = straight(jnp.where(c == 1, before, ends[0]), half)
     query = new_query.astype(F32)
     new_size = jax.nn.softplus(new_step + step_bias)
     keep = jnp.repeat(jnp.exp(-decay_rate * new_size), HEAD_DIM, axis=1)

time: 126 us -> 127 us (level)
  the two profiles are of different devices: /device:TPU:1 before, /device:TPU:16 now
where the time goes in v1:
time: 127 us; the launch traced here: 126 us
  starting transfers between devices  58.4 us (46%)
  blocking collectives  21.7 us (17%)
  Pallas kernels  16.3 us (13%)
  waiting for transfers between devices  12.4 us (10%)
  local copies, waits for them, and re-layouts  7.91 us (6%)
  other arithmetic  7.21 us (6%)
  between operations  1.3 us (1%)
    all_to_all x1, blocking collectives, per_device(): got = lax.all_to_all(sent, 'sp', 0, 0, tiled=True)  21.7 us
    ppermute x7, starting transfers between devices, onward(): return lax.ppermute(v, ('y', 'c'), pairs)  20.8 us
    ppermute x4, starting transfers between devices, straight(): return lax.ppermute(v, ('y', 'c'), pairs)  17.7 us
    pallas_call x5, Pallas kernels, piece_states(): pl.pallas_call(body, out_shape=[jax.ShapeDtypeStruct(own.shape, F32)] * 2...  14.8 us
    ppermute x7, waiting for transfers between devices, onward(): return lax.ppermute(v, ('y', 'c'), pairs)  11.1 us
    all_to_all x1, starting transfers between devices, per_device(): steps = lax.all_to_all(steps, ('y', 'c'), 0, 0, tiled=True)  8.73 us
    ppermute x4, starting transfers between devices, swap(): return lax.ppermute(v, 'c', [(0, 1), (1, 0)])  7.8 us
    unnamed x42, local copies, waits for them, and re-layouts  4.85 us
  transfers between devices with their start and end apart: 17, of which 4 were waited for; matrix products, arithmetic and copies ran while one was open for 8% of the time, Pallas kernels for 10%

profile of v1, /device:TPU:16, one launch (start us, length us, event | category | flops | bytes accessed | tf_op | source)
XLA Modules:
  0.0 125.5 jit_solution(11787456477901248798)
XLA Ops:
  0.7 2.1 %collective-permute-start.3 = (bf16[192,2048]{1,0:T(8,128)(2,1)}, bf16[192,2048]{1,0:T(8,128)(2,1)S(1)}, u32[]{:S(2)}, u32[]{:S(2)}) collective-permute-start(bf16[192,2048]{1,0:T(8,128)(2,1)} %bitcast.61), channel_id=1, source_target_pairs={{0,1},{1,0},{2,3},{3,2},{4,5},{5,4},{6,7},{7,6},{8,9},{9,8},{10,11... | collective-permute-start | bytes 2359304 | tf_op jit(solution)/shard_map/ppermute | solution.py:185
  2.7 3.5 %collective-permute-start = (bf16[192,2048]{1,0:T(8,128)(2,1)}, bf16[192,2048]{1,0:T(8,128)(2,1)}, u32[]{:S(2)}, u32[]{:S(2)}) collective-permute-start(bf16[192,2048]{1,0:T(8,128)(2,1)} %bitcast.62), channel_id=1, source_target_pairs={{0,2},{1,15},{2,4},{3,1},{4,6},{5,3},{6,8},{7,5},{8,10},{9,7},{10,... | collective-permute-start | bytes 2359304 | tf_op jit(solution)/shard_map/ppermute | solution.py:192
  6.2 1.0 copy-done.2
  7.3 1.0 copy-done.3
  8.3 0.7 copy-done.5
  9.0 0.7 copy-done.6
  9.9 1.9 %collective-permute-start.9 = (bf16[2052,256]{1,0:T(8,128)(2,1)S(1)}, bf16[2052,256]{1,0:T(8,128)(2,1)}, u32[]{:S(2)}, u32[]{:S(2)}) collective-permute-start(bf16[2052,256]{1,0:T(8,128)(2,1)S(1)} %joined.1.refs_2_.refs_3_), channel_id=1, source_target_pairs={{0,1},{1,0},{2,3},{3,2},{4,5},{5,4},{6,7},{7,6},{8,9},{9,8},{10,11... | collective-permute-start | bytes 3151880 | tf_op jit(solution)/shard_map/ppermute | solution.py:185
  12.6 0.6 add_add_fusion.3.place
  13.2 0.6 add_add_fusion.2.place
  13.8 0.6 add_add_fusion.1.place
  14.4 0.6 add_add_fusion.place
  14.9 0.7 add_add_fusion.4.place
  15.6 0.3 convolution_convert_fusion
  16.1 0.6 copy.40
  16.7 8.7 %all-to-all-start = ((bf16[16,2,2,96]{3,2,1,0:T(2,128)(2,1)}), bf16[16,2,2,96]{3,2,1,0:T(2,128)(2,1)S(1)}, u32[]{:S(2)}, u32[]{:S(2)}) async-start(bf16[16,2,2,96]{3,2,1,0:T(2,128)(2,1)} %bitcast.59), calls=%async_computation | async-start | bytes 32768 | tf_op jit(solution)/shard_map/all_to_all | solution.py:215
  25.5 3.4 %collective-permute-start.7 = (bf16[8,2048]{1,0:T(8,128)(2,1)S(1)}, bf16[8,2048]{1,0:T(8,128)(2,1)}, u32[]{:S(2)}, u32[]{:S(2)}) collective-permute-start(bf16[8,2048]{1,0:T(8,128)(2,1)S(1)} %broadcast_select_fusion.2), channel_id=1, source_target_pairs={{0,2},{1,3},{2,4},{3,5},{4,6},{5,7},{6,8},{7,9},{8,10},{9,11},{10,... | collective-permute-start | bytes 98312 | tf_op jit(solution)/shard_map/ppermute | solution.py:204
  28.9 4.6 %collective-permute-start.4 = (bf16[192,2048]{1,0:T(8,128)(2,1)S(1)}, bf16[192,2048]{1,0:T(8,128)(2,1)}, u32[]{:S(2)}, u32[]{:S(2)}) collective-permute-start(bf16[192,2048]{1,0:T(8,128)(2,1)S(1)} %collective-permute-done.3), channel_id=1, source_target_pairs={{0,2},{1,15},{2,4},{3,1},{4,6},{5,3},{6,8},{7,5},{8,10},{9,7},{10,... | collective-permute-start | bytes 2359304 | tf_op jit(solution)/shard_map/ppermute | solution.py:192
  33.5 2.5 %collective-permute-start.1 = (bf16[192,2048]{1,0:T(8,128)(2,1)}, bf16[192,2048]{1,0:T(8,128)(2,1)}, u32[]{:S(2)}, u32[]{:S(2)}) collective-permute-start(bf16[192,2048]{1,0:T(8,128)(2,1)} %collective-permute-done.refs_0_), channel_id=1, source_target_pairs={{0,2},{1,15},{2,4},{3,1},{4,6},{5,3},{6,8},{7,5},{8,10},{9,7},{10,... | collective-permute-start | bytes 2359304 | tf_op jit(solution)/shard_map/ppermute | solution.py:192
  36.1 0.2 fusion.13
  36.4 1.2 reduce-window.6
  37.7 0.4 reduce-window.9
  38.6 1.9 %collective-permute-start.10 = (f32[16,192,2]{1,0,2:T(8,128)S(1)}, f32[16,192,2]{1,0,2:T(8,128)S(1)}, u32[]{:S(2)}, u32[]{:S(2)}) collective-permute-start(f32[16,192,2]{1,0,2:T(8,128)S(1)} %reshape.67), channel_id=1, source_target_pairs={{0,1},{1,0},{2,3},{3,2},{4,5},{5,4},{6,7},{7,6},{8,9},{9,8},{10,11... | collective-permute-start | bytes 73736 | tf_op jit(solution)/shard_map/ppermute | solution.py:185
  40.5 2.5 %collective-permute-done.4.refs_1_ = bf16[192,2048]{1,0:T(8,128)(2,1)} collective-permute-done((bf16[192,2048]{1,0:T(8,128)(2,1)S(1)}, bf16[192,2048]{1,0:T(8,128)(2,1)}, u32[]{:S(2)}, u32[]{:S(2)}) %collective-permute-start.4) | collective-permute-done | bytes 786464 | tf_op jit(solution)/shard_map/ppermute | solution.py:192
  43.0 4.5 %collective-permute-start.5 = (bf16[192,2048]{1,0:T(8,128)(2,1)}, bf16[192,2048]{1,0:T(8,128)(2,1)}, u32[]{:S(2)}, u32[]{:S(2)}) collective-permute-start(bf16[192,2048]{1,0:T(8,128)(2,1)} %collective-permute-done.4.refs_1_), channel_id=1, source_target_pairs={{0,2},{1,15},{2,4},{3,1},{4,6},{5,3},{6,8},{7,5},{8,10},{9,7},{10,... | collective-permute-start | bytes 2359304 | tf_op jit(solution)/shard_map/ppermute | solution.py:192
  47.5 1.4 %broadcast_select_fusion.1 = (bf16[8,2048]{1,0:T(8,128)(2,1)}, bf16[8,2048]{1,0:T(8,128)(2,1)}) fusion(bf16[8,2048]{1,0:T(8,128)(2,1)} %collective-permute-done.7, bf16[8,2048]{1,0:T(8,128)(2,1)S(1)} %reshape.61, pred[]{:T(512)S(6)} %eq.20, bf16[8,2048]{1,0:T(8,128)(2,1)S(1)} %reshape.63, pred[]{:T(512)S(6)} %eq.19), kind=kLoop, calls=%fused_computation.17 | loop fusion | flops 32768 | bytes 163842 | tf_op jit(solution)/shard_map/jit(_where)/select_n | solution.py:241
  48.9 1.9 %collective-permute-start.14 = (bf16[8,2048]{1,0:T(8,128)(2,1)}, bf16[8,2048]{1,0:T(8,128)(2,1)}, u32[]{:S(2)}, u32[]{:S(2)}) collective-permute-start(bf16[8,2048]{1,0:T(8,128)(2,1)} %get-tuple-element.40), channel_id=1, source_target_pairs={{1,8},{0,9},{3,10},{2,11},{5,12},{4,13},{7,14},{6,15},{9,0},{8,1},... | collective-permute-start | bytes 98312 | tf_op jit(solution)/shard_map/ppermute | solution.py:211
  50.8 3.6 %collective-permute-start.12 = (bf16[8,2048]{1,0:T(8,128)(2,1)}, bf16[8,2048]{1,0:T(8,128)(2,1)}, u32[]{:S(2)}, u32[]{:S(2)}) collective-permute-start(bf16[8,2048]{1,0:T(8,128)(2,1)} %collective-permute-done.7), channel_id=1, source_target_pairs={{1,2},{0,15},{3,4},{2,1},{5,6},{4,3},{7,8},{6,5},{9,10},{8,7},{11,... | collective-permute-start | bytes 98312 | tf_op jit(solution)/shard_map/ppermute | solution.py:211
  54.5 0.6 pad_maximum_fusion
  55.1 1.4 %copy.35.refs_4_.refs_5_ = f32[16,192,4]{2,1,0:T(8,128)S(1)} copy(f32[16,192,4]{1,0,2:T(8,128)} %pad_maximum_fusion) | data formatting | bytes 98304 | tf_op jit(solution)/shard_map/concatenate | solution.py:223
  56.5 3.5 %collective-permute-start.11 = (bf16[8,2048]{1,0:T(8,128)(2,1)}, bf16[8,2048]{1,0:T(8,128)(2,1)S(1)}, u32[]{:S(2)}, u32[]{:S(2)}) collective-permute-start(bf16[8,2048]{1,0:T(8,128)(2,1)} %collective-permute-done.7), channel_id=1, source_target_pairs={{1,4},{0,13},{3,6},{2,15},{5,8},{4,1},{7,10},{6,3},{9,12},{8,5},{1... | collective-permute-start | bytes 98312 | tf_op jit(solution)/shard_map/ppermute | solution.py:211
  60.0 1.9 %collective-permute-start.2 = (bf16[192,2048]{1,0:T(8,128)(2,1)}, bf16[192,2048]{1,0:T(8,128)(2,1)S(1)}, u32[]{:S(2)}, u32[]{:S(2)}) collective-permute-start(bf16[192,2048]{1,0:T(8,128)(2,1)} %collective-permute-done.1.refs_0_), channel_id=1, source_target_pairs={{0,2},{1,15},{2,4},{3,1},{4,6},{5,3},{6,8},{7,5},{8,10},{9,7},{10,... | collective-permute-start | bytes 2359304 | tf_op jit(solution)/shard_map/ppermute | solution.py:192
  61.9 0.7 copy-done.4
  62.7 0.6 copy-done.11
  63.3 2.4 %piece_states.5 = (f32[2,128,128]{2,1,0:T(8,128)S(1)}, f32[2,128,128]{2,1,0:T(8,128)S(1)}) custom-call(s32[3]{0:T(128)S(1)} %copy-done.11, bf16[192,2048]{1,0:T(8,128)(2,1)S(1)} %bitcast.64, bf16[8,2048]{1,0:T(8,128)(2,1)S(1)} %copy-done.4, bf16[2052,256]{1,0:T(8,128)(2,1)S(1)} %joined.1.refs_2_.refs_3_, ...), custom_call_target="tpu_custom_call" | custom-call | flops 3227516928 | bytes 2101248 | tf_op jit(solution)/shard_map/piece_states/pallas_call | solution.py:66
  65.7 8.7 %collective-permute-start.8 = (bf16[8,2048]{1,0:T(8,128)(2,1)}, bf16[8,2048]{1,0:T(8,128)(2,1)S(1)}, u32[]{:S(2)}, u32[]{:S(2)}) collective-permute-start(bf16[8,2048]{1,0:T(8,128)(2,1)} %collective-permute-done.7), channel_id=1, source_target_pairs={{1,6},{0,11},{3,8},{2,13},{5,10},{4,15},{7,12},{6,1},{9,14},{8,3},... | collective-permute-start | bytes 98312 | tf_op jit(solution)/shard_map/ppermute | solution.py:211
  74.4 1.9 %collective-permute-start.6 = (bf16[192,2048]{1,0:T(8,128)(2,1)}, bf16[192,2048]{1,0:T(8,128)(2,1)S(1)}, u32[]{:S(2)}, u32[]{:S(2)}) collective-permute-start(bf16[192,2048]{1,0:T(8,128)(2,1)} %collective-permute-done.5.refs_1_), channel_id=1, source_target_pairs={{0,2},{1,15},{2,4},{3,1},{4,6},{5,3},{6,8},{7,5},{8,10},{9,7},{10,... | collective-permute-start | bytes 2359304 | tf_op jit(solution)/shard_map/ppermute | solution.py:192
  76.3 3.5 %piece_states.6 = (f32[2,128,128]{2,1,0:T(8,128)S(1)}, f32[2,128,128]{2,1,0:T(8,128)S(1)}) custom-call(s32[3]{0:T(128)S(1)} %copy-done.10, bf16[192,2048]{1,0:T(8,128)(2,1)} %collective-permute-done.refs_0_, bf16[192,2048]{1,0:T(8,128)(2,1)} %collective-permute-done.4.refs_1_, bf16[8,2048]{1,0:T(8,128)(2,1)} %collective-permute-done.12.refs_2_, ...), custom_call_target="tpu_custom_call" | custom-call | flops 6455033856 | bytes 2101248 | tf_op jit(solution)/shard_map/piece_states/pallas_call | solution.py:66
  79.8 1.9 %collective-permute-start.13 = (bf16[192,2048]{1,0:T(8,128)(2,1)S(1)}, bf16[192,2048]{1,0:T(8,128)(2,1)S(1)}, u32[]{:S(2)}, u32[]{:S(2)}) collective-permute-start(bf16[192,2048]{1,0:T(8,128)(2,1)S(1)} %collective-permute-done.2.refs_0_), channel_id=1, source_target_pairs={{0,2},{1,15},{2,4},{3,1},{4,6},{5,3},{6,8},{7,5},{8,10},{9,7},{10,... | collective-permute-start | bytes 2359304 | tf_op jit(solution)/shard_map/ppermute | solution.py:192
  81.8 3.5 %piece_states.7 = (f32[2,128,128]{2,1,0:T(8,128)S(1)}, f32[2,128,128]{2,1,0:T(8,128)S(1)}) custom-call(s32[3]{0:T(128)S(1)} %copy-done.9, bf16[192,2048]{1,0:T(8,128)(2,1)} %collective-permute-done.1.refs_0_, bf16[192,2048]{1,0:T(8,128)(2,1)} %collective-permute-done.5.refs_1_, bf16[8,2048]{1,0:T(8,128)(2,1)S(1)} %collective-permute-done.11.refs_2_, ...), custom_call_target="tpu_custom_call" | custom-call | flops 6455033856 | bytes 2101248 | tf_op jit(solution)/shard_map/piece_states/pallas_call | solution.py:66
  85.3 3.2 %collective-permute-done.6.refs_1_ = bf16[192,2048]{1,0:T(8,128)(2,1)S(1)} collective-permute-done((bf16[192,2048]{1,0:T(8,128)(2,1)}, bf16[192,2048]{1,0:T(8,128)(2,1)S(1)}, u32[]{:S(2)}, u32[]{:S(2)}) %collective-permute-start.6) | collective-permute-done | bytes 786464 | tf_op jit(solution)/shard_map/ppermute | solution.py:192
  88.5 3.0 %piece_states.8 = (f32[2,128,128]{2,1,0:T(8,128)S(1)}, f32[2,128,128]{2,1,0:T(8,128)S(1)}) custom-call(s32[3]{0:T(128)S(1)} %copy-done.8, bf16[192,2048]{1,0:T(8,128)(2,1)S(1)} %collective-permute-done.2.refs_0_, bf16[192,2048]{1,0:T(8,128)(2,1)S(1)} %collective-permute-done.6.refs_1_, bf16[8,2048]{1,0:T(8,128)(2,1)S(1)} %collective-permute-done.8.refs_2_, ...), custom_call_target="tpu_custom_call" | custom-call | flops 6455033856 | bytes 2101248 | tf_op jit(solution)/shard_map/piece_states/pallas_call | solution.py:66
  91.5 5.4 %collective-permute-done.13.refs_0_ = bf16[192,2048]{1,0:T(8,128)(2,1)S(1)} collective-permute-done((bf16[192,2048]{1,0:T(8,128)(2,1)S(1)}, bf16[192,2048]{1,0:T(8,128)(2,1)S(1)}, u32[]{:S(2)}, u32[]{:S(2)}) %collective-permute-start.13) | collective-permute-done | bytes 786464 | tf_op jit(solution)/shard_map/ppermute | solution.py:192
  96.9 2.4 %piece_states.9 = (f32[2,128,128]{2,1,0:T(8,128)S(1)}, f32[2,128,128]{2,1,0:T(8,128)S(1)}) custom-call(s32[3]{0:T(128)S(1)} %copy-done.7, bf16[192,2048]{1,0:T(8,128)(2,1)S(1)} %collective-permute-done.13.refs_0_, bf16[8,2048]{1,0:T(8,128)(2,1)} %collective-permute-done.14.refs_1_, bf16[2052,256]{1,0:T(8,128)(2,1)S(1)} %joined.1.refs_2_.refs_3_, ...), custom_call_target="tpu_custom_call" | custom-call | flops 3227516928 | bytes 2101248 | tf_op jit(solution)/shard_map/piece_states/pallas_call | solution.py:66
  99.3 1.9 %collective-permute-start.15 = (f32[2,128,128]{2,1,0:T(8,128)S(1)}, f32[2,128,128]{2,1,0:T(8,128)S(1)}, u32[]{:S(2)}, u32[]{:S(2)}) collective-permute-start(f32[2,128,128]{2,1,0:T(8,128)S(1)} %get-tuple-element.34), channel_id=1, source_target_pairs={{0,1},{1,0},{2,3},{3,2},{4,5},{5,4},{6,7},{7,6},{8,9},{9,8},{10,11... | collective-permute-start | bytes 393224 | tf_op jit(solution)/shard_map/ppermute | solution.py:185
  101.3 1.3 %collective-permute-done.15.b_ref = f32[2,128,128]{2,1,0:T(8,128)S(1)} collective-permute-done((f32[2,128,128]{2,1,0:T(8,128)S(1)}, f32[2,128,128]{2,1,0:T(8,128)S(1)}, u32[]{:S(2)}, u32[]{:S(2)}) %collective-permute-start.15) | collective-permute-done | bytes 131104 | tf_op jit(solution)/shard_map/ppermute | solution.py:185
  102.6 0.2 packed.1
  102.8 21.7 %all_to_all.10.got_ref = bf16[32,16,128]{2,1,0:T(8,128)(2,1)S(1)} all-to-all(bf16[32,16,128]{2,1,0:T(8,128)(2,1)S(1)} %packed.1), channel_id=1, replica_groups=mesh['sp'=32,'y'=8,'c'=2] {'sp'}, dimensions={0} | all-to-all | bytes 262144 | tf_op jit(solution)/shard_map/all_to_all | solution.py:255
  124.4 1.1 finished.1
  (80 shorter events, 1.8 us)
Async XLA Ops:
  0.6 15.0 %copy-start = (bf16[2048,32]{0,1:T(8,128)(2,1)S(1)}, bf16[2048,32]{0,1:T(8,128)(2,1)}, u32[]{:S(2)}) copy-start(bf16[2048,32]{0,1:T(8,128)(2,1)} %param.18) | copy-start | bytes 393220
  0.6 11.5 %copy-start.13 = (f32[2]{0:T(128)S(1)}, f32[2]{0:T(128)}, u32[]{:S(2)}) copy-start(f32[2]{0:T(128)} %param.21) | copy-start | bytes 28
  0.7 11.5 %copy-start.14 = (f32[2,2]{1,0:T(2,128)S(1)}, f32[2,2]{1,0:T(2,128)}, u32[]{:S(2)}) copy-start(f32[2,2]{1,0:T(2,128)} %param.28) | copy-start | bytes 52
  0.7 15.0 %copy-start.1 = (bf16[2,96,2048]{2,1,0:T(8,128)(2,1)S(1)}, bf16[2,96,2048]{2,1,0:T(8,128)(2,1)}, u32[]{:S(2)}) copy-start(bf16[2,96,2048]{2,1,0:T(8,128)(2,1)} %param.15) | copy-start | bytes 2359300
  0.7 14.9 %collective-permute-start.3 = (bf16[192,2048]{1,0:T(8,128)(2,1)}, bf16[192,2048]{1,0:T(8,128)(2,1)S(1)}, u32[]{:S(2)}, u32[]{:S(2)}) collective-permute-start(bf16[192,2048]{1,0:T(8,128)(2,1)} %bitcast.61), channel_id=1, source_target_pairs={{0,1},{1,0},{2,3},{3,2},{4,5},{5,4},{6,7},{7,6},{8,9},{9,8},{10,11... | collective-permute-start | bytes 2359304 | tf_op jit(solution)/shard_map/ppermute | solution.py:185
  2.7 30.8 %collective-permute-start = (bf16[192,2048]{1,0:T(8,128)(2,1)}, bf16[192,2048]{1,0:T(8,128)(2,1)}, u32[]{:S(2)}, u32[]{:S(2)}) collective-permute-start(bf16[192,2048]{1,0:T(8,128)(2,1)} %bitcast.62), channel_id=1, source_target_pairs={{0,2},{1,15},{2,4},{3,1},{4,6},{5,3},{6,8},{7,5},{8,10},{9,7},{10,... | collective-permute-start | bytes 2359304 | tf_op jit(solution)/shard_map/ppermute | solution.py:192
  6.2 1.0 copy-start.2
  7.3 1.0 copy-start.3
  8.3 0.7 copy-start.5
  9.0 0.7 copy-start.6
  9.7 2.3 %copy-start.18 = (bf16[2,128]{1,0:T(2,128)(2,1)S(1)}, bf16[2,128]{1,0:T(2,128)(2,1)}, u32[]{:S(2)}) copy-start(bf16[2,128]{1,0:T(2,128)(2,1)} %param.26) | copy-start | bytes 1540
  9.7 2.3 %copy-start.19 = (bf16[2,128]{1,0:T(2,128)(2,1)S(1)}, bf16[2,128]{1,0:T(2,128)(2,1)}, u32[]{:S(2)}) copy-start(bf16[2,128]{1,0:T(2,128)(2,1)} %param.25) | copy-start | bytes 1540
  9.7 2.4 %copy-start.15 = (f32[2]{0:T(128)S(1)}, f32[2]{0:T(128)}, u32[]{:S(2)}) copy-start(f32[2]{0:T(128)} %param.22) | copy-start | bytes 28
  9.7 2.4 %copy-start.20 = (bf16[128]{0:T(256)(128)(2,1)S(1)}, bf16[128]{0:T(256)(128)(2,1)}, u32[]{:S(2)}) copy-start(bf16[128]{0:T(256)(128)(2,1)} %param.29) | copy-start | bytes 772
  9.7 2.8 %copy-start.16 = (bf16[2,128]{1,0:T(2,128)(2,1)S(1)}, bf16[2,128]{1,0:T(2,128)(2,1)}, u32[]{:S(2)}) copy-start(bf16[2,128]{1,0:T(2,128)(2,1)} %param.27) | copy-start | bytes 1540
  9.7 2.8 %copy-start.17 = (bf16[2,128]{1,0:T(2,128)(2,1)S(1)}, bf16[2,128]{1,0:T(2,128)(2,1)}, u32[]{:S(2)}) copy-start(bf16[2,128]{1,0:T(2,128)(2,1)} %param.24) | copy-start | bytes 1540
  9.9 26.2 %copy-start.12 = (f32[2,1536,2]{1,2,0:T(2,128)S(1)}, f32[2,1536,2]{1,2,0:T(2,128)}, u32[]{:S(2)}) copy-start(f32[2,1536,2]{1,2,0:T(2,128)} %param.23) | copy-start | bytes 73732
  9.9 46.6 %collective-permute-start.9 = (bf16[2052,256]{1,0:T(8,128)(2,1)S(1)}, bf16[2052,256]{1,0:T(8,128)(2,1)}, u32[]{:S(2)}, u32[]{:S(2)}) collective-permute-start(bf16[2052,256]{1,0:T(8,128)(2,1)S(1)} %joined.1.refs_2_.refs_3_), channel_id=1, source_target_pairs={{0,1},{1,0},{2,3},{3,2},{4,5},{5,4},{6,7},{7,6},{8,9},{9,8},{10,11... | collective-permute-start | bytes 3151880 | tf_op jit(solution)/shard_map/ppermute | solution.py:185
  16.7 19.3 %all-to-all-start = ((bf16[16,2,2,96]{3,2,1,0:T(2,128)(2,1)}), bf16[16,2,2,96]{3,2,1,0:T(2,128)(2,1)S(1)}, u32[]{:S(2)}, u32[]{:S(2)}) async-start(bf16[16,2,2,96]{3,2,1,0:T(2,128)(2,1)} %bitcast.59), calls=%async_computation | async-start | bytes 32768 | tf_op jit(solution)/shard_map/all_to_all | solution.py:215
  25.5 22.0 %collective-permute-start.7 = (bf16[8,2048]{1,0:T(8,128)(2,1)S(1)}, bf16[8,2048]{1,0:T(8,128)(2,1)}, u32[]{:S(2)}, u32[]{:S(2)}) collective-permute-start(bf16[8,2048]{1,0:T(8,128)(2,1)S(1)} %broadcast_select_fusion.2), channel_id=1, source_target_pairs={{0,2},{1,3},{2,4},{3,5},{4,6},{5,7},{6,8},{7,9},{8,10},{9,11},{10,... | collective-permute-start | bytes 98312 | tf_op jit(solution)/shard_map/ppermute | solution.py:204
  28.9 14.1 %collective-permute-start.4 = (bf16[192,2048]{1,0:T(8,128)(2,1)S(1)}, bf16[192,2048]{1,0:T(8,128)(2,1)}, u32[]{:S(2)}, u32[]{:S(2)}) collective-permute-start(bf16[192,2048]{1,0:T(8,128)(2,1)S(1)} %collective-permute-done.3), channel_id=1, source_target_pairs={{0,2},{1,15},{2,4},{3,1},{4,6},{5,3},{6,8},{7,5},{8,10},{9,7},{10,... | collective-permute-start | bytes 2359304 | tf_op jit(solution)/shard_map/ppermute | solution.py:192
  33.5 26.4 %collective-permute-start.1 = (bf16[192,2048]{1,0:T(8,128)(2,1)}, bf16[192,2048]{1,0:T(8,128)(2,1)}, u32[]{:S(2)}, u32[]{:S(2)}) collective-permute-start(bf16[192,2048]{1,0:T(8,128)(2,1)} %collective-permute-done.refs_0_), channel_id=1, source_target_pairs={{0,2},{1,15},{2,4},{3,1},{4,6},{5,3},{6,8},{7,5},{8,10},{9,7},{10,... | collective-permute-start | bytes 2359304 | tf_op jit(solution)/shard_map/ppermute | solution.py:192
  38.6 12.3 %collective-permute-start.10 = (f32[16,192,2]{1,0,2:T(8,128)S(1)}, f32[16,192,2]{1,0,2:T(8,128)S(1)}, u32[]{:S(2)}, u32[]{:S(2)}) collective-permute-start(f32[16,192,2]{1,0,2:T(8,128)S(1)} %reshape.67), channel_id=1, source_target_pairs={{0,1},{1,0},{2,3},{3,2},{4,5},{5,4},{6,7},{7,6},{8,9},{9,8},{10,11... | collective-permute-start | bytes 73736 | tf_op jit(solution)/shard_map/ppermute | solution.py:185
  43.0 31.4 %collective-permute-start.5 = (bf16[192,2048]{1,0:T(8,128)(2,1)}, bf16[192,2048]{1,0:T(8,128)(2,1)}, u32[]{:S(2)}, u32[]{:S(2)}) collective-permute-start(bf16[192,2048]{1,0:T(8,128)(2,1)} %collective-permute-done.4.refs_1_), channel_id=1, source_target_pairs={{0,2},{1,15},{2,4},{3,1},{4,6},{5,3},{6,8},{7,5},{8,10},{9,7},{10,... | collective-permute-start | bytes 2359304 | tf_op jit(solution)/shard_map/ppermute | solution.py:192
  48.9 42.6 %collective-permute-start.14 = (bf16[8,2048]{1,0:T(8,128)(2,1)}, bf16[8,2048]{1,0:T(8,128)(2,1)}, u32[]{:S(2)}, u32[]{:S(2)}) collective-permute-start(bf16[8,2048]{1,0:T(8,128)(2,1)} %get-tuple-element.40), channel_id=1, source_target_pairs={{1,8},{0,9},{3,10},{2,11},{5,12},{4,13},{7,14},{6,15},{9,0},{8,1},... | collective-permute-start | bytes 98312 | tf_op jit(solution)/shard_map/ppermute | solution.py:211
  50.8 14.8 %collective-permute-start.12 = (bf16[8,2048]{1,0:T(8,128)(2,1)}, bf16[8,2048]{1,0:T(8,128)(2,1)}, u32[]{:S(2)}, u32[]{:S(2)}) collective-permute-start(bf16[8,2048]{1,0:T(8,128)(2,1)} %collective-permute-done.7), channel_id=1, source_target_pairs={{1,2},{0,15},{3,4},{2,1},{5,6},{4,3},{7,8},{6,5},{9,10},{8,7},{11,... | collective-permute-start | bytes 98312 | tf_op jit(solution)/shard_map/ppermute | solution.py:211
  56.5 25.3 %collective-permute-start.11 = (bf16[8,2048]{1,0:T(8,128)(2,1)}, bf16[8,2048]{1,0:T(8,128)(2,1)S(1)}, u32[]{:S(2)}, u32[]{:S(2)}) collective-permute-start(bf16[8,2048]{1,0:T(8,128)(2,1)} %collective-permute-done.7), channel_id=1, source_target_pairs={{1,4},{0,13},{3,6},{2,15},{5,8},{4,1},{7,10},{6,3},{9,12},{8,5},{1... | collective-permute-start | bytes 98312 | tf_op jit(solution)/shard_map/ppermute | solution.py:211
  60.0 19.8 %collective-permute-start.2 = (bf16[192,2048]{1,0:T(8,128)(2,1)}, bf16[192,2048]{1,0:T(8,128)(2,1)S(1)}, u32[]{:S(2)}, u32[]{:S(2)}) collective-permute-start(bf16[192,2048]{1,0:T(8,128)(2,1)} %collective-permute-done.1.refs_0_), channel_id=1, source_target_pairs={{0,2},{1,15},{2,4},{3,1},{4,6},{5,3},{6,8},{7,5},{8,10},{9,7},{10,... | collective-permute-start | bytes 2359304 | tf_op jit(solution)/shard_map/ppermute | solution.py:192
  61.9 0.8 copy-start.4
  62.7 0.6 copy-start.11
  63.3 13.0 %copy-start.10 = (s32[3]{0:T(128)S(1)}, s32[3]{0:T(128)}, u32[]{:S(2)}) copy-start(s32[3]{0:T(128)} %add_add_fusion.2.place) | copy-start | bytes 40
  65.7 19.6 %collective-permute-start.8 = (bf16[8,2048]{1,0:T(8,128)(2,1)}, bf16[8,2048]{1,0:T(8,128)(2,1)S(1)}, u32[]{:S(2)}, u32[]{:S(2)}) collective-permute-start(bf16[8,2048]{1,0:T(8,128)(2,1)} %collective-permute-done.7), channel_id=1, source_target_pairs={{1,6},{0,11},{3,8},{2,13},{5,10},{4,15},{7,12},{6,1},{9,14},{8,3},... | collective-permute-start | bytes 98312 | tf_op jit(solution)/shard_map/ppermute | solution.py:211
  74.4 14.1 %collective-permute-start.6 = (bf16[192,2048]{1,0:T(8,128)(2,1)}, bf16[192,2048]{1,0:T(8,128)(2,1)S(1)}, u32[]{:S(2)}, u32[]{:S(2)}) collective-permute-start(bf16[192,2048]{1,0:T(8,128)(2,1)} %collective-permute-done.5.refs_1_), channel_id=1, source_target_pairs={{0,2},{1,15},{2,4},{3,1},{4,6},{5,3},{6,8},{7,5},{8,10},{9,7},{10,... | collective-permute-start | bytes 2359304 | tf_op jit(solution)/shard_map/ppermute | solution.py:192
  76.3 5.4 %copy-start.9 = (s32[3]{0:T(128)S(1)}, s32[3]{0:T(128)}, u32[]{:S(2)}) copy-start(s32[3]{0:T(128)} %add_add_fusion.1.place) | copy-start | bytes 40
  79.8 17.1 %collective-permute-start.13 = (bf16[192,2048]{1,0:T(8,128)(2,1)S(1)}, bf16[192,2048]{1,0:T(8,128)(2,1)S(1)}, u32[]{:S(2)}, u32[]{:S(2)}) collective-permute-start(bf16[192,2048]{1,0:T(8,128)(2,1)S(1)} %collective-permute-done.2.refs_0_), channel_id=1, source_target_pairs={{0,2},{1,15},{2,4},{3,1},{4,6},{5,3},{6,8},{7,5},{8,10},{9,7},{10,... | collective-permute-start | bytes 2359304 | tf_op jit(solution)/shard_map/ppermute | solution.py:192
  81.8 6.7 %copy-start.8 = (s32[3]{0:T(128)S(1)}, s32[3]{0:T(128)}, u32[]{:S(2)}) copy-start(s32[3]{0:T(128)} %add_add_fusion.place) | copy-start | bytes 40
  88.5 8.4 %copy-start.7 = (s32[3]{0:T(128)S(1)}, s32[3]{0:T(128)}, u32[]{:S(2)}) copy-start(s32[3]{0:T(128)} %add_add_fusion.4.place) | copy-start | bytes 40
  99.3 3.2 %collective-permute-start.15 = (f32[2,128,128]{2,1,0:T(8,128)S(1)}, f32[2,128,128]{2,1,0:T(8,128)S(1)}, u32[]{:S(2)}, u32[]{:S(2)}) collective-permute-start(f32[2,128,128]{2,1,0:T(8,128)S(1)} %get-tuple-element.34), channel_id=1, source_target_pairs={{0,1},{1,0},{2,3},{3,2},{4,5},{5,4},{6,7},{7,6},{8,9},{9,8},{10,11... | collective-permute-start | bytes 393224 | tf_op jit(solution)/shard_map/ppermute | solution.py:185

commit v2 on v1

v2 whole, which is shorter than its diff:
```python
import jax
import jax.numpy as jnp
from jax import lax
from jax.experimental import pallas as pl
from jax.experimental.pallas import tpu as pltpu
from jax.sharding import Mesh
from jax.sharding import PartitionSpec as P

HEAD_DIM = 64
EPSILON = 1e-05
BF = jnp.bfloat16
F32 = jnp.float32
GRANT = pltpu.CompilerParams(vmem_limit_bytes=16 * 1024 * 1024)
VMEM = pl.BlockSpec(memory_space=pltpu.VMEM)
SMEM = pl.BlockSpec(memory_space=pltpu.SMEM)


def mm(a, b, dims, precision=None):
    return lax.dot_general(a, b, (dims, ((), ())), preferred_element_type=F32, precision=precision)


def softplus(v):
    return jnp.maximum(v, 0.0) + jnp.log1p(jnp.exp(-jnp.abs(v)))


def piece_states(meta, xs, far, end, w_step, w, jump, rates, runs, rows, chips):
    depth = w[0].shape[0] - 4
    many, both = len(xs), 2 * rows
    given = [] if runs is None else list(runs)

    def body(m_ref, *refs):
        x_refs = refs[:many]
        s_ref, wa_ref, wb_ref, j_ref, r_ref = refs[many : many + 5]
        ins = refs[many + 5 : many + 5 + len(given)]
        own_out, other_out, ext = refs[many + 5 + len(given) :]
        outs = (own_out, other_out)
        y, c = m_ref[0], m_ref[1]
        low = c == 0
        away = jnp.where(low, y - far, y + far)
        wrapped = jnp.logical_or(away < 0, away >= chips)
        chip = jnp.where(away < 0, away + chips, jnp.where(away >= chips, away - chips, away))
        run = 2 if end else jnp.where(wrapped, 1, 0)
        place = (2 * chip + c, 2 * chip + 1 - c)
        for g in range(2):
            if given:
                outs[g][...] = ins[g][...]
            else:
                outs[g][...] = jnp.zeros(outs[g].shape, F32)

        lane = lax.broadcasted_iota(jnp.int32, (8, both), 1)
        i = lax.broadcasted_iota(jnp.int32, (both, both), 0)
        j = lax.broadcasted_iota(jnp.int32, (both, both), 1)
        below = jnp.where(jnp.logical_and(i > j, (i >= rows) == (j >= rows)), 1.0, 0.0)
        sizes, afters, sums = [], [], []
        for n in range(many):
            step = mm(s_ref[...], x_refs[n][...], ((1,), (1,))).astype(BF).astype(F32)[:, :both]
            size = softplus(step + r_ref[0][:, 0:1])
            decay = j_ref[place[n]] - r_ref[1][:, 0:1] * size
            sizes.append(size)
            afters.append(mm(decay, below, ((1,), (0,)), lax.Precision.HIGHEST))
            sums.append([
                jnp.sum(jnp.where(lane < rows, decay, 0.0), axis=1, keepdims=True),
                jnp.sum(jnp.where(lane < rows, 0.0, decay), axis=1, keepdims=True),
            ])
        total = [sum(v[s] for v in sums) for s in range(2)]
        before = [own_out[run, s, 128:136, :] for s in range(2)]
        lead = [jnp.where(low, v[:, 0:1], 0.0) for v in before]
        lifts = []
        for n in range(many):
            more = list(lead)
            if many == 2:
                first = low if n == 0 else jnp.logical_not(low)
                more = [more[s] + jnp.where(first, sums[1 - n][s], 0.0) for s in range(2)]
            weight = sizes[n] * jnp.exp(afters[n] + jnp.where(lane < rows, more[0], more[1]))
            weight = jnp.concatenate([weight, jnp.zeros((8, 256 - both), F32)], axis=1)
            lifts.append(jnp.transpose(weight))

        taps = jnp.concatenate([r[depth : depth + 4, :] for r in (wa_ref, wb_ref)], axis=1).astype(F32)
        for n in range(many):
            x = x_refs[n][...]
            for g, r in enumerate((wa_ref, wb_ref)):
                p = mm(x, r[:depth, :], ((1,), (0,))).astype(BF).astype(F32)
                for s in range(2):
                    ext[2 * n + s, 4:8, 256 * g : 256 * g + 256] = p[both + 4 * s : both + 4 * s + 4, :]
                    ext[2 * n + s, 8 : 8 + rows, 256 * g : 256 * g + 256] = p[s * rows : (s + 1) * rows, :]
        for s in range(2):
            states = [jnp.zeros((128, 128), F32)] * 2
            for n in range(many):
                mixed = ext[2 * n + s, 5 : 5 + rows, :] * taps[0:1, :]
                for k in range(1, 4):
                    mixed = mixed + ext[2 * n + s, 5 + k : 5 + k + rows, :] * taps[k : k + 1, :]
                mixed = mixed / (1.0 + jnp.exp(-mixed))
                lift = lifts[n][s * rows : (s + 1) * rows, :]
                for g in range(2):
                    parts = [
                        mixed[:, 256 * g + 64 * e : 256 * g + 64 * e + 64] * lift[:, 2 * g + e : 2 * g + e + 1]
                        for e in range(2)
                    ]
                    values = jnp.concatenate(parts, axis=1).astype(BF)
                    keys = mixed[:, 256 * g + 128 : 256 * g + 256].astype(BF)
                    states[g] = states[g] + mm(values, keys, ((0,), (0,)))
            fade = jnp.where(low, 1.0, jnp.exp(total[s]))
            for g in range(2):
                for e in range(2):
                    part = slice(64 * e, 64 * e + 64)
                    old = outs[g][run, s, part, :]
                    outs[g][run, s, part, :] = old * fade[2 * g + e : 2 * g + e + 1, :] + states[g][part, :]
                outs[g][run, s, 128:136, :] = before[s] + total[s]

    shape = (3, 2, 136, 128)
    return pl.pallas_call(
        body,
        out_shape=[jax.ShapeDtypeStruct(shape, F32)] * 2,
        in_specs=[SMEM] + [VMEM] * (many + 5 + len(given)),
        out_specs=[VMEM] * 2,
        scratch_shapes=[pltpu.VMEM((2 * many, rows + 8, 512), F32)],
        cost_estimate=pl.CostEstimate(
            flops=32 * sum(x.shape[0] for x in xs) * w[0].size,
            transcendentals=0,
            bytes_accessed=4 * w[0].size,
        ),
        compiler_params=GRANT,
        name="piece_states",
    )(meta, *xs, w_step, *w, jump, rates, *given)


def joined(w_value, w_key, conv_value, conv_key):
    depth = w_value.shape[0]

    def body(v_ref, k_ref, cv_ref, ck_ref, out_ref):
        out_ref[:depth, :128] = v_ref[...]
        out_ref[:depth, 128:] = k_ref[...]
        out_ref[depth:, :128] = cv_ref[...]
        out_ref[depth:, 128:] = ck_ref[...]

    return pl.pallas_call(
        body,
        out_shape=jax.ShapeDtypeStruct((depth + conv_value.shape[0], 256), BF),
        in_specs=[VMEM] * 4,
        out_specs=VMEM,
        compiler_params=GRANT,
        name="joined",
    )(w_value, w_key, conv_value, conv_key)


def terms(step_bias, decay_rate, new_step, new_value, new_key, new_query, new_gate, read_gain):
    def body(b_ref, r_ref, n_ref, v_ref, k_ref, q_ref, g_ref, gain_ref, out_ref, query_ref):
        lane = lax.broadcasted_iota(jnp.int32, (1, 128), 1)

        def spread(a, b):
            return jnp.where(lane < HEAD_DIM, a, b)

        query = q_ref[...].astype(F32)
        query_ref[...] = query
        value, key, gate = (r[...].astype(F32) for r in (v_ref, k_ref, g_ref))
        match = jnp.sum(key * query, axis=1, keepdims=True)
        gates = gate / (1.0 + jnp.exp(-gate))
        rate = spread(r_ref[0], r_ref[1])
        for s in range(2):
            size = softplus(spread(n_ref[s, 0] + b_ref[0], n_ref[s, 1] + b_ref[1]))
            out_ref[s : s + 1, :] = jnp.exp(-rate * size)
            out_ref[2 + s : 3 + s, :] = size * match[s : s + 1, :] * value[s : s + 1, :]
        out_ref[4:6, :] = gates
        out_ref[6:7, :] = gain_ref[...].astype(F32)
        out_ref[7:8, :] = jnp.zeros((1, 128), F32)

    return pl.pallas_call(
        body,
        out_shape=[jax.ShapeDtypeStruct((8, 128), F32), jax.ShapeDtypeStruct((2, 128), F32)],
        in_specs=[SMEM] * 3 + [VMEM] * 5,
        out_specs=[VMEM] * 2,
        compiler_params=GRANT,
        name="terms",
    )(step_bias, decay_rate, new_step, new_value, new_key, new_query, new_gate, read_gain.reshape(1, 128))


def packed(meta, own, got, query, sp_count, chips):
    share = HEAD_DIM // sp_count

    def body(m_ref, a_ref, b_ref, q_ref, out_ref):
        def put(row, value):
            out_ref[:, row : row + 1, :] = jnp.broadcast_to(value[None], (sp_count, 1, 128))

        low = m_ref[1] == 0
        late = m_ref[0] < chips // 2
        lane = lax.broadcasted_iota(jnp.int32, (1, 128), 1)
        left = jnp.zeros((1, 128), F32)
        for s in range(2):
            mine = [a_ref[r, s, 128:130, :] for r in range(3)]
            theirs = [b_ref[r, s, 130:132, :] for r in range(3)]
            d1, d2, d3 = (jnp.where(low, m, t) for m, t in zip(mine, theirs))
            u1, u2, u3 = (jnp.where(low, t, m) for m, t in zip(mine, theirs))
            last = d3 + u3
            after_u1 = d2 + jnp.where(late, last, 0.0)
            after_d1 = after_u1 + u1
            after_u3 = jnp.where(late, d2, after_d1 + d1)
            after_d3 = after_u3 + u3
            after_u2 = after_d1 + d1 + jnp.where(late, 0.0, last)
            total = after_u2 + u2
            for e in range(2):
                left = jnp.where(lane == 2 * s + e, total[e : e + 1, :], left)
            down = [jnp.exp(v) for v in (after_d1, jnp.zeros_like(d2), after_d3)]
            up = [jnp.exp(v) for v in (after_u1, after_u2, after_u3)]
            reads = []
            for e in range(2):
                state = jnp.zeros((64, 128), F32)
                for r in range(3):
                    part = slice(64 * e, 64 * e + 64)
                    scale_a = jnp.where(low, down[r], up[r])[e : e + 1, :]
                    scale_b = jnp.where(low, up[r], down[r])[e : e + 1, :]
                    state = state + a_ref[r, s, part, :] * scale_a + b_ref[r, s, part, :] * scale_b
                reads.append(jnp.sum(state * q_ref[s : s + 1, :], axis=1).reshape(1, 64))
                cut = state.astype(BF).reshape(sp_count, share, 128)
                out_ref[:, 4 * s + 2 * e : 4 * s + 2 * e + share, :] = cut
            read = jnp.concatenate(reads, axis=1)
            high = read.astype(BF)
            put(8 + s, high)
            put(10 + s, (read - high.astype(F32)).astype(BF))
        for k in range(3):
            part = left.astype(BF)
            left = left - part.astype(F32)
            put(12 + k, part)
        put(15, jnp.zeros((1, 128), BF))

    return pl.pallas_call(
        body,
        out_shape=jax.ShapeDtypeStruct((sp_count, 16, 128), BF),
        in_specs=[SMEM] + [VMEM] * 3,
        out_specs=VMEM,
        compiler_params=GRANT,
        name="packed",
    )(meta, own, got, query)


def finished(meta, got, fixed):
    sp_count = got.shape[0]

    def body(m_ref, got_ref, fix_ref, state_out, read_out):
        run = jnp.zeros((1, 128), F32)
        total = jnp.zeros((16, 128), F32)
        for j in reversed(range(sp_count)):
            g = got_ref[j].astype(F32)
            e = jnp.exp(run)
            one = [jnp.broadcast_to(e[:, i : i + 1], (1, 128)) for i in range(4)]
            both = [jnp.concatenate([one[2 * s][:, :64], one[2 * s + 1][:, 64:]], axis=1) for s in range(2)]
            scale = jnp.concatenate([one[i // 2] for i in range(8)] + both * 4, axis=0)
            total = total + g * scale
            run = run + g[12:13] + g[13:14] + g[14:15]
        for s in range(2):
            for h in range(2):
                state_out[s, h] = total[4 * s + 2 * h : 4 * s + 2 * h + 2].astype(BF)
        read = total[8:10] + total[10:12]
        gated = (fix_ref[0:2] * read + fix_ref[2:4]) * fix_ref[4:6]
        mean = jnp.mean(gated * gated, axis=1, keepdims=True)
        out = gated * lax.rsqrt(mean + EPSILON) * fix_ref[6:7]
        out = jnp.concatenate([out, jnp.zeros((6, 128), F32)], axis=0)
        out = pltpu.roll(out, m_ref[2], 1)
        for s in range(2):
            for h in range(2):
                read_out[s, h : h + 1, :] = out[s : s + 1, 64 * h : 64 * h + 2].astype(BF)

    return pl.pallas_call(
        body,
        out_shape=[jax.ShapeDtypeStruct((2, 2, 2, 128), BF), jax.ShapeDtypeStruct((2, 2, 2), BF)],
        in_specs=[SMEM, VMEM, VMEM],
        out_specs=[VMEM] * 2,
        compiler_params=GRANT,
        name="finished",
    )(meta, got, fixed)


def per_device(
    hidden_in, w_value, w_key, w_step, conv_value, conv_key, step_bias, decay_rate, decay_jump,
    new_value, new_key, new_query, new_gate, new_step, read_gain,
):
    sp_count, y_count, c_count = (lax.axis_size(a) for a in ("sp", "y", "c"))
    sp, y, c = (lax.axis_index(a) for a in ("sp", "y", "c"))
    tp_count = y_count * c_count
    count = sp_count * tp_count
    rows, width = hidden_in.shape[1:]
    heads = step_bias.shape[0]
    share = HEAD_DIM // sp_count
    half = y_count // 2

    def swap(v):
        return lax.ppermute(v, "c", [(0, 1), (1, 0)])

    def onward(v):
        pairs = []
        for i in range(y_count):
            pairs.append((2 * i, 2 * ((i + 1) % y_count)))
            pairs.append((2 * i + 1, 2 * ((i - 1) % y_count) + 1))
        return lax.ppermute(v, ("y", "c"), pairs)

    meta = jnp.stack([y, c, (128 - sp * share) % 128]).astype(jnp.int32)

    ends = hidden_in[:, rows - 4 :, :].reshape(8, width)
    ends = lax.ppermute(ends, ("sp", "y", "c"), [(i, i + 1) for i in range(count - 1)])
    a = [jnp.concatenate([hidden_in.reshape(2 * rows, width), ends], axis=0)]
    a.append(onward(a[0]))
    b = [swap(a[0])]
    b.append(onward(b[0]))

    w_own = joined(w_value, w_key, conv_value, conv_key)
    w_both = w_own, swap(w_own)
    pair = lax.dynamic_slice_in_dim(w_step.T, y * 2 * heads, 2 * heads, 0)
    pair = jnp.where(c == 0, pair, jnp.roll(pair, heads, axis=0))
    w_steps = jnp.pad(pair, ((0, 8 - 2 * heads), (0, 0)))
    rates = jnp.broadcast_to(jnp.stack([step_bias, decay_rate])[:, :, None], (2, heads, 128))
    jump = jnp.concatenate([decay_jump.transpose(0, 2, 1), rates], axis=2)
    jump = jnp.concatenate([jump, swap(jump)], axis=1)
    jump = jnp.pad(jump, ((0, 0), (0, 8 - 2 * heads), (0, 0)))
    rates = jump[:, :, tp_count * rows :]
    jump = jump[:, :, : tp_count * rows].reshape(2, 8, tp_count, rows).transpose(2, 1, 0, 3)
    jump = jump.reshape(tp_count, 8, 2 * rows)

    def add(runs, xs, far, end):
        return piece_states(meta, xs, far, end, w_steps, w_both, jump, rates, runs, rows, y_count)

    runs = add(None, [a[0]], 0, False)
    for s in range(1, half):
        a.append(onward(a[s]))
        if s + 1 < half:
            b.append(onward(b[s]))
        runs = add(runs, [a[s], b[s]], s, False)

    fixed, query = terms(step_bias, decay_rate, new_step, new_value, new_key, new_query, new_gate, read_gain)
    runs, fixed, query = lax.optimization_barrier((runs, fixed, query))
    own, other = add(runs, [a[half]], half, True)
    sent = packed(meta, own, swap(other), query, sp_count, y_count)
    got = lax.all_to_all(sent, "sp", 0, 0, tiled=True)
    return tuple(finished(meta, got, fixed))


def solution(mesh):
    tp = ("y", "c")
    chips = Mesh(mesh.devices.reshape(mesh.shape["sp"], mesh.shape["tp"] // 2, 2), ("sp", *tp))

    return jax.shard_map(
        per_device,
        mesh=chips,
        in_specs=(
            P(None, ("sp", *tp), None), P(None, tp), P(None, tp), P(), P(None, tp), P(None, tp), P(tp), P(tp),
            P(None, "sp", tp), P(None, tp), P(None, tp), P(None, tp), P(None, tp), P(None, tp), P(tp),
        ),
        out_specs=(P(None, tp, "sp", None), P(None, tp, "sp")),
        check_vma=False,
    )
```

time: 127 us -> 114 us (0.90)
  the two profiles are of different devices: /device:TPU:16 before, /device:TPU:1 now
where the time goes in v2:
time: 114 us; the launch traced here: 113 us
  starting transfers between devices  40.8 us (36%)
  waiting for transfers between devices  23.8 us (21%)
  blocking collectives  22.4 us (20%)
  Pallas kernels  20.9 us (18%)
  local copies, waits for them, and re-layouts  2.24 us (2%)
  other arithmetic  2.12 us (2%)
    ppermute x7, starting transfers between devices, onward(): return lax.ppermute(v, ('y', 'c'), pairs)  25.9 us
    all_to_all x1, blocking collectives, per_device(): got = lax.all_to_all(sent, 'sp', 0, 0, tiled=True)  22.4 us
    ppermute x7, waiting for transfers between devices, onward(): return lax.ppermute(v, ('y', 'c'), pairs)  18.2 us
    pallas_call x5, Pallas kernels, piece_states(): pl.pallas_call(body, out_shape=[jax.ShapeDtypeStruct(shape, F32)] * 2, in...  17.7 us
    ppermute x4, starting transfers between devices, swap(): return lax.ppermute(v, 'c', [(0, 1), (1, 0)])  10.4 us
    ppermute x1, starting transfers between devices, per_device(): lax.ppermute(ends, ('sp', 'y', 'c'), [(i, i + 1) for i in range(count - 1)])  4.58 us
    ppermute x1, waiting for transfers between devices, per_device(): lax.ppermute(ends, ('sp', 'y', 'c'), [(i, i + 1) for i in range(count - 1)])  4.22 us
  transfers between devices with their start and end apart: 12, of which 9 were waited for; matrix products, arithmetic and copies ran while one was open for 2% of the time, Pallas kernels for 14%

profile of v2, /device:TPU:1, one launch (start us, length us, event | category | flops | bytes accessed | tf_op | source)
XLA Modules:
  0.0 113.4 jit_solution(7529871931123702700)
XLA Ops:
  0.7 0.9 slice.17
  1.6 4.6 %collective-permute-start = (bf16[8,2048]{1,0:T(8,128)(2,1)S(1)}, bf16[8,2048]{1,0:T(8,128)(2,1)S(1)}, u32[]{:S(2)}, u32[]{:S(2)}) collective-permute-start(bf16[8,2048]{1,0:T(8,128)(2,1)S(1)} %reshape.21), channel_id=1, source_target_pairs={{0,1},{1,2},{2,3},{3,4},{4,5},{5,6},{6,7},{7,8},{8,9},{9,10},{10,1... | collective-permute-start | bytes 98312 | tf_op jit(solution)/shard_map/ppermute | solution.py:298
  6.2 4.2 %collective-permute-done = bf16[8,2048]{1,0:T(8,128)(2,1)S(1)} collective-permute-done((bf16[8,2048]{1,0:T(8,128)(2,1)S(1)}, bf16[8,2048]{1,0:T(8,128)(2,1)S(1)}, u32[]{:S(2)}, u32[]{:S(2)}) %collective-permute-start) | collective-permute-done | bytes 32800 | tf_op jit(solution)/shard_map/ppermute | solution.py:298
  10.5 1.2 %pad_maximum_fusion.refs_0_ = bf16[200,2048]{1,0:T(8,128)(2,1)S(1)} fusion(bf16[8,2048]{1,0:T(8,128)(2,1)S(1)} %collective-permute-done, bf16[192,2048]{1,0:T(8,128)(2,1)} %bitcast.16), kind=kLoop, calls=%fused_computation | loop fusion | flops 1638400 | bytes 1638400 | tf_op jit(solution)/shard_map/concatenate | solution.py:299
  11.6 0.0 copy-start.2
  11.7 0.0 copy-start.3
  11.7 0.0 copy-start.12
  11.7 0.0 copy-start.6
  11.7 0.0 copy-start.7
  11.7 0.0 copy-start.8
  11.7 0.0 copy-start.9
  11.7 0.0 copy-start.11
  11.8 2.2 %collective-permute-start.7 = (bf16[200,2048]{1,0:T(8,128)(2,1)S(1)}, bf16[200,2048]{1,0:T(8,128)(2,1)}, u32[]{:S(2)}, u32[]{:S(2)}) collective-permute-start(bf16[200,2048]{1,0:T(8,128)(2,1)S(1)} %pad_maximum_fusion.refs_0_), channel_id=1, source_target_pairs={{0,1},{1,0},{2,3},{3,2},{4,5},{5,4},{6,7},{7,6},{8,9},{9,8},{10,11... | collective-permute-start | bytes 2457608 | tf_op jit(solution)/shard_map/ppermute | solution.py:286
  14.0 2.8 %collective-permute-start.1 = (bf16[200,2048]{1,0:T(8,128)(2,1)S(1)}, bf16[200,2048]{1,0:T(8,128)(2,1)}, u32[]{:S(2)}, u32[]{:S(2)}) collective-permute-start(bf16[200,2048]{1,0:T(8,128)(2,1)S(1)} %pad_maximum_fusion.refs_0_), channel_id=1, source_target_pairs={{0,2},{1,15},{2,4},{3,1},{4,6},{5,3},{6,8},{7,5},{8,10},{9,7},{10,... | collective-permute-start | bytes 2457608 | tf_op jit(solution)/shard_map/ppermute | solution.py:293
  16.9 0.2 joined.1.refs_2_.refs_3_
  17.0 1.9 %collective-permute-start.5 = (bf16[2052,256]{1,0:T(8,128)(2,1)S(1)}, bf16[2052,256]{1,0:T(8,128)(2,1)}, u32[]{:S(2)}, u32[]{:S(2)}) collective-permute-start(bf16[2052,256]{1,0:T(8,128)(2,1)S(1)} %joined.1.refs_2_.refs_3_), channel_id=1, source_target_pairs={{0,1},{1,0},{2,3},{3,2},{4,5},{5,4},{6,7},{7,6},{8,9},{9,8},{10,11... | collective-permute-start | bytes 3151880 | tf_op jit(solution)/shard_map/ppermute | solution.py:286
  19.0 4.3 %collective-permute-start.8 = (bf16[200,2048]{1,0:T(8,128)(2,1)}, bf16[200,2048]{1,0:T(8,128)(2,1)S(1)}, u32[]{:S(2)}, u32[]{:S(2)}) collective-permute-start(bf16[200,2048]{1,0:T(8,128)(2,1)} %collective-permute-done.7), channel_id=1, source_target_pairs={{0,2},{1,15},{2,4},{3,1},{4,6},{5,3},{6,8},{7,5},{8,10},{9,7},{10,... | collective-permute-start | bytes 2457608 | tf_op jit(solution)/shard_map/ppermute | solution.py:293
  23.3 0.1 broadcast_in_dim.2
  23.4 1.9 %collective-permute-start.6 = (f32[2,2,1664]{2,1,0:T(2,128)S(1)}, f32[2,2,1664]{2,1,0:T(2,128)S(1)}, u32[]{:S(2)}, u32[]{:S(2)}) collective-permute-start(f32[2,2,1664]{2,1,0:T(2,128)S(1)} %pad_maximum_fusion.1), channel_id=1, source_target_pairs={{0,1},{1,0},{2,3},{3,2},{4,5},{5,4},{6,7},{7,6},{8,9},{9,8},{10,11... | collective-permute-start | bytes 79880 | tf_op jit(solution)/shard_map/ppermute | solution.py:286
  25.3 0.8 dynamic-slice_bitcast_fusion
  26.1 1.3 %collective-permute-done.1.refs_0_ = bf16[200,2048]{1,0:T(8,128)(2,1)} collective-permute-done((bf16[200,2048]{1,0:T(8,128)(2,1)S(1)}, bf16[200,2048]{1,0:T(8,128)(2,1)}, u32[]{:S(2)}, u32[]{:S(2)}) %collective-permute-start.1) | collective-permute-done | bytes 819232 | tf_op jit(solution)/shard_map/ppermute | solution.py:293
  27.4 3.8 %collective-permute-start.2 = (bf16[200,2048]{1,0:T(8,128)(2,1)}, bf16[200,2048]{1,0:T(8,128)(2,1)}, u32[]{:S(2)}, u32[]{:S(2)}) collective-permute-start(bf16[200,2048]{1,0:T(8,128)(2,1)} %collective-permute-done.1.refs_0_), channel_id=1, source_target_pairs={{0,2},{1,15},{2,4},{3,1},{4,6},{5,3},{6,8},{7,5},{8,10},{9,7},{10,... | collective-permute-start | bytes 2457608 | tf_op jit(solution)/shard_map/ppermute | solution.py:293
  31.2 4.9 %collective-permute-done.8.refs_1_ = bf16[200,2048]{1,0:T(8,128)(2,1)S(1)} collective-permute-done((bf16[200,2048]{1,0:T(8,128)(2,1)}, bf16[200,2048]{1,0:T(8,128)(2,1)S(1)}, u32[]{:S(2)}, u32[]{:S(2)}) %collective-permute-start.8) | collective-permute-done | bytes 819232 | tf_op jit(solution)/shard_map/ppermute | solution.py:293
  36.1 3.8 %collective-permute-start.9 = (bf16[200,2048]{1,0:T(8,128)(2,1)S(1)}, bf16[200,2048]{1,0:T(8,128)(2,1)}, u32[]{:S(2)}, u32[]{:S(2)}) collective-permute-start(bf16[200,2048]{1,0:T(8,128)(2,1)S(1)} %collective-permute-done.8.refs_1_), channel_id=1, source_target_pairs={{0,2},{1,15},{2,4},{3,1},{4,6},{5,3},{6,8},{7,5},{8,10},{9,7},{10,... | collective-permute-start | bytes 2457608 | tf_op jit(solution)/shard_map/ppermute | solution.py:293
  39.9 0.8 maximum_select_fusion
  40.7 0.1 pad_add_fusion.m_ref
  40.8 0.6 terms.1
  41.5 0.1 reshape.22
  41.6 0.1 copy.17
  41.8 0.1 reshape.23.refs_4_.refs_5_
  41.9 3.1 %collective-permute-done.2.refs_0_ = bf16[200,2048]{1,0:T(8,128)(2,1)} collective-permute-done((bf16[200,2048]{1,0:T(8,128)(2,1)}, bf16[200,2048]{1,0:T(8,128)(2,1)}, u32[]{:S(2)}, u32[]{:S(2)}) %collective-permute-start.2) | collective-permute-done | bytes 819232 | tf_op jit(solution)/shard_map/ppermute | solution.py:293
  45.0 3.8 %collective-permute-start.3 = (bf16[200,2048]{1,0:T(8,128)(2,1)}, bf16[200,2048]{1,0:T(8,128)(2,1)S(1)}, u32[]{:S(2)}, u32[]{:S(2)}) collective-permute-start(bf16[200,2048]{1,0:T(8,128)(2,1)} %collective-permute-done.2.refs_0_), channel_id=1, source_target_pairs={{0,2},{1,15},{2,4},{3,1},{4,6},{5,3},{6,8},{7,5},{8,10},{9,7},{10,... | collective-permute-start | bytes 2457608 | tf_op jit(solution)/shard_map/ppermute | solution.py:293
  48.8 2.9 %piece_states.5 = (f32[3,2,136,128]{3,2,1,0:T(8,128)S(1)}, f32[3,2,136,128]{3,2,1,0:T(8,128)S(1)}) custom-call(s32[3]{0:T(128)S(1)} %pad_add_fusion.m_ref, bf16[200,2048]{1,0:T(8,128)(2,1)S(1)} %pad_maximum_fusion.refs_0_, bf16[8,2048]{1,0:T(8,128)(2,1)S(1)} %pad.8.refs_1_.refs_2_, bf16[2052,256]{1,0:T(8,128)(2,1)S(1)} %joined.1.refs_2_.refs_3_, ...), custom_call_target="tpu_custom_call" | custom-call | flops 3361996800 | bytes 2101248 | tf_op jit(solution)/shard_map/piece_states/pallas_call | solution.py:111
  51.6 2.1 %collective-permute-done.9.refs_1_ = bf16[200,2048]{1,0:T(8,128)(2,1)} collective-permute-done((bf16[200,2048]{1,0:T(8,128)(2,1)S(1)}, bf16[200,2048]{1,0:T(8,128)(2,1)}, u32[]{:S(2)}, u32[]{:S(2)}) %collective-permute-start.9) | collective-permute-done | bytes 819232 | tf_op jit(solution)/shard_map/ppermute | solution.py:293
  53.8 3.8 %collective-permute-start.10 = (bf16[200,2048]{1,0:T(8,128)(2,1)}, bf16[200,2048]{1,0:T(8,128)(2,1)S(1)}, u32[]{:S(2)}, u32[]{:S(2)}) collective-permute-start(bf16[200,2048]{1,0:T(8,128)(2,1)} %collective-permute-done.9.refs_1_), channel_id=1, source_target_pairs={{0,2},{1,15},{2,4},{3,1},{4,6},{5,3},{6,8},{7,5},{8,10},{9,7},{10,... | collective-permute-start | bytes 2457608 | tf_op jit(solution)/shard_map/ppermute | solution.py:293
  57.5 4.0 %piece_states.6 = (f32[3,2,136,128]{3,2,1,0:T(8,128)S(1)}, f32[3,2,136,128]{3,2,1,0:T(8,128)S(1)}) custom-call(s32[3]{0:T(128)S(1)} %pad_add_fusion.m_ref, bf16[200,2048]{1,0:T(8,128)(2,1)} %collective-permute-done.1.refs_0_, bf16[200,2048]{1,0:T(8,128)(2,1)S(1)} %collective-permute-done.8.refs_1_, bf16[8,2048]{1,0:T(8,128)(2,1)S(1)} %pad.8.refs_1_.refs_2_, ...), custom_call_target="tpu_custom_call" | custom-call | flops 6723993600 | bytes 2101248 | tf_op jit(solution)/shard_map/piece_states/pallas_call | solution.py:111
  61.5 0.9 collective-permute-done.3.refs_0_
  62.5 3.8 %collective-permute-start.4 = (bf16[200,2048]{1,0:T(8,128)(2,1)S(1)}, bf16[200,2048]{1,0:T(8,128)(2,1)S(1)}, u32[]{:S(2)}, u32[]{:S(2)}) collective-permute-start(bf16[200,2048]{1,0:T(8,128)(2,1)S(1)} %collective-permute-done.3.refs_0_), channel_id=1, source_target_pairs={{0,2},{1,15},{2,4},{3,1},{4,6},{5,3},{6,8},{7,5},{8,10},{9,7},{10,... | collective-permute-start | bytes 2457608 | tf_op jit(solution)/shard_map/ppermute | solution.py:293
  66.2 4.2 %piece_states.7 = (f32[3,2,136,128]{3,2,1,0:T(8,128)S(1)}, f32[3,2,136,128]{3,2,1,0:T(8,128)S(1)}) custom-call(s32[3]{0:T(128)S(1)} %pad_add_fusion.m_ref, bf16[200,2048]{1,0:T(8,128)(2,1)} %collective-permute-done.2.refs_0_, bf16[200,2048]{1,0:T(8,128)(2,1)} %collective-permute-done.9.refs_1_, bf16[8,2048]{1,0:T(8,128)(2,1)S(1)} %pad.8.refs_1_.refs_2_, ...), custom_call_target="tpu_custom_call" | custom-call | flops 6723993600 | bytes 2101248 | tf_op jit(solution)/shard_map/piece_states/pallas_call | solution.py:111
  70.4 0.8 collective-permute-done.10.refs_1_
  71.2 3.8 %piece_states.8 = (f32[3,2,136,128]{3,2,1,0:T(8,128)S(1)}, f32[3,2,136,128]{3,2,1,0:T(8,128)S(1)}) custom-call(s32[3]{0:T(128)S(1)} %pad_add_fusion.m_ref, bf16[200,2048]{1,0:T(8,128)(2,1)S(1)} %collective-permute-done.3.refs_0_, bf16[200,2048]{1,0:T(8,128)(2,1)S(1)} %collective-permute-done.10.refs_1_, bf16[8,2048]{1,0:T(8,128)(2,1)S(1)} %pad.8.refs_1_.refs_2_, ...), custom_call_target="tpu_custom_call" | custom-call | flops 6723993600 | bytes 2101248 | tf_op jit(solution)/shard_map/piece_states/pallas_call | solution.py:111
  75.0 5.0 %collective-permute-done.4.refs_0_ = bf16[200,2048]{1,0:T(8,128)(2,1)S(1)} collective-permute-done((bf16[200,2048]{1,0:T(8,128)(2,1)S(1)}, bf16[200,2048]{1,0:T(8,128)(2,1)S(1)}, u32[]{:S(2)}, u32[]{:S(2)}) %collective-permute-start.4) | collective-permute-done | bytes 819232 | tf_op jit(solution)/shard_map/ppermute | solution.py:293
  80.0 2.8 %piece_states.9 = (f32[3,2,136,128]{3,2,1,0:T(8,128)S(1)}, f32[3,2,136,128]{3,2,1,0:T(8,128)S(1)}) custom-call(s32[3]{0:T(128)S(1)} %pad_add_fusion.m_ref, bf16[200,2048]{1,0:T(8,128)(2,1)S(1)} %collective-permute-done.4.refs_0_, bf16[8,2048]{1,0:T(8,128)(2,1)S(1)} %pad.8.refs_1_.refs_2_, bf16[2052,256]{1,0:T(8,128)(2,1)S(1)} %joined.1.refs_2_.refs_3_, ...), custom_call_target="tpu_custom_call" | custom-call | flops 3361996800 | bytes 2101248 | tf_op jit(solution)/shard_map/piece_states/pallas_call | solution.py:111
  82.8 4.3 %collective-permute-start.11 = (f32[3,2,136,128]{3,2,1,0:T(8,128)S(1)}, f32[3,2,136,128]{3,2,1,0:T(8,128)S(1)}, u32[]{:S(2)}, u32[]{:S(2)}) collective-permute-start(f32[3,2,136,128]{3,2,1,0:T(8,128)S(1)} %get-tuple-element.31), channel_id=1, source_target_pairs={{0,1},{1,0},{2,3},{3,2},{4,5},{5,4},{6,7},{7,6},{8,9},{9,8},{10,11... | collective-permute-start | bytes 1253384 | tf_op jit(solution)/shard_map/ppermute | solution.py:286
  87.2 1.4 %collective-permute-done.11.b_ref = f32[3,2,136,128]{3,2,1,0:T(8,128)S(1)} collective-permute-done((f32[3,2,136,128]{3,2,1,0:T(8,128)S(1)}, f32[3,2,136,128]{3,2,1,0:T(8,128)S(1)}, u32[]{:S(2)}, u32[]{:S(2)}) %collective-permute-start.11) | collective-permute-done | bytes 417824 | tf_op jit(solution)/shard_map/ppermute | solution.py:286
  88.5 0.8 packed.1
  89.4 22.4 %all_to_all.5.got_ref = bf16[32,16,128]{2,1,0:T(8,128)(2,1)S(1)} all-to-all(bf16[32,16,128]{2,1,0:T(8,128)(2,1)S(1)} %packed.1), channel_id=1, replica_groups=mesh['sp'=32,'y'=8,'c'=2] {'sp'}, dimensions={0} | all-to-all | bytes 262144 | tf_op jit(solution)/shard_map/all_to_all | solution.py:331
  111.8 1.6 %finished.1 = (bf16[2,2,2,128]{3,2,1,0:T(2,128)(2,1)}, bf16[2,2,2]{2,1,0:T(2,128)(2,1)}) custom-call(s32[3]{0:T(128)S(1)} %pad_add_fusion.m_ref, bf16[32,16,128]{2,1,0:T(8,128)(2,1)S(1)} %all_to_all.5.got_ref, f32[8,128]{1,0:T(8,128)S(1)} %get-tuple-element.33.fix_ref), custom_call_target="tpu_custom_call" | custom-call | tf_op jit(solution)/shard_map/finished/pallas_call | solution.py:262
  (29 shorter events, 0.2 us)
Async XLA Ops:
  0.6 16.2 %copy-start = (bf16[2048,128]{1,0:T(8,128)(2,1)S(1)}, bf16[2048,128]{1,0:T(8,128)(2,1)}, u32[]{:S(2)}) copy-start(bf16[2048,128]{1,0:T(8,128)(2,1)} %v_ref.2) | copy-start | bytes 1572868
  0.6 16.2 %copy-start.1 = (bf16[2048,128]{1,0:T(8,128)(2,1)S(1)}, bf16[2048,128]{1,0:T(8,128)(2,1)}, u32[]{:S(2)}) copy-start(bf16[2048,128]{1,0:T(8,128)(2,1)} %k_ref.2) | copy-start | bytes 1572868
  0.7 16.2 %copy-start.4 = (bf16[4,128]{1,0:T(4,128)(2,1)S(1)}, bf16[4,128]{1,0:T(4,128)(2,1)}, u32[]{:S(2)}) copy-start(bf16[4,128]{1,0:T(4,128)(2,1)} %cv_ref.1) | copy-start | bytes 3076
  0.7 16.2 %copy-start.5 = (bf16[4,128]{1,0:T(4,128)(2,1)S(1)}, bf16[4,128]{1,0:T(4,128)(2,1)}, u32[]{:S(2)}) copy-start(bf16[4,128]{1,0:T(4,128)(2,1)} %ck_ref.1) | copy-start | bytes 3076
  1.6 8.8 %collective-permute-start = (bf16[8,2048]{1,0:T(8,128)(2,1)S(1)}, bf16[8,2048]{1,0:T(8,128)(2,1)S(1)}, u32[]{:S(2)}, u32[]{:S(2)}) collective-permute-start(bf16[8,2048]{1,0:T(8,128)(2,1)S(1)} %reshape.21), channel_id=1, source_target_pairs={{0,1},{1,2},{2,3},{3,4},{4,5},{5,6},{6,7},{7,8},{8,9},{9,10},{10,1... | collective-permute-start | bytes 98312 | tf_op jit(solution)/shard_map/ppermute | solution.py:298
  11.6 7.3 %copy-start.2 = (f32[2]{0:T(128)S(1)}, f32[2]{0:T(128)}, u32[]{:S(2)}) copy-start(f32[2]{0:T(128)} %r_ref.1) | copy-start | bytes 28
  11.7 7.3 %copy-start.3 = (f32[2]{0:T(128)S(1)}, f32[2]{0:T(128)}, u32[]{:S(2)}) copy-start(f32[2]{0:T(128)} %b_ref.1) | copy-start | bytes 28
  11.7 11.7 %copy-start.12 = (f32[2,1536,2]{1,2,0:T(2,128)S(1)}, f32[2,1536,2]{1,2,0:T(2,128)}, u32[]{:S(2)}) copy-start(f32[2,1536,2]{1,2,0:T(2,128)} %param.23) | copy-start | bytes 73732
  11.7 29.1 %copy-start.6 = (f32[2,2]{1,0:T(2,128)S(1)}, f32[2,2]{1,0:T(2,128)}, u32[]{:S(2)}) copy-start(f32[2,2]{1,0:T(2,128)} %n_ref.1) | copy-start | bytes 52
  11.7 29.1 %copy-start.7 = (bf16[2,128]{1,0:T(2,128)(2,1)S(1)}, bf16[2,128]{1,0:T(2,128)(2,1)}, u32[]{:S(2)}) copy-start(bf16[2,128]{1,0:T(2,128)(2,1)} %v_ref.3) | copy-start | bytes 1540
  11.7 29.1 %copy-start.8 = (bf16[2,128]{1,0:T(2,128)(2,1)S(1)}, bf16[2,128]{1,0:T(2,128)(2,1)}, u32[]{:S(2)}) copy-start(bf16[2,128]{1,0:T(2,128)(2,1)} %k_ref.3) | copy-start | bytes 1540
  11.7 29.1 %copy-start.9 = (bf16[2,128]{1,0:T(2,128)(2,1)S(1)}, bf16[2,128]{1,0:T(2,128)(2,1)}, u32[]{:S(2)}) copy-start(bf16[2,128]{1,0:T(2,128)(2,1)} %q_ref.1) | copy-start | bytes 1540
  11.7 29.1 %copy-start.10 = (bf16[2,128]{1,0:T(2,128)(2,1)S(1)}, bf16[2,128]{1,0:T(2,128)(2,1)}, u32[]{:S(2)}) copy-start(bf16[2,128]{1,0:T(2,128)(2,1)} %g_ref.1) | copy-start | bytes 1540
  11.7 29.1 %copy-start.11 = (bf16[128]{0:T(256)(128)(2,1)S(1)}, bf16[128]{0:T(256)(128)(2,1)}, u32[]{:S(2)}) copy-start(bf16[128]{0:T(256)(128)(2,1)} %param.29) | copy-start | bytes 772
  11.8 7.3 %collective-permute-start.7 = (bf16[200,2048]{1,0:T(8,128)(2,1)S(1)}, bf16[200,2048]{1,0:T(8,128)(2,1)}, u32[]{:S(2)}, u32[]{:S(2)}) collective-permute-start(bf16[200,2048]{1,0:T(8,128)(2,1)S(1)} %pad_maximum_fusion.refs_0_), channel_id=1, source_target_pairs={{0,1},{1,0},{2,3},{3,2},{4,5},{5,4},{6,7},{7,6},{8,9},{9,8},{10,11... | collective-permute-start | bytes 2457608 | tf_op jit(solution)/shard_map/ppermute | solution.py:286
  14.0 13.5 %collective-permute-start.1 = (bf16[200,2048]{1,0:T(8,128)(2,1)S(1)}, bf16[200,2048]{1,0:T(8,128)(2,1)}, u32[]{:S(2)}, u32[]{:S(2)}) collective-permute-start(bf16[200,2048]{1,0:T(8,128)(2,1)S(1)} %pad_maximum_fusion.refs_0_), channel_id=1, source_target_pairs={{0,2},{1,15},{2,4},{3,1},{4,6},{5,3},{6,8},{7,5},{8,10},{9,7},{10,... | collective-permute-start | bytes 2457608 | tf_op jit(solution)/shard_map/ppermute | solution.py:293
  17.0 31.7 %collective-permute-start.5 = (bf16[2052,256]{1,0:T(8,128)(2,1)S(1)}, bf16[2052,256]{1,0:T(8,128)(2,1)}, u32[]{:S(2)}, u32[]{:S(2)}) collective-permute-start(bf16[2052,256]{1,0:T(8,128)(2,1)S(1)} %joined.1.refs_2_.refs_3_), channel_id=1, source_target_pairs={{0,1},{1,0},{2,3},{3,2},{4,5},{5,4},{6,7},{7,6},{8,9},{9,8},{10,11... | collective-permute-start | bytes 3151880 | tf_op jit(solution)/shard_map/ppermute | solution.py:286
  19.0 17.1 %collective-permute-start.8 = (bf16[200,2048]{1,0:T(8,128)(2,1)}, bf16[200,2048]{1,0:T(8,128)(2,1)S(1)}, u32[]{:S(2)}, u32[]{:S(2)}) collective-permute-start(bf16[200,2048]{1,0:T(8,128)(2,1)} %collective-permute-done.7), channel_id=1, source_target_pairs={{0,2},{1,15},{2,4},{3,1},{4,6},{5,3},{6,8},{7,5},{8,10},{9,7},{10,... | collective-permute-start | bytes 2457608 | tf_op jit(solution)/shard_map/ppermute | solution.py:293
  23.4 18.1 %collective-permute-start.6 = (f32[2,2,1664]{2,1,0:T(2,128)S(1)}, f32[2,2,1664]{2,1,0:T(2,128)S(1)}, u32[]{:S(2)}, u32[]{:S(2)}) collective-permute-start(f32[2,2,1664]{2,1,0:T(2,128)S(1)} %pad_maximum_fusion.1), channel_id=1, source_target_pairs={{0,1},{1,0},{2,3},{3,2},{4,5},{5,4},{6,7},{7,6},{8,9},{9,8},{10,11... | collective-permute-start | bytes 79880 | tf_op jit(solution)/shard_map/ppermute | solution.py:286
  27.4 17.6 %collective-permute-start.2 = (bf16[200,2048]{1,0:T(8,128)(2,1)}, bf16[200,2048]{1,0:T(8,128)(2,1)}, u32[]{:S(2)}, u32[]{:S(2)}) collective-permute-start(bf16[200,2048]{1,0:T(8,128)(2,1)} %collective-permute-done.1.refs_0_), channel_id=1, source_target_pairs={{0,2},{1,15},{2,4},{3,1},{4,6},{5,3},{6,8},{7,5},{8,10},{9,7},{10,... | collective-permute-start | bytes 2457608 | tf_op jit(solution)/shard_map/ppermute | solution.py:293
  36.1 17.7 %collective-permute-start.9 = (bf16[200,2048]{1,0:T(8,128)(2,1)S(1)}, bf16[200,2048]{1,0:T(8,128)(2,1)}, u32[]{:S(2)}, u32[]{:S(2)}) collective-permute-start(bf16[200,2048]{1,0:T(8,128)(2,1)S(1)} %collective-permute-done.8.refs_1_), channel_id=1, source_target_pairs={{0,2},{1,15},{2,4},{3,1},{4,6},{5,3},{6,8},{7,5},{8,10},{9,7},{10,... | collective-permute-start | bytes 2457608 | tf_op jit(solution)/shard_map/ppermute | solution.py:293
  45.0 17.4 %collective-permute-start.3 = (bf16[200,2048]{1,0:T(8,128)(2,1)}, bf16[200,2048]{1,0:T(8,128)(2,1)S(1)}, u32[]{:S(2)}, u32[]{:S(2)}) collective-permute-start(bf16[200,2048]{1,0:T(8,128)(2,1)} %collective-permute-done.2.refs_0_), channel_id=1, source_target_pairs={{0,2},{1,15},{2,4},{3,1},{4,6},{5,3},{6,8},{7,5},{8,10},{9,7},{10,... | collective-permute-start | bytes 2457608 | tf_op jit(solution)/shard_map/ppermute | solution.py:293
  53.8 17.4 %collective-permute-start.10 = (bf16[200,2048]{1,0:T(8,128)(2,1)}, bf16[200,2048]{1,0:T(8,128)(2,1)S(1)}, u32[]{:S(2)}, u32[]{:S(2)}) collective-permute-start(bf16[200,2048]{1,0:T(8,128)(2,1)} %collective-permute-done.9.refs_1_), channel_id=1, source_target_pairs={{0,2},{1,15},{2,4},{3,1},{4,6},{5,3},{6,8},{7,5},{8,10},{9,7},{10,... | collective-permute-start | bytes 2457608 | tf_op jit(solution)/shard_map/ppermute | solution.py:293
  62.5 17.6 %collective-permute-start.4 = (bf16[200,2048]{1,0:T(8,128)(2,1)S(1)}, bf16[200,2048]{1,0:T(8,128)(2,1)S(1)}, u32[]{:S(2)}, u32[]{:S(2)}) collective-permute-start(bf16[200,2048]{1,0:T(8,128)(2,1)S(1)} %collective-permute-done.3.refs_0_), channel_id=1, source_target_pairs={{0,2},{1,15},{2,4},{3,1},{4,6},{5,3},{6,8},{7,5},{8,10},{9,7},{10,... | collective-permute-start | bytes 2457608 | tf_op jit(solution)/shard_map/ppermute | solution.py:293
  82.8 5.7 %collective-permute-start.11 = (f32[3,2,136,128]{3,2,1,0:T(8,128)S(1)}, f32[3,2,136,128]{3,2,1,0:T(8,128)S(1)}, u32[]{:S(2)}, u32[]{:S(2)}) collective-permute-start(f32[3,2,136,128]{3,2,1,0:T(8,128)S(1)} %get-tuple-element.31), channel_id=1, source_target_pairs={{0,1},{1,0},{2,3},{3,2},{4,5},{5,4},{6,7},{7,6},{8,9},{9,8},{10,11... | collective-permute-start | bytes 1253384 | tf_op jit(solution)/shard_map/ppermute | solution.py:286

commit v3 on v2

--- a/solution.py
+++ b/solution.py
@@ -19,20 +19,30 @@
     return lax.dot_general(a, b, (dims, ((), ())), preferred_element_type=F32, precision=precision)
 
 
+def halves(v):
+    high = v.astype(BF)
+    return high, (v - high.astype(F32)).astype(BF)
+
+
+def product(a, b):
+    (ah, al), (bh, bl) = halves(a), halves(b)
+    dims = ((0,), (0,))
+    return mm(ah, bh, dims) + (mm(al, bh, dims) + mm(ah, bl, dims))
+
+
 def softplus(v):
     return jnp.maximum(v, 0.0) + jnp.log1p(jnp.exp(-jnp.abs(v)))
 
 
-def piece_states(meta, xs, far, end, w_step, w, jump, rates, runs, rows, chips):
-    depth = w[0].shape[0] - 4
+def piece_states(meta, xs, far, end, w_step, w, taps, jump, rates, runs, base, rows, chips):
     many, both = len(xs), 2 * rows
     given = [] if runs is None else list(runs)
 
     def body(m_ref, *refs):
         x_refs = refs[:many]
-        s_ref, wa_ref, wb_ref, j_ref, r_ref = refs[many : many + 5]
-        ins = refs[many + 5 : many + 5 + len(given)]
-        own_out, other_out, ext = refs[many + 5 + len(given) :]
+        s_ref, wa_ref, wb_ref, t_ref, j_ref, r_ref = refs[many : many + 6]
+        ins = refs[many + 6 : many + 6 + len(given)]
+        own_out, other_out, ext = refs[many + 6 + len(given) :]
         outs = (own_out, other_out)
         y, c = m_ref[0], m_ref[1]
         low = c == 0
@@ -75,43 +85,42 @@
             weight = jnp.concatenate([weight, jnp.zeros((8, 256 - both), F32)], axis=1)
             lifts.append(jnp.transpose(weight))
 
-        taps = jnp.concatenate([r[depth : depth + 4, :] for r in (wa_ref, wb_ref)], axis=1).astype(F32)
         for n in range(many):
             x = x_refs[n][...]
             for g, r in enumerate((wa_ref, wb_ref)):
-                p = mm(x, r[:depth, :], ((1,), (0,))).astype(BF).astype(F32)
+                p = mm(x, r[...], ((1,), (0,))).astype(BF).astype(F32)
                 for s in range(2):
                     ext[2 * n + s, 4:8, 256 * g : 256 * g + 256] = p[both + 4 * s : both + 4 * s + 4, :]
                     ext[2 * n + s, 8 : 8 + rows, 256 * g : 256 * g + 256] = p[s * rows : (s + 1) * rows, :]
         for s in range(2):
             states = [jnp.zeros((128, 128), F32)] * 2
             for n in range(many):
-                mixed = ext[2 * n + s, 5 : 5 + rows, :] * taps[0:1, :]
+                mixed = ext[2 * n + s, 5 : 5 + rows, :] * t_ref[0:1, :]
                 for k in range(1, 4):
-                    mixed = mixed + ext[2 * n + s, 5 + k : 5 + k + rows, :] * taps[k : k + 1, :]
+                    mixed = mixed + ext[2 * n + s, 5 + k : 5 + k + rows, :] * t_ref[k : k + 1, :]
                 mixed = mixed / (1.0 + jnp.exp(-mixed))
                 lift = lifts[n][s * rows : (s + 1) * rows, :]
                 for g in range(2):
                     parts = [
-                        mixed[:, 256 * g + 64 * e : 256 * g + 64 * e + 64] * lift[:, 2 * g + e : 2 * g + e + 1]
+                        mixed[:, 256 * g + 64 * e : 256 * g + 64 * e + 64] * lift[:, base + 2 * g + e : base + 2 * g + e + 1]
                         for e in range(2)
                     ]
-                    values = jnp.concatenate(parts, axis=1).astype(BF)
-                    keys = mixed[:, 256 * g + 128 : 256 * g + 256].astype(BF)
-                    states[g] = states[g] + mm(values, keys, ((0,), (0,)))
+                    values = jnp.concatenate(parts, axis=1)
+                    keys = mixed[:, 256 * g + 128 : 256 * g + 256]
+                    states[g] = states[g] + product(values, keys)
             fade = jnp.where(low, 1.0, jnp.exp(total[s]))
             for g in range(2):
                 for e in range(2):
                     part = slice(64 * e, 64 * e + 64)
                     old = outs[g][run, s, part, :]
-                    outs[g][run, s, part, :] = old * fade[2 * g + e : 2 * g + e + 1, :] + states[g][part, :]
+                    outs[g][run, s, part, :] = old * fade[base + 2 * g + e : base + 2 * g + e + 1, :] + states[g][part, :]
                 outs[g][run, s, 128:136, :] = before[s] + total[s]
 
     shape = (3, 2, 136, 128)
     return pl.pallas_call(
         body,
         out_shape=[jax.ShapeDtypeStruct(shape, F32)] * 2,
-        in_specs=[SMEM] + [VMEM] * (many + 5 + len(given)),
+        in_specs=[SMEM] + [VMEM] * (many + 6 + len(given)),
         out_specs=[VMEM] * 2,
         scratch_shapes=[pltpu.VMEM((2 * many, rows + 8, 512), F32)],
         cost_estimate=pl.CostEstimate(
@@ -121,26 +130,28 @@
         ),
         compiler_params=GRANT,
         name="piece_states",
-    )(meta, *xs, w_step, *w, jump, rates, *given)
-
-
-def joined(w_value, w_key, conv_value, conv_key):
+    )(meta, *xs, w_step, *w, taps, jump, rates, *given)
+
+
+def joined(meta, w_value, w_key, parts):
     depth = w_value.shape[0]
-
-    def body(v_ref, k_ref, cv_ref, ck_ref, out_ref):
-        out_ref[:depth, :128] = v_ref[...]
-        out_ref[:depth, 128:] = k_ref[...]
-        out_ref[depth:, :128] = cv_ref[...]
-        out_ref[depth:, 128:] = ck_ref[...]
-
-    return pl.pallas_call(
-        body,
-        out_shape=jax.ShapeDtypeStruct((depth + conv_value.shape[0], 256), BF),
-        in_specs=[VMEM] * 4,
-        out_specs=VMEM,
+    cut = depth // parts
+
+    def body(m_ref, v_ref, k_ref, out_ref, part_ref):
+        out_ref[:, :128] = v_ref[...]
+        out_ref[:, 128:] = k_ref[...]
+        start = pl.multiple_of(m_ref[3] * cut, cut)
+        part_ref[:, :128] = v_ref[pl.ds(start, cut), :]
+        part_ref[:, 128:] = k_ref[pl.ds(start, cut), :]
+
+    return pl.pallas_call(
+        body,
+        out_shape=[jax.ShapeDtypeStruct((depth, 256), BF), jax.ShapeDtypeStruct((cut, 256), BF)],
+        in_specs=[SMEM] + [VMEM] * 2,
+        out_specs=[VMEM] * 2,
         compiler_params=GRANT,
         name="joined",
-    )(w_value, w_key, conv_value, conv_key)
+    )(meta, w_value, w_key)
 
 
 def terms(step_bias, decay_rate, new_step, new_value, new_key, new_query, new_gate, read_gain):
@@ -174,62 +185,106 @@
     )(step_bias, decay_rate, new_step, new_value, new_key, new_query, new_gate, read_gain.reshape(1, 128))
 
 
-def packed(meta, own, got, query, sp_count, chips):
+def merged(meta, groups, decays, chips):
+    def body(m_ref, *refs):
+        g_refs, d_refs = refs[:4], refs[4:8]
+        keep_out, send_out, total_out = refs[8:]
+        y, c = m_ref[0], m_ref[1]
+        lane = lax.broadcasted_iota(jnp.int32, (1, 128), 1)
+
+        def turned(v):
+            return jnp.where(v < 0, v + chips, jnp.where(v >= chips, v - chips, v))
+
+        places = []
+        for o in range(4):
+            q = turned(y + chips // 2) if o >= 2 else y
+            low = (c == 0) if o % 2 == 0 else (c != 0)
+            reach = chips // 4
+            first = jnp.where(low, 2 * jnp.maximum(q - reach + 1, 0), 2 * q + 1)
+            second = jnp.where(low, 2 * jnp.minimum(q - reach + 1 + chips, chips), 0)
+            third = jnp.where(low, 2 * turned(q - reach), 2 * turned(q + reach) + 1)
+            places.append((first, second, third))
+        left = jnp.zeros((1, 128), F32)
+        for s in range(2):
+            for g in range(4):
+                after = [jnp.zeros((2, 128), F32)] * 3
+                for o in range(4):
+                    for k in range(3):
+                        row = 2 * (g ^ o)
+                        decay = d_refs[o][k, s, row : row + 2, :]
+                        after = [v + jnp.where(places[o][k] > places[0][r], decay, 0.0) for r, v in enumerate(after)]
+                        if g == 0:
+                            for e in range(2):
+                                left = left + jnp.where(lane == 2 * s + e, decay[e : e + 1, :], 0.0)
+                scale = [jnp.exp(v) for v in after]
+                for e in range(2):
+                    part = slice(64 * e, 64 * e + 64)
+                    state = sum(g_refs[g][r, s, part, :] * scale[r][e : e + 1, :] for r in range(3))
+                    (keep_out if g % 2 == 0 else send_out)[g // 2, s, part, :] = state
+        for k in range(3):
+            part = left.astype(BF).astype(F32)
+            left = left - part
+            total_out[k : k + 1, :] = part
+        total_out[3:, :] = jnp.zeros((5, 128), F32)
+
+    return pl.pallas_call(
+        body,
+        out_shape=[jax.ShapeDtypeStruct((2, 2, 128, 128), F32)] * 2 + [jax.ShapeDtypeStruct((8, 128), F32)],
+        in_specs=[SMEM] + [VMEM] * 8,
+        out_specs=[VMEM] * 3,
+        compiler_params=GRANT,
+        name="merged",
+    )(meta, *groups, *decays)
+
+
+def summed(keep, got, query):
+    def body(a_ref, b_ref, q_ref, own_out, far_out):
+        own_out[...] = a_ref[0] + b_ref[0]
+        for s in range(2):
+            state = a_ref[1, s] + b_ref[1, s]
+            far_out[s, :128, :] = state.astype(BF)
+            read = jnp.sum(state * q_ref[s : s + 1, :], axis=1).reshape(1, 128)
+            high, low = halves(read)
+            far_out[s, 128:144, :] = jnp.concatenate([high, low, jnp.zeros((14, 128), BF)], axis=0)
+
+    return pl.pallas_call(
+        body,
+        out_shape=[jax.ShapeDtypeStruct((2, 128, 128), F32), jax.ShapeDtypeStruct((2, 144, 128), BF)],
+        in_specs=[VMEM] * 3,
+        out_specs=[VMEM] * 2,
+        compiler_params=GRANT,
+        name="summed",
+    )(keep, got, query)
+
+
+def packed(own, got, query, total, sp_count):
     share = HEAD_DIM // sp_count
 
-    def body(m_ref, a_ref, b_ref, q_ref, out_ref):
+    def body(a_ref, b_ref, q_ref, t_ref, out_ref):
         def put(row, value):
             out_ref[:, row : row + 1, :] = jnp.broadcast_to(value[None], (sp_count, 1, 128))
 
-        low = m_ref[1] == 0
-        late = m_ref[0] < chips // 2
-        lane = lax.broadcasted_iota(jnp.int32, (1, 128), 1)
-        left = jnp.zeros((1, 128), F32)
-        for s in range(2):
-            mine = [a_ref[r, s, 128:130, :] for r in range(3)]
-            theirs = [b_ref[r, s, 130:132, :] for r in range(3)]
-            d1, d2, d3 = (jnp.where(low, m, t) for m, t in zip(mine, theirs))
-            u1, u2, u3 = (jnp.where(low, t, m) for m, t in zip(mine, theirs))
-            last = d3 + u3
-            after_u1 = d2 + jnp.where(late, last, 0.0)
-            after_d1 = after_u1 + u1
-            after_u3 = jnp.where(late, d2, after_d1 + d1)
-            after_d3 = after_u3 + u3
-            after_u2 = after_d1 + d1 + jnp.where(late, 0.0, last)
-            total = after_u2 + u2
+        for s in range(2):
+            state = a_ref[s] + b_ref[s, :128, :].astype(F32)
+            far = b_ref[s, 128:144, :].astype(F32)
+            read = jnp.sum(a_ref[s] * q_ref[s : s + 1, :], axis=1).reshape(1, 128)
+            high, low = halves(read + far[0:1] + far[1:2])
+            put(8 + s, high)
+            put(10 + s, low)
             for e in range(2):
-                left = jnp.where(lane == 2 * s + e, total[e : e + 1, :], left)
-            down = [jnp.exp(v) for v in (after_d1, jnp.zeros_like(d2), after_d3)]
-            up = [jnp.exp(v) for v in (after_u1, after_u2, after_u3)]
-            reads = []
-            for e in range(2):
-                state = jnp.zeros((64, 128), F32)
-                for r in range(3):
-                    part = slice(64 * e, 64 * e + 64)
-                    scale_a = jnp.where(low, down[r], up[r])[e : e + 1, :]
-                    scale_b = jnp.where(low, up[r], down[r])[e : e + 1, :]
-                    state = state + a_ref[r, s, part, :] * scale_a + b_ref[r, s, part, :] * scale_b
-                reads.append(jnp.sum(state * q_ref[s : s + 1, :], axis=1).reshape(1, 64))
-                cut = state.astype(BF).reshape(sp_count, share, 128)
+                cut = state[64 * e : 64 * e + 64, :].astype(BF).reshape(sp_count, share, 128)
                 out_ref[:, 4 * s + 2 * e : 4 * s + 2 * e + share, :] = cut
-            read = jnp.concatenate(reads, axis=1)
-            high = read.astype(BF)
-            put(8 + s, high)
-            put(10 + s, (read - high.astype(F32)).astype(BF))
-        for k in range(3):
-            part = left.astype(BF)
-            left = left - part.astype(F32)
-            put(12 + k, part)
-        put(15, jnp.zeros((1, 128), BF))
+        for k in range(4):
+            put(12 + k, t_ref[k : k + 1, :].astype(BF))
 
     return pl.pallas_call(
         body,
         out_shape=jax.ShapeDtypeStruct((sp_count, 16, 128), BF),
-        in_specs=[SMEM] + [VMEM] * 3,
+        in_specs=[VMEM] * 4,
         out_specs=VMEM,
         compiler_params=GRANT,
         name="packed",
-    )(meta, own, got, query)
+    )(own, got, query, total)
 
 
 def finished(meta, got, fixed):
@@ -280,7 +335,7 @@
     rows, width = hidden_in.shape[1:]
     heads = step_bias.shape[0]
     share = HEAD_DIM // sp_count
-    half = y_count // 2
+    half, reach = y_count // 2, y_count // 4
 
     def swap(v):
         return lax.ppermute(v, "c", [(0, 1), (1, 0)])
@@ -292,7 +347,16 @@
             pairs.append((2 * i + 1, 2 * ((i - 1) % y_count) + 1))
         return lax.ppermute(v, ("y", "c"), pairs)
 
-    meta = jnp.stack([y, c, (128 - sp * share) % 128]).astype(jnp.int32)
+    def across(v):
+        return lax.ppermute(v, "y", [(i, (i + half) % y_count) for i in range(y_count)])
+
+    meta = jnp.stack([y, c, (128 - sp * share) % 128, sp]).astype(jnp.int32)
+
+    w_own, w_part = joined(meta, w_value, w_key, sp_count)
+    w_part = jnp.broadcast_to(across(w_part)[None], (sp_count, *w_part.shape))
+    w_far = lax.all_to_all(w_part, "sp", 0, 0, tiled=True).reshape(w_own.shape)
+    w_near = w_own, swap(w_own)
+    w_far = w_far, swap(w_far)
 
     ends = hidden_in[:, rows - 4 :, :].reshape(8, width)
     ends = lax.ppermute(ends, ("sp", "y", "c"), [(i, i + 1) for i in range(count - 1)])
@@ -301,33 +365,52 @@
     b = [swap(a[0])]
     b.append(onward(b[0]))
 
-    w_own = joined(w_value, w_key, conv_value, conv_key)
-    w_both = w_own, swap(w_own)
-    pair = lax.dynamic_slice_in_dim(w_step.T, y * 2 * heads, 2 * heads, 0)
-    pair = jnp.where(c == 0, pair, jnp.roll(pair, heads, axis=0))
-    w_steps = jnp.pad(pair, ((0, 8 - 2 * heads), (0, 0)))
+    def ordered(v):
+        return jnp.where(c == 0, v, jnp.roll(v, heads, axis=0))
+
+    steps = w_step.T
+    pairs = (lax.dynamic_slice_in_dim(steps, v * 2 * heads, 2 * heads, 0) for v in (y, (y + half) % y_count))
+    w_steps = jnp.concatenate([ordered(v) for v in pairs], axis=0)
     rates = jnp.broadcast_to(jnp.stack([step_bias, decay_rate])[:, :, None], (2, heads, 128))
-    jump = jnp.concatenate([decay_jump.transpose(0, 2, 1), rates], axis=2)
-    jump = jnp.concatenate([jump, swap(jump)], axis=1)
-    jump = jnp.pad(jump, ((0, 0), (0, 8 - 2 * heads), (0, 0)))
-    rates = jump[:, :, tp_count * rows :]
-    jump = jump[:, :, : tp_count * rows].reshape(2, 8, tp_count, rows).transpose(2, 1, 0, 3)
+    taps = jnp.concatenate([conv_value, conv_key], axis=1).astype(F32).reshape(2, heads, 256)
+    asked = new_query.astype(F32).reshape(2, heads, HEAD_DIM)
+    small = jnp.concatenate([decay_jump.transpose(0, 2, 1), rates, taps, asked], axis=2)
+    small = jnp.concatenate([small, swap(small)], axis=1)
+    small = jnp.concatenate([small, across(small)], axis=1)
+    length = tp_count * rows
+    rates, taps = small[:, :, length : length + 128], small[:, :, length + 128 : length + 384]
+    asked = small[:, 4 : 4 + heads, length + 384 :].reshape(2, heads * HEAD_DIM)
+    taps = taps.reshape(2, 4, 2, 256).transpose(0, 2, 1, 3).reshape(4, 1024)
+    jump = small[:, :, :length].reshape(2, 8, tp_count, rows).transpose(2, 1, 0, 3)
     jump = jump.reshape(tp_count, 8, 2 * rows)
 
-    def add(runs, xs, far, end):
-        return piece_states(meta, xs, far, end, w_steps, w_both, jump, rates, runs, rows, y_count)
-
-    runs = add(None, [a[0]], 0, False)
-    for s in range(1, half):
-        a.append(onward(a[s]))
-        if s + 1 < half:
-            b.append(onward(b[s]))
-        runs = add(runs, [a[s], b[s]], s, False)
+    for k in range(1, reach):
+        if k + 1 < reach:
+            b.append(onward(b[k]))
+        a.append(onward(a[k]))
+
+    def add(runs, k, w, base):
+        ends = k == 0 or k == reach
+        xs = [a[k]] if ends else [a[k], b[k]]
+        part = taps[:, 128 * base : 128 * base + 512]
+        return piece_states(meta, xs, k, k == reach, w_steps, w, part, jump, rates, runs, base, rows, y_count)
+
+    near = None
+    for k in range(reach + 1):
+        near = add(near, k, w_near, 0)
+    decays = near[0][:, :, 128:, :]
+    decays = [decays, swap(decays)]
+    apart = across(jnp.concatenate(decays, axis=0))
+    decays += [apart[:3], apart[3:]]
 
     fixed, query = terms(step_bias, decay_rate, new_step, new_value, new_key, new_query, new_gate, read_gain)
-    runs, fixed, query = lax.optimization_barrier((runs, fixed, query))
-    own, other = add(runs, [a[half]], half, True)
-    sent = packed(meta, own, swap(other), query, sp_count, y_count)
+    near, decays, fixed, query, asked = lax.optimization_barrier((near, decays, fixed, query, asked))
+    away = None
+    for k in range(reach + 1):
+        away = add(away, k, w_far, 4)
+    keep, send, total = merged(meta, [*near, *away], decays, y_count)
+    own, apart = summed(keep, swap(send), asked)
+    sent = packed(own, across(apart), query, total, sp_count)
     got = lax.all_to_all(sent, "sp", 0, 0, tiled=True)
     return tuple(finished(meta, got, fixed))
 

time: 114 us -> 146 us (1.28)
  the two profiles are of different devices: /device:TPU:1 before, /device:TPU:8 now
where the time goes in v3:
time: 146 us; the launch traced here: 144 us
  starting transfers between devices  59.7 us (41%)
  waiting for transfers between devices  27.9 us (19%)
  Pallas kernels  27.7 us (19%)
  blocking collectives  20.3 us (14%)
  local copies, waits for them, and re-layouts  7.32 us (5%)
    pallas_call x6, Pallas kernels, piece_states(): pl.pallas_call(body, out_shape=[jax.ShapeDtypeStruct(shape, F32)] * 2, in...  22.6 us
    ppermute x4, starting transfers between devices, across(): lax.ppermute(v, 'y', [(i, (i + half) % y_count) for i in range(y_count)])  21.5 us
    all_to_all x1, blocking collectives, per_device(): got = lax.all_to_all(sent, 'sp', 0, 0, tiled=True)  20.3 us
    ppermute x4, waiting for transfers between devices, across(): lax.ppermute(v, 'y', [(i, (i + half) % y_count) for i in range(y_count)])  17.1 us
    all_to_all x1, starting transfers between devices, per_device(): w_far = lax.all_to_all(w_part, 'sp', 0, 0, tiled=True).reshape(w_own.shape)  13.3 us
    ppermute x6, starting transfers between devices, swap(): return lax.ppermute(v, 'c', [(0, 1), (1, 0)])  13.2 us
    ppermute x3, starting transfers between devices, onward(): return lax.ppermute(v, ('y', 'c'), pairs)  9.82 us
    ppermute x3, waiting for transfers between devices, onward(): return lax.ppermute(v, ('y', 'c'), pairs)  8.12 us
  transfers between devices with their start and end apart: 15, of which 8 were waited for; matrix products, arithmetic and copies ran while one was open for 2% of the time, Pallas kernels for 10%

profile of v3, /device:TPU:8, one launch (start us, length us, event | category | flops | bytes accessed | tf_op | source)
XLA Modules:
  0.0 144.4 jit_solution(18206374092090537130)
XLA Ops:
  0.7 0.9 slice.48
  1.6 1.9 %collective-permute-start = (bf16[8,2048]{1,0:T(8,128)(2,1)S(1)}, bf16[8,2048]{1,0:T(8,128)(2,1)S(1)}, u32[]{:S(2)}, u32[]{:S(2)}) collective-permute-start(bf16[8,2048]{1,0:T(8,128)(2,1)S(1)} %reshape.43), channel_id=1, source_target_pairs={{0,1},{1,2},{2,3},{3,4},{4,5},{5,6},{6,7},{7,8},{8,9},{9,10},{10,1... | collective-permute-start | bytes 98312 | tf_op jit(solution)/shard_map/ppermute | solution.py:362
  3.6 1.0 copy-done
  4.7 1.0 copy-done.1
  5.7 1.7 %joined.1 = (bf16[2048,256]{1,0:T(8,128)(2,1)}, bf16[64,256]{1,0:T(8,128)(2,1)S(1)}) custom-call(s32[4]{0:T(128)S(1)} %pad_add_fusion.m_ref, bf16[2048,128]{1,0:T(8,128)(2,1)S(1)} %copy-done, bf16[2048,128]{1,0:T(8,128)(2,1)S(1)} %copy-done.1), custom_call_target="tpu_custom_call" | custom-call | tf_op jit(solution)/shard_map/joined/pallas_call | solution.py:147
  7.4 3.6 %collective-permute-start.3 = (bf16[2048,256]{1,0:T(8,128)(2,1)}, bf16[2048,256]{1,0:T(8,128)(2,1)}, u32[]{:S(2)}, u32[]{:S(2)}) collective-permute-start(bf16[2048,256]{1,0:T(8,128)(2,1)} %get-tuple-element.32.refs_2_.refs_3_), channel_id=1, source_target_pairs={{0,1},{1,0},{2,3},{3,2},{4,5},{5,4},{6,7},{7,6},{8,9},{9,8},{10,11... | collective-permute-start | bytes 3145736 | tf_op jit(solution)/shard_map/ppermute | solution.py:341
  11.0 0.1 reshape.54
  11.3 1.9 %collective-permute-start.4 = (f32[2,2,1984]{2,1,0:T(2,128)S(1)}, f32[2,2,1984]{2,1,0:T(2,128)S(1)}, u32[]{:S(2)}, u32[]{:S(2)}) collective-permute-start(f32[2,2,1984]{2,1,0:T(2,128)S(1)} %pad_maximum_fusion.5), channel_id=1, source_target_pairs={{0,1},{1,0},{2,3},{3,2},{4,5},{5,4},{6,7},{7,6},{8,9},{9,8},{10,11... | collective-permute-start | bytes 95240 | tf_op jit(solution)/shard_map/ppermute | solution.py:341
  13.2 5.9 %collective-permute-start.10 = (bf16[64,256]{1,0:T(8,128)(2,1)S(1)}, bf16[64,256]{1,0:T(8,128)(2,1)S(1)}, u32[]{:S(2)}, u32[]{:S(2)}) collective-permute-start(bf16[64,256]{1,0:T(8,128)(2,1)S(1)} %get-tuple-element.43), channel_id=1, source_target_pairs={{0,8},{2,10},{4,12},{6,14},{8,0},{10,2},{12,4},{14,6},{1,9},{3,11}... | collective-permute-start | bytes 98312 | tf_op jit(solution)/shard_map/ppermute | solution.py:351
  19.1 0.8 dynamic-slice_bitcast_fusion.1
  20.0 2.9 %collective-permute-done.10 = bf16[64,256]{1,0:T(8,128)(2,1)S(1)} collective-permute-done((bf16[64,256]{1,0:T(8,128)(2,1)S(1)}, bf16[64,256]{1,0:T(8,128)(2,1)S(1)}, u32[]{:S(2)}, u32[]{:S(2)}) %collective-permute-start.10) | collective-permute-done | bytes 32800 | tf_op jit(solution)/shard_map/ppermute | solution.py:351
  22.9 1.1 broadcast_in_dim.5
  24.0 13.3 %all-to-all-start = ((bf16[32,64,256]{2,1,0:T(8,128)(2,1)}), bf16[32,64,256]{2,1,0:T(8,128)(2,1)S(1)}, u32[]{:S(2)}, u32[]{:S(2)}) async-start(bf16[32,64,256]{2,1,0:T(8,128)(2,1)} %broadcast_in_dim.5), calls=%async_computation | async-start | bytes 2097152 | tf_op jit(solution)/shard_map/all_to_all | solution.py:357
  37.4 1.9 %collective-permute-start.6 = (bf16[200,2048]{1,0:T(8,128)(2,1)S(1)}, bf16[200,2048]{1,0:T(8,128)(2,1)}, u32[]{:S(2)}, u32[]{:S(2)}) collective-permute-start(bf16[200,2048]{1,0:T(8,128)(2,1)S(1)} %pad_maximum_fusion.refs_0_), channel_id=1, source_target_pairs={{0,1},{1,0},{2,3},{3,2},{4,5},{5,4},{6,7},{7,6},{8,9},{9,8},{10,11... | collective-permute-start | bytes 2457608 | tf_op jit(solution)/shard_map/ppermute | solution.py:341
  39.4 6.5 %collective-permute-start.5 = (f32[2,4,1984]{2,1,0:T(4,128)S(1)}, f32[2,4,1984]{2,1,0:T(4,128)S(1)}, u32[]{:S(2)}, u32[]{:S(2)}) collective-permute-start(f32[2,4,1984]{2,1,0:T(4,128)S(1)} %pad_maximum_fusion.2), channel_id=1, source_target_pairs={{0,8},{2,10},{4,12},{6,14},{8,0},{10,2},{12,4},{14,6},{1,9},{3,11}... | collective-permute-start | bytes 190472 | tf_op jit(solution)/shard_map/ppermute | solution.py:351
  45.9 2.1 %collective-permute-start.1 = (bf16[200,2048]{1,0:T(8,128)(2,1)S(1)}, bf16[200,2048]{1,0:T(8,128)(2,1)S(1)}, u32[]{:S(2)}, u32[]{:S(2)}) collective-permute-start(bf16[200,2048]{1,0:T(8,128)(2,1)S(1)} %pad_maximum_fusion.refs_0_), channel_id=1, source_target_pairs={{0,2},{1,15},{2,4},{3,1},{4,6},{5,3},{6,8},{7,5},{8,10},{9,7},{10,... | collective-permute-start | bytes 2457608 | tf_op jit(solution)/shard_map/ppermute | solution.py:348
  48.0 1.7 %collective-permute-done.5 = f32[2,4,1984]{2,1,0:T(4,128)S(1)} collective-permute-done((f32[2,4,1984]{2,1,0:T(4,128)S(1)}, f32[2,4,1984]{2,1,0:T(4,128)S(1)}, u32[]{:S(2)}, u32[]{:S(2)}) %collective-permute-start.5) | collective-permute-done | bytes 63520 | tf_op jit(solution)/shard_map/ppermute | solution.py:351
  49.8 4.7 %collective-permute-start.7 = (bf16[200,2048]{1,0:T(8,128)(2,1)}, bf16[200,2048]{1,0:T(8,128)(2,1)}, u32[]{:S(2)}, u32[]{:S(2)}) collective-permute-start(bf16[200,2048]{1,0:T(8,128)(2,1)} %collective-permute-done.6), channel_id=1, source_target_pairs={{0,2},{1,15},{2,4},{3,1},{4,6},{5,3},{6,8},{7,5},{8,10},{9,7},{10,... | collective-permute-start | bytes 2457608 | tf_op jit(solution)/shard_map/ppermute | solution.py:348
  54.7 0.1 reshape.48
  54.8 0.1 copy.18
  54.9 0.1 reshape.49.refs_5_.refs_6_
  55.0 5.1 %collective-permute-done.1.refs_0_ = bf16[200,2048]{1,0:T(8,128)(2,1)S(1)} collective-permute-done((bf16[200,2048]{1,0:T(8,128)(2,1)S(1)}, bf16[200,2048]{1,0:T(8,128)(2,1)S(1)}, u32[]{:S(2)}, u32[]{:S(2)}) %collective-permute-start.1) | collective-permute-done | bytes 819232 | tf_op jit(solution)/shard_map/ppermute | solution.py:348
  60.2 3.0 %collective-permute-start.2 = (bf16[200,2048]{1,0:T(8,128)(2,1)S(1)}, bf16[200,2048]{1,0:T(8,128)(2,1)}, u32[]{:S(2)}, u32[]{:S(2)}) collective-permute-start(bf16[200,2048]{1,0:T(8,128)(2,1)S(1)} %collective-permute-done.1.refs_0_), channel_id=1, source_target_pairs={{0,2},{1,15},{2,4},{3,1},{4,6},{5,3},{6,8},{7,5},{8,10},{9,7},{10,... | collective-permute-start | bytes 2457608 | tf_op jit(solution)/shard_map/ppermute | solution.py:348
  63.2 3.5 %piece_states.6 = (f32[3,2,136,128]{3,2,1,0:T(8,128)S(1)}, f32[3,2,136,128]{3,2,1,0:T(8,128)S(1)}) custom-call(s32[4]{0:T(128)S(1)} %pad_add_fusion.m_ref, bf16[200,2048]{1,0:T(8,128)(2,1)S(1)} %pad_maximum_fusion.refs_0_, bf16[8,2048]{1,0:T(8,128)(2,1)S(1)} %pad_maximum_fusion.4.refs_1_.refs_2_, bf16[2048,256]{1,0:T(8,128)(2,1)} %get-tuple-element.32.refs_2_.refs_3_, ...), custom_call_target="tpu_custom_call" | custom-call | flops 3355443200 | bytes 2097152 | tf_op jit(solution)/shard_map/piece_states/pallas_call | solution.py:120
  66.7 0.7 copy-done.12
  67.5 1.9 %collective-permute-start.11 = (bf16[2048,256]{1,0:T(8,128)(2,1)S(1)}, bf16[2048,256]{1,0:T(8,128)(2,1)}, u32[]{:S(2)}, u32[]{:S(2)}) collective-permute-start(bf16[2048,256]{1,0:T(8,128)(2,1)S(1)} %bitcast.21), channel_id=1, source_target_pairs={{0,1},{1,0},{2,3},{3,2},{4,5},{5,4},{6,7},{7,6},{8,9},{9,8},{10,11... | collective-permute-start | bytes 3145736 | tf_op jit(solution)/shard_map/ppermute | solution.py:341
  69.4 1.0 copy-done.13
  70.4 4.4 %piece_states.7 = (f32[3,2,136,128]{3,2,1,0:T(8,128)S(1)}, f32[3,2,136,128]{3,2,1,0:T(8,128)S(1)}) custom-call(s32[4]{0:T(128)S(1)} %pad_add_fusion.m_ref, bf16[200,2048]{1,0:T(8,128)(2,1)S(1)} %collective-permute-done.1.refs_0_, bf16[200,2048]{1,0:T(8,128)(2,1)} %collective-permute-done.7.refs_1_, bf16[8,2048]{1,0:T(8,128)(2,1)S(1)} %pad_maximum_fusion.4.refs_1_.refs_2_, ...), custom_call_target="tpu_custom_call" | custom-call | flops 6710886400 | bytes 2097152 | tf_op jit(solution)/shard_map/piece_states/pallas_call | solution.py:120
  74.8 3.0 %collective-permute-done.2.refs_0_ = bf16[200,2048]{1,0:T(8,128)(2,1)} collective-permute-done((bf16[200,2048]{1,0:T(8,128)(2,1)S(1)}, bf16[200,2048]{1,0:T(8,128)(2,1)}, u32[]{:S(2)}, u32[]{:S(2)}) %collective-permute-start.2) | collective-permute-done | bytes 819232 | tf_op jit(solution)/shard_map/ppermute | solution.py:348
  77.8 3.8 %piece_states.8 = (f32[3,2,136,128]{3,2,1,0:T(8,128)S(1)}, f32[3,2,136,128]{3,2,1,0:T(8,128)S(1)}) custom-call(s32[4]{0:T(128)S(1)} %pad_add_fusion.m_ref, bf16[200,2048]{1,0:T(8,128)(2,1)} %collective-permute-done.2.refs_0_, bf16[8,2048]{1,0:T(8,128)(2,1)S(1)} %pad_maximum_fusion.4.refs_1_.refs_2_, bf16[2048,256]{1,0:T(8,128)(2,1)} %get-tuple-element.32.refs_2_.refs_3_, ...), custom_call_target="tpu_custom_call" | custom-call | flops 3355443200 | bytes 2097152 | tf_op jit(solution)/shard_map/piece_states/pallas_call | solution.py:120
  81.7 1.9 %collective-permute-start.8 = (f32[3,2,8,128]{3,2,1,0:T(8,128)S(1)}, f32[3,2,8,128]{3,2,1,0:T(8,128)S(1)}, u32[]{:S(2)}, u32[]{:S(2)}) collective-permute-start(f32[3,2,8,128]{3,2,1,0:T(8,128)S(1)} %slice.57.refs_4_), channel_id=1, source_target_pairs={{0,1},{1,0},{2,3},{3,2},{4,5},{5,4},{6,7},{7,6},{8,9},{9,8},{10,11... | collective-permute-start | bytes 73736 | tf_op jit(solution)/shard_map/ppermute | solution.py:341
  83.6 1.2 collective-permute-done.8.refs_5_
  84.8 5.2 %collective-permute-start.9 = (f32[6,2,8,128]{3,2,1,0:T(8,128)S(1)}, f32[6,2,8,128]{3,2,1,0:T(8,128)S(1)}, u32[]{:S(2)}, u32[]{:S(2)}) collective-permute-start(f32[6,2,8,128]{3,2,1,0:T(8,128)S(1)} %pad_maximum_fusion.3), channel_id=1, source_target_pairs={{0,8},{2,10},{4,12},{6,14},{8,0},{10,2},{12,4},{14,6},{1,9},{3,11}... | collective-permute-start | bytes 147464 | tf_op jit(solution)/shard_map/ppermute | solution.py:351
  90.0 0.6 terms.1
  90.6 0.1 reshape.51.q_ref
  90.7 5.0 %collective-permute-done.9 = f32[6,2,8,128]{3,2,1,0:T(8,128)S(1)} collective-permute-done((f32[6,2,8,128]{3,2,1,0:T(8,128)S(1)}, f32[6,2,8,128]{3,2,1,0:T(8,128)S(1)}, u32[]{:S(2)}, u32[]{:S(2)}) %collective-permute-start.9) | collective-permute-done | bytes 49184 | tf_op jit(solution)/shard_map/ppermute | solution.py:351
  95.7 3.3 %piece_states.9 = (f32[3,2,136,128]{3,2,1,0:T(8,128)S(1)}, f32[3,2,136,128]{3,2,1,0:T(8,128)S(1)}) custom-call(s32[4]{0:T(128)S(1)} %pad_add_fusion.m_ref, bf16[200,2048]{1,0:T(8,128)(2,1)S(1)} %pad_maximum_fusion.refs_0_, bf16[8,2048]{1,0:T(8,128)(2,1)S(1)} %pad_maximum_fusion.4.refs_1_.refs_2_, bf16[2048,256]{1,0:T(8,128)(2,1)S(1)} %bitcast.22, ...), custom_call_target="tpu_custom_call" | custom-call | flops 3355443200 | bytes 2097152 | tf_op jit(solution)/shard_map/piece_states/pallas_call | solution.py:120
  99.0 4.1 %piece_states.10 = (f32[3,2,136,128]{3,2,1,0:T(8,128)S(1)}, f32[3,2,136,128]{3,2,1,0:T(8,128)S(1)}) custom-call(s32[4]{0:T(128)S(1)} %pad_add_fusion.m_ref, bf16[200,2048]{1,0:T(8,128)(2,1)S(1)} %copy-done.11, bf16[200,2048]{1,0:T(8,128)(2,1)} %collective-permute-done.7.refs_1_, bf16[8,2048]{1,0:T(8,128)(2,1)S(1)} %pad_maximum_fusion.4.refs_1_.refs_2_, ...), custom_call_target="tpu_custom_call" | custom-call | flops 6710886400 | bytes 2097152 | tf_op jit(solution)/shard_map/piece_states/pallas_call | solution.py:120
  103.1 3.4 %piece_states.11 = (f32[3,2,136,128]{3,2,1,0:T(8,128)S(1)}, f32[3,2,136,128]{3,2,1,0:T(8,128)S(1)}) custom-call(s32[4]{0:T(128)S(1)} %pad_add_fusion.m_ref, bf16[200,2048]{1,0:T(8,128)(2,1)} %collective-permute-done.2.refs_0_, bf16[8,2048]{1,0:T(8,128)(2,1)S(1)} %pad_maximum_fusion.4.refs_1_.refs_2_, bf16[2048,256]{1,0:T(8,128)(2,1)S(1)} %bitcast.24, ...), custom_call_target="tpu_custom_call" | custom-call | flops 3355443200 | bytes 2097152 | tf_op jit(solution)/shard_map/piece_states/pallas_call | solution.py:120
  106.6 0.8 merged.1
  107.4 1.9 %collective-permute-start.12 = (f32[2,2,128,128]{3,2,1,0:T(8,128)S(1)}, f32[2,2,128,128]{3,2,1,0:T(8,128)S(1)}, u32[]{:S(2)}, u32[]{:S(2)}) collective-permute-start(f32[2,2,128,128]{3,2,1,0:T(8,128)S(1)} %get-tuple-element.55), channel_id=1, source_target_pairs={{0,1},{1,0},{2,3},{3,2},{4,5},{5,4},{6,7},{7,6},{8,9},{9,8},{10,11... | collective-permute-start | bytes 786440 | tf_op jit(solution)/shard_map/ppermute | solution.py:341
  109.3 1.5 %collective-permute-done.12.b_ref = f32[2,2,128,128]{3,2,1,0:T(8,128)S(1)} collective-permute-done((f32[2,2,128,128]{3,2,1,0:T(8,128)S(1)}, f32[2,2,128,128]{3,2,1,0:T(8,128)S(1)}, u32[]{:S(2)}, u32[]{:S(2)}) %collective-permute-start.12) | collective-permute-done | bytes 262176 | tf_op jit(solution)/shard_map/ppermute | solution.py:341
  110.8 0.1 summed.1
  111.0 4.0 %collective-permute-start.13 = (bf16[2,144,128]{2,1,0:T(8,128)(2,1)S(1)}, bf16[2,144,128]{2,1,0:T(8,128)(2,1)S(1)}, u32[]{:S(2)}, u32[]{:S(2)}) collective-permute-start(bf16[2,144,128]{2,1,0:T(8,128)(2,1)S(1)} %get-tuple-element.58), channel_id=1, source_target_pairs={{0,8},{2,10},{4,12},{6,14},{8,0},{10,2},{12,4},{14,6},{1,9},{3,11}... | collective-permute-start | bytes 221192 | tf_op jit(solution)/shard_map/ppermute | solution.py:351
  114.9 7.4 %collective-permute-done.13.b_ref = bf16[2,144,128]{2,1,0:T(8,128)(2,1)S(1)} collective-permute-done((bf16[2,144,128]{2,1,0:T(8,128)(2,1)S(1)}, bf16[2,144,128]{2,1,0:T(8,128)(2,1)S(1)}, u32[]{:S(2)}, u32[]{:S(2)}) %collective-permute-start.13) | collective-permute-done | bytes 73760 | tf_op jit(solution)/shard_map/ppermute | solution.py:351
  122.4 0.2 packed.1
  122.5 20.3 %all_to_all.10.got_ref = bf16[32,16,128]{2,1,0:T(8,128)(2,1)S(1)} all-to-all(bf16[32,16,128]{2,1,0:T(8,128)(2,1)S(1)} %packed.1), channel_id=1, replica_groups=mesh['sp'=32,'y'=8,'c'=2] {'sp'}, dimensions={0} | all-to-all | bytes 262144 | tf_op jit(solution)/shard_map/all_to_all | solution.py:414
  142.8 1.6 %finished.1 = (bf16[2,2,2,128]{3,2,1,0:T(2,128)(2,1)}, bf16[2,2,2]{2,1,0:T(2,128)(2,1)}) custom-call(s32[4]{0:T(128)S(1)} %pad_add_fusion.m_ref, bf16[32,16,128]{2,1,0:T(8,128)(2,1)S(1)} %all_to_all.10.got_ref, f32[8,128]{1,0:T(8,128)S(1)} %get-tuple-element.61.fix_ref), custom_call_target="tpu_custom_call" | custom-call | tf_op jit(solution)/shard_map/finished/pallas_call | solution.py:317
  (63 shorter events, 0.6 us)
Async XLA Ops:
  0.6 10.4 %copy-start.2 = (bf16[2,128]{1,0:T(2,128)(2,1)S(1)}, bf16[2,128]{1,0:T(2,128)(2,1)}, u32[]{:S(2)}) copy-start(bf16[2,128]{1,0:T(2,128)(2,1)} %q_ref.1) | copy-start | bytes 1540
  0.6 10.5 %copy-start.16 = (bf16[4,128]{1,0:T(4,128)(2,1)S(1)}, bf16[4,128]{1,0:T(4,128)(2,1)}, u32[]{:S(2)}) copy-start(bf16[4,128]{1,0:T(4,128)(2,1)} %param.20) | copy-start | bytes 3076
  0.7 10.5 %copy-start.17 = (bf16[4,128]{1,0:T(4,128)(2,1)S(1)}, bf16[4,128]{1,0:T(4,128)(2,1)}, u32[]{:S(2)}) copy-start(bf16[4,128]{1,0:T(4,128)(2,1)} %param.19) | copy-start | bytes 3076
  0.7 10.5 %copy-start.3 = (f32[2]{0:T(128)S(1)}, f32[2]{0:T(128)}, u32[]{:S(2)}) copy-start(f32[2]{0:T(128)} %r_ref.1) | copy-start | bytes 28
  0.7 10.5 %copy-start.4 = (f32[2]{0:T(128)S(1)}, f32[2]{0:T(128)}, u32[]{:S(2)}) copy-start(f32[2]{0:T(128)} %b_ref.1) | copy-start | bytes 28
  0.7 10.6 %copy-start.15 = (f32[2,1536,2]{1,2,0:T(2,128)S(1)}, f32[2,1536,2]{1,2,0:T(2,128)}, u32[]{:S(2)}) copy-start(f32[2,1536,2]{1,2,0:T(2,128)} %param.23) | copy-start | bytes 73732
  1.6 35.7 %collective-permute-start = (bf16[8,2048]{1,0:T(8,128)(2,1)S(1)}, bf16[8,2048]{1,0:T(8,128)(2,1)S(1)}, u32[]{:S(2)}, u32[]{:S(2)}) collective-permute-start(bf16[8,2048]{1,0:T(8,128)(2,1)S(1)} %reshape.43), channel_id=1, source_target_pairs={{0,1},{1,2},{2,3},{3,4},{4,5},{5,6},{6,7},{7,8},{8,9},{9,10},{10,1... | collective-permute-start | bytes 98312 | tf_op jit(solution)/shard_map/ppermute | solution.py:362
  3.6 1.0 copy-start
  4.7 1.0 copy-start.1
  7.4 55.7 %collective-permute-start.3 = (bf16[2048,256]{1,0:T(8,128)(2,1)}, bf16[2048,256]{1,0:T(8,128)(2,1)}, u32[]{:S(2)}, u32[]{:S(2)}) collective-permute-start(bf16[2048,256]{1,0:T(8,128)(2,1)} %get-tuple-element.32.refs_2_.refs_3_), channel_id=1, source_target_pairs={{0,1},{1,0},{2,3},{3,2},{4,5},{5,4},{6,7},{7,6},{8,9},{9,8},{10,11... | collective-permute-start | bytes 3145736 | tf_op jit(solution)/shard_map/ppermute | solution.py:341
  11.3 28.1 %collective-permute-start.4 = (f32[2,2,1984]{2,1,0:T(2,128)S(1)}, f32[2,2,1984]{2,1,0:T(2,128)S(1)}, u32[]{:S(2)}, u32[]{:S(2)}) collective-permute-start(f32[2,2,1984]{2,1,0:T(2,128)S(1)} %pad_maximum_fusion.5), channel_id=1, source_target_pairs={{0,1},{1,0},{2,3},{3,2},{4,5},{5,4},{6,7},{7,6},{8,9},{9,8},{10,11... | collective-permute-start | bytes 95240 | tf_op jit(solution)/shard_map/ppermute | solution.py:341
  13.2 9.7 %collective-permute-start.10 = (bf16[64,256]{1,0:T(8,128)(2,1)S(1)}, bf16[64,256]{1,0:T(8,128)(2,1)S(1)}, u32[]{:S(2)}, u32[]{:S(2)}) collective-permute-start(bf16[64,256]{1,0:T(8,128)(2,1)S(1)} %get-tuple-element.43), channel_id=1, source_target_pairs={{0,8},{2,10},{4,12},{6,14},{8,0},{10,2},{12,4},{14,6},{1,9},{3,11}... | collective-permute-start | bytes 98312 | tf_op jit(solution)/shard_map/ppermute | solution.py:351
  24.0 13.3 %copy-start.14 = (bf16[2,96,2048]{2,1,0:T(8,128)(2,1)S(1)}, bf16[2,96,2048]{2,1,0:T(8,128)(2,1)}, u32[]{:S(2)}) copy-start(bf16[2,96,2048]{2,1,0:T(8,128)(2,1)} %param.15) | copy-start | bytes 2359300
  24.0 43.5 %all-to-all-start = ((bf16[32,64,256]{2,1,0:T(8,128)(2,1)}), bf16[32,64,256]{2,1,0:T(8,128)(2,1)S(1)}, u32[]{:S(2)}, u32[]{:S(2)}) async-start(bf16[32,64,256]{2,1,0:T(8,128)(2,1)} %broadcast_in_dim.5), calls=%async_computation | async-start | bytes 2097152 | tf_op jit(solution)/shard_map/all_to_all | solution.py:357
  37.4 12.4 %collective-permute-start.6 = (bf16[200,2048]{1,0:T(8,128)(2,1)S(1)}, bf16[200,2048]{1,0:T(8,128)(2,1)}, u32[]{:S(2)}, u32[]{:S(2)}) collective-permute-start(bf16[200,2048]{1,0:T(8,128)(2,1)S(1)} %pad_maximum_fusion.refs_0_), channel_id=1, source_target_pairs={{0,1},{1,0},{2,3},{3,2},{4,5},{5,4},{6,7},{7,6},{8,9},{9,8},{10,11... | collective-permute-start | bytes 2457608 | tf_op jit(solution)/shard_map/ppermute | solution.py:341
  39.4 10.3 %collective-permute-start.5 = (f32[2,4,1984]{2,1,0:T(4,128)S(1)}, f32[2,4,1984]{2,1,0:T(4,128)S(1)}, u32[]{:S(2)}, u32[]{:S(2)}) collective-permute-start(f32[2,4,1984]{2,1,0:T(4,128)S(1)} %pad_maximum_fusion.2), channel_id=1, source_target_pairs={{0,8},{2,10},{4,12},{6,14},{8,0},{10,2},{12,4},{14,6},{1,9},{3,11}... | collective-permute-start | bytes 190472 | tf_op jit(solution)/shard_map/ppermute | solution.py:351
  45.9 14.2 %collective-permute-start.1 = (bf16[200,2048]{1,0:T(8,128)(2,1)S(1)}, bf16[200,2048]{1,0:T(8,128)(2,1)S(1)}, u32[]{:S(2)}, u32[]{:S(2)}) collective-permute-start(bf16[200,2048]{1,0:T(8,128)(2,1)S(1)} %pad_maximum_fusion.refs_0_), channel_id=1, source_target_pairs={{0,2},{1,15},{2,4},{3,1},{4,6},{5,3},{6,8},{7,5},{8,10},{9,7},{10,... | collective-permute-start | bytes 2457608 | tf_op jit(solution)/shard_map/ppermute | solution.py:348
  49.8 19.5 %collective-permute-start.7 = (bf16[200,2048]{1,0:T(8,128)(2,1)}, bf16[200,2048]{1,0:T(8,128)(2,1)}, u32[]{:S(2)}, u32[]{:S(2)}) collective-permute-start(bf16[200,2048]{1,0:T(8,128)(2,1)} %collective-permute-done.6), channel_id=1, source_target_pairs={{0,2},{1,15},{2,4},{3,1},{4,6},{5,3},{6,8},{7,5},{8,10},{9,7},{10,... | collective-permute-start | bytes 2457608 | tf_op jit(solution)/shard_map/ppermute | solution.py:348
  60.1 9.2 %copy-start.10 = (bf16[200,2048]{1,0:T(8,128)(2,1)}, bf16[200,2048]{1,0:T(8,128)(2,1)S(1)}, u32[]{:S(2)}) copy-start(bf16[200,2048]{1,0:T(8,128)(2,1)S(1)} %collective-permute-done.1.refs_0_) | copy-start | bytes 2457604
  60.2 17.7 %collective-permute-start.2 = (bf16[200,2048]{1,0:T(8,128)(2,1)S(1)}, bf16[200,2048]{1,0:T(8,128)(2,1)}, u32[]{:S(2)}, u32[]{:S(2)}) collective-permute-start(bf16[200,2048]{1,0:T(8,128)(2,1)S(1)} %collective-permute-done.1.refs_0_), channel_id=1, source_target_pairs={{0,2},{1,15},{2,4},{3,1},{4,6},{5,3},{6,8},{7,5},{8,10},{9,7},{10,... | collective-permute-start | bytes 2457608 | tf_op jit(solution)/shard_map/ppermute | solution.py:348
  66.7 0.7 copy-start.12
  67.5 28.2 %collective-permute-start.11 = (bf16[2048,256]{1,0:T(8,128)(2,1)S(1)}, bf16[2048,256]{1,0:T(8,128)(2,1)}, u32[]{:S(2)}, u32[]{:S(2)}) collective-permute-start(bf16[2048,256]{1,0:T(8,128)(2,1)S(1)} %bitcast.21), channel_id=1, source_target_pairs={{0,1},{1,0},{2,3},{3,2},{4,5},{5,4},{6,7},{7,6},{8,9},{9,8},{10,11... | collective-permute-start | bytes 3145736 | tf_op jit(solution)/shard_map/ppermute | solution.py:341
  69.4 1.0 copy-start.13
  77.8 12.1 %copy-start.5 = (f32[2,2]{1,0:T(2,128)S(1)}, f32[2,2]{1,0:T(2,128)}, u32[]{:S(2)}) copy-start(f32[2,2]{1,0:T(2,128)} %n_ref.1) | copy-start | bytes 52
  77.8 12.1 %copy-start.6 = (bf16[2,128]{1,0:T(2,128)(2,1)S(1)}, bf16[2,128]{1,0:T(2,128)(2,1)}, u32[]{:S(2)}) copy-start(bf16[2,128]{1,0:T(2,128)(2,1)} %v_ref.3) | copy-start | bytes 1540
  77.8 12.1 %copy-start.7 = (bf16[2,128]{1,0:T(2,128)(2,1)S(1)}, bf16[2,128]{1,0:T(2,128)(2,1)}, u32[]{:S(2)}) copy-start(bf16[2,128]{1,0:T(2,128)(2,1)} %k_ref.3) | copy-start | bytes 1540
  77.8 12.2 %copy-start.8 = (bf16[2,128]{1,0:T(2,128)(2,1)S(1)}, bf16[2,128]{1,0:T(2,128)(2,1)}, u32[]{:S(2)}) copy-start(bf16[2,128]{1,0:T(2,128)(2,1)} %g_ref.1) | copy-start | bytes 1540
  77.8 12.2 %copy-start.9 = (bf16[128]{0:T(256)(128)(2,1)S(1)}, bf16[128]{0:T(256)(128)(2,1)}, u32[]{:S(2)}) copy-start(bf16[128]{0:T(256)(128)(2,1)} %param.29) | copy-start | bytes 772
  81.7 3.1 %collective-permute-start.8 = (f32[3,2,8,128]{3,2,1,0:T(8,128)S(1)}, f32[3,2,8,128]{3,2,1,0:T(8,128)S(1)}, u32[]{:S(2)}, u32[]{:S(2)}) collective-permute-start(f32[3,2,8,128]{3,2,1,0:T(8,128)S(1)} %slice.57.refs_4_), channel_id=1, source_target_pairs={{0,1},{1,0},{2,3},{3,2},{4,5},{5,4},{6,7},{7,6},{8,9},{9,8},{10,11... | collective-permute-start | bytes 73736 | tf_op jit(solution)/shard_map/ppermute | solution.py:341
  84.8 10.9 %collective-permute-start.9 = (f32[6,2,8,128]{3,2,1,0:T(8,128)S(1)}, f32[6,2,8,128]{3,2,1,0:T(8,128)S(1)}, u32[]{:S(2)}, u32[]{:S(2)}) collective-permute-start(f32[6,2,8,128]{3,2,1,0:T(8,128)S(1)} %pad_maximum_fusion.3), channel_id=1, source_target_pairs={{0,8},{2,10},{4,12},{6,14},{8,0},{10,2},{12,4},{14,6},{1,9},{3,11}... | collective-permute-start | bytes 147464 | tf_op jit(solution)/shard_map/ppermute | solution.py:351
  95.7 3.3 %copy-start.11 = (bf16[200,2048]{1,0:T(8,128)(2,1)S(1)}, bf16[200,2048]{1,0:T(8,128)(2,1)}, u32[]{:S(2)}) copy-start(bf16[200,2048]{1,0:T(8,128)(2,1)} %copy-done.10) | copy-start | bytes 2457604
  107.4 3.4 %collective-permute-start.12 = (f32[2,2,128,128]{3,2,1,0:T(8,128)S(1)}, f32[2,2,128,128]{3,2,1,0:T(8,128)S(1)}, u32[]{:S(2)}, u32[]{:S(2)}) collective-permute-start(f32[2,2,128,128]{3,2,1,0:T(8,128)S(1)} %get-tuple-element.55), channel_id=1, source_target_pairs={{0,1},{1,0},{2,3},{3,2},{4,5},{5,4},{6,7},{7,6},{8,9},{9,8},{10,11... | collective-permute-start | bytes 786440 | tf_op jit(solution)/shard_map/ppermute | solution.py:341
  111.0 11.4 %collective-permute-start.13 = (bf16[2,144,128]{2,1,0:T(8,128)(2,1)S(1)}, bf16[2,144,128]{2,1,0:T(8,128)(2,1)S(1)}, u32[]{:S(2)}, u32[]{:S(2)}) collective-permute-start(bf16[2,144,128]{2,1,0:T(8,128)(2,1)S(1)} %get-tuple-element.58), channel_id=1, source_target_pairs={{0,8},{2,10},{4,12},{6,14},{8,0},{10,2},{12,4},{14,6},{1,9},{3,11}... | collective-permute-start | bytes 221192 | tf_op jit(solution)/shard_map/ppermute | solution.py:351

commit v4 on v2

--- a/solution.py
+++ b/solution.py
@@ -17,6 +17,17 @@
 
 def mm(a, b, dims, precision=None):
     return lax.dot_general(a, b, (dims, ((), ())), preferred_element_type=F32, precision=precision)
+
+
+def halves(v):
+    high = v.astype(BF)
+    return high, (v - high.astype(F32)).astype(BF)
+
+
+def product(a, b):
+    (ah, al), (bh, bl) = halves(a), halves(b)
+    dims = ((0,), (0,))
+    return mm(ah, bh, dims) + (mm(al, bh, dims) + mm(ah, bl, dims))
 
 
 def softplus(v):
@@ -96,9 +107,9 @@
                         mixed[:, 256 * g + 64 * e : 256 * g + 64 * e + 64] * lift[:, 2 * g + e : 2 * g + e + 1]
                         for e in range(2)
                     ]
-                    values = jnp.concatenate(parts, axis=1).astype(BF)
-                    keys = mixed[:, 256 * g + 128 : 256 * g + 256].astype(BF)
-                    states[g] = states[g] + mm(values, keys, ((0,), (0,)))
+                    values = jnp.concatenate(parts, axis=1)
+                    keys = mixed[:, 256 * g + 128 : 256 * g + 256]
+                    states[g] = states[g] + product(values, keys)
             fade = jnp.where(low, 1.0, jnp.exp(total[s]))
             for g in range(2):
                 for e in range(2):
@@ -213,9 +224,9 @@
                 cut = state.astype(BF).reshape(sp_count, share, 128)
                 out_ref[:, 4 * s + 2 * e : 4 * s + 2 * e + share, :] = cut
             read = jnp.concatenate(reads, axis=1)
-            high = read.astype(BF)
+            high, low_part = halves(read)
             put(8 + s, high)
-            put(10 + s, (read - high.astype(F32)).astype(BF))
+            put(10 + s, low_part)
         for k in range(3):
             part = left.astype(BF)
             left = left - part.astype(F32)
@@ -236,16 +247,23 @@
     sp_count = got.shape[0]
 
     def body(m_ref, got_ref, fix_ref, state_out, read_out):
-        run = jnp.zeros((1, 128), F32)
-        total = jnp.zeros((16, 128), F32)
-        for j in reversed(range(sp_count)):
-            g = got_ref[j].astype(F32)
-            e = jnp.exp(run)
-            one = [jnp.broadcast_to(e[:, i : i + 1], (1, 128)) for i in range(4)]
-            both = [jnp.concatenate([one[2 * s][:, :64], one[2 * s + 1][:, 64:]], axis=1) for s in range(2)]
-            scale = jnp.concatenate([one[i // 2] for i in range(8)] + both * 4, axis=0)
-            total = total + g * scale
-            run = run + g[12:13] + g[13:14] + g[14:15]
+        blocks = [got_ref[j].astype(F32) for j in range(sp_count)]
+        decay = jnp.concatenate([g[12:13] + g[13:14] + g[14:15] for g in blocks], axis=0)
+        i = lax.broadcasted_iota(jnp.int32, (sp_count, sp_count), 0)
+        j = lax.broadcasted_iota(jnp.int32, (sp_count, sp_count), 1)
+        after = jnp.where(j > i, 1.0, 0.0)
+        fade = jnp.exp(mm(after, decay, ((1,), (0,)), lax.Precision.HIGHEST))
+        one = [jnp.broadcast_to(fade[:, i : i + 1], (sp_count, 128)) for i in range(4)]
+        lane = lax.broadcasted_iota(jnp.int32, (sp_count, 128), 1)
+        both = [jnp.where(lane < HEAD_DIM, one[2 * s], one[2 * s + 1]) for s in range(2)]
+        row = lax.broadcasted_iota(jnp.int32, (8, 128), 0)
+        total = [jnp.zeros((8, 128), F32)] * 2
+        for j, g in enumerate(blocks):
+            a, b, c, d = (v[j : j + 1] for v in one)
+            scale = jnp.where(row < 4, jnp.where(row < 2, a, b), jnp.where(row < 6, c, d))
+            total[0] = total[0] + g[:8] * scale
+            total[1] = total[1] + g[8:] * jnp.where(row % 2 == 0, both[0][j : j + 1], both[1][j : j + 1])
+        total = jnp.concatenate(total, axis=0)
         for s in range(2):
             for h in range(2):
                 state_out[s, h] = total[4 * s + 2 * h : 4 * s + 2 * h + 2].astype(BF)
@@ -294,12 +312,19 @@
 
     meta = jnp.stack([y, c, (128 - sp * share) % 128]).astype(jnp.int32)
 
+    x = hidden_in.reshape(2 * rows, width)
+    bare = onward(x)
     ends = hidden_in[:, rows - 4 :, :].reshape(8, width)
     ends = lax.ppermute(ends, ("sp", "y", "c"), [(i, i + 1) for i in range(count - 1)])
-    a = [jnp.concatenate([hidden_in.reshape(2 * rows, width), ends], axis=0)]
-    a.append(onward(a[0]))
+    a = [jnp.concatenate([x, ends], axis=0)]
     b = [swap(a[0])]
     b.append(onward(b[0]))
+    pairs = []
+    for i in range(y_count):
+        pairs.append((2 * i + 1, 2 * ((i + 1) % y_count)))
+        pairs.append((2 * i, 2 * ((i - 1) % y_count) + 1))
+    near = lax.ppermute(b[0][2 * rows :], ("y", "c"), pairs)
+    a.append(jnp.concatenate([bare, near], axis=0))
 
     w_own = joined(w_value, w_key, conv_value, conv_key)
     w_both = w_own, swap(w_own)

time: 114 us -> 119 us (1.044)
  starting transfers between devices: 40.8 us -> 48.7 us
  waiting for transfers between devices: 23.8 us -> 17.6 us
  local copies, waits for them, and re-layouts: 2.24 us -> 4.19 us
  Pallas kernels: 20.9 us -> 22.1 us
    ppermute x7, waiting for transfers between devices: 18.2 us -> 12 us  [onward(): return lax.ppermute(v, ('y', 'c'), pairs)]
    ppermute x7, starting transfers between devices: 25.9 us -> 29.4 us  [onward(): return lax.ppermute(v, ('y', 'c'), pairs)]
    ppermute x0 -> x1, starting transfers between devices: none -> 2.32 us  [per_device(): near = lax.ppermute(b[0][2 * rows:], ('y', 'c'), pairs)]
    ppermute x4, starting transfers between devices: 10.4 us -> 12.5 us  [swap(): return lax.ppermute(v, 'c', [(0, 1), (1, 0)])]
  transfers between devices with their start and end apart: 12 -> 13, of which waited for: 9 -> 6; matrix products, arithmetic and copies ran while one was open for 2% -> 3% of each run, Pallas kernels for 14% -> 14%
where the time goes in v4:
time: 119 us; the launch traced here: 118 us
  starting transfers between devices  48.7 us (41%)
  blocking collectives  22.4 us (19%)
  Pallas kernels  22.1 us (19%)
  waiting for transfers between devices  17.6 us (15%)
  local copies, waits for them, and re-layouts  4.19 us (4%)
  other arithmetic  2.12 us (2%)
    ppermute x7, starting transfers between devices, onward(): return lax.ppermute(v, ('y', 'c'), pairs)  29.4 us
    all_to_all x1, blocking collectives, per_device(): got = lax.all_to_all(sent, 'sp', 0, 0, tiled=True)  22.4 us
    pallas_call x5, Pallas kernels, piece_states(): pl.pallas_call(body, out_shape=[jax.ShapeDtypeStruct(shape, F32)] * 2, in...  18.8 us
    ppermute x4, starting transfers between devices, swap(): return lax.ppermute(v, 'c', [(0, 1), (1, 0)])  12.5 us
    ppermute x7, waiting for transfers between devices, onward(): return lax.ppermute(v, ('y', 'c'), pairs)  12 us
    ppermute x1, starting transfers between devices, per_device(): lax.ppermute(ends, ('sp', 'y', 'c'), [(i, i + 1) for i in range(count - 1)])  4.58 us
    ppermute x1, waiting for transfers between devices, per_device(): lax.ppermute(ends, ('sp', 'y', 'c'), [(i, i + 1) for i in range(count - 1)])  4.22 us
  transfers between devices with their start and end apart: 13, of which 6 were waited for; matrix products, arithmetic and copies ran while one was open for 3% of the time, Pallas kernels for 14%

profile of v4, /device:TPU:1, one launch (start us, length us, event | category | flops | bytes accessed | tf_op | source)
XLA Modules:
  0.0 118.3 jit_solution(132912644645410138)
XLA Ops:
  0.7 0.9 slice.20
  1.6 4.6 %collective-permute-start.1 = (bf16[8,2048]{1,0:T(8,128)(2,1)S(1)}, bf16[8,2048]{1,0:T(8,128)(2,1)S(1)}, u32[]{:S(2)}, u32[]{:S(2)}) collective-permute-start(bf16[8,2048]{1,0:T(8,128)(2,1)S(1)} %reshape.21), channel_id=1, source_target_pairs={{0,1},{1,2},{2,3},{3,4},{4,5},{5,6},{6,7},{7,8},{8,9},{9,10},{10,1... | collective-permute-start | bytes 98312 | tf_op jit(solution)/shard_map/ppermute | solution.py:318
  6.2 4.2 %collective-permute-done.1 = bf16[8,2048]{1,0:T(8,128)(2,1)S(1)} collective-permute-done((bf16[8,2048]{1,0:T(8,128)(2,1)S(1)}, bf16[8,2048]{1,0:T(8,128)(2,1)S(1)}, u32[]{:S(2)}, u32[]{:S(2)}) %collective-permute-start.1) | collective-permute-done | bytes 32800 | tf_op jit(solution)/shard_map/ppermute | solution.py:318
  10.5 1.2 %pad_maximum_fusion.refs_0_ = bf16[200,2048]{1,0:T(8,128)(2,1)S(1)} fusion(bf16[8,2048]{1,0:T(8,128)(2,1)S(1)} %collective-permute-done.1, bf16[192,2048]{1,0:T(8,128)(2,1)} %bitcast.16), kind=kLoop, calls=%fused_computation | loop fusion | flops 1638400 | bytes 1638400 | tf_op jit(solution)/shard_map/concatenate | solution.py:319
  11.6 0.0 copy-start.2
  11.7 0.0 copy-start.3
  11.7 0.0 copy-start.12
  11.7 2.2 %collective-permute-start.2 = (bf16[200,2048]{1,0:T(8,128)(2,1)S(1)}, bf16[200,2048]{1,0:T(8,128)(2,1)}, u32[]{:S(2)}, u32[]{:S(2)}) collective-permute-start(bf16[200,2048]{1,0:T(8,128)(2,1)S(1)} %pad_maximum_fusion.refs_0_), channel_id=1, source_target_pairs={{0,1},{1,0},{2,3},{3,2},{4,5},{5,4},{6,7},{7,6},{8,9},{9,8},{10,11... | collective-permute-start | bytes 2457608 | tf_op jit(solution)/shard_map/ppermute | solution.py:304
  13.9 2.8 %collective-permute-start = (bf16[192,2048]{1,0:T(8,128)(2,1)}, bf16[192,2048]{1,0:T(8,128)(2,1)}, u32[]{:S(2)}, u32[]{:S(2)}) collective-permute-start(bf16[192,2048]{1,0:T(8,128)(2,1)} %bitcast.17), channel_id=1, source_target_pairs={{0,2},{1,15},{2,4},{3,1},{4,6},{5,3},{6,8},{7,5},{8,10},{9,7},{10,... | collective-permute-start | bytes 2359304 | tf_op jit(solution)/shard_map/ppermute | solution.py:311
  16.8 0.2 joined.1.refs_2_.refs_3_
  17.0 0.0 copy-start.6
  17.0 0.0 copy-start.7
  17.0 0.0 copy-start.8
  17.0 0.0 copy-start.9
  17.0 0.0 copy-start.10
  17.1 2.1 %collective-permute-start.7 = (bf16[2052,256]{1,0:T(8,128)(2,1)S(1)}, bf16[2052,256]{1,0:T(8,128)(2,1)}, u32[]{:S(2)}, u32[]{:S(2)}) collective-permute-start(bf16[2052,256]{1,0:T(8,128)(2,1)S(1)} %joined.1.refs_2_.refs_3_), channel_id=1, source_target_pairs={{0,1},{1,0},{2,3},{3,2},{4,5},{5,4},{6,7},{7,6},{8,9},{9,8},{10,11... | collective-permute-start | bytes 3151880 | tf_op jit(solution)/shard_map/ppermute | solution.py:304
  19.1 0.1 broadcast_in_dim.2
  19.2 2.4 %collective-permute-start.8 = (f32[2,2,1664]{2,1,0:T(2,128)S(1)}, f32[2,2,1664]{2,1,0:T(2,128)S(1)}, u32[]{:S(2)}, u32[]{:S(2)}) collective-permute-start(f32[2,2,1664]{2,1,0:T(2,128)S(1)} %pad_maximum_fusion.1), channel_id=1, source_target_pairs={{0,1},{1,0},{2,3},{3,2},{4,5},{5,4},{6,7},{7,6},{8,9},{9,8},{10,11... | collective-permute-start | bytes 79880 | tf_op jit(solution)/shard_map/ppermute | solution.py:304
  21.7 0.8 dynamic-slice_bitcast_fusion
  22.5 0.8 slice.26
  23.2 2.3 %collective-permute-start.3 = (bf16[8,2048]{1,0:T(8,128)(2,1)S(1)}, bf16[8,2048]{1,0:T(8,128)(2,1)S(1)}, u32[]{:S(2)}, u32[]{:S(2)}) collective-permute-start(bf16[8,2048]{1,0:T(8,128)(2,1)S(1)} %slice.26), channel_id=1, source_target_pairs={{1,2},{0,15},{3,4},{2,1},{5,6},{4,3},{7,8},{6,5},{9,10},{8,7},{11,... | collective-permute-start | bytes 98312 | tf_op jit(solution)/shard_map/ppermute | solution.py:326
  25.6 4.1 %collective-permute-start.9 = (bf16[200,2048]{1,0:T(8,128)(2,1)}, bf16[200,2048]{1,0:T(8,128)(2,1)}, u32[]{:S(2)}, u32[]{:S(2)}) collective-permute-start(bf16[200,2048]{1,0:T(8,128)(2,1)} %collective-permute-done.2), channel_id=1, source_target_pairs={{0,2},{1,15},{2,4},{3,1},{4,6},{5,3},{6,8},{7,5},{8,10},{9,7},{10,... | collective-permute-start | bytes 2457608 | tf_op jit(solution)/shard_map/ppermute | solution.py:311
  29.6 1.2 %constant_dynamic-update-slice_fusion.1 = bf16[200,2048]{1,0:T(8,128)(2,1)S(1)} fusion(bf16[192,2048]{1,0:T(8,128)(2,1)} %collective-permute-done), kind=kLoop, calls=%fused_computation.8 | loop fusion | bytes 1572864
  30.8 3.1 %collective-permute-start.4 = (bf16[200,2048]{1,0:T(8,128)(2,1)S(1)}, bf16[200,2048]{1,0:T(8,128)(2,1)}, u32[]{:S(2)}, u32[]{:S(2)}) collective-permute-start(bf16[200,2048]{1,0:T(8,128)(2,1)S(1)} %constant_dynamic-update-slice_fusion.refs_0_), channel_id=1, source_target_pairs={{0,2},{1,15},{2,4},{3,1},{4,6},{5,3},{6,8},{7,5},{8,10},{9,7},{10,... | collective-permute-start | bytes 2457608 | tf_op jit(solution)/shard_map/ppermute | solution.py:311
  33.9 5.3 %collective-permute-done.9.refs_1_ = bf16[200,2048]{1,0:T(8,128)(2,1)} collective-permute-done((bf16[200,2048]{1,0:T(8,128)(2,1)}, bf16[200,2048]{1,0:T(8,128)(2,1)}, u32[]{:S(2)}, u32[]{:S(2)}) %collective-permute-start.9) | collective-permute-done | bytes 819232 | tf_op jit(solution)/shard_map/ppermute | solution.py:311
  39.3 5.0 %collective-permute-start.10 = (bf16[200,2048]{1,0:T(8,128)(2,1)}, bf16[200,2048]{1,0:T(8,128)(2,1)}, u32[]{:S(2)}, u32[]{:S(2)}) collective-permute-start(bf16[200,2048]{1,0:T(8,128)(2,1)} %collective-permute-done.9.refs_1_), channel_id=1, source_target_pairs={{0,2},{1,15},{2,4},{3,1},{4,6},{5,3},{6,8},{7,5},{8,10},{9,7},{10,... | collective-permute-start | bytes 2457608 | tf_op jit(solution)/shard_map/ppermute | solution.py:311
  44.2 0.8 maximum_select_fusion
  45.0 0.1 pad_add_fusion.m_ref
  45.2 0.6 terms.1
  45.9 0.1 reshape.22
  46.0 0.1 copy.17
  46.1 0.1 reshape.23.refs_4_.refs_5_
  46.2 1.8 %collective-permute-done.4.refs_0_ = bf16[200,2048]{1,0:T(8,128)(2,1)} collective-permute-done((bf16[200,2048]{1,0:T(8,128)(2,1)S(1)}, bf16[200,2048]{1,0:T(8,128)(2,1)}, u32[]{:S(2)}, u32[]{:S(2)}) %collective-permute-start.4) | collective-permute-done | bytes 819232 | tf_op jit(solution)/shard_map/ppermute | solution.py:311
  48.0 5.0 %collective-permute-start.5 = (bf16[200,2048]{1,0:T(8,128)(2,1)}, bf16[200,2048]{1,0:T(8,128)(2,1)S(1)}, u32[]{:S(2)}, u32[]{:S(2)}) collective-permute-start(bf16[200,2048]{1,0:T(8,128)(2,1)} %collective-permute-done.4.refs_0_), channel_id=1, source_target_pairs={{0,2},{1,15},{2,4},{3,1},{4,6},{5,3},{6,8},{7,5},{8,10},{9,7},{10,... | collective-permute-start | bytes 2457608 | tf_op jit(solution)/shard_map/ppermute | solution.py:311
  53.0 3.2 %piece_states.5 = (f32[3,2,136,128]{3,2,1,0:T(8,128)S(1)}, f32[3,2,136,128]{3,2,1,0:T(8,128)S(1)}) custom-call(s32[3]{0:T(128)S(1)} %pad_add_fusion.m_ref, bf16[200,2048]{1,0:T(8,128)(2,1)S(1)} %pad_maximum_fusion.refs_0_, bf16[8,2048]{1,0:T(8,128)(2,1)S(1)} %pad.8.refs_1_.refs_2_, bf16[2052,256]{1,0:T(8,128)(2,1)S(1)} %joined.1.refs_2_.refs_3_, ...), custom_call_target="tpu_custom_call" | custom-call | flops 3361996800 | bytes 2101248 | tf_op jit(solution)/shard_map/piece_states/pallas_call | solution.py:122
  56.2 0.6 collective-permute-done.10.refs_1_
  56.8 5.0 %collective-permute-start.11 = (bf16[200,2048]{1,0:T(8,128)(2,1)}, bf16[200,2048]{1,0:T(8,128)(2,1)S(1)}, u32[]{:S(2)}, u32[]{:S(2)}) collective-permute-start(bf16[200,2048]{1,0:T(8,128)(2,1)} %collective-permute-done.10.refs_1_), channel_id=1, source_target_pairs={{0,2},{1,15},{2,4},{3,1},{4,6},{5,3},{6,8},{7,5},{8,10},{9,7},{10,... | collective-permute-start | bytes 2457608 | tf_op jit(solution)/shard_map/ppermute | solution.py:311
  61.8 4.1 %piece_states.6 = (f32[3,2,136,128]{3,2,1,0:T(8,128)S(1)}, f32[3,2,136,128]{3,2,1,0:T(8,128)S(1)}) custom-call(s32[3]{0:T(128)S(1)} %pad_add_fusion.m_ref, bf16[200,2048]{1,0:T(8,128)(2,1)S(1)} %constant_dynamic-update-slice_fusion.refs_0_, bf16[200,2048]{1,0:T(8,128)(2,1)} %collective-permute-done.9.refs_1_, bf16[8,2048]{1,0:T(8,128)(2,1)S(1)} %pad.8.refs_1_.refs_2_, ...), custom_call_target="tpu_custom_call" | custom-call | flops 6723993600 | bytes 2101248 | tf_op jit(solution)/shard_map/piece_states/pallas_call | solution.py:122
  65.9 4.5 %collective-permute-start.6 = (bf16[200,2048]{1,0:T(8,128)(2,1)S(1)}, bf16[200,2048]{1,0:T(8,128)(2,1)S(1)}, u32[]{:S(2)}, u32[]{:S(2)}) collective-permute-start(bf16[200,2048]{1,0:T(8,128)(2,1)S(1)} %collective-permute-done.5.refs_0_), channel_id=1, source_target_pairs={{0,2},{1,15},{2,4},{3,1},{4,6},{5,3},{6,8},{7,5},{8,10},{9,7},{10,... | collective-permute-start | bytes 2457608 | tf_op jit(solution)/shard_map/ppermute | solution.py:311
  70.5 4.4 %piece_states.7 = (f32[3,2,136,128]{3,2,1,0:T(8,128)S(1)}, f32[3,2,136,128]{3,2,1,0:T(8,128)S(1)}) custom-call(s32[3]{0:T(128)S(1)} %pad_add_fusion.m_ref, bf16[200,2048]{1,0:T(8,128)(2,1)} %collective-permute-done.4.refs_0_, bf16[200,2048]{1,0:T(8,128)(2,1)} %collective-permute-done.10.refs_1_, bf16[8,2048]{1,0:T(8,128)(2,1)S(1)} %pad.8.refs_1_.refs_2_, ...), custom_call_target="tpu_custom_call" | custom-call | flops 6723993600 | bytes 2101248 | tf_op jit(solution)/shard_map/piece_states/pallas_call | solution.py:122
  74.8 3.9 %piece_states.8 = (f32[3,2,136,128]{3,2,1,0:T(8,128)S(1)}, f32[3,2,136,128]{3,2,1,0:T(8,128)S(1)}) custom-call(s32[3]{0:T(128)S(1)} %pad_add_fusion.m_ref, bf16[200,2048]{1,0:T(8,128)(2,1)S(1)} %collective-permute-done.5.refs_0_, bf16[200,2048]{1,0:T(8,128)(2,1)S(1)} %collective-permute-done.11.refs_1_, bf16[8,2048]{1,0:T(8,128)(2,1)S(1)} %pad.8.refs_1_.refs_2_, ...), custom_call_target="tpu_custom_call" | custom-call | flops 6723993600 | bytes 2101248 | tf_op jit(solution)/shard_map/piece_states/pallas_call | solution.py:122
  78.7 4.3 %collective-permute-done.6.refs_0_ = bf16[200,2048]{1,0:T(8,128)(2,1)S(1)} collective-permute-done((bf16[200,2048]{1,0:T(8,128)(2,1)S(1)}, bf16[200,2048]{1,0:T(8,128)(2,1)S(1)}, u32[]{:S(2)}, u32[]{:S(2)}) %collective-permute-start.6) | collective-permute-done | bytes 819232 | tf_op jit(solution)/shard_map/ppermute | solution.py:311
  83.0 3.2 %piece_states.9 = (f32[3,2,136,128]{3,2,1,0:T(8,128)S(1)}, f32[3,2,136,128]{3,2,1,0:T(8,128)S(1)}) custom-call(s32[3]{0:T(128)S(1)} %pad_add_fusion.m_ref, bf16[200,2048]{1,0:T(8,128)(2,1)S(1)} %collective-permute-done.6.refs_0_, bf16[8,2048]{1,0:T(8,128)(2,1)S(1)} %pad.8.refs_1_.refs_2_, bf16[2052,256]{1,0:T(8,128)(2,1)S(1)} %joined.1.refs_2_.refs_3_, ...), custom_call_target="tpu_custom_call" | custom-call | flops 3361996800 | bytes 2101248 | tf_op jit(solution)/shard_map/piece_states/pallas_call | solution.py:122
  86.2 5.8 %collective-permute-start.12 = (f32[3,2,136,128]{3,2,1,0:T(8,128)S(1)}, f32[3,2,136,128]{3,2,1,0:T(8,128)S(1)}, u32[]{:S(2)}, u32[]{:S(2)}) collective-permute-start(f32[3,2,136,128]{3,2,1,0:T(8,128)S(1)} %get-tuple-element.31), channel_id=1, source_target_pairs={{0,1},{1,0},{2,3},{3,2},{4,5},{5,4},{6,7},{7,6},{8,9},{9,8},{10,11... | collective-permute-start | bytes 1253384 | tf_op jit(solution)/shard_map/ppermute | solution.py:304
  92.1 1.4 %collective-permute-done.12.b_ref = f32[3,2,136,128]{3,2,1,0:T(8,128)S(1)} collective-permute-done((f32[3,2,136,128]{3,2,1,0:T(8,128)S(1)}, f32[3,2,136,128]{3,2,1,0:T(8,128)S(1)}, u32[]{:S(2)}, u32[]{:S(2)}) %collective-permute-start.12) | collective-permute-done | bytes 417824 | tf_op jit(solution)/shard_map/ppermute | solution.py:304
  93.4 0.8 packed.1
  94.2 22.4 %all_to_all.5.got_ref = bf16[32,16,128]{2,1,0:T(8,128)(2,1)S(1)} all-to-all(bf16[32,16,128]{2,1,0:T(8,128)(2,1)S(1)} %packed.1), channel_id=1, replica_groups=mesh['sp'=32,'y'=8,'c'=2] {'sp'}, dimensions={0} | all-to-all | bytes 262144 | tf_op jit(solution)/shard_map/all_to_all | solution.py:356
  116.6 1.6 %finished.1 = (bf16[2,2,2,128]{3,2,1,0:T(2,128)(2,1)}, bf16[2,2,2]{2,1,0:T(2,128)(2,1)}) custom-call(s32[3]{0:T(128)S(1)} %pad_add_fusion.m_ref, bf16[32,16,128]{2,1,0:T(8,128)(2,1)S(1)} %all_to_all.5.got_ref, f32[8,128]{1,0:T(8,128)S(1)} %get-tuple-element.33.fix_ref), custom_call_target="tpu_custom_call" | custom-call | tf_op jit(solution)/shard_map/finished/pallas_call | solution.py:280
  (34 shorter events, 0.2 us)
Async XLA Ops:
  0.6 16.1 %copy-start = (bf16[2048,128]{1,0:T(8,128)(2,1)S(1)}, bf16[2048,128]{1,0:T(8,128)(2,1)}, u32[]{:S(2)}) copy-start(bf16[2048,128]{1,0:T(8,128)(2,1)} %v_ref.2) | copy-start | bytes 1572868
  0.6 16.1 %copy-start.1 = (bf16[2048,128]{1,0:T(8,128)(2,1)S(1)}, bf16[2048,128]{1,0:T(8,128)(2,1)}, u32[]{:S(2)}) copy-start(bf16[2048,128]{1,0:T(8,128)(2,1)} %k_ref.2) | copy-start | bytes 1572868
  0.7 16.1 %copy-start.4 = (bf16[4,128]{1,0:T(4,128)(2,1)S(1)}, bf16[4,128]{1,0:T(4,128)(2,1)}, u32[]{:S(2)}) copy-start(bf16[4,128]{1,0:T(4,128)(2,1)} %cv_ref.1) | copy-start | bytes 3076
  0.7 16.1 %copy-start.5 = (bf16[4,128]{1,0:T(4,128)(2,1)S(1)}, bf16[4,128]{1,0:T(4,128)(2,1)}, u32[]{:S(2)}) copy-start(bf16[4,128]{1,0:T(4,128)(2,1)} %ck_ref.1) | copy-start | bytes 3076
  1.6 8.8 %collective-permute-start.1 = (bf16[8,2048]{1,0:T(8,128)(2,1)S(1)}, bf16[8,2048]{1,0:T(8,128)(2,1)S(1)}, u32[]{:S(2)}, u32[]{:S(2)}) collective-permute-start(bf16[8,2048]{1,0:T(8,128)(2,1)S(1)} %reshape.21), channel_id=1, source_target_pairs={{0,1},{1,2},{2,3},{3,4},{4,5},{5,6},{6,7},{7,8},{8,9},{9,10},{10,1... | collective-permute-start | bytes 98312 | tf_op jit(solution)/shard_map/ppermute | solution.py:318
  11.6 7.5 %copy-start.2 = (f32[2]{0:T(128)S(1)}, f32[2]{0:T(128)}, u32[]{:S(2)}) copy-start(f32[2]{0:T(128)} %r_ref.1) | copy-start | bytes 28
  11.7 7.5 %copy-start.3 = (f32[2]{0:T(128)S(1)}, f32[2]{0:T(128)}, u32[]{:S(2)}) copy-start(f32[2]{0:T(128)} %b_ref.1) | copy-start | bytes 28
  11.7 7.6 %copy-start.12 = (f32[2,1536,2]{1,2,0:T(2,128)S(1)}, f32[2,1536,2]{1,2,0:T(2,128)}, u32[]{:S(2)}) copy-start(f32[2,1536,2]{1,2,0:T(2,128)} %param.23) | copy-start | bytes 73732
  11.7 10.8 %collective-permute-start.2 = (bf16[200,2048]{1,0:T(8,128)(2,1)S(1)}, bf16[200,2048]{1,0:T(8,128)(2,1)}, u32[]{:S(2)}, u32[]{:S(2)}) collective-permute-start(bf16[200,2048]{1,0:T(8,128)(2,1)S(1)} %pad_maximum_fusion.refs_0_), channel_id=1, source_target_pairs={{0,1},{1,0},{2,3},{3,2},{4,5},{5,4},{6,7},{7,6},{8,9},{9,8},{10,11... | collective-permute-start | bytes 2457608 | tf_op jit(solution)/shard_map/ppermute | solution.py:304
  13.9 15.7 %collective-permute-start = (bf16[192,2048]{1,0:T(8,128)(2,1)}, bf16[192,2048]{1,0:T(8,128)(2,1)}, u32[]{:S(2)}, u32[]{:S(2)}) collective-permute-start(bf16[192,2048]{1,0:T(8,128)(2,1)} %bitcast.17), channel_id=1, source_target_pairs={{0,2},{1,15},{2,4},{3,1},{4,6},{5,3},{6,8},{7,5},{8,10},{9,7},{10,... | collective-permute-start | bytes 2359304 | tf_op jit(solution)/shard_map/ppermute | solution.py:311
  17.0 28.1 %copy-start.6 = (f32[2,2]{1,0:T(2,128)S(1)}, f32[2,2]{1,0:T(2,128)}, u32[]{:S(2)}) copy-start(f32[2,2]{1,0:T(2,128)} %n_ref.1) | copy-start | bytes 52
  17.0 28.1 %copy-start.7 = (bf16[2,128]{1,0:T(2,128)(2,1)S(1)}, bf16[2,128]{1,0:T(2,128)(2,1)}, u32[]{:S(2)}) copy-start(bf16[2,128]{1,0:T(2,128)(2,1)} %v_ref.3) | copy-start | bytes 1540
  17.0 28.1 %copy-start.8 = (bf16[2,128]{1,0:T(2,128)(2,1)S(1)}, bf16[2,128]{1,0:T(2,128)(2,1)}, u32[]{:S(2)}) copy-start(bf16[2,128]{1,0:T(2,128)(2,1)} %k_ref.3) | copy-start | bytes 1540
  17.0 28.1 %copy-start.9 = (bf16[2,128]{1,0:T(2,128)(2,1)S(1)}, bf16[2,128]{1,0:T(2,128)(2,1)}, u32[]{:S(2)}) copy-start(bf16[2,128]{1,0:T(2,128)(2,1)} %q_ref.1) | copy-start | bytes 1540
  17.0 28.1 %copy-start.10 = (bf16[2,128]{1,0:T(2,128)(2,1)S(1)}, bf16[2,128]{1,0:T(2,128)(2,1)}, u32[]{:S(2)}) copy-start(bf16[2,128]{1,0:T(2,128)(2,1)} %g_ref.1) | copy-start | bytes 1540
  17.0 28.1 %copy-start.11 = (bf16[128]{0:T(256)(128)(2,1)S(1)}, bf16[128]{0:T(256)(128)(2,1)}, u32[]{:S(2)}) copy-start(bf16[128]{0:T(256)(128)(2,1)} %param.29) | copy-start | bytes 772
  17.1 36.0 %collective-permute-start.7 = (bf16[2052,256]{1,0:T(8,128)(2,1)S(1)}, bf16[2052,256]{1,0:T(8,128)(2,1)}, u32[]{:S(2)}, u32[]{:S(2)}) collective-permute-start(bf16[2052,256]{1,0:T(8,128)(2,1)S(1)} %joined.1.refs_2_.refs_3_), channel_id=1, source_target_pairs={{0,1},{1,0},{2,3},{3,2},{4,5},{5,4},{6,7},{7,6},{8,9},{9,8},{10,11... | collective-permute-start | bytes 3151880 | tf_op jit(solution)/shard_map/ppermute | solution.py:304
  19.2 26.6 %collective-permute-start.8 = (f32[2,2,1664]{2,1,0:T(2,128)S(1)}, f32[2,2,1664]{2,1,0:T(2,128)S(1)}, u32[]{:S(2)}, u32[]{:S(2)}) collective-permute-start(f32[2,2,1664]{2,1,0:T(2,128)S(1)} %pad_maximum_fusion.1), channel_id=1, source_target_pairs={{0,1},{1,0},{2,3},{3,2},{4,5},{5,4},{6,7},{7,6},{8,9},{9,8},{10,11... | collective-permute-start | bytes 79880 | tf_op jit(solution)/shard_map/ppermute | solution.py:304
  23.2 7.6 %collective-permute-start.3 = (bf16[8,2048]{1,0:T(8,128)(2,1)S(1)}, bf16[8,2048]{1,0:T(8,128)(2,1)S(1)}, u32[]{:S(2)}, u32[]{:S(2)}) collective-permute-start(bf16[8,2048]{1,0:T(8,128)(2,1)S(1)} %slice.26), channel_id=1, source_target_pairs={{1,2},{0,15},{3,4},{2,1},{5,6},{4,3},{7,8},{6,5},{9,10},{8,7},{11,... | collective-permute-start | bytes 98312 | tf_op jit(solution)/shard_map/ppermute | solution.py:326
  25.6 13.7 %collective-permute-start.9 = (bf16[200,2048]{1,0:T(8,128)(2,1)}, bf16[200,2048]{1,0:T(8,128)(2,1)}, u32[]{:S(2)}, u32[]{:S(2)}) collective-permute-start(bf16[200,2048]{1,0:T(8,128)(2,1)} %collective-permute-done.2), channel_id=1, source_target_pairs={{0,2},{1,15},{2,4},{3,1},{4,6},{5,3},{6,8},{7,5},{8,10},{9,7},{10,... | collective-permute-start | bytes 2457608 | tf_op jit(solution)/shard_map/ppermute | solution.py:311
  30.8 17.2 %collective-permute-start.4 = (bf16[200,2048]{1,0:T(8,128)(2,1)S(1)}, bf16[200,2048]{1,0:T(8,128)(2,1)}, u32[]{:S(2)}, u32[]{:S(2)}) collective-permute-start(bf16[200,2048]{1,0:T(8,128)(2,1)S(1)} %constant_dynamic-update-slice_fusion.refs_0_), channel_id=1, source_target_pairs={{0,2},{1,15},{2,4},{3,1},{4,6},{5,3},{6,8},{7,5},{8,10},{9,7},{10,... | collective-permute-start | bytes 2457608 | tf_op jit(solution)/shard_map/ppermute | solution.py:311
  39.3 17.6 %collective-permute-start.10 = (bf16[200,2048]{1,0:T(8,128)(2,1)}, bf16[200,2048]{1,0:T(8,128)(2,1)}, u32[]{:S(2)}, u32[]{:S(2)}) collective-permute-start(bf16[200,2048]{1,0:T(8,128)(2,1)} %collective-permute-done.9.refs_1_), channel_id=1, source_target_pairs={{0,2},{1,15},{2,4},{3,1},{4,6},{5,3},{6,8},{7,5},{8,10},{9,7},{10,... | collective-permute-start | bytes 2457608 | tf_op jit(solution)/shard_map/ppermute | solution.py:311
  48.0 17.9 %collective-permute-start.5 = (bf16[200,2048]{1,0:T(8,128)(2,1)}, bf16[200,2048]{1,0:T(8,128)(2,1)S(1)}, u32[]{:S(2)}, u32[]{:S(2)}) collective-permute-start(bf16[200,2048]{1,0:T(8,128)(2,1)} %collective-permute-done.4.refs_0_), channel_id=1, source_target_pairs={{0,2},{1,15},{2,4},{3,1},{4,6},{5,3},{6,8},{7,5},{8,10},{9,7},{10,... | collective-permute-start | bytes 2457608 | tf_op jit(solution)/shard_map/ppermute | solution.py:311
  56.8 18.0 %collective-permute-start.11 = (bf16[200,2048]{1,0:T(8,128)(2,1)}, bf16[200,2048]{1,0:T(8,128)(2,1)S(1)}, u32[]{:S(2)}, u32[]{:S(2)}) collective-permute-start(bf16[200,2048]{1,0:T(8,128)(2,1)} %collective-permute-done.10.refs_1_), channel_id=1, source_target_pairs={{0,2},{1,15},{2,4},{3,1},{4,6},{5,3},{6,8},{7,5},{8,10},{9,7},{10,... | collective-permute-start | bytes 2457608 | tf_op jit(solution)/shard_map/ppermute | solution.py:311
  65.9 17.1 %collective-permute-start.6 = (bf16[200,2048]{1,0:T(8,128)(2,1)S(1)}, bf16[200,2048]{1,0:T(8,128)(2,1)S(1)}, u32[]{:S(2)}, u32[]{:S(2)}) collective-permute-start(bf16[200,2048]{1,0:T(8,128)(2,1)S(1)} %collective-permute-done.5.refs_0_), channel_id=1, source_target_pairs={{0,2},{1,15},{2,4},{3,1},{4,6},{5,3},{6,8},{7,5},{8,10},{9,7},{10,... | collective-permute-start | bytes 2457608 | tf_op jit(solution)/shard_map/ppermute | solution.py:311
  86.2 7.2 %collective-permute-start.12 = (f32[3,2,136,128]{3,2,1,0:T(8,128)S(1)}, f32[3,2,136,128]{3,2,1,0:T(8,128)S(1)}, u32[]{:S(2)}, u32[]{:S(2)}) collective-permute-start(f32[3,2,136,128]{3,2,1,0:T(8,128)S(1)} %get-tuple-element.31), channel_id=1, source_target_pairs={{0,1},{1,0},{2,3},{3,2},{4,5},{5,4},{6,7},{7,6},{8,9},{9,8},{10,11... | collective-permute-start | bytes 1253384 | tf_op jit(solution)/shard_map/ppermute | solution.py:304

commit v5 on v4

--- a/solution.py
+++ b/solution.py
@@ -34,16 +34,16 @@
     return jnp.maximum(v, 0.0) + jnp.log1p(jnp.exp(-jnp.abs(v)))
 
 
-def piece_states(meta, xs, far, end, w_step, w, jump, rates, runs, rows, chips):
+def piece_states(meta, xs, halo, far, end, w_step, w, jump, rates, runs, rows, chips):
     depth = w[0].shape[0] - 4
     many, both = len(xs), 2 * rows
     given = [] if runs is None else list(runs)
 
     def body(m_ref, *refs):
         x_refs = refs[:many]
-        s_ref, wa_ref, wb_ref, j_ref, r_ref = refs[many : many + 5]
-        ins = refs[many + 5 : many + 5 + len(given)]
-        own_out, other_out, ext = refs[many + 5 + len(given) :]
+        h_ref, s_ref, wa_ref, wb_ref, j_ref, r_ref = refs[many : many + 6]
+        ins = refs[many + 6 : many + 6 + len(given)]
+        own_out, other_out, ext, full = refs[many + 6 + len(given) :]
         outs = (own_out, other_out)
         y, c = m_ref[0], m_ref[1]
         low = c == 0
@@ -64,7 +64,7 @@
         below = jnp.where(jnp.logical_and(i > j, (i >= rows) == (j >= rows)), 1.0, 0.0)
         sizes, afters, sums = [], [], []
         for n in range(many):
-            step = mm(s_ref[...], x_refs[n][...], ((1,), (1,))).astype(BF).astype(F32)[:, :both]
+            step = mm(s_ref[...], x_refs[n][...], ((1,), (1,))).astype(BF).astype(F32)
             size = softplus(step + r_ref[0][:, 0:1])
             decay = j_ref[place[n]] - r_ref[1][:, 0:1] * size
             sizes.append(size)
@@ -87,13 +87,23 @@
             lifts.append(jnp.transpose(weight))
 
         taps = jnp.concatenate([r[depth : depth + 4, :] for r in (wa_ref, wb_ref)], axis=1).astype(F32)
-        for n in range(many):
-            x = x_refs[n][...]
-            for g, r in enumerate((wa_ref, wb_ref)):
-                p = mm(x, r[:depth, :], ((1,), (0,))).astype(BF).astype(F32)
-                for s in range(2):
-                    ext[2 * n + s, 4:8, 256 * g : 256 * g + 256] = p[both + 4 * s : both + 4 * s + 4, :]
-                    ext[2 * n + s, 8 : 8 + rows, 256 * g : 256 * g + 256] = p[s * rows : (s + 1) * rows, :]
+        full[:both, :] = x_refs[0][...]
+        full[both:, :] = h_ref[...]
+        for g, r in enumerate((wa_ref, wb_ref)):
+            cols = slice(256 * g, 256 * g + 256)
+            p = [
+                mm((full if n == 0 else x_refs[n])[...], r[:depth, :], ((1,), (0,))).astype(BF).astype(F32)
+                for n in range(many)
+            ]
+            for s in range(2):
+                before_row = [p[0][both + 4 * s : both + 4 * s + 4, :]]
+                if many == 2:
+                    last = [v[(s + 1) * rows - 4 : (s + 1) * rows, :] for v in p]
+                    outer = before_row[0]
+                    before_row = [jnp.where(low, outer, last[1]), jnp.where(low, last[0], outer)]
+                for n in range(many):
+                    ext[2 * n + s, 4:8, cols] = before_row[n]
+                    ext[2 * n + s, 8 : 8 + rows, cols] = p[n][s * rows : (s + 1) * rows, :]
         for s in range(2):
             states = [jnp.zeros((128, 128), F32)] * 2
             for n in range(many):
@@ -122,9 +132,9 @@
     return pl.pallas_call(
         body,
         out_shape=[jax.ShapeDtypeStruct(shape, F32)] * 2,
-        in_specs=[SMEM] + [VMEM] * (many + 5 + len(given)),
+        in_specs=[SMEM] + [VMEM] * (many + 6 + len(given)),
         out_specs=[VMEM] * 2,
-        scratch_shapes=[pltpu.VMEM((2 * many, rows + 8, 512), F32)],
+        scratch_shapes=[pltpu.VMEM((2 * many, rows + 8, 512), F32), pltpu.VMEM((both + 8, depth), BF)],
         cost_estimate=pl.CostEstimate(
             flops=32 * sum(x.shape[0] for x in xs) * w[0].size,
             transcendentals=0,
@@ -132,7 +142,7 @@
         ),
         compiler_params=GRANT,
         name="piece_states",
-    )(meta, *xs, w_step, *w, jump, rates, *given)
+    )(meta, *xs, halo, w_step, *w, jump, rates, *given)
 
 
 def joined(w_value, w_key, conv_value, conv_key):
@@ -312,19 +322,23 @@
 
     meta = jnp.stack([y, c, (128 - sp * share) % 128]).astype(jnp.int32)
 
-    x = hidden_in.reshape(2 * rows, width)
-    bare = onward(x)
-    ends = hidden_in[:, rows - 4 :, :].reshape(8, width)
-    ends = lax.ppermute(ends, ("sp", "y", "c"), [(i, i + 1) for i in range(count - 1)])
-    a = [jnp.concatenate([x, ends], axis=0)]
+    def last(v):
+        return v.reshape(2, rows, width)[:, rows - 4 :, :].reshape(8, width)
+
+    a = [hidden_in.reshape(2 * rows, width)]
+    a.append(onward(a[0]))
     b = [swap(a[0])]
     b.append(onward(b[0]))
-    pairs = []
-    for i in range(y_count):
-        pairs.append((2 * i + 1, 2 * ((i + 1) % y_count)))
-        pairs.append((2 * i, 2 * ((i - 1) % y_count) + 1))
-    near = lax.ppermute(b[0][2 * rows :], ("y", "c"), pairs)
-    a.append(jnp.concatenate([bare, near], axis=0))
+    ends = last(a[0]), last(b[0])
+    before = jnp.where(c == 1, *ends)
+    before = lax.ppermute(before, ("sp", "y", "c"), [(i, i + 2) for i in range(count - 2)])
+
+    def straight(v, far):
+        pairs = []
+        for i in range(y_count):
+            pairs.append((2 * i + 1, 2 * ((i + far) % y_count)))
+            pairs.append((2 * i, 2 * ((i - far) % y_count) + 1))
+        return lax.ppermute(v, ("y", "c"), pairs)
 
     w_own = joined(w_value, w_key, conv_value, conv_key)
     w_both = w_own, swap(w_own)
@@ -339,19 +353,20 @@
     jump = jump[:, :, : tp_count * rows].reshape(2, 8, tp_count, rows).transpose(2, 1, 0, 3)
     jump = jump.reshape(tp_count, 8, 2 * rows)
 
-    def add(runs, xs, far, end):
-        return piece_states(meta, xs, far, end, w_steps, w_both, jump, rates, runs, rows, y_count)
-
-    runs = add(None, [a[0]], 0, False)
+    def add(runs, xs, halo, far, end):
+        return piece_states(meta, xs, halo, far, end, w_steps, w_both, jump, rates, runs, rows, y_count)
+
+    runs = add(None, [a[0]], jnp.where(c == 0, before, ends[1]), 0, False)
     for s in range(1, half):
         a.append(onward(a[s]))
         if s + 1 < half:
             b.append(onward(b[s]))
-        runs = add(runs, [a[s], b[s]], s, False)
+        runs = add(runs, [a[s], b[s]], straight(before, s), s, False)
 
     fixed, query = terms(step_bias, decay_rate, new_step, new_value, new_key, new_query, new_gate, read_gain)
-    runs, fixed, query = lax.optimization_barrier((runs, fixed, query))
-    own, other = add(runs, [a[half]], half, True)
+    end = straight(jnp.where(c == 1, before, ends[0]), half)
+    runs, fixed, query, end = lax.optimization_barrier((runs, fixed, query, end))
+    own, other = add(runs, [a[half]], end, half, True)
     sent = packed(meta, own, swap(other), query, sp_count, y_count)
     got = lax.all_to_all(sent, "sp", 0, 0, tiled=True)
     return tuple(finished(meta, got, fixed))

time: 119 us -> 118 us (level)
  the two profiles are of different devices: /device:TPU:1 before, /device:TPU:16 now
where the time goes in v5:
time: 118 us; the launch traced here: 117 us
  starting transfers between devices  50 us (42%)
  blocking collectives  22.4 us (19%)
  Pallas kernels  19 us (16%)
  waiting for transfers between devices  17.5 us (15%)
  local copies, waits for them, and re-layouts  5.61 us (5%)
    all_to_all x1, blocking collectives, per_device(): got = lax.all_to_all(sent, 'sp', 0, 0, tiled=True)  22.4 us
    ppermute x7, starting transfers between devices, onward(): return lax.ppermute(v, ('y', 'c'), pairs)  21.8 us
    pallas_call x5, Pallas kernels, piece_states(): pl.pallas_call(body, out_shape=[jax.ShapeDtypeStruct(shape, F32)] * 2, in...  15.7 us
    ppermute x4, starting transfers between devices, straight(): return lax.ppermute(v, ('y', 'c'), pairs)  15.1 us
    ppermute x4, starting transfers between devices, swap(): return lax.ppermute(v, 'c', [(0, 1), (1, 0)])  10.1 us
    ppermute x7, waiting for transfers between devices, onward(): return lax.ppermute(v, ('y', 'c'), pairs)  9.88 us
    ppermute x1, waiting for transfers between devices, per_device(): lax.ppermute(before, ('sp', 'y', 'c'), [(i, i + 2) for i in range(count -...  6.28 us
    unnamed x28, local copies, waits for them, and re-layouts  3.48 us
  transfers between devices with their start and end apart: 16, of which 5 were waited for; matrix products, arithmetic and copies ran while one was open for 3% of the time, Pallas kernels for 12%

profile of v5, /device:TPU:16, one launch (start us, length us, event | category | flops | bytes accessed | tf_op | source)
XLA Modules:
  0.0 116.7 jit_solution(10665114184284944991)
XLA Ops:
  0.7 2.1 %collective-permute-start.4 = (bf16[192,2048]{1,0:T(8,128)(2,1)}, bf16[192,2048]{1,0:T(8,128)(2,1)}, u32[]{:S(2)}, u32[]{:S(2)}) collective-permute-start(bf16[192,2048]{1,0:T(8,128)(2,1)} %bitcast.16), channel_id=1, source_target_pairs={{0,1},{1,0},{2,3},{3,2},{4,5},{5,4},{6,7},{7,6},{8,9},{9,8},{10,11... | collective-permute-start | bytes 2359304 | tf_op jit(solution)/shard_map/ppermute | solution.py:314
  2.7 3.5 %collective-permute-start = (bf16[192,2048]{1,0:T(8,128)(2,1)}, bf16[192,2048]{1,0:T(8,128)(2,1)}, u32[]{:S(2)}, u32[]{:S(2)}) collective-permute-start(bf16[192,2048]{1,0:T(8,128)(2,1)} %bitcast.17), channel_id=1, source_target_pairs={{0,2},{1,15},{2,4},{3,1},{4,6},{5,3},{6,8},{7,5},{8,10},{9,7},{10,... | collective-permute-start | bytes 2359304 | tf_op jit(solution)/shard_map/ppermute | solution.py:321
  6.2 1.0 copy-done
  7.3 1.0 copy-done.1
  8.3 0.7 copy-done.5
  9.0 0.7 copy-done.6
  9.7 0.0 copy-start.10
  9.7 0.0 copy-start.11
  9.7 0.0 copy-start.12
  9.7 0.2 joined.1.refs_3_.refs_4_
  9.9 2.1 %collective-permute-start.10 = (bf16[2052,256]{1,0:T(8,128)(2,1)S(1)}, bf16[2052,256]{1,0:T(8,128)(2,1)S(1)}, u32[]{:S(2)}, u32[]{:S(2)}) collective-permute-start(bf16[2052,256]{1,0:T(8,128)(2,1)S(1)} %joined.1.refs_3_.refs_4_), channel_id=1, source_target_pairs={{0,1},{1,0},{2,3},{3,2},{4,5},{5,4},{6,7},{7,6},{8,9},{9,8},{10,11... | collective-permute-start | bytes 3151880 | tf_op jit(solution)/shard_map/ppermute | solution.py:314
  12.0 0.1 broadcast_in_dim.2
  12.1 2.4 %collective-permute-start.11 = (f32[2,2,1664]{2,1,0:T(2,128)S(1)}, f32[2,2,1664]{2,1,0:T(2,128)S(1)}, u32[]{:S(2)}, u32[]{:S(2)}) collective-permute-start(f32[2,2,1664]{2,1,0:T(2,128)S(1)} %pad_maximum_fusion), channel_id=1, source_target_pairs={{0,1},{1,0},{2,3},{3,2},{4,5},{5,4},{6,7},{7,6},{8,9},{9,8},{10,11... | collective-permute-start | bytes 79880 | tf_op jit(solution)/shard_map/ppermute | solution.py:314
  14.6 0.8 dynamic-slice_bitcast_fusion
  15.4 4.7 %collective-permute-start.5 = (bf16[192,2048]{1,0:T(8,128)(2,1)}, bf16[192,2048]{1,0:T(8,128)(2,1)}, u32[]{:S(2)}, u32[]{:S(2)}) collective-permute-start(bf16[192,2048]{1,0:T(8,128)(2,1)} %collective-permute-done.4), channel_id=1, source_target_pairs={{0,2},{1,15},{2,4},{3,1},{4,6},{5,3},{6,8},{7,5},{8,10},{9,7},{10,... | collective-permute-start | bytes 2359304 | tf_op jit(solution)/shard_map/ppermute | solution.py:321
  20.1 0.8 maximum_select_fusion
  21.0 0.6 terms.1
  21.6 0.1 pad_add_fusion.m_ref
  21.7 0.9 slice.26
  22.6 2.6 %collective-permute-start.1 = (bf16[192,2048]{1,0:T(8,128)(2,1)}, bf16[192,2048]{1,0:T(8,128)(2,1)}, u32[]{:S(2)}, u32[]{:S(2)}) collective-permute-start(bf16[192,2048]{1,0:T(8,128)(2,1)} %collective-permute-done.refs_0_), channel_id=1, source_target_pairs={{0,2},{1,15},{2,4},{3,1},{4,6},{5,3},{6,8},{7,5},{8,10},{9,7},{10,... | collective-permute-start | bytes 2359304 | tf_op jit(solution)/shard_map/ppermute | solution.py:321
  25.2 3.0 %collective-permute-start.8 = (bf16[8,2048]{1,0:T(8,128)(2,1)S(1)}, bf16[8,2048]{1,0:T(8,128)(2,1)S(1)}, u32[]{:S(2)}, u32[]{:S(2)}) collective-permute-start(bf16[8,2048]{1,0:T(8,128)(2,1)S(1)} %broadcast_select_fusion.2), channel_id=1, source_target_pairs={{0,2},{1,3},{2,4},{3,5},{4,6},{5,7},{6,8},{7,9},{8,10},{9,11},{10,... | collective-permute-start | bytes 98312 | tf_op jit(solution)/shard_map/ppermute | solution.py:334
  28.2 3.8 %collective-permute-done.5.refs_1_ = bf16[192,2048]{1,0:T(8,128)(2,1)} collective-permute-done((bf16[192,2048]{1,0:T(8,128)(2,1)}, bf16[192,2048]{1,0:T(8,128)(2,1)}, u32[]{:S(2)}, u32[]{:S(2)}) %collective-permute-start.5) | collective-permute-done | bytes 786464 | tf_op jit(solution)/shard_map/ppermute | solution.py:321
  32.0 2.3 %collective-permute-start.6 = (bf16[192,2048]{1,0:T(8,128)(2,1)}, bf16[192,2048]{1,0:T(8,128)(2,1)}, u32[]{:S(2)}, u32[]{:S(2)}) collective-permute-start(bf16[192,2048]{1,0:T(8,128)(2,1)} %collective-permute-done.5.refs_1_), channel_id=1, source_target_pairs={{0,2},{1,15},{2,4},{3,1},{4,6},{5,3},{6,8},{7,5},{8,10},{9,7},{10,... | collective-permute-start | bytes 2359304 | tf_op jit(solution)/shard_map/ppermute | solution.py:321
  34.3 0.0 collective-permute-done.11
  34.4 0.1 reshape.30
  34.5 0.1 copy.17
  34.6 0.1 reshape.31.refs_5_.refs_6_
  34.7 6.3 %collective-permute-done.8 = bf16[8,2048]{1,0:T(8,128)(2,1)S(1)} collective-permute-done((bf16[8,2048]{1,0:T(8,128)(2,1)S(1)}, bf16[8,2048]{1,0:T(8,128)(2,1)S(1)}, u32[]{:S(2)}, u32[]{:S(2)}) %collective-permute-start.8) | collective-permute-done | bytes 32800 | tf_op jit(solution)/shard_map/ppermute | solution.py:334
  41.0 1.9 %collective-permute-start.14 = (bf16[8,2048]{1,0:T(8,128)(2,1)S(1)}, bf16[8,2048]{1,0:T(8,128)(2,1)S(1)}, u32[]{:S(2)}, u32[]{:S(2)}) collective-permute-start(bf16[8,2048]{1,0:T(8,128)(2,1)S(1)} %get-tuple-element.36), channel_id=1, source_target_pairs={{1,8},{0,9},{3,10},{2,11},{5,12},{4,13},{7,14},{6,15},{9,0},{8,1},... | collective-permute-start | bytes 98312 | tf_op jit(solution)/shard_map/ppermute | solution.py:341
  42.9 4.1 %collective-permute-start.13 = (bf16[8,2048]{1,0:T(8,128)(2,1)S(1)}, bf16[8,2048]{1,0:T(8,128)(2,1)S(1)}, u32[]{:S(2)}, u32[]{:S(2)}) collective-permute-start(bf16[8,2048]{1,0:T(8,128)(2,1)S(1)} %collective-permute-done.8), channel_id=1, source_target_pairs={{1,2},{0,15},{3,4},{2,1},{5,6},{4,3},{7,8},{6,5},{9,10},{8,7},{11,... | collective-permute-start | bytes 98312 | tf_op jit(solution)/shard_map/ppermute | solution.py:341
  47.1 3.5 %collective-permute-start.12 = (bf16[8,2048]{1,0:T(8,128)(2,1)S(1)}, bf16[8,2048]{1,0:T(8,128)(2,1)S(1)}, u32[]{:S(2)}, u32[]{:S(2)}) collective-permute-start(bf16[8,2048]{1,0:T(8,128)(2,1)S(1)} %collective-permute-done.8), channel_id=1, source_target_pairs={{1,4},{0,13},{3,6},{2,15},{5,8},{4,1},{7,10},{6,3},{9,12},{8,5},{1... | collective-permute-start | bytes 98312 | tf_op jit(solution)/shard_map/ppermute | solution.py:341
  50.6 0.0 collective-permute-done.1.refs_0_
  50.6 3.2 %collective-permute-start.2 = (bf16[192,2048]{1,0:T(8,128)(2,1)}, bf16[192,2048]{1,0:T(8,128)(2,1)S(1)}, u32[]{:S(2)}, u32[]{:S(2)}) collective-permute-start(bf16[192,2048]{1,0:T(8,128)(2,1)} %collective-permute-done.1.refs_0_), channel_id=1, source_target_pairs={{0,2},{1,15},{2,4},{3,1},{4,6},{5,3},{6,8},{7,5},{8,10},{9,7},{10,... | collective-permute-start | bytes 2359304 | tf_op jit(solution)/shard_map/ppermute | solution.py:321
  53.8 2.4 %piece_states.5 = (f32[3,2,136,128]{3,2,1,0:T(8,128)S(1)}, f32[3,2,136,128]{3,2,1,0:T(8,128)S(1)}) custom-call(s32[3]{0:T(128)S(1)} %pad_add_fusion.m_ref, bf16[192,2048]{1,0:T(8,128)(2,1)S(1)} %bitcast.18, bf16[8,2048]{1,0:T(8,128)(2,1)S(1)} %get-tuple-element.37.refs_1_, bf16[8,2048]{1,0:T(8,128)(2,1)S(1)} %pad.8.refs_2_.refs_3_, ...), custom_call_target="tpu_custom_call" | custom-call | flops 3227516928 | bytes 2101248 | tf_op jit(solution)/shard_map/piece_states/pallas_call | solution.py:132
  56.3 5.5 %collective-permute-start.9 = (bf16[8,2048]{1,0:T(8,128)(2,1)S(1)}, bf16[8,2048]{1,0:T(8,128)(2,1)S(1)}, u32[]{:S(2)}, u32[]{:S(2)}) collective-permute-start(bf16[8,2048]{1,0:T(8,128)(2,1)S(1)} %collective-permute-done.8), channel_id=1, source_target_pairs={{1,6},{0,11},{3,8},{2,13},{5,10},{4,15},{7,12},{6,1},{9,14},{8,3},... | collective-permute-start | bytes 98312 | tf_op jit(solution)/shard_map/ppermute | solution.py:341
  61.8 2.6 %collective-permute-start.7 = (bf16[192,2048]{1,0:T(8,128)(2,1)}, bf16[192,2048]{1,0:T(8,128)(2,1)S(1)}, u32[]{:S(2)}, u32[]{:S(2)}) collective-permute-start(bf16[192,2048]{1,0:T(8,128)(2,1)} %collective-permute-done.6.refs_1_), channel_id=1, source_target_pairs={{0,2},{1,15},{2,4},{3,1},{4,6},{5,3},{6,8},{7,5},{8,10},{9,7},{10,... | collective-permute-start | bytes 2359304 | tf_op jit(solution)/shard_map/ppermute | solution.py:321
  64.4 3.9 %piece_states.6 = (f32[3,2,136,128]{3,2,1,0:T(8,128)S(1)}, f32[3,2,136,128]{3,2,1,0:T(8,128)S(1)}) custom-call(s32[3]{0:T(128)S(1)} %pad_add_fusion.m_ref, bf16[192,2048]{1,0:T(8,128)(2,1)} %collective-permute-done.refs_0_, bf16[192,2048]{1,0:T(8,128)(2,1)} %collective-permute-done.5.refs_1_, bf16[8,2048]{1,0:T(8,128)(2,1)S(1)} %collective-permute-done.13.refs_2_, ...), custom_call_target="tpu_custom_call" | custom-call | flops 6455033856 | bytes 2101248 | tf_op jit(solution)/shard_map/piece_states/pallas_call | solution.py:132
  68.3 2.9 %collective-permute-start.3 = (bf16[192,2048]{1,0:T(8,128)(2,1)S(1)}, bf16[192,2048]{1,0:T(8,128)(2,1)S(1)}, u32[]{:S(2)}, u32[]{:S(2)}) collective-permute-start(bf16[192,2048]{1,0:T(8,128)(2,1)S(1)} %collective-permute-done.2.refs_0_), channel_id=1, source_target_pairs={{0,2},{1,15},{2,4},{3,1},{4,6},{5,3},{6,8},{7,5},{8,10},{9,7},{10,... | collective-permute-start | bytes 2359304 | tf_op jit(solution)/shard_map/ppermute | solution.py:321
  71.3 3.9 %piece_states.7 = (f32[3,2,136,128]{3,2,1,0:T(8,128)S(1)}, f32[3,2,136,128]{3,2,1,0:T(8,128)S(1)}) custom-call(s32[3]{0:T(128)S(1)} %pad_add_fusion.m_ref, bf16[192,2048]{1,0:T(8,128)(2,1)} %collective-permute-done.1.refs_0_, bf16[192,2048]{1,0:T(8,128)(2,1)} %collective-permute-done.6.refs_1_, bf16[8,2048]{1,0:T(8,128)(2,1)S(1)} %collective-permute-done.12.refs_2_, ...), custom_call_target="tpu_custom_call" | custom-call | flops 6455033856 | bytes 2101248 | tf_op jit(solution)/shard_map/piece_states/pallas_call | solution.py:132
  75.2 0.7 collective-permute-done.7.refs_1_
  75.9 3.1 %piece_states.8 = (f32[3,2,136,128]{3,2,1,0:T(8,128)S(1)}, f32[3,2,136,128]{3,2,1,0:T(8,128)S(1)}) custom-call(s32[3]{0:T(128)S(1)} %pad_add_fusion.m_ref, bf16[192,2048]{1,0:T(8,128)(2,1)S(1)} %collective-permute-done.2.refs_0_, bf16[192,2048]{1,0:T(8,128)(2,1)S(1)} %collective-permute-done.7.refs_1_, bf16[8,2048]{1,0:T(8,128)(2,1)S(1)} %collective-permute-done.9.refs_2_, ...), custom_call_target="tpu_custom_call" | custom-call | flops 6455033856 | bytes 2101248 | tf_op jit(solution)/shard_map/piece_states/pallas_call | solution.py:132
  79.0 5.4 %collective-permute-done.3.refs_0_ = bf16[192,2048]{1,0:T(8,128)(2,1)S(1)} collective-permute-done((bf16[192,2048]{1,0:T(8,128)(2,1)S(1)}, bf16[192,2048]{1,0:T(8,128)(2,1)S(1)}, u32[]{:S(2)}, u32[]{:S(2)}) %collective-permute-start.3) | collective-permute-done | bytes 786464 | tf_op jit(solution)/shard_map/ppermute | solution.py:321
  84.3 2.5 %piece_states.9 = (f32[3,2,136,128]{3,2,1,0:T(8,128)S(1)}, f32[3,2,136,128]{3,2,1,0:T(8,128)S(1)}) custom-call(s32[3]{0:T(128)S(1)} %pad_add_fusion.m_ref, bf16[192,2048]{1,0:T(8,128)(2,1)S(1)} %collective-permute-done.3.refs_0_, bf16[8,2048]{1,0:T(8,128)(2,1)S(1)} %collective-permute-done.14.refs_1_, bf16[8,2048]{1,0:T(8,128)(2,1)S(1)} %pad.8.refs_2_.refs_3_, ...), custom_call_target="tpu_custom_call" | custom-call | flops 3227516928 | bytes 2101248 | tf_op jit(solution)/shard_map/piece_states/pallas_call | solution.py:132
  86.8 3.6 %collective-permute-start.15 = (f32[3,2,136,128]{3,2,1,0:T(8,128)S(1)}, f32[3,2,136,128]{3,2,1,0:T(8,128)S(1)}, u32[]{:S(2)}, u32[]{:S(2)}) collective-permute-start(f32[3,2,136,128]{3,2,1,0:T(8,128)S(1)} %get-tuple-element.33), channel_id=1, source_target_pairs={{0,1},{1,0},{2,3},{3,2},{4,5},{5,4},{6,7},{7,6},{8,9},{9,8},{10,11... | collective-permute-start | bytes 1253384 | tf_op jit(solution)/shard_map/ppermute | solution.py:314
  90.4 1.4 %collective-permute-done.15.b_ref = f32[3,2,136,128]{3,2,1,0:T(8,128)S(1)} collective-permute-done((f32[3,2,136,128]{3,2,1,0:T(8,128)S(1)}, f32[3,2,136,128]{3,2,1,0:T(8,128)S(1)}, u32[]{:S(2)}, u32[]{:S(2)}) %collective-permute-start.15) | collective-permute-done | bytes 417824 | tf_op jit(solution)/shard_map/ppermute | solution.py:314
  91.8 0.8 packed.1
  92.6 22.4 %all_to_all.5.got_ref = bf16[32,16,128]{2,1,0:T(8,128)(2,1)S(1)} all-to-all(bf16[32,16,128]{2,1,0:T(8,128)(2,1)S(1)} %packed.1), channel_id=1, replica_groups=mesh['sp'=32,'y'=8,'c'=2] {'sp'}, dimensions={0} | all-to-all | bytes 262144 | tf_op jit(solution)/shard_map/all_to_all | solution.py:371
  115.0 1.6 %finished.1 = (bf16[2,2,2,128]{3,2,1,0:T(2,128)(2,1)}, bf16[2,2,2]{2,1,0:T(2,128)(2,1)}) custom-call(s32[3]{0:T(128)S(1)} %pad_add_fusion.m_ref, bf16[32,16,128]{2,1,0:T(8,128)(2,1)S(1)} %all_to_all.5.got_ref, f32[8,128]{1,0:T(8,128)S(1)} %get-tuple-element.35.fix_ref), custom_call_target="tpu_custom_call" | custom-call | tf_op jit(solution)/shard_map/finished/pallas_call | solution.py:290
  (42 shorter events, 0.2 us)
Async XLA Ops:
  0.6 11.3 %copy-start.2 = (f32[2]{0:T(128)S(1)}, f32[2]{0:T(128)}, u32[]{:S(2)}) copy-start(f32[2]{0:T(128)} %r_ref.1) | copy-start | bytes 28
  0.6 11.3 %copy-start.3 = (f32[2]{0:T(128)S(1)}, f32[2]{0:T(128)}, u32[]{:S(2)}) copy-start(f32[2]{0:T(128)} %b_ref.1) | copy-start | bytes 28
  0.7 20.3 %copy-start.8 = (bf16[2,128]{1,0:T(2,128)(2,1)S(1)}, bf16[2,128]{1,0:T(2,128)(2,1)}, u32[]{:S(2)}) copy-start(bf16[2,128]{1,0:T(2,128)(2,1)} %v_ref.3) | copy-start | bytes 1540
  0.7 14.7 %collective-permute-start.4 = (bf16[192,2048]{1,0:T(8,128)(2,1)}, bf16[192,2048]{1,0:T(8,128)(2,1)}, u32[]{:S(2)}, u32[]{:S(2)}) collective-permute-start(bf16[192,2048]{1,0:T(8,128)(2,1)} %bitcast.16), channel_id=1, source_target_pairs={{0,1},{1,0},{2,3},{3,2},{4,5},{5,4},{6,7},{7,6},{8,9},{9,8},{10,11... | collective-permute-start | bytes 2359304 | tf_op jit(solution)/shard_map/ppermute | solution.py:314
  2.7 19.9 %collective-permute-start = (bf16[192,2048]{1,0:T(8,128)(2,1)}, bf16[192,2048]{1,0:T(8,128)(2,1)}, u32[]{:S(2)}, u32[]{:S(2)}) collective-permute-start(bf16[192,2048]{1,0:T(8,128)(2,1)} %bitcast.17), channel_id=1, source_target_pairs={{0,2},{1,15},{2,4},{3,1},{4,6},{5,3},{6,8},{7,5},{8,10},{9,7},{10,... | collective-permute-start | bytes 2359304 | tf_op jit(solution)/shard_map/ppermute | solution.py:321
  6.2 1.0 copy-start
  7.3 1.0 copy-start.1
  8.3 0.7 copy-start.5
  9.0 0.7 copy-start.6
  9.7 2.4 %copy-start.13 = (f32[2,1536,2]{1,2,0:T(2,128)S(1)}, f32[2,1536,2]{1,2,0:T(2,128)}, u32[]{:S(2)}) copy-start(f32[2,1536,2]{1,2,0:T(2,128)} %param.23) | copy-start | bytes 73732
  9.7 4.9 %copy-start.4 = (bf16[2,96,2048]{2,1,0:T(8,128)(2,1)S(1)}, bf16[2,96,2048]{2,1,0:T(8,128)(2,1)}, u32[]{:S(2)}) copy-start(bf16[2,96,2048]{2,1,0:T(8,128)(2,1)} %param.15) | copy-start | bytes 2359300
  9.7 11.3 %copy-start.7 = (f32[2,2]{1,0:T(2,128)S(1)}, f32[2,2]{1,0:T(2,128)}, u32[]{:S(2)}) copy-start(f32[2,2]{1,0:T(2,128)} %n_ref.1) | copy-start | bytes 52
  9.7 11.3 %copy-start.9 = (bf16[2,128]{1,0:T(2,128)(2,1)S(1)}, bf16[2,128]{1,0:T(2,128)(2,1)}, u32[]{:S(2)}) copy-start(bf16[2,128]{1,0:T(2,128)(2,1)} %k_ref.3) | copy-start | bytes 1540
  9.7 11.3 %copy-start.10 = (bf16[2,128]{1,0:T(2,128)(2,1)S(1)}, bf16[2,128]{1,0:T(2,128)(2,1)}, u32[]{:S(2)}) copy-start(bf16[2,128]{1,0:T(2,128)(2,1)} %q_ref.1) | copy-start | bytes 1540
  9.7 11.3 %copy-start.11 = (bf16[2,128]{1,0:T(2,128)(2,1)S(1)}, bf16[2,128]{1,0:T(2,128)(2,1)}, u32[]{:S(2)}) copy-start(bf16[2,128]{1,0:T(2,128)(2,1)} %g_ref.1) | copy-start | bytes 1540
  9.7 11.3 %copy-start.12 = (bf16[128]{0:T(256)(128)(2,1)S(1)}, bf16[128]{0:T(256)(128)(2,1)}, u32[]{:S(2)}) copy-start(bf16[128]{0:T(256)(128)(2,1)} %param.29) | copy-start | bytes 772
  9.9 37.2 %collective-permute-start.10 = (bf16[2052,256]{1,0:T(8,128)(2,1)S(1)}, bf16[2052,256]{1,0:T(8,128)(2,1)S(1)}, u32[]{:S(2)}, u32[]{:S(2)}) collective-permute-start(bf16[2052,256]{1,0:T(8,128)(2,1)S(1)} %joined.1.refs_3_.refs_4_), channel_id=1, source_target_pairs={{0,1},{1,0},{2,3},{3,2},{4,5},{5,4},{6,7},{7,6},{8,9},{9,8},{10,11... | collective-permute-start | bytes 3151880 | tf_op jit(solution)/shard_map/ppermute | solution.py:314
  12.1 22.2 %collective-permute-start.11 = (f32[2,2,1664]{2,1,0:T(2,128)S(1)}, f32[2,2,1664]{2,1,0:T(2,128)S(1)}, u32[]{:S(2)}, u32[]{:S(2)}) collective-permute-start(f32[2,2,1664]{2,1,0:T(2,128)S(1)} %pad_maximum_fusion), channel_id=1, source_target_pairs={{0,1},{1,0},{2,3},{3,2},{4,5},{5,4},{6,7},{7,6},{8,9},{9,8},{10,11... | collective-permute-start | bytes 79880 | tf_op jit(solution)/shard_map/ppermute | solution.py:314
  15.4 16.6 %collective-permute-start.5 = (bf16[192,2048]{1,0:T(8,128)(2,1)}, bf16[192,2048]{1,0:T(8,128)(2,1)}, u32[]{:S(2)}, u32[]{:S(2)}) collective-permute-start(bf16[192,2048]{1,0:T(8,128)(2,1)} %collective-permute-done.4), channel_id=1, source_target_pairs={{0,2},{1,15},{2,4},{3,1},{4,6},{5,3},{6,8},{7,5},{8,10},{9,7},{10,... | collective-permute-start | bytes 2359304 | tf_op jit(solution)/shard_map/ppermute | solution.py:321
  22.6 28.0 %collective-permute-start.1 = (bf16[192,2048]{1,0:T(8,128)(2,1)}, bf16[192,2048]{1,0:T(8,128)(2,1)}, u32[]{:S(2)}, u32[]{:S(2)}) collective-permute-start(bf16[192,2048]{1,0:T(8,128)(2,1)} %collective-permute-done.refs_0_), channel_id=1, source_target_pairs={{0,2},{1,15},{2,4},{3,1},{4,6},{5,3},{6,8},{7,5},{8,10},{9,7},{10,... | collective-permute-start | bytes 2359304 | tf_op jit(solution)/shard_map/ppermute | solution.py:321
  25.2 15.8 %collective-permute-start.8 = (bf16[8,2048]{1,0:T(8,128)(2,1)S(1)}, bf16[8,2048]{1,0:T(8,128)(2,1)S(1)}, u32[]{:S(2)}, u32[]{:S(2)}) collective-permute-start(bf16[8,2048]{1,0:T(8,128)(2,1)S(1)} %broadcast_select_fusion.2), channel_id=1, source_target_pairs={{0,2},{1,3},{2,4},{3,5},{4,6},{5,7},{6,8},{7,9},{8,10},{9,11},{10,... | collective-permute-start | bytes 98312 | tf_op jit(solution)/shard_map/ppermute | solution.py:334
  32.0 29.8 %collective-permute-start.6 = (bf16[192,2048]{1,0:T(8,128)(2,1)}, bf16[192,2048]{1,0:T(8,128)(2,1)}, u32[]{:S(2)}, u32[]{:S(2)}) collective-permute-start(bf16[192,2048]{1,0:T(8,128)(2,1)} %collective-permute-done.5.refs_1_), channel_id=1, source_target_pairs={{0,2},{1,15},{2,4},{3,1},{4,6},{5,3},{6,8},{7,5},{8,10},{9,7},{10,... | collective-permute-start | bytes 2359304 | tf_op jit(solution)/shard_map/ppermute | solution.py:321
  41.0 37.9 %collective-permute-start.14 = (bf16[8,2048]{1,0:T(8,128)(2,1)S(1)}, bf16[8,2048]{1,0:T(8,128)(2,1)S(1)}, u32[]{:S(2)}, u32[]{:S(2)}) collective-permute-start(bf16[8,2048]{1,0:T(8,128)(2,1)S(1)} %get-tuple-element.36), channel_id=1, source_target_pairs={{1,8},{0,9},{3,10},{2,11},{5,12},{4,13},{7,14},{6,15},{9,0},{8,1},... | collective-permute-start | bytes 98312 | tf_op jit(solution)/shard_map/ppermute | solution.py:341
  42.9 13.3 %collective-permute-start.13 = (bf16[8,2048]{1,0:T(8,128)(2,1)S(1)}, bf16[8,2048]{1,0:T(8,128)(2,1)S(1)}, u32[]{:S(2)}, u32[]{:S(2)}) collective-permute-start(bf16[8,2048]{1,0:T(8,128)(2,1)S(1)} %collective-permute-done.8), channel_id=1, source_target_pairs={{1,2},{0,15},{3,4},{2,1},{5,6},{4,3},{7,8},{6,5},{9,10},{8,7},{11,... | collective-permute-start | bytes 98312 | tf_op jit(solution)/shard_map/ppermute | solution.py:341
  47.1 24.2 %collective-permute-start.12 = (bf16[8,2048]{1,0:T(8,128)(2,1)S(1)}, bf16[8,2048]{1,0:T(8,128)(2,1)S(1)}, u32[]{:S(2)}, u32[]{:S(2)}) collective-permute-start(bf16[8,2048]{1,0:T(8,128)(2,1)S(1)} %collective-permute-done.8), channel_id=1, source_target_pairs={{1,4},{0,13},{3,6},{2,15},{5,8},{4,1},{7,10},{6,3},{9,12},{8,5},{1... | collective-permute-start | bytes 98312 | tf_op jit(solution)/shard_map/ppermute | solution.py:341
  50.6 17.7 %collective-permute-start.2 = (bf16[192,2048]{1,0:T(8,128)(2,1)}, bf16[192,2048]{1,0:T(8,128)(2,1)S(1)}, u32[]{:S(2)}, u32[]{:S(2)}) collective-permute-start(bf16[192,2048]{1,0:T(8,128)(2,1)} %collective-permute-done.1.refs_0_), channel_id=1, source_target_pairs={{0,2},{1,15},{2,4},{3,1},{4,6},{5,3},{6,8},{7,5},{8,10},{9,7},{10,... | collective-permute-start | bytes 2359304 | tf_op jit(solution)/shard_map/ppermute | solution.py:321
  56.3 18.9 %collective-permute-start.9 = (bf16[8,2048]{1,0:T(8,128)(2,1)S(1)}, bf16[8,2048]{1,0:T(8,128)(2,1)S(1)}, u32[]{:S(2)}, u32[]{:S(2)}) collective-permute-start(bf16[8,2048]{1,0:T(8,128)(2,1)S(1)} %collective-permute-done.8), channel_id=1, source_target_pairs={{1,6},{0,11},{3,8},{2,13},{5,10},{4,15},{7,12},{6,1},{9,14},{8,3},... | collective-permute-start | bytes 98312 | tf_op jit(solution)/shard_map/ppermute | solution.py:341
  61.8 14.1 %collective-permute-start.7 = (bf16[192,2048]{1,0:T(8,128)(2,1)}, bf16[192,2048]{1,0:T(8,128)(2,1)S(1)}, u32[]{:S(2)}, u32[]{:S(2)}) collective-permute-start(bf16[192,2048]{1,0:T(8,128)(2,1)} %collective-permute-done.6.refs_1_), channel_id=1, source_target_pairs={{0,2},{1,15},{2,4},{3,1},{4,6},{5,3},{6,8},{7,5},{8,10},{9,7},{10,... | collective-permute-start | bytes 2359304 | tf_op jit(solution)/shard_map/ppermute | solution.py:321
  68.3 16.0 %collective-permute-start.3 = (bf16[192,2048]{1,0:T(8,128)(2,1)S(1)}, bf16[192,2048]{1,0:T(8,128)(2,1)S(1)}, u32[]{:S(2)}, u32[]{:S(2)}) collective-permute-start(bf16[192,2048]{1,0:T(8,128)(2,1)S(1)} %collective-permute-done.2.refs_0_), channel_id=1, source_target_pairs={{0,2},{1,15},{2,4},{3,1},{4,6},{5,3},{6,8},{7,5},{8,10},{9,7},{10,... | collective-permute-start | bytes 2359304 | tf_op jit(solution)/shard_map/ppermute | solution.py:321
  86.8 5.0 %collective-permute-start.15 = (f32[3,2,136,128]{3,2,1,0:T(8,128)S(1)}, f32[3,2,136,128]{3,2,1,0:T(8,128)S(1)}, u32[]{:S(2)}, u32[]{:S(2)}) collective-permute-start(f32[3,2,136,128]{3,2,1,0:T(8,128)S(1)} %get-tuple-element.33), channel_id=1, source_target_pairs={{0,1},{1,0},{2,3},{3,2},{4,5},{5,4},{6,7},{7,6},{8,9},{9,8},{10,11... | collective-permute-start | bytes 1253384 | tf_op jit(solution)/shard_map/ppermute | solution.py:314

commit v6 on v5

--- a/solution.py
+++ b/solution.py
@@ -38,12 +38,14 @@
     depth = w[0].shape[0] - 4
     many, both = len(xs), 2 * rows
     given = [] if runs is None else list(runs)
+    xs = xs if halo is None else [*xs, halo]
+    held = len(xs)
 
     def body(m_ref, *refs):
-        x_refs = refs[:many]
-        h_ref, s_ref, wa_ref, wb_ref, j_ref, r_ref = refs[many : many + 6]
-        ins = refs[many + 6 : many + 6 + len(given)]
-        own_out, other_out, ext, full = refs[many + 6 + len(given) :]
+        x_refs = refs[:held]
+        s_ref, wa_ref, wb_ref, j_ref, r_ref = refs[held : held + 5]
+        ins = refs[held + 5 : held + 5 + len(given)]
+        own_out, other_out, ext, full = refs[held + 5 + len(given) :]
         outs = (own_out, other_out)
         y, c = m_ref[0], m_ref[1]
         low = c == 0
@@ -64,7 +66,7 @@
         below = jnp.where(jnp.logical_and(i > j, (i >= rows) == (j >= rows)), 1.0, 0.0)
         sizes, afters, sums = [], [], []
         for n in range(many):
-            step = mm(s_ref[...], x_refs[n][...], ((1,), (1,))).astype(BF).astype(F32)
+            step = mm(s_ref[...], x_refs[n][...], ((1,), (1,))).astype(BF).astype(F32)[:, :both]
             size = softplus(step + r_ref[0][:, 0:1])
             decay = j_ref[place[n]] - r_ref[1][:, 0:1] * size
             sizes.append(size)
@@ -87,16 +89,18 @@
             lifts.append(jnp.transpose(weight))
 
         taps = jnp.concatenate([r[depth : depth + 4, :] for r in (wa_ref, wb_ref)], axis=1).astype(F32)
-        full[:both, :] = x_refs[0][...]
-        full[both:, :] = h_ref[...]
+        if many == 1:
+            full[:both, :] = x_refs[0][...]
+            full[both:, :] = x_refs[1][...]
+        inputs = [full] if many == 1 else x_refs
         for g, r in enumerate((wa_ref, wb_ref)):
             cols = slice(256 * g, 256 * g + 256)
             p = [
-                mm((full if n == 0 else x_refs[n])[...], r[:depth, :], ((1,), (0,))).astype(BF).astype(F32)
-                for n in range(many)
+                mm(v[...], r[:depth, :], ((1,), (0,))).astype(BF).astype(F32)
+                for v in inputs
             ]
             for s in range(2):
-                before_row = [p[0][both + 4 * s : both + 4 * s + 4, :]]
+                before_row = [p[many - 1][both + 4 * s : both + 4 * s + 4, :]]
                 if many == 2:
                     last = [v[(s + 1) * rows - 4 : (s + 1) * rows, :] for v in p]
                     outer = before_row[0]
@@ -132,7 +136,7 @@
     return pl.pallas_call(
         body,
         out_shape=[jax.ShapeDtypeStruct(shape, F32)] * 2,
-        in_specs=[SMEM] + [VMEM] * (many + 6 + len(given)),
+        in_specs=[SMEM] + [VMEM] * (held + 5 + len(given)),
         out_specs=[VMEM] * 2,
         scratch_shapes=[pltpu.VMEM((2 * many, rows + 8, 512), F32), pltpu.VMEM((both + 8, depth), BF)],
         cost_estimate=pl.CostEstimate(
@@ -142,7 +146,7 @@
         ),
         compiler_params=GRANT,
         name="piece_states",
-    )(meta, *xs, halo, w_step, *w, jump, rates, *given)
+    )(meta, *xs, w_step, *w, jump, rates, *given)
 
 
 def joined(w_value, w_key, conv_value, conv_key):
@@ -333,12 +337,12 @@
     before = jnp.where(c == 1, *ends)
     before = lax.ppermute(before, ("sp", "y", "c"), [(i, i + 2) for i in range(count - 2)])
 
-    def straight(v, far):
-        pairs = []
-        for i in range(y_count):
-            pairs.append((2 * i + 1, 2 * ((i + far) % y_count)))
-            pairs.append((2 * i, 2 * ((i - far) % y_count) + 1))
-        return lax.ppermute(v, ("y", "c"), pairs)
+    near = onward(before)
+    b[1] = jnp.concatenate([b[1], near], axis=0)
+
+    later = (w_value, w_key, conv_value, conv_key, w_step, decay_jump, step_bias, decay_rate)
+    a[1], *later = lax.optimization_barrier((a[1], *later))
+    w_value, w_key, conv_value, conv_key, w_step, decay_jump, step_bias, decay_rate = later
 
     w_own = joined(w_value, w_key, conv_value, conv_key)
     w_both = w_own, swap(w_own)
@@ -361,10 +365,13 @@
         a.append(onward(a[s]))
         if s + 1 < half:
             b.append(onward(b[s]))
-        runs = add(runs, [a[s], b[s]], straight(before, s), s, False)
+        if s == half - 2:
+            a[s + 1], runs = lax.optimization_barrier((a[s + 1], runs))
+        runs = add(runs, [a[s], b[s]], None, s, False)
 
     fixed, query = terms(step_bias, decay_rate, new_step, new_value, new_key, new_query, new_gate, read_gain)
-    end = straight(jnp.where(c == 1, before, ends[0]), half)
+    end = b[half - 1]
+    end = onward(jnp.where(c == 0, end[2 * rows :], last(end[: 2 * rows])))
     runs, fixed, query, end = lax.optimization_barrier((runs, fixed, query, end))
     own, other = add(runs, [a[half]], end, half, True)
     sent = packed(meta, own, swap(other), query, sp_count, y_count)

time: 118 us -> 129 us (1.093)
  the two profiles are of different devices: /device:TPU:16 before, /device:TPU:24 now
where the time goes in v6:
time: 129 us; the launch traced here: 128 us
  starting transfers between devices  45.1 us (35%)
  waiting for transfers between devices  25.4 us (20%)
  blocking collectives  23.8 us (18%)
  Pallas kernels  22.2 us (17%)
  local copies, waits for them, and re-layouts  7.5 us (6%)
  other arithmetic  2.37 us (2%)
    ppermute x9, starting transfers between devices, onward(): return lax.ppermute(v, ('y', 'c'), pairs)  31.4 us
    all_to_all x1, blocking collectives, per_device(): got = lax.all_to_all(sent, 'sp', 0, 0, tiled=True)  23.8 us
    ppermute x9, waiting for transfers between devices, onward(): return lax.ppermute(v, ('y', 'c'), pairs)  23.7 us
    pallas_call x5, Pallas kernels, piece_states(): pl.pallas_call(body, out_shape=[jax.ShapeDtypeStruct(shape, F32)] * 2, in...  18.9 us
    ppermute x4, starting transfers between devices, swap(): return lax.ppermute(v, 'c', [(0, 1), (1, 0)])  8.17 us
    ppermute x1, starting transfers between devices, per_device(): lax.ppermute(before, ('sp', 'y', 'c'), [(i, i + 2) for i in range(count -...  5.6 us
    unnamed x33, local copies, waits for them, and re-layouts  5.29 us
  transfers between devices with their start and end apart: 14, of which 5 were waited for; matrix products, arithmetic and copies ran while one was open for 4% of the time, Pallas kernels for 13%

profile of v6, /device:TPU:24, one launch (start us, length us, event | category | flops | bytes accessed | tf_op | source)
XLA Modules:
  0.0 127.5 jit_solution(2521686550744713227)
XLA Ops:
  0.6 4.7 %collective-permute-start = (bf16[192,2048]{1,0:T(8,128)(2,1)}, bf16[192,2048]{1,0:T(8,128)(2,1)}, u32[]{:S(2)}, u32[]{:S(2)}) collective-permute-start(bf16[192,2048]{1,0:T(8,128)(2,1)} %bitcast.17), channel_id=1, source_target_pairs={{0,2},{1,15},{2,4},{3,1},{4,6},{5,3},{6,8},{7,5},{8,10},{9,7},{10,... | collective-permute-start | bytes 2359304 | tf_op jit(solution)/shard_map/ppermute | solution.py:325
  5.3 1.9 %collective-permute-start.3 = (bf16[192,2048]{1,0:T(8,128)(2,1)}, bf16[192,2048]{1,0:T(8,128)(2,1)S(1)}, u32[]{:S(2)}, u32[]{:S(2)}) collective-permute-start(bf16[192,2048]{1,0:T(8,128)(2,1)} %bitcast.18), channel_id=1, source_target_pairs={{0,1},{1,0},{2,3},{3,2},{4,5},{5,4},{6,7},{7,6},{8,9},{9,8},{10,11... | collective-permute-start | bytes 2359304 | tf_op jit(solution)/shard_map/ppermute | solution.py:318
  7.3 0.9 slice.29
  8.2 0.1 pad_add_fusion.m_ref
  8.3 6.9 %collective-permute-done.refs_0_ = bf16[192,2048]{1,0:T(8,128)(2,1)} collective-permute-done((bf16[192,2048]{1,0:T(8,128)(2,1)}, bf16[192,2048]{1,0:T(8,128)(2,1)}, u32[]{:S(2)}, u32[]{:S(2)}) %collective-permute-start) | collective-permute-done | bytes 786464 | tf_op jit(solution)/shard_map/ppermute | solution.py:325
  15.1 0.7 pad_maximum_fusion.1
  15.8 0.1 broadcast_in_dim.2
  15.9 0.8 pad_maximum_fusion
  16.6 1.9 %collective-permute-start.8 = (f32[2,2,1664]{2,1,0:T(2,128)S(1)}, f32[2,2,1664]{2,1,0:T(2,128)S(1)}, u32[]{:S(2)}, u32[]{:S(2)}) collective-permute-start(f32[2,2,1664]{2,1,0:T(2,128)S(1)} %pad_maximum_fusion), channel_id=1, source_target_pairs={{0,1},{1,0},{2,3},{3,2},{4,5},{5,4},{6,7},{7,6},{8,9},{9,8},{10,11... | collective-permute-start | bytes 79880 | tf_op jit(solution)/shard_map/ppermute | solution.py:318
  18.6 0.0 copy-start
  18.6 1.0 copy-done
  19.6 1.0 copy-done.1
  20.7 0.7 copy-done.5
  21.3 0.7 copy-done.6
  22.1 0.2 joined.1.refs_3_
  22.3 2.4 %collective-permute-start.7 = (bf16[2052,256]{1,0:T(8,128)(2,1)S(1)}, bf16[2052,256]{1,0:T(8,128)(2,1)}, u32[]{:S(2)}, u32[]{:S(2)}) collective-permute-start(bf16[2052,256]{1,0:T(8,128)(2,1)S(1)} %joined.1.refs_3_), channel_id=1, source_target_pairs={{0,1},{1,0},{2,3},{3,2},{4,5},{5,4},{6,7},{7,6},{8,9},{9,8},{10,11... | collective-permute-start | bytes 3151880 | tf_op jit(solution)/shard_map/ppermute | solution.py:318
  24.8 5.6 %collective-permute-start.5 = (bf16[8,2048]{1,0:T(8,128)(2,1)S(1)}, bf16[8,2048]{1,0:T(8,128)(2,1)S(1)}, u32[]{:S(2)}, u32[]{:S(2)}) collective-permute-start(bf16[8,2048]{1,0:T(8,128)(2,1)S(1)} %broadcast_select_fusion.1), channel_id=1, source_target_pairs={{0,2},{1,3},{2,4},{3,5},{4,6},{5,7},{6,8},{7,9},{8,10},{9,11},{10,... | collective-permute-start | bytes 98312 | tf_op jit(solution)/shard_map/ppermute | solution.py:338
  30.4 1.9 %collective-permute-start.1 = (bf16[192,2048]{1,0:T(8,128)(2,1)}, bf16[192,2048]{1,0:T(8,128)(2,1)}, u32[]{:S(2)}, u32[]{:S(2)}) collective-permute-start(bf16[192,2048]{1,0:T(8,128)(2,1)} %collective-permute-done.refs_0_), channel_id=1, source_target_pairs={{0,2},{1,15},{2,4},{3,1},{4,6},{5,3},{6,8},{7,5},{8,10},{9,7},{10,... | collective-permute-start | bytes 2359304 | tf_op jit(solution)/shard_map/ppermute | solution.py:325
  32.3 2.0 %collective-permute-start.4 = (bf16[192,2048]{1,0:T(8,128)(2,1)S(1)}, bf16[192,2048]{1,0:T(8,128)(2,1)S(1)}, u32[]{:S(2)}, u32[]{:S(2)}) collective-permute-start(bf16[192,2048]{1,0:T(8,128)(2,1)S(1)} %collective-permute-done.3), channel_id=1, source_target_pairs={{0,2},{1,15},{2,4},{3,1},{4,6},{5,3},{6,8},{7,5},{8,10},{9,7},{10,... | collective-permute-start | bytes 2359304 | tf_op jit(solution)/shard_map/ppermute | solution.py:325
  34.4 0.8 dynamic-slice_bitcast_fusion
  35.2 0.8 maximum_select_fusion
  36.1 0.6 terms.1
  36.7 5.3 %collective-permute-start.6 = (bf16[8,2048]{1,0:T(8,128)(2,1)S(1)}, bf16[8,2048]{1,0:T(8,128)(2,1)S(1)}, u32[]{:S(2)}, u32[]{:S(2)}) collective-permute-start(bf16[8,2048]{1,0:T(8,128)(2,1)S(1)} %collective-permute-done.5), channel_id=1, source_target_pairs={{0,2},{1,15},{2,4},{3,1},{4,6},{5,3},{6,8},{7,5},{8,10},{9,7},{10,... | collective-permute-start | bytes 98312 | tf_op jit(solution)/shard_map/ppermute | solution.py:325
  42.0 10.9 %collective-permute-done.4 = bf16[192,2048]{1,0:T(8,128)(2,1)S(1)} collective-permute-done((bf16[192,2048]{1,0:T(8,128)(2,1)S(1)}, bf16[192,2048]{1,0:T(8,128)(2,1)S(1)}, u32[]{:S(2)}, u32[]{:S(2)}) %collective-permute-start.4) | collective-permute-done | bytes 786464 | tf_op jit(solution)/shard_map/ppermute | solution.py:325
  52.9 0.1 constant_dynamic-update-slice_fusion.1
  53.0 0.3 collective-permute-done.6
  53.3 3.1 %collective-permute-start.10 = (bf16[200,2048]{1,0:T(8,128)(2,1)S(1)}, bf16[200,2048]{1,0:T(8,128)(2,1)}, u32[]{:S(2)}, u32[]{:S(2)}) collective-permute-start(bf16[200,2048]{1,0:T(8,128)(2,1)S(1)} %constant_dynamic-update-slice_fusion.refs_1_), channel_id=1, source_target_pairs={{0,2},{1,15},{2,4},{3,1},{4,6},{5,3},{6,8},{7,5},{8,10},{9,7},{10,... | collective-permute-start | bytes 2457608 | tf_op jit(solution)/shard_map/ppermute | solution.py:325
  56.5 0.1 reshape.36
  56.6 0.1 copy.17
  56.7 0.1 reshape.37.refs_5_
  56.8 1.9 %collective-permute-start.2 = (bf16[192,2048]{1,0:T(8,128)(2,1)}, bf16[192,2048]{1,0:T(8,128)(2,1)}, u32[]{:S(2)}, u32[]{:S(2)}) collective-permute-start(bf16[192,2048]{1,0:T(8,128)(2,1)} %collective-permute-done.1.refs_0_), channel_id=1, source_target_pairs={{0,2},{1,15},{2,4},{3,1},{4,6},{5,3},{6,8},{7,5},{8,10},{9,7},{10,... | collective-permute-start | bytes 2359304 | tf_op jit(solution)/shard_map/ppermute | solution.py:325
  58.8 3.1 %piece_states.5 = (f32[3,2,136,128]{3,2,1,0:T(8,128)S(1)}, f32[3,2,136,128]{3,2,1,0:T(8,128)S(1)}) custom-call(s32[3]{0:T(128)S(1)} %pad_add_fusion.m_ref, bf16[192,2048]{1,0:T(8,128)(2,1)S(1)} %bitcast.19, bf16[8,2048]{1,0:T(8,128)(2,1)S(1)} %broadcast_select_fusion.refs_1_, bf16[8,2048]{1,0:T(8,128)(2,1)S(1)} %pad.8.refs_2_, ...), custom_call_target="tpu_custom_call" | custom-call | flops 3361996800 | bytes 2101248 | tf_op jit(solution)/shard_map/piece_states/pallas_call | solution.py:136
  61.9 5.6 %collective-permute-done.10.refs_1_ = bf16[200,2048]{1,0:T(8,128)(2,1)} collective-permute-done((bf16[200,2048]{1,0:T(8,128)(2,1)S(1)}, bf16[200,2048]{1,0:T(8,128)(2,1)}, u32[]{:S(2)}, u32[]{:S(2)}) %collective-permute-start.10) | collective-permute-done | bytes 819232 | tf_op jit(solution)/shard_map/ppermute | solution.py:325
  67.6 4.3 %collective-permute-start.11 = (bf16[200,2048]{1,0:T(8,128)(2,1)}, bf16[200,2048]{1,0:T(8,128)(2,1)S(1)}, u32[]{:S(2)}, u32[]{:S(2)}) collective-permute-start(bf16[200,2048]{1,0:T(8,128)(2,1)} %collective-permute-done.10.refs_1_), channel_id=1, source_target_pairs={{0,2},{1,15},{2,4},{3,1},{4,6},{5,3},{6,8},{7,5},{8,10},{9,7},{10,... | collective-permute-start | bytes 2457608 | tf_op jit(solution)/shard_map/ppermute | solution.py:325
  71.9 4.1 %piece_states.6 = (f32[3,2,136,128]{3,2,1,0:T(8,128)S(1)}, f32[3,2,136,128]{3,2,1,0:T(8,128)S(1)}) custom-call(s32[3]{0:T(128)S(1)} %pad_add_fusion.m_ref, bf16[192,2048]{1,0:T(8,128)(2,1)} %collective-permute-done.refs_0_, bf16[200,2048]{1,0:T(8,128)(2,1)S(1)} %constant_dynamic-update-slice_fusion.refs_1_, bf16[8,2048]{1,0:T(8,128)(2,1)S(1)} %pad.8.refs_2_, ...), custom_call_target="tpu_custom_call" | custom-call | flops 6589513728 | bytes 2101248 | tf_op jit(solution)/shard_map/piece_states/pallas_call | solution.py:136
  76.1 4.3 %collective-permute-start.9 = (bf16[192,2048]{1,0:T(8,128)(2,1)}, bf16[192,2048]{1,0:T(8,128)(2,1)S(1)}, u32[]{:S(2)}, u32[]{:S(2)}) collective-permute-start(bf16[192,2048]{1,0:T(8,128)(2,1)} %collective-permute-done.2.refs_0_), channel_id=1, source_target_pairs={{0,2},{1,15},{2,4},{3,1},{4,6},{5,3},{6,8},{7,5},{8,10},{9,7},{10,... | collective-permute-start | bytes 2359304 | tf_op jit(solution)/shard_map/ppermute | solution.py:325
  80.4 4.4 %piece_states.7 = (f32[3,2,136,128]{3,2,1,0:T(8,128)S(1)}, f32[3,2,136,128]{3,2,1,0:T(8,128)S(1)}) custom-call(s32[3]{0:T(128)S(1)} %pad_add_fusion.m_ref, bf16[192,2048]{1,0:T(8,128)(2,1)} %collective-permute-done.1.refs_0_, bf16[200,2048]{1,0:T(8,128)(2,1)} %collective-permute-done.10.refs_1_, bf16[8,2048]{1,0:T(8,128)(2,1)S(1)} %pad.8.refs_2_, ...), custom_call_target="tpu_custom_call" | custom-call | flops 6589513728 | bytes 2101248 | tf_op jit(solution)/shard_map/piece_states/pallas_call | solution.py:136
  84.7 0.8 copy-done.13
  85.5 0.1 slice.44
  85.6 3.7 %collective-permute-start.12 = (bf16[8,2048]{1,0:T(8,128)(2,1)S(1)}, bf16[8,2048]{1,0:T(8,128)(2,1)S(1)}, u32[]{:S(2)}, u32[]{:S(2)}) collective-permute-start(bf16[8,2048]{1,0:T(8,128)(2,1)S(1)} %slice_select_fusion), channel_id=1, source_target_pairs={{0,2},{1,15},{2,4},{3,1},{4,6},{5,3},{6,8},{7,5},{8,10},{9,7},{10,... | collective-permute-start | bytes 98312 | tf_op jit(solution)/shard_map/ppermute | solution.py:325
  89.3 1.0 copy-done.14
  90.3 4.1 %piece_states.8 = (f32[3,2,136,128]{3,2,1,0:T(8,128)S(1)}, f32[3,2,136,128]{3,2,1,0:T(8,128)S(1)}) custom-call(s32[3]{0:T(128)S(1)} %pad_add_fusion.m_ref, bf16[192,2048]{1,0:T(8,128)(2,1)} %collective-permute-done.2.refs_0_, bf16[200,2048]{1,0:T(8,128)(2,1)S(1)} %collective-permute-done.11.refs_1_, bf16[8,2048]{1,0:T(8,128)(2,1)S(1)} %pad.8.refs_2_, ...), custom_call_target="tpu_custom_call" | custom-call | flops 6589513728 | bytes 2101248 | tf_op jit(solution)/shard_map/piece_states/pallas_call | solution.py:136
  94.5 3.1 %piece_states.9 = (f32[3,2,136,128]{3,2,1,0:T(8,128)S(1)}, f32[3,2,136,128]{3,2,1,0:T(8,128)S(1)}) custom-call(s32[3]{0:T(128)S(1)} %pad_add_fusion.m_ref, bf16[192,2048]{1,0:T(8,128)(2,1)S(1)} %collective-permute-done.9.refs_0_, bf16[8,2048]{1,0:T(8,128)(2,1)S(1)} %collective-permute-done.12.refs_1_, bf16[8,2048]{1,0:T(8,128)(2,1)S(1)} %pad.8.refs_2_, ...), custom_call_target="tpu_custom_call" | custom-call | flops 3361996800 | bytes 2101248 | tf_op jit(solution)/shard_map/piece_states/pallas_call | solution.py:136
  97.7 1.9 %collective-permute-start.13 = (f32[3,2,136,128]{3,2,1,0:T(8,128)S(1)}, f32[3,2,136,128]{3,2,1,0:T(8,128)S(1)}, u32[]{:S(2)}, u32[]{:S(2)}) collective-permute-start(f32[3,2,136,128]{3,2,1,0:T(8,128)S(1)} %get-tuple-element.57), channel_id=1, source_target_pairs={{0,1},{1,0},{2,3},{3,2},{4,5},{5,4},{6,7},{7,6},{8,9},{9,8},{10,11... | collective-permute-start | bytes 1253384 | tf_op jit(solution)/shard_map/ppermute | solution.py:318
  99.6 1.7 %collective-permute-done.13.b_ref = f32[3,2,136,128]{3,2,1,0:T(8,128)S(1)} collective-permute-done((f32[3,2,136,128]{3,2,1,0:T(8,128)S(1)}, f32[3,2,136,128]{3,2,1,0:T(8,128)S(1)}, u32[]{:S(2)}, u32[]{:S(2)}) %collective-permute-start.13) | collective-permute-done | bytes 417824 | tf_op jit(solution)/shard_map/ppermute | solution.py:318
  101.3 0.8 packed.1
  102.1 23.8 %all_to_all.5.got_ref = bf16[32,16,128]{2,1,0:T(8,128)(2,1)S(1)} all-to-all(bf16[32,16,128]{2,1,0:T(8,128)(2,1)S(1)} %packed.1), channel_id=1, replica_groups=mesh['sp'=32,'y'=8,'c'=2] {'sp'}, dimensions={0} | all-to-all | bytes 262144 | tf_op jit(solution)/shard_map/all_to_all | solution.py:378
  125.9 1.6 %finished.1 = (bf16[2,2,2,128]{3,2,1,0:T(2,128)(2,1)}, bf16[2,2,2]{2,1,0:T(2,128)(2,1)}) custom-call(s32[3]{0:T(128)S(1)} %pad_add_fusion.m_ref, bf16[32,16,128]{2,1,0:T(8,128)(2,1)S(1)} %all_to_all.5.got_ref, f32[8,128]{1,0:T(8,128)S(1)} %get-tuple-element.59.fix_ref), custom_call_target="tpu_custom_call" | custom-call | tf_op jit(solution)/shard_map/finished/pallas_call | solution.py:294
  (48 shorter events, 0.3 us)
Async XLA Ops:
  0.6 14.5 %collective-permute-start = (bf16[192,2048]{1,0:T(8,128)(2,1)}, bf16[192,2048]{1,0:T(8,128)(2,1)}, u32[]{:S(2)}, u32[]{:S(2)}) collective-permute-start(bf16[192,2048]{1,0:T(8,128)(2,1)} %bitcast.17), channel_id=1, source_target_pairs={{0,2},{1,15},{2,4},{3,1},{4,6},{5,3},{6,8},{7,5},{8,10},{9,7},{10,... | collective-permute-start | bytes 2359304 | tf_op jit(solution)/shard_map/ppermute | solution.py:325
  5.3 19.4 %collective-permute-start.3 = (bf16[192,2048]{1,0:T(8,128)(2,1)}, bf16[192,2048]{1,0:T(8,128)(2,1)S(1)}, u32[]{:S(2)}, u32[]{:S(2)}) collective-permute-start(bf16[192,2048]{1,0:T(8,128)(2,1)} %bitcast.18), channel_id=1, source_target_pairs={{0,1},{1,0},{2,3},{3,2},{4,5},{5,4},{6,7},{7,6},{8,9},{9,8},{10,11... | collective-permute-start | bytes 2359304 | tf_op jit(solution)/shard_map/ppermute | solution.py:318
  16.6 39.7 %collective-permute-start.8 = (f32[2,2,1664]{2,1,0:T(2,128)S(1)}, f32[2,2,1664]{2,1,0:T(2,128)S(1)}, u32[]{:S(2)}, u32[]{:S(2)}) collective-permute-start(f32[2,2,1664]{2,1,0:T(2,128)S(1)} %pad_maximum_fusion), channel_id=1, source_target_pairs={{0,1},{1,0},{2,3},{3,2},{4,5},{5,4},{6,7},{7,6},{8,9},{9,8},{10,11... | collective-permute-start | bytes 79880 | tf_op jit(solution)/shard_map/ppermute | solution.py:318
  18.6 1.0 copy-start
  19.6 1.0 copy-start.1
  20.7 0.7 copy-start.5
  21.3 0.7 copy-start.6
  22.0 14.0 %copy-start.2 = (f32[2]{0:T(128)S(1)}, f32[2]{0:T(128)}, u32[]{:S(2)}) copy-start(f32[2]{0:T(128)} %r_ref) | copy-start | bytes 28
  22.0 14.0 %copy-start.3 = (f32[2]{0:T(128)S(1)}, f32[2]{0:T(128)}, u32[]{:S(2)}) copy-start(f32[2]{0:T(128)} %b_ref) | copy-start | bytes 28
  22.0 14.0 %copy-start.7 = (f32[2,2]{1,0:T(2,128)S(1)}, f32[2,2]{1,0:T(2,128)}, u32[]{:S(2)}) copy-start(f32[2,2]{1,0:T(2,128)} %n_ref.1) | copy-start | bytes 52
  22.0 14.0 %copy-start.8 = (bf16[2,128]{1,0:T(2,128)(2,1)S(1)}, bf16[2,128]{1,0:T(2,128)(2,1)}, u32[]{:S(2)}) copy-start(bf16[2,128]{1,0:T(2,128)(2,1)} %v_ref.2) | copy-start | bytes 1540
  22.0 14.0 %copy-start.9 = (bf16[2,128]{1,0:T(2,128)(2,1)S(1)}, bf16[2,128]{1,0:T(2,128)(2,1)}, u32[]{:S(2)}) copy-start(bf16[2,128]{1,0:T(2,128)(2,1)} %k_ref.2) | copy-start | bytes 1540
  22.0 14.0 %copy-start.10 = (bf16[2,128]{1,0:T(2,128)(2,1)S(1)}, bf16[2,128]{1,0:T(2,128)(2,1)}, u32[]{:S(2)}) copy-start(bf16[2,128]{1,0:T(2,128)(2,1)} %q_ref.1) | copy-start | bytes 1540
  22.1 14.0 %copy-start.11 = (bf16[2,128]{1,0:T(2,128)(2,1)S(1)}, bf16[2,128]{1,0:T(2,128)(2,1)}, u32[]{:S(2)}) copy-start(bf16[2,128]{1,0:T(2,128)(2,1)} %g_ref.1) | copy-start | bytes 1540
  22.1 14.0 %copy-start.12 = (bf16[128]{0:T(256)(128)(2,1)S(1)}, bf16[128]{0:T(256)(128)(2,1)}, u32[]{:S(2)}) copy-start(bf16[128]{0:T(256)(128)(2,1)} %param.29) | copy-start | bytes 772
  22.3 34.1 %copy-start.15 = (f32[2,1536,2]{1,2,0:T(2,128)S(1)}, f32[2,1536,2]{1,2,0:T(2,128)}, u32[]{:S(2)}) copy-start(f32[2,1536,2]{1,2,0:T(2,128)} %param.23) | copy-start | bytes 73732
  22.3 36.5 %collective-permute-start.7 = (bf16[2052,256]{1,0:T(8,128)(2,1)S(1)}, bf16[2052,256]{1,0:T(8,128)(2,1)}, u32[]{:S(2)}, u32[]{:S(2)}) collective-permute-start(bf16[2052,256]{1,0:T(8,128)(2,1)S(1)} %joined.1.refs_3_), channel_id=1, source_target_pairs={{0,1},{1,0},{2,3},{3,2},{4,5},{5,4},{6,7},{7,6},{8,9},{9,8},{10,11... | collective-permute-start | bytes 3151880 | tf_op jit(solution)/shard_map/ppermute | solution.py:318
  24.8 11.9 %collective-permute-start.5 = (bf16[8,2048]{1,0:T(8,128)(2,1)S(1)}, bf16[8,2048]{1,0:T(8,128)(2,1)S(1)}, u32[]{:S(2)}, u32[]{:S(2)}) collective-permute-start(bf16[8,2048]{1,0:T(8,128)(2,1)S(1)} %broadcast_select_fusion.1), channel_id=1, source_target_pairs={{0,2},{1,3},{2,4},{3,5},{4,6},{5,7},{6,8},{7,9},{8,10},{9,11},{10,... | collective-permute-start | bytes 98312 | tf_op jit(solution)/shard_map/ppermute | solution.py:338
  30.4 26.4 %collective-permute-start.1 = (bf16[192,2048]{1,0:T(8,128)(2,1)}, bf16[192,2048]{1,0:T(8,128)(2,1)}, u32[]{:S(2)}, u32[]{:S(2)}) collective-permute-start(bf16[192,2048]{1,0:T(8,128)(2,1)} %collective-permute-done.refs_0_), channel_id=1, source_target_pairs={{0,2},{1,15},{2,4},{3,1},{4,6},{5,3},{6,8},{7,5},{8,10},{9,7},{10,... | collective-permute-start | bytes 2359304 | tf_op jit(solution)/shard_map/ppermute | solution.py:325
  32.3 20.6 %collective-permute-start.4 = (bf16[192,2048]{1,0:T(8,128)(2,1)S(1)}, bf16[192,2048]{1,0:T(8,128)(2,1)S(1)}, u32[]{:S(2)}, u32[]{:S(2)}) collective-permute-start(bf16[192,2048]{1,0:T(8,128)(2,1)S(1)} %collective-permute-done.3), channel_id=1, source_target_pairs={{0,2},{1,15},{2,4},{3,1},{4,6},{5,3},{6,8},{7,5},{8,10},{9,7},{10,... | collective-permute-start | bytes 2359304 | tf_op jit(solution)/shard_map/ppermute | solution.py:325
  36.7 22.1 %copy-start.4 = (bf16[2,96,2048]{2,1,0:T(8,128)(2,1)S(1)}, bf16[2,96,2048]{2,1,0:T(8,128)(2,1)}, u32[]{:S(2)}) copy-start(bf16[2,96,2048]{2,1,0:T(8,128)(2,1)} %param.15) | copy-start | bytes 2359300
  36.7 16.6 %collective-permute-start.6 = (bf16[8,2048]{1,0:T(8,128)(2,1)S(1)}, bf16[8,2048]{1,0:T(8,128)(2,1)S(1)}, u32[]{:S(2)}, u32[]{:S(2)}) collective-permute-start(bf16[8,2048]{1,0:T(8,128)(2,1)S(1)} %collective-permute-done.5), channel_id=1, source_target_pairs={{0,2},{1,15},{2,4},{3,1},{4,6},{5,3},{6,8},{7,5},{8,10},{9,7},{10,... | collective-permute-start | bytes 98312 | tf_op jit(solution)/shard_map/ppermute | solution.py:325
  53.3 14.3 %collective-permute-start.10 = (bf16[200,2048]{1,0:T(8,128)(2,1)S(1)}, bf16[200,2048]{1,0:T(8,128)(2,1)}, u32[]{:S(2)}, u32[]{:S(2)}) collective-permute-start(bf16[200,2048]{1,0:T(8,128)(2,1)S(1)} %constant_dynamic-update-slice_fusion.refs_1_), channel_id=1, source_target_pairs={{0,2},{1,15},{2,4},{3,1},{4,6},{5,3},{6,8},{7,5},{8,10},{9,7},{10,... | collective-permute-start | bytes 2457608 | tf_op jit(solution)/shard_map/ppermute | solution.py:325
  56.8 19.2 %collective-permute-start.2 = (bf16[192,2048]{1,0:T(8,128)(2,1)}, bf16[192,2048]{1,0:T(8,128)(2,1)}, u32[]{:S(2)}, u32[]{:S(2)}) collective-permute-start(bf16[192,2048]{1,0:T(8,128)(2,1)} %collective-permute-done.1.refs_0_), channel_id=1, source_target_pairs={{0,2},{1,15},{2,4},{3,1},{4,6},{5,3},{6,8},{7,5},{8,10},{9,7},{10,... | collective-permute-start | bytes 2359304 | tf_op jit(solution)/shard_map/ppermute | solution.py:325
  67.6 17.9 %collective-permute-start.11 = (bf16[200,2048]{1,0:T(8,128)(2,1)}, bf16[200,2048]{1,0:T(8,128)(2,1)S(1)}, u32[]{:S(2)}, u32[]{:S(2)}) collective-permute-start(bf16[200,2048]{1,0:T(8,128)(2,1)} %collective-permute-done.10.refs_1_), channel_id=1, source_target_pairs={{0,2},{1,15},{2,4},{3,1},{4,6},{5,3},{6,8},{7,5},{8,10},{9,7},{10,... | collective-permute-start | bytes 2457608 | tf_op jit(solution)/shard_map/ppermute | solution.py:325
  76.1 18.4 %collective-permute-start.9 = (bf16[192,2048]{1,0:T(8,128)(2,1)}, bf16[192,2048]{1,0:T(8,128)(2,1)S(1)}, u32[]{:S(2)}, u32[]{:S(2)}) collective-permute-start(bf16[192,2048]{1,0:T(8,128)(2,1)} %collective-permute-done.2.refs_0_), channel_id=1, source_target_pairs={{0,2},{1,15},{2,4},{3,1},{4,6},{5,3},{6,8},{7,5},{8,10},{9,7},{10,... | collective-permute-start | bytes 2359304 | tf_op jit(solution)/shard_map/ppermute | solution.py:325
  84.7 0.8 copy-start.13
  85.6 8.9 %collective-permute-start.12 = (bf16[8,2048]{1,0:T(8,128)(2,1)S(1)}, bf16[8,2048]{1,0:T(8,128)(2,1)S(1)}, u32[]{:S(2)}, u32[]{:S(2)}) collective-permute-start(bf16[8,2048]{1,0:T(8,128)(2,1)S(1)} %slice_select_fusion), channel_id=1, source_target_pairs={{0,2},{1,15},{2,4},{3,1},{4,6},{5,3},{6,8},{7,5},{8,10},{9,7},{10,... | collective-permute-start | bytes 98312 | tf_op jit(solution)/shard_map/ppermute | solution.py:325
  89.3 1.0 copy-start.14
  97.7 3.7 %collective-permute-start.13 = (f32[3,2,136,128]{3,2,1,0:T(8,128)S(1)}, f32[3,2,136,128]{3,2,1,0:T(8,128)S(1)}, u32[]{:S(2)}, u32[]{:S(2)}) collective-permute-start(f32[3,2,136,128]{3,2,1,0:T(8,128)S(1)} %get-tuple-element.57), channel_id=1, source_target_pairs={{0,1},{1,0},{2,3},{3,2},{4,5},{5,4},{6,7},{7,6},{8,9},{9,8},{10,11... | collective-permute-start | bytes 1253384 | tf_op jit(solution)/shard_map/ppermute | solution.py:318

commit v7 on v6

--- a/solution.py
+++ b/solution.py
@@ -338,11 +338,12 @@
     before = lax.ppermute(before, ("sp", "y", "c"), [(i, i + 2) for i in range(count - 2)])
 
     near = onward(before)
+    edge = jnp.where(c == 0, before, ends[1])
+
+    later = (w_value, w_key, conv_value, conv_key, w_step, decay_jump, step_bias, decay_rate)
+    b[1], *later = lax.optimization_barrier((b[1], *later))
+    w_value, w_key, conv_value, conv_key, w_step, decay_jump, step_bias, decay_rate = later
     b[1] = jnp.concatenate([b[1], near], axis=0)
-
-    later = (w_value, w_key, conv_value, conv_key, w_step, decay_jump, step_bias, decay_rate)
-    a[1], *later = lax.optimization_barrier((a[1], *later))
-    w_value, w_key, conv_value, conv_key, w_step, decay_jump, step_bias, decay_rate = later
 
     w_own = joined(w_value, w_key, conv_value, conv_key)
     w_both = w_own, swap(w_own)
@@ -360,7 +361,7 @@
     def add(runs, xs, halo, far, end):
         return piece_states(meta, xs, halo, far, end, w_steps, w_both, jump, rates, runs, rows, y_count)
 
-    runs = add(None, [a[0]], jnp.where(c == 0, before, ends[1]), 0, False)
+    runs = add(None, [a[0]], edge, 0, False)
     for s in range(1, half):
         a.append(onward(a[s]))
         if s + 1 < half:

time: 129 us -> 119 us (0.922)
  the two profiles are of different devices: /device:TPU:24 before, /device:TPU:8 now
where the time goes in v7:
time: 119 us; the launch traced here: 118 us
  starting transfers between devices  41.4 us (35%)
  blocking collectives  23.7 us (20%)
  Pallas kernels  22.1 us (19%)
  waiting for transfers between devices  18.4 us (15%)
  local copies, waits for them, and re-layouts  8.71 us (7%)
  other arithmetic  2.37 us (2%)
  between operations  1.21 us (1%)
    ppermute x9, starting transfers between devices, onward(): return lax.ppermute(v, ('y', 'c'), pairs)  28.4 us
    all_to_all x1, blocking collectives, per_device(): got = lax.all_to_all(sent, 'sp', 0, 0, tiled=True)  23.7 us
    pallas_call x5, Pallas kernels, piece_states(): pl.pallas_call(body, out_shape=[jax.ShapeDtypeStruct(shape, F32)] * 2, in...  18.8 us
    ppermute x9, waiting for transfers between devices, onward(): return lax.ppermute(v, ('y', 'c'), pairs)  9.85 us
    ppermute x4, starting transfers between devices, swap(): return lax.ppermute(v, 'c', [(0, 1), (1, 0)])  8.3 us
    ppermute x1, waiting for transfers between devices, per_device(): lax.ppermute(before, ('sp', 'y', 'c'), [(i, i + 2) for i in range(count -...  6.86 us
    unnamed x37, local copies, waits for them, and re-layouts  6.44 us
    ppermute x1, starting transfers between devices, per_device(): lax.ppermute(before, ('sp', 'y', 'c'), [(i, i + 2) for i in range(count -...  4.7 us
  transfers between devices with their start and end apart: 14, of which 4 were waited for; matrix products, arithmetic and copies ran while one was open for 4% of the time, Pallas kernels for 14%

profile of v7, /device:TPU:8, one launch (start us, length us, event | category | flops | bytes accessed | tf_op | source)
XLA Modules:
  0.0 118.0 jit_solution(8220459562227230030)
XLA Ops:
  0.6 1.9 %collective-permute-start.3 = (bf16[192,2048]{1,0:T(8,128)(2,1)}, bf16[192,2048]{1,0:T(8,128)(2,1)S(1)}, u32[]{:S(2)}, u32[]{:S(2)}) collective-permute-start(bf16[192,2048]{1,0:T(8,128)(2,1)} %bitcast.17), channel_id=1, source_target_pairs={{0,1},{1,0},{2,3},{3,2},{4,5},{5,4},{6,7},{7,6},{8,9},{9,8},{10,11... | collective-permute-start | bytes 2359304 | tf_op jit(solution)/shard_map/ppermute | solution.py:318
  2.6 3.5 %collective-permute-start = (bf16[192,2048]{1,0:T(8,128)(2,1)}, bf16[192,2048]{1,0:T(8,128)(2,1)S(1)}, u32[]{:S(2)}, u32[]{:S(2)}) collective-permute-start(bf16[192,2048]{1,0:T(8,128)(2,1)} %bitcast.18), channel_id=1, source_target_pairs={{0,2},{1,15},{2,4},{3,1},{4,6},{5,3},{6,8},{7,5},{8,10},{9,7},{10,... | collective-permute-start | bytes 2359304 | tf_op jit(solution)/shard_map/ppermute | solution.py:325
  6.1 0.9 slice.29
  7.1 3.5 %collective-permute-start.4 = (bf16[192,2048]{1,0:T(8,128)(2,1)S(1)}, bf16[192,2048]{1,0:T(8,128)(2,1)S(1)}, u32[]{:S(2)}, u32[]{:S(2)}) collective-permute-start(bf16[192,2048]{1,0:T(8,128)(2,1)S(1)} %collective-permute-done.3), channel_id=1, source_target_pairs={{0,2},{1,15},{2,4},{3,1},{4,6},{5,3},{6,8},{7,5},{8,10},{9,7},{10,... | collective-permute-start | bytes 2359304 | tf_op jit(solution)/shard_map/ppermute | solution.py:325
  10.6 4.7 %collective-permute-start.5 = (bf16[8,2048]{1,0:T(8,128)(2,1)S(1)}, bf16[8,2048]{1,0:T(8,128)(2,1)S(1)}, u32[]{:S(2)}, u32[]{:S(2)}) collective-permute-start(bf16[8,2048]{1,0:T(8,128)(2,1)S(1)} %broadcast_select_fusion.1), channel_id=1, source_target_pairs={{0,2},{1,3},{2,4},{3,5},{4,6},{5,7},{6,8},{7,9},{8,10},{9,11},{10,... | collective-permute-start | bytes 98312 | tf_op jit(solution)/shard_map/ppermute | solution.py:338
  15.3 0.1 pad_add_fusion.m_ref
  15.3 5.4 %collective-permute-done.refs_0_ = bf16[192,2048]{1,0:T(8,128)(2,1)S(1)} collective-permute-done((bf16[192,2048]{1,0:T(8,128)(2,1)}, bf16[192,2048]{1,0:T(8,128)(2,1)S(1)}, u32[]{:S(2)}, u32[]{:S(2)}) %collective-permute-start) | collective-permute-done | bytes 786464 | tf_op jit(solution)/shard_map/ppermute | solution.py:325
  20.8 1.9 %collective-permute-start.1 = (bf16[192,2048]{1,0:T(8,128)(2,1)S(1)}, bf16[192,2048]{1,0:T(8,128)(2,1)}, u32[]{:S(2)}, u32[]{:S(2)}) collective-permute-start(bf16[192,2048]{1,0:T(8,128)(2,1)S(1)} %collective-permute-done.refs_0_), channel_id=1, source_target_pairs={{0,2},{1,15},{2,4},{3,1},{4,6},{5,3},{6,8},{7,5},{8,10},{9,7},{10,... | collective-permute-start | bytes 2359304 | tf_op jit(solution)/shard_map/ppermute | solution.py:325
  22.7 6.9 %collective-permute-done.5 = bf16[8,2048]{1,0:T(8,128)(2,1)S(1)} collective-permute-done((bf16[8,2048]{1,0:T(8,128)(2,1)S(1)}, bf16[8,2048]{1,0:T(8,128)(2,1)S(1)}, u32[]{:S(2)}, u32[]{:S(2)}) %collective-permute-start.5) | collective-permute-done | bytes 32800 | tf_op jit(solution)/shard_map/ppermute | solution.py:338
  29.6 1.9 %collective-permute-start.6 = (bf16[8,2048]{1,0:T(8,128)(2,1)S(1)}, bf16[8,2048]{1,0:T(8,128)(2,1)S(1)}, u32[]{:S(2)}, u32[]{:S(2)}) collective-permute-start(bf16[8,2048]{1,0:T(8,128)(2,1)S(1)} %collective-permute-done.5), channel_id=1, source_target_pairs={{0,2},{1,15},{2,4},{3,1},{4,6},{5,3},{6,8},{7,5},{8,10},{9,7},{10,... | collective-permute-start | bytes 98312 | tf_op jit(solution)/shard_map/ppermute | solution.py:325
  31.5 0.7 pad_maximum_fusion.1
  32.2 0.1 broadcast_in_dim.2
  32.3 0.8 pad_maximum_fusion
  33.0 1.9 %collective-permute-start.8 = (f32[2,2,1664]{2,1,0:T(2,128)S(1)}, f32[2,2,1664]{2,1,0:T(2,128)S(1)}, u32[]{:S(2)}, u32[]{:S(2)}) collective-permute-start(f32[2,2,1664]{2,1,0:T(2,128)S(1)} %pad_maximum_fusion), channel_id=1, source_target_pairs={{0,1},{1,0},{2,3},{3,2},{4,5},{5,4},{6,7},{7,6},{8,9},{9,8},{10,11... | collective-permute-start | bytes 79880 | tf_op jit(solution)/shard_map/ppermute | solution.py:318
  34.9 0.0 copy-start
  35.0 1.0 copy-done
  36.0 1.0 copy-done.1
  37.0 0.7 copy-done.5
  37.7 0.7 copy-done.6
  38.4 0.2 joined.1.refs_3_
  38.7 2.5 %collective-permute-start.7 = (bf16[2052,256]{1,0:T(8,128)(2,1)S(1)}, bf16[2052,256]{1,0:T(8,128)(2,1)}, u32[]{:S(2)}, u32[]{:S(2)}) collective-permute-start(bf16[2052,256]{1,0:T(8,128)(2,1)S(1)} %joined.1.refs_3_), channel_id=1, source_target_pairs={{0,1},{1,0},{2,3},{3,2},{4,5},{5,4},{6,7},{7,6},{8,9},{9,8},{10,11... | collective-permute-start | bytes 3151880 | tf_op jit(solution)/shard_map/ppermute | solution.py:318
  41.2 0.1 constant_dynamic-update-slice_fusion.1
  41.3 1.9 %collective-permute-start.10 = (bf16[200,2048]{1,0:T(8,128)(2,1)S(1)}, bf16[200,2048]{1,0:T(8,128)(2,1)}, u32[]{:S(2)}, u32[]{:S(2)}) collective-permute-start(bf16[200,2048]{1,0:T(8,128)(2,1)S(1)} %constant_dynamic-update-slice_fusion.refs_1_), channel_id=1, source_target_pairs={{0,2},{1,15},{2,4},{3,1},{4,6},{5,3},{6,8},{7,5},{8,10},{9,7},{10,... | collective-permute-start | bytes 2457608 | tf_op jit(solution)/shard_map/ppermute | solution.py:325
  43.3 0.8 dynamic-slice_bitcast_fusion
  44.1 0.8 maximum_select_fusion
  45.0 0.6 terms.1
  45.6 5.3 %collective-permute-start.2 = (bf16[192,2048]{1,0:T(8,128)(2,1)}, bf16[192,2048]{1,0:T(8,128)(2,1)}, u32[]{:S(2)}, u32[]{:S(2)}) collective-permute-start(bf16[192,2048]{1,0:T(8,128)(2,1)} %collective-permute-done.1.refs_0_), channel_id=1, source_target_pairs={{0,2},{1,15},{2,4},{3,1},{4,6},{5,3},{6,8},{7,5},{8,10},{9,7},{10,... | collective-permute-start | bytes 2359304 | tf_op jit(solution)/shard_map/ppermute | solution.py:325
  51.0 0.1 reshape.36
  51.1 0.1 copy.17
  51.2 0.1 reshape.37.refs_5_
  51.3 4.4 %collective-permute-done.10.refs_1_ = bf16[200,2048]{1,0:T(8,128)(2,1)} collective-permute-done((bf16[200,2048]{1,0:T(8,128)(2,1)S(1)}, bf16[200,2048]{1,0:T(8,128)(2,1)}, u32[]{:S(2)}, u32[]{:S(2)}) %collective-permute-start.10) | collective-permute-done | bytes 819232 | tf_op jit(solution)/shard_map/ppermute | solution.py:325
  55.7 2.7 %collective-permute-start.11 = (bf16[200,2048]{1,0:T(8,128)(2,1)}, bf16[200,2048]{1,0:T(8,128)(2,1)S(1)}, u32[]{:S(2)}, u32[]{:S(2)}) collective-permute-start(bf16[200,2048]{1,0:T(8,128)(2,1)} %collective-permute-done.10.refs_1_), channel_id=1, source_target_pairs={{0,2},{1,15},{2,4},{3,1},{4,6},{5,3},{6,8},{7,5},{8,10},{9,7},{10,... | collective-permute-start | bytes 2457608 | tf_op jit(solution)/shard_map/ppermute | solution.py:325
  58.4 1.1 copy-done.4
  59.5 3.2 %piece_states.5 = (f32[3,2,136,128]{3,2,1,0:T(8,128)S(1)}, f32[3,2,136,128]{3,2,1,0:T(8,128)S(1)}) custom-call(s32[3]{0:T(128)S(1)} %pad_add_fusion.m_ref, bf16[192,2048]{1,0:T(8,128)(2,1)S(1)} %bitcast.19, bf16[8,2048]{1,0:T(8,128)(2,1)S(1)} %broadcast_select_fusion.refs_1_, bf16[8,2048]{1,0:T(8,128)(2,1)S(1)} %pad.8.refs_2_, ...), custom_call_target="tpu_custom_call" | custom-call | flops 3361996800 | bytes 2101248 | tf_op jit(solution)/shard_map/piece_states/pallas_call | solution.py:136
  62.7 3.9 %piece_states.6 = (f32[3,2,136,128]{3,2,1,0:T(8,128)S(1)}, f32[3,2,136,128]{3,2,1,0:T(8,128)S(1)}) custom-call(s32[3]{0:T(128)S(1)} %pad_add_fusion.m_ref, bf16[192,2048]{1,0:T(8,128)(2,1)S(1)} %copy-done.14, bf16[200,2048]{1,0:T(8,128)(2,1)S(1)} %constant_dynamic-update-slice_fusion.refs_1_, bf16[8,2048]{1,0:T(8,128)(2,1)S(1)} %pad.8.refs_2_, ...), custom_call_target="tpu_custom_call" | custom-call | flops 6589513728 | bytes 2101248 | tf_op jit(solution)/shard_map/piece_states/pallas_call | solution.py:136
  66.7 4.5 %collective-permute-start.9 = (bf16[192,2048]{1,0:T(8,128)(2,1)}, bf16[192,2048]{1,0:T(8,128)(2,1)S(1)}, u32[]{:S(2)}, u32[]{:S(2)}) collective-permute-start(bf16[192,2048]{1,0:T(8,128)(2,1)} %collective-permute-done.2.refs_0_), channel_id=1, source_target_pairs={{0,2},{1,15},{2,4},{3,1},{4,6},{5,3},{6,8},{7,5},{8,10},{9,7},{10,... | collective-permute-start | bytes 2359304 | tf_op jit(solution)/shard_map/ppermute | solution.py:325
  71.2 4.4 %piece_states.7 = (f32[3,2,136,128]{3,2,1,0:T(8,128)S(1)}, f32[3,2,136,128]{3,2,1,0:T(8,128)S(1)}) custom-call(s32[3]{0:T(128)S(1)} %pad_add_fusion.m_ref, bf16[192,2048]{1,0:T(8,128)(2,1)} %collective-permute-done.1.refs_0_, bf16[200,2048]{1,0:T(8,128)(2,1)} %collective-permute-done.10.refs_1_, bf16[8,2048]{1,0:T(8,128)(2,1)S(1)} %pad.8.refs_2_, ...), custom_call_target="tpu_custom_call" | custom-call | flops 6589513728 | bytes 2101248 | tf_op jit(solution)/shard_map/piece_states/pallas_call | solution.py:136
  75.6 0.7 copy-done.15
  76.3 0.1 slice.44
  76.5 3.3 %collective-permute-start.12 = (bf16[8,2048]{1,0:T(8,128)(2,1)S(1)}, bf16[8,2048]{1,0:T(8,128)(2,1)S(1)}, u32[]{:S(2)}, u32[]{:S(2)}) collective-permute-start(bf16[8,2048]{1,0:T(8,128)(2,1)S(1)} %slice_select_fusion), channel_id=1, source_target_pairs={{0,2},{1,15},{2,4},{3,1},{4,6},{5,3},{6,8},{7,5},{8,10},{9,7},{10,... | collective-permute-start | bytes 98312 | tf_op jit(solution)/shard_map/ppermute | solution.py:325
  79.8 1.0 copy-done.16
  80.8 4.1 %piece_states.8 = (f32[3,2,136,128]{3,2,1,0:T(8,128)S(1)}, f32[3,2,136,128]{3,2,1,0:T(8,128)S(1)}) custom-call(s32[3]{0:T(128)S(1)} %pad_add_fusion.m_ref, bf16[192,2048]{1,0:T(8,128)(2,1)} %collective-permute-done.2.refs_0_, bf16[200,2048]{1,0:T(8,128)(2,1)S(1)} %collective-permute-done.11.refs_1_, bf16[8,2048]{1,0:T(8,128)(2,1)S(1)} %pad.8.refs_2_, ...), custom_call_target="tpu_custom_call" | custom-call | flops 6589513728 | bytes 2101248 | tf_op jit(solution)/shard_map/piece_states/pallas_call | solution.py:136
  84.9 3.1 %piece_states.9 = (f32[3,2,136,128]{3,2,1,0:T(8,128)S(1)}, f32[3,2,136,128]{3,2,1,0:T(8,128)S(1)}) custom-call(s32[3]{0:T(128)S(1)} %pad_add_fusion.m_ref, bf16[192,2048]{1,0:T(8,128)(2,1)S(1)} %collective-permute-done.9.refs_0_, bf16[8,2048]{1,0:T(8,128)(2,1)S(1)} %collective-permute-done.12.refs_1_, bf16[8,2048]{1,0:T(8,128)(2,1)S(1)} %pad.8.refs_2_, ...), custom_call_target="tpu_custom_call" | custom-call | flops 3361996800 | bytes 2101248 | tf_op jit(solution)/shard_map/piece_states/pallas_call | solution.py:136
  88.1 1.9 %collective-permute-start.13 = (f32[3,2,136,128]{3,2,1,0:T(8,128)S(1)}, f32[3,2,136,128]{3,2,1,0:T(8,128)S(1)}, u32[]{:S(2)}, u32[]{:S(2)}) collective-permute-start(f32[3,2,136,128]{3,2,1,0:T(8,128)S(1)} %get-tuple-element.57), channel_id=1, source_target_pairs={{0,1},{1,0},{2,3},{3,2},{4,5},{5,4},{6,7},{7,6},{8,9},{9,8},{10,11... | collective-permute-start | bytes 1253384 | tf_op jit(solution)/shard_map/ppermute | solution.py:318
  90.0 1.7 %collective-permute-done.13.b_ref = f32[3,2,136,128]{3,2,1,0:T(8,128)S(1)} collective-permute-done((f32[3,2,136,128]{3,2,1,0:T(8,128)S(1)}, f32[3,2,136,128]{3,2,1,0:T(8,128)S(1)}, u32[]{:S(2)}, u32[]{:S(2)}) %collective-permute-start.13) | collective-permute-done | bytes 417824 | tf_op jit(solution)/shard_map/ppermute | solution.py:318
  91.8 0.8 packed.1
  92.6 23.7 %all_to_all.5.got_ref = bf16[32,16,128]{2,1,0:T(8,128)(2,1)S(1)} all-to-all(bf16[32,16,128]{2,1,0:T(8,128)(2,1)S(1)} %packed.1), channel_id=1, replica_groups=mesh['sp'=32,'y'=8,'c'=2] {'sp'}, dimensions={0} | all-to-all | bytes 262144 | tf_op jit(solution)/shard_map/all_to_all | solution.py:379
  116.3 1.6 %finished.1 = (bf16[2,2,2,128]{3,2,1,0:T(2,128)(2,1)}, bf16[2,2,2]{2,1,0:T(2,128)(2,1)}) custom-call(s32[3]{0:T(128)S(1)} %pad_add_fusion.m_ref, bf16[32,16,128]{2,1,0:T(8,128)(2,1)S(1)} %all_to_all.5.got_ref, f32[8,128]{1,0:T(8,128)S(1)} %get-tuple-element.59.fix_ref), custom_call_target="tpu_custom_call" | custom-call | tf_op jit(solution)/shard_map/finished/pallas_call | solution.py:294
  (52 shorter events, 0.3 us)
Async XLA Ops:
  0.6 6.4 %collective-permute-start.3 = (bf16[192,2048]{1,0:T(8,128)(2,1)}, bf16[192,2048]{1,0:T(8,128)(2,1)S(1)}, u32[]{:S(2)}, u32[]{:S(2)}) collective-permute-start(bf16[192,2048]{1,0:T(8,128)(2,1)} %bitcast.17), channel_id=1, source_target_pairs={{0,1},{1,0},{2,3},{3,2},{4,5},{5,4},{6,7},{7,6},{8,9},{9,8},{10,11... | collective-permute-start | bytes 2359304 | tf_op jit(solution)/shard_map/ppermute | solution.py:318
  2.6 18.2 %collective-permute-start = (bf16[192,2048]{1,0:T(8,128)(2,1)}, bf16[192,2048]{1,0:T(8,128)(2,1)S(1)}, u32[]{:S(2)}, u32[]{:S(2)}) collective-permute-start(bf16[192,2048]{1,0:T(8,128)(2,1)} %bitcast.18), channel_id=1, source_target_pairs={{0,2},{1,15},{2,4},{3,1},{4,6},{5,3},{6,8},{7,5},{8,10},{9,7},{10,... | collective-permute-start | bytes 2359304 | tf_op jit(solution)/shard_map/ppermute | solution.py:325
  7.1 24.4 %collective-permute-start.4 = (bf16[192,2048]{1,0:T(8,128)(2,1)S(1)}, bf16[192,2048]{1,0:T(8,128)(2,1)S(1)}, u32[]{:S(2)}, u32[]{:S(2)}) collective-permute-start(bf16[192,2048]{1,0:T(8,128)(2,1)S(1)} %collective-permute-done.3), channel_id=1, source_target_pairs={{0,2},{1,15},{2,4},{3,1},{4,6},{5,3},{6,8},{7,5},{8,10},{9,7},{10,... | collective-permute-start | bytes 2359304 | tf_op jit(solution)/shard_map/ppermute | solution.py:325
  10.6 19.0 %collective-permute-start.5 = (bf16[8,2048]{1,0:T(8,128)(2,1)S(1)}, bf16[8,2048]{1,0:T(8,128)(2,1)S(1)}, u32[]{:S(2)}, u32[]{:S(2)}) collective-permute-start(bf16[8,2048]{1,0:T(8,128)(2,1)S(1)} %broadcast_select_fusion.1), channel_id=1, source_target_pairs={{0,2},{1,3},{2,4},{3,5},{4,6},{5,7},{6,8},{7,9},{8,10},{9,11},{10,... | collective-permute-start | bytes 98312 | tf_op jit(solution)/shard_map/ppermute | solution.py:338
  20.8 17.8 %copy-start.13 = (bf16[192,2048]{1,0:T(8,128)(2,1)}, bf16[192,2048]{1,0:T(8,128)(2,1)S(1)}, u32[]{:S(2)}) copy-start(bf16[192,2048]{1,0:T(8,128)(2,1)S(1)} %collective-permute-done.refs_0_) | copy-start | bytes 2359300
  20.8 24.8 %collective-permute-start.1 = (bf16[192,2048]{1,0:T(8,128)(2,1)S(1)}, bf16[192,2048]{1,0:T(8,128)(2,1)}, u32[]{:S(2)}, u32[]{:S(2)}) collective-permute-start(bf16[192,2048]{1,0:T(8,128)(2,1)S(1)} %collective-permute-done.refs_0_), channel_id=1, source_target_pairs={{0,2},{1,15},{2,4},{3,1},{4,6},{5,3},{6,8},{7,5},{8,10},{9,7},{10,... | collective-permute-start | bytes 2359304 | tf_op jit(solution)/shard_map/ppermute | solution.py:325
  29.6 11.8 %collective-permute-start.6 = (bf16[8,2048]{1,0:T(8,128)(2,1)S(1)}, bf16[8,2048]{1,0:T(8,128)(2,1)S(1)}, u32[]{:S(2)}, u32[]{:S(2)}) collective-permute-start(bf16[8,2048]{1,0:T(8,128)(2,1)S(1)} %collective-permute-done.5), channel_id=1, source_target_pairs={{0,2},{1,15},{2,4},{3,1},{4,6},{5,3},{6,8},{7,5},{8,10},{9,7},{10,... | collective-permute-start | bytes 98312 | tf_op jit(solution)/shard_map/ppermute | solution.py:325
  33.0 17.9 %collective-permute-start.8 = (f32[2,2,1664]{2,1,0:T(2,128)S(1)}, f32[2,2,1664]{2,1,0:T(2,128)S(1)}, u32[]{:S(2)}, u32[]{:S(2)}) collective-permute-start(f32[2,2,1664]{2,1,0:T(2,128)S(1)} %pad_maximum_fusion), channel_id=1, source_target_pairs={{0,1},{1,0},{2,3},{3,2},{4,5},{5,4},{6,7},{7,6},{8,9},{9,8},{10,11... | collective-permute-start | bytes 79880 | tf_op jit(solution)/shard_map/ppermute | solution.py:318
  34.9 1.0 copy-start
  36.0 1.0 copy-start.1
  37.0 0.7 copy-start.5
  37.7 0.7 copy-start.6
  38.6 6.3 %copy-start.2 = (f32[2]{0:T(128)S(1)}, f32[2]{0:T(128)}, u32[]{:S(2)}) copy-start(f32[2]{0:T(128)} %r_ref) | copy-start | bytes 28
  38.6 6.3 %copy-start.3 = (f32[2]{0:T(128)S(1)}, f32[2]{0:T(128)}, u32[]{:S(2)}) copy-start(f32[2]{0:T(128)} %b_ref) | copy-start | bytes 28
  38.6 6.3 %copy-start.7 = (f32[2,2]{1,0:T(2,128)S(1)}, f32[2,2]{1,0:T(2,128)}, u32[]{:S(2)}) copy-start(f32[2,2]{1,0:T(2,128)} %n_ref.1) | copy-start | bytes 52
  38.6 6.3 %copy-start.8 = (bf16[2,128]{1,0:T(2,128)(2,1)S(1)}, bf16[2,128]{1,0:T(2,128)(2,1)}, u32[]{:S(2)}) copy-start(bf16[2,128]{1,0:T(2,128)(2,1)} %v_ref.2) | copy-start | bytes 1540
  38.6 6.3 %copy-start.9 = (bf16[2,128]{1,0:T(2,128)(2,1)S(1)}, bf16[2,128]{1,0:T(2,128)(2,1)}, u32[]{:S(2)}) copy-start(bf16[2,128]{1,0:T(2,128)(2,1)} %k_ref.2) | copy-start | bytes 1540
  38.6 6.3 %copy-start.10 = (bf16[2,128]{1,0:T(2,128)(2,1)S(1)}, bf16[2,128]{1,0:T(2,128)(2,1)}, u32[]{:S(2)}) copy-start(bf16[2,128]{1,0:T(2,128)(2,1)} %q_ref.1) | copy-start | bytes 1540
  38.7 6.3 %copy-start.11 = (bf16[2,128]{1,0:T(2,128)(2,1)S(1)}, bf16[2,128]{1,0:T(2,128)(2,1)}, u32[]{:S(2)}) copy-start(bf16[2,128]{1,0:T(2,128)(2,1)} %g_ref.1) | copy-start | bytes 1540
  38.7 6.3 %copy-start.12 = (bf16[128]{0:T(256)(128)(2,1)S(1)}, bf16[128]{0:T(256)(128)(2,1)}, u32[]{:S(2)}) copy-start(bf16[128]{0:T(256)(128)(2,1)} %param.29) | copy-start | bytes 772
  38.7 12.2 %copy-start.17 = (f32[2,1536,2]{1,2,0:T(2,128)S(1)}, f32[2,1536,2]{1,2,0:T(2,128)}, u32[]{:S(2)}) copy-start(f32[2,1536,2]{1,2,0:T(2,128)} %param.23) | copy-start | bytes 73732
  38.7 19.7 %collective-permute-start.7 = (bf16[2052,256]{1,0:T(8,128)(2,1)S(1)}, bf16[2052,256]{1,0:T(8,128)(2,1)}, u32[]{:S(2)}, u32[]{:S(2)}) collective-permute-start(bf16[2052,256]{1,0:T(8,128)(2,1)S(1)} %joined.1.refs_3_), channel_id=1, source_target_pairs={{0,1},{1,0},{2,3},{3,2},{4,5},{5,4},{6,7},{7,6},{8,9},{9,8},{10,11... | collective-permute-start | bytes 3151880 | tf_op jit(solution)/shard_map/ppermute | solution.py:318
  41.3 14.3 %collective-permute-start.10 = (bf16[200,2048]{1,0:T(8,128)(2,1)S(1)}, bf16[200,2048]{1,0:T(8,128)(2,1)}, u32[]{:S(2)}, u32[]{:S(2)}) collective-permute-start(bf16[200,2048]{1,0:T(8,128)(2,1)S(1)} %constant_dynamic-update-slice_fusion.refs_1_), channel_id=1, source_target_pairs={{0,2},{1,15},{2,4},{3,1},{4,6},{5,3},{6,8},{7,5},{8,10},{9,7},{10,... | collective-permute-start | bytes 2457608 | tf_op jit(solution)/shard_map/ppermute | solution.py:325
  45.6 21.1 %collective-permute-start.2 = (bf16[192,2048]{1,0:T(8,128)(2,1)}, bf16[192,2048]{1,0:T(8,128)(2,1)}, u32[]{:S(2)}, u32[]{:S(2)}) collective-permute-start(bf16[192,2048]{1,0:T(8,128)(2,1)} %collective-permute-done.1.refs_0_), channel_id=1, source_target_pairs={{0,2},{1,15},{2,4},{3,1},{4,6},{5,3},{6,8},{7,5},{8,10},{9,7},{10,... | collective-permute-start | bytes 2359304 | tf_op jit(solution)/shard_map/ppermute | solution.py:325
  55.7 20.6 %collective-permute-start.11 = (bf16[200,2048]{1,0:T(8,128)(2,1)}, bf16[200,2048]{1,0:T(8,128)(2,1)S(1)}, u32[]{:S(2)}, u32[]{:S(2)}) collective-permute-start(bf16[200,2048]{1,0:T(8,128)(2,1)} %collective-permute-done.10.refs_1_), channel_id=1, source_target_pairs={{0,2},{1,15},{2,4},{3,1},{4,6},{5,3},{6,8},{7,5},{8,10},{9,7},{10,... | collective-permute-start | bytes 2457608 | tf_op jit(solution)/shard_map/ppermute | solution.py:325
  58.4 1.1 copy-start.4
  59.5 3.2 %copy-start.14 = (bf16[192,2048]{1,0:T(8,128)(2,1)S(1)}, bf16[192,2048]{1,0:T(8,128)(2,1)}, u32[]{:S(2)}) copy-start(bf16[192,2048]{1,0:T(8,128)(2,1)} %copy-done.13) | copy-start | bytes 2359300
  66.7 18.3 %collective-permute-start.9 = (bf16[192,2048]{1,0:T(8,128)(2,1)}, bf16[192,2048]{1,0:T(8,128)(2,1)S(1)}, u32[]{:S(2)}, u32[]{:S(2)}) collective-permute-start(bf16[192,2048]{1,0:T(8,128)(2,1)} %collective-permute-done.2.refs_0_), channel_id=1, source_target_pairs={{0,2},{1,15},{2,4},{3,1},{4,6},{5,3},{6,8},{7,5},{8,10},{9,7},{10,... | collective-permute-start | bytes 2359304 | tf_op jit(solution)/shard_map/ppermute | solution.py:325
  75.6 0.8 copy-start.15
  76.5 8.5 %collective-permute-start.12 = (bf16[8,2048]{1,0:T(8,128)(2,1)S(1)}, bf16[8,2048]{1,0:T(8,128)(2,1)S(1)}, u32[]{:S(2)}, u32[]{:S(2)}) collective-permute-start(bf16[8,2048]{1,0:T(8,128)(2,1)S(1)} %slice_select_fusion), channel_id=1, source_target_pairs={{0,2},{1,15},{2,4},{3,1},{4,6},{5,3},{6,8},{7,5},{8,10},{9,7},{10,... | collective-permute-start | bytes 98312 | tf_op jit(solution)/shard_map/ppermute | solution.py:325
  79.8 1.0 copy-start.16
  88.1 3.7 %collective-permute-start.13 = (f32[3,2,136,128]{3,2,1,0:T(8,128)S(1)}, f32[3,2,136,128]{3,2,1,0:T(8,128)S(1)}, u32[]{:S(2)}, u32[]{:S(2)}) collective-permute-start(f32[3,2,136,128]{3,2,1,0:T(8,128)S(1)} %get-tuple-element.57), channel_id=1, source_target_pairs={{0,1},{1,0},{2,3},{3,2},{4,5},{5,4},{6,7},{7,6},{8,9},{9,8},{10,11... | collective-permute-start | bytes 1253384 | tf_op jit(solution)/shard_map/ppermute | solution.py:318

commit v8 on v4

--- a/solution.py
+++ b/solution.py
@@ -34,16 +34,22 @@
     return jnp.maximum(v, 0.0) + jnp.log1p(jnp.exp(-jnp.abs(v)))
 
 
-def piece_states(meta, xs, far, end, w_step, w, jump, rates, runs, rows, chips):
+def piece_states(meta, xs, halo, far, end, w_step, w, jump, rates, runs, rows, chips):
+    many, both = len(xs), 2 * rows
     depth = w[0].shape[0] - 4
-    many, both = len(xs), 2 * rows
     given = [] if runs is None else list(runs)
+    xs = xs if halo is None else [*xs, halo]
+    held = len(xs)
 
     def body(m_ref, *refs):
-        x_refs = refs[:many]
-        s_ref, wa_ref, wb_ref, j_ref, r_ref = refs[many : many + 5]
-        ins = refs[many + 5 : many + 5 + len(given)]
-        own_out, other_out, ext = refs[many + 5 + len(given) :]
+        x_refs = list(refs[:held])
+        s_ref, wa_ref, wb_ref, j_ref, r_ref = refs[held : held + 5]
+        ins = refs[held + 5 : held + 5 + len(given)]
+        own_out, other_out, ext, full = refs[held + 5 + len(given) :]
+        if held > many:
+            full[:both, :] = x_refs[0][...]
+            full[both:, :] = x_refs[1][...]
+            x_refs = [full]
         outs = (own_out, other_out)
         y, c = m_ref[0], m_ref[1]
         low = c == 0
@@ -87,13 +93,14 @@
             lifts.append(jnp.transpose(weight))
 
         taps = jnp.concatenate([r[depth : depth + 4, :] for r in (wa_ref, wb_ref)], axis=1).astype(F32)
-        for n in range(many):
-            x = x_refs[n][...]
-            for g, r in enumerate((wa_ref, wb_ref)):
-                p = mm(x, r[:depth, :], ((1,), (0,))).astype(BF).astype(F32)
+        for g, r in enumerate((wa_ref, wb_ref)):
+            cols = slice(256 * g, 256 * g + 256)
+            p = [mm(v[...], r[:depth, :], ((1,), (0,))).astype(BF).astype(F32) for v in x_refs]
+            for n in range(many):
+                base = both + 8 * (many - 1 - n)
                 for s in range(2):
-                    ext[2 * n + s, 4:8, 256 * g : 256 * g + 256] = p[both + 4 * s : both + 4 * s + 4, :]
-                    ext[2 * n + s, 8 : 8 + rows, 256 * g : 256 * g + 256] = p[s * rows : (s + 1) * rows, :]
+                    ext[2 * n + s, 4:8, cols] = p[-1][base + 4 * s : base + 4 * s + 4, :]
+                    ext[2 * n + s, 8 : 8 + rows, cols] = p[n][s * rows : (s + 1) * rows, :]
         for s in range(2):
             states = [jnp.zeros((128, 128), F32)] * 2
             for n in range(many):
@@ -122,9 +129,9 @@
     return pl.pallas_call(
         body,
         out_shape=[jax.ShapeDtypeStruct(shape, F32)] * 2,
-        in_specs=[SMEM] + [VMEM] * (many + 5 + len(given)),
+        in_specs=[SMEM] + [VMEM] * (held + 5 + len(given)),
         out_specs=[VMEM] * 2,
-        scratch_shapes=[pltpu.VMEM((2 * many, rows + 8, 512), F32)],
+        scratch_shapes=[pltpu.VMEM((2 * many, rows + 8, 512), F32), pltpu.VMEM((both + 8, depth), BF)],
         cost_estimate=pl.CostEstimate(
             flops=32 * sum(x.shape[0] for x in xs) * w[0].size,
             transcendentals=0,
@@ -313,18 +320,12 @@
     meta = jnp.stack([y, c, (128 - sp * share) % 128]).astype(jnp.int32)
 
     x = hidden_in.reshape(2 * rows, width)
-    bare = onward(x)
     ends = hidden_in[:, rows - 4 :, :].reshape(8, width)
     ends = lax.ppermute(ends, ("sp", "y", "c"), [(i, i + 1) for i in range(count - 1)])
-    a = [jnp.concatenate([x, ends], axis=0)]
-    b = [swap(a[0])]
+    a = [x, onward(x)]
+    first = jnp.concatenate([x, ends], axis=0)
+    b = [jnp.concatenate([swap(first), ends], axis=0)]
     b.append(onward(b[0]))
-    pairs = []
-    for i in range(y_count):
-        pairs.append((2 * i + 1, 2 * ((i + 1) % y_count)))
-        pairs.append((2 * i, 2 * ((i - 1) % y_count) + 1))
-    near = lax.ppermute(b[0][2 * rows :], ("y", "c"), pairs)
-    a.append(jnp.concatenate([bare, near], axis=0))
 
     w_own = joined(w_value, w_key, conv_value, conv_key)
     w_both = w_own, swap(w_own)
@@ -339,19 +340,20 @@
     jump = jump[:, :, : tp_count * rows].reshape(2, 8, tp_count, rows).transpose(2, 1, 0, 3)
     jump = jump.reshape(tp_count, 8, 2 * rows)
 
-    def add(runs, xs, far, end):
-        return piece_states(meta, xs, far, end, w_steps, w_both, jump, rates, runs, rows, y_count)
-
-    runs = add(None, [a[0]], 0, False)
+    def add(runs, xs, halo, far, end):
+        return piece_states(meta, xs, halo, far, end, w_steps, w_both, jump, rates, runs, rows, y_count)
+
+    runs = add(None, [first], None, 0, False)
     for s in range(1, half):
         a.append(onward(a[s]))
         if s + 1 < half:
             b.append(onward(b[s]))
-        runs = add(runs, [a[s], b[s]], s, False)
+        runs = add(runs, [a[s], b[s]], None, s, False)
 
     fixed, query = terms(step_bias, decay_rate, new_step, new_value, new_key, new_query, new_gate, read_gain)
     runs, fixed, query = lax.optimization_barrier((runs, fixed, query))
-    own, other = add(runs, [a[half]], half, True)
+    last = onward(b[half - 1][2 * rows + 8 :])
+    own, other = add(runs, [a[half]], last, half, True)
     sent = packed(meta, own, swap(other), query, sp_count, y_count)
     got = lax.all_to_all(sent, "sp", 0, 0, tiled=True)
     return tuple(finished(meta, got, fixed))

time: 119 us -> 115 us (0.966)
  starting transfers between devices: 48.7 us -> 44.5 us
  local copies, waits for them, and re-layouts: 4.19 us -> 2.24 us
    ppermute x1 -> x0, starting transfers between devices: 2.32 us -> none  [per_device(): near = lax.ppermute(b[0][2 * rows:], ('y', 'c'), pairs)]
    ppermute x4, starting transfers between devices: 12.5 us -> 10.4 us  [swap(): return lax.ppermute(v, 'c', [(0, 1), (1, 0)])]
    ppermute x7 -> x8, waiting for transfers between devices: 12 us -> 12.6 us  [onward(): return lax.ppermute(v, ('y', 'c'), pairs)]
    ppermute x7 -> x8, starting transfers between devices: 29.4 us -> 29.6 us  [onward(): return lax.ppermute(v, ('y', 'c'), pairs)]
  transfers between devices with their start and end apart: 13 -> 13, of which waited for: 6 -> 9; matrix products, arithmetic and copies ran while one was open for 3% -> 3% of each run, Pallas kernels for 14% -> 14%
where the time goes in v8:
time: 115 us; the launch traced here: 114 us
  starting transfers between devices  44.5 us (39%)
  blocking collectives  22.4 us (19%)
  Pallas kernels  22.1 us (19%)
  waiting for transfers between devices  18.2 us (16%)
  other arithmetic  3.13 us (3%)
  local copies, waits for them, and re-layouts  2.24 us (2%)
    ppermute x8, starting transfers between devices, onward(): return lax.ppermute(v, ('y', 'c'), pairs)  29.6 us
    all_to_all x1, blocking collectives, per_device(): got = lax.all_to_all(sent, 'sp', 0, 0, tiled=True)  22.4 us
    pallas_call x5, Pallas kernels, piece_states(): pl.pallas_call(body, out_shape=[jax.ShapeDtypeStruct(shape, F32)] * 2, in...  18.8 us
    ppermute x8, waiting for transfers between devices, onward(): return lax.ppermute(v, ('y', 'c'), pairs)  12.6 us
    ppermute x4, starting transfers between devices, swap(): return lax.ppermute(v, 'c', [(0, 1), (1, 0)])  10.4 us
    ppermute x1, starting transfers between devices, per_device(): lax.ppermute(ends, ('sp', 'y', 'c'), [(i, i + 1) for i in range(count - 1)])  4.58 us
    ppermute x1, waiting for transfers between devices, per_device(): lax.ppermute(ends, ('sp', 'y', 'c'), [(i, i + 1) for i in range(count - 1)])  4.22 us
  transfers between devices with their start and end apart: 13, of which 9 were waited for; matrix products, arithmetic and copies ran while one was open for 3% of the time, Pallas kernels for 14%

profile of v8, /device:TPU:1, one launch (start us, length us, event | category | flops | bytes accessed | tf_op | source)
XLA Modules:
  0.0 113.8 jit_solution(14264971558882474476)
XLA Ops:
  0.7 0.9 slice.20
  1.6 4.6 %collective-permute-start.4 = (bf16[8,2048]{1,0:T(8,128)(2,1)S(1)}, bf16[8,2048]{1,0:T(8,128)(2,1)S(1)}, u32[]{:S(2)}, u32[]{:S(2)}) collective-permute-start(bf16[8,2048]{1,0:T(8,128)(2,1)S(1)} %reshape.21), channel_id=1, source_target_pairs={{0,1},{1,2},{2,3},{3,4},{4,5},{5,6},{6,7},{7,8},{8,9},{9,10},{10,1... | collective-permute-start | bytes 98312 | tf_op jit(solution)/shard_map/ppermute | solution.py:324
  6.2 4.2 %collective-permute-done.4 = bf16[8,2048]{1,0:T(8,128)(2,1)S(1)} collective-permute-done((bf16[8,2048]{1,0:T(8,128)(2,1)S(1)}, bf16[8,2048]{1,0:T(8,128)(2,1)S(1)}, u32[]{:S(2)}, u32[]{:S(2)}) %collective-permute-start.4) | collective-permute-done | bytes 32800 | tf_op jit(solution)/shard_map/ppermute | solution.py:324
  10.5 1.2 %pad_maximum_fusion.1.refs_0_ = bf16[200,2048]{1,0:T(8,128)(2,1)S(1)} fusion(bf16[8,2048]{1,0:T(8,128)(2,1)S(1)} %collective-permute-done.4, bf16[192,2048]{1,0:T(8,128)(2,1)} %bitcast.16), kind=kLoop, calls=%fused_computation.1 | loop fusion | flops 1638400 | bytes 1638400 | tf_op jit(solution)/shard_map/concatenate | solution.py:326
  11.6 0.0 copy-start.2
  11.7 0.0 copy-start.3
  11.7 2.1 %collective-permute-start.5 = (bf16[200,2048]{1,0:T(8,128)(2,1)S(1)}, bf16[200,2048]{1,0:T(8,128)(2,1)S(1)}, u32[]{:S(2)}, u32[]{:S(2)}) collective-permute-start(bf16[200,2048]{1,0:T(8,128)(2,1)S(1)} %pad_maximum_fusion.1.refs_0_), channel_id=1, source_target_pairs={{0,1},{1,0},{2,3},{3,2},{4,5},{5,4},{6,7},{7,6},{8,9},{9,8},{10,11... | collective-permute-start | bytes 2457608 | tf_op jit(solution)/shard_map/ppermute | solution.py:311
  13.7 2.8 %collective-permute-start = (bf16[192,2048]{1,0:T(8,128)(2,1)}, bf16[192,2048]{1,0:T(8,128)(2,1)}, u32[]{:S(2)}, u32[]{:S(2)}) collective-permute-start(bf16[192,2048]{1,0:T(8,128)(2,1)} %bitcast.17), channel_id=1, source_target_pairs={{0,2},{1,15},{2,4},{3,1},{4,6},{5,3},{6,8},{7,5},{8,10},{9,7},{10,... | collective-permute-start | bytes 2359304 | tf_op jit(solution)/shard_map/ppermute | solution.py:318
  16.6 0.2 joined.1.refs_2_.refs_3_
  16.8 0.0 copy-start.6
  16.9 0.0 copy-start.7
  16.9 0.0 copy-start.10
  16.9 0.0 copy-start.11
  16.9 2.1 %collective-permute-start.10 = (bf16[2052,256]{1,0:T(8,128)(2,1)S(1)}, bf16[2052,256]{1,0:T(8,128)(2,1)}, u32[]{:S(2)}, u32[]{:S(2)}) collective-permute-start(bf16[2052,256]{1,0:T(8,128)(2,1)S(1)} %joined.1.refs_2_.refs_3_), channel_id=1, source_target_pairs={{0,1},{1,0},{2,3},{3,2},{4,5},{5,4},{6,7},{7,6},{8,9},{9,8},{10,11... | collective-permute-start | bytes 3151880 | tf_op jit(solution)/shard_map/ppermute | solution.py:311
  19.0 1.0 pad_maximum_fusion
  20.0 4.2 %collective-permute-start.6 = (bf16[208,2048]{1,0:T(8,128)(2,1)}, bf16[208,2048]{1,0:T(8,128)(2,1)S(1)}, u32[]{:S(2)}, u32[]{:S(2)}) collective-permute-start(bf16[208,2048]{1,0:T(8,128)(2,1)} %pad_maximum_fusion), channel_id=1, source_target_pairs={{0,2},{1,15},{2,4},{3,1},{4,6},{5,3},{6,8},{7,5},{8,10},{9,7},{10,... | collective-permute-start | bytes 2555912 | tf_op jit(solution)/shard_map/ppermute | solution.py:318
  24.3 0.1 broadcast_in_dim.2
  24.4 1.9 %collective-permute-start.11 = (f32[2,2,1664]{2,1,0:T(2,128)S(1)}, f32[2,2,1664]{2,1,0:T(2,128)S(1)}, u32[]{:S(2)}, u32[]{:S(2)}) collective-permute-start(f32[2,2,1664]{2,1,0:T(2,128)S(1)} %pad_maximum_fusion.2), channel_id=1, source_target_pairs={{0,1},{1,0},{2,3},{3,2},{4,5},{5,4},{6,7},{7,6},{8,9},{9,8},{10,11... | collective-permute-start | bytes 79880 | tf_op jit(solution)/shard_map/ppermute | solution.py:311
  26.3 0.8 dynamic-slice_bitcast_fusion
  27.1 3.7 %collective-permute-start.1 = (bf16[192,2048]{1,0:T(8,128)(2,1)}, bf16[192,2048]{1,0:T(8,128)(2,1)}, u32[]{:S(2)}, u32[]{:S(2)}) collective-permute-start(bf16[192,2048]{1,0:T(8,128)(2,1)} %collective-permute-done.refs_0_), channel_id=1, source_target_pairs={{0,2},{1,15},{2,4},{3,1},{4,6},{5,3},{6,8},{7,5},{8,10},{9,7},{10,... | collective-permute-start | bytes 2359304 | tf_op jit(solution)/shard_map/ppermute | solution.py:318
  30.9 5.2 %collective-permute-done.6.refs_1_ = bf16[208,2048]{1,0:T(8,128)(2,1)S(1)} collective-permute-done((bf16[208,2048]{1,0:T(8,128)(2,1)}, bf16[208,2048]{1,0:T(8,128)(2,1)S(1)}, u32[]{:S(2)}, u32[]{:S(2)}) %collective-permute-start.6) | collective-permute-done | bytes 852000 | tf_op jit(solution)/shard_map/ppermute | solution.py:318
  36.1 3.8 %collective-permute-start.7 = (bf16[208,2048]{1,0:T(8,128)(2,1)S(1)}, bf16[208,2048]{1,0:T(8,128)(2,1)}, u32[]{:S(2)}, u32[]{:S(2)}) collective-permute-start(bf16[208,2048]{1,0:T(8,128)(2,1)S(1)} %collective-permute-done.6.refs_1_), channel_id=1, source_target_pairs={{0,2},{1,15},{2,4},{3,1},{4,6},{5,3},{6,8},{7,5},{8,10},{9,7},{10,... | collective-permute-start | bytes 2555912 | tf_op jit(solution)/shard_map/ppermute | solution.py:318
  39.9 0.8 maximum_select_fusion
  40.7 0.1 pad_add_fusion.m_ref
  40.8 0.6 terms.1
  41.5 0.1 reshape.22
  41.6 0.1 copy.17
  41.8 0.1 reshape.23.refs_4_.refs_5_
  41.9 2.8 %collective-permute-done.1.refs_0_ = bf16[192,2048]{1,0:T(8,128)(2,1)} collective-permute-done((bf16[192,2048]{1,0:T(8,128)(2,1)}, bf16[192,2048]{1,0:T(8,128)(2,1)}, u32[]{:S(2)}, u32[]{:S(2)}) %collective-permute-start.1) | collective-permute-done | bytes 786464 | tf_op jit(solution)/shard_map/ppermute | solution.py:318
  44.6 3.8 %collective-permute-start.2 = (bf16[192,2048]{1,0:T(8,128)(2,1)}, bf16[192,2048]{1,0:T(8,128)(2,1)S(1)}, u32[]{:S(2)}, u32[]{:S(2)}) collective-permute-start(bf16[192,2048]{1,0:T(8,128)(2,1)} %collective-permute-done.1.refs_0_), channel_id=1, source_target_pairs={{0,2},{1,15},{2,4},{3,1},{4,6},{5,3},{6,8},{7,5},{8,10},{9,7},{10,... | collective-permute-start | bytes 2359304 | tf_op jit(solution)/shard_map/ppermute | solution.py:318
  48.4 3.2 %piece_states.5 = (f32[3,2,136,128]{3,2,1,0:T(8,128)S(1)}, f32[3,2,136,128]{3,2,1,0:T(8,128)S(1)}) custom-call(s32[3]{0:T(128)S(1)} %pad_add_fusion.m_ref, bf16[200,2048]{1,0:T(8,128)(2,1)S(1)} %pad_maximum_fusion.1.refs_0_, bf16[8,2048]{1,0:T(8,128)(2,1)S(1)} %pad.8.refs_1_.refs_2_, bf16[2052,256]{1,0:T(8,128)(2,1)S(1)} %joined.1.refs_2_.refs_3_, ...), custom_call_target="tpu_custom_call" | custom-call | flops 3361996800 | bytes 2101248 | tf_op jit(solution)/shard_map/piece_states/pallas_call | solution.py:129
  51.6 2.1 %collective-permute-done.7.refs_1_ = bf16[208,2048]{1,0:T(8,128)(2,1)} collective-permute-done((bf16[208,2048]{1,0:T(8,128)(2,1)S(1)}, bf16[208,2048]{1,0:T(8,128)(2,1)}, u32[]{:S(2)}, u32[]{:S(2)}) %collective-permute-start.7) | collective-permute-done | bytes 852000 | tf_op jit(solution)/shard_map/ppermute | solution.py:318
  53.8 3.8 %collective-permute-start.8 = (bf16[208,2048]{1,0:T(8,128)(2,1)}, bf16[208,2048]{1,0:T(8,128)(2,1)S(1)}, u32[]{:S(2)}, u32[]{:S(2)}) collective-permute-start(bf16[208,2048]{1,0:T(8,128)(2,1)} %collective-permute-done.7.refs_1_), channel_id=1, source_target_pairs={{0,2},{1,15},{2,4},{3,1},{4,6},{5,3},{6,8},{7,5},{8,10},{9,7},{10,... | collective-permute-start | bytes 2555912 | tf_op jit(solution)/shard_map/ppermute | solution.py:318
  57.5 4.2 %piece_states.6 = (f32[3,2,136,128]{3,2,1,0:T(8,128)S(1)}, f32[3,2,136,128]{3,2,1,0:T(8,128)S(1)}) custom-call(s32[3]{0:T(128)S(1)} %pad_add_fusion.m_ref, bf16[192,2048]{1,0:T(8,128)(2,1)} %collective-permute-done.refs_0_, bf16[208,2048]{1,0:T(8,128)(2,1)S(1)} %collective-permute-done.6.refs_1_, bf16[8,2048]{1,0:T(8,128)(2,1)S(1)} %pad.8.refs_1_.refs_2_, ...), custom_call_target="tpu_custom_call" | custom-call | flops 6723993600 | bytes 2101248 | tf_op jit(solution)/shard_map/piece_states/pallas_call | solution.py:129
  61.7 0.4 collective-permute-done.2.refs_0_
  62.1 3.8 %collective-permute-start.3 = (bf16[192,2048]{1,0:T(8,128)(2,1)S(1)}, bf16[192,2048]{1,0:T(8,128)(2,1)S(1)}, u32[]{:S(2)}, u32[]{:S(2)}) collective-permute-start(bf16[192,2048]{1,0:T(8,128)(2,1)S(1)} %collective-permute-done.2.refs_0_), channel_id=1, source_target_pairs={{0,2},{1,15},{2,4},{3,1},{4,6},{5,3},{6,8},{7,5},{8,10},{9,7},{10,... | collective-permute-start | bytes 2359304 | tf_op jit(solution)/shard_map/ppermute | solution.py:318
  65.9 4.4 %piece_states.7 = (f32[3,2,136,128]{3,2,1,0:T(8,128)S(1)}, f32[3,2,136,128]{3,2,1,0:T(8,128)S(1)}) custom-call(s32[3]{0:T(128)S(1)} %pad_add_fusion.m_ref, bf16[192,2048]{1,0:T(8,128)(2,1)} %collective-permute-done.1.refs_0_, bf16[208,2048]{1,0:T(8,128)(2,1)} %collective-permute-done.7.refs_1_, bf16[8,2048]{1,0:T(8,128)(2,1)S(1)} %pad.8.refs_1_.refs_2_, ...), custom_call_target="tpu_custom_call" | custom-call | flops 6723993600 | bytes 2101248 | tf_op jit(solution)/shard_map/piece_states/pallas_call | solution.py:129
  70.2 1.0 collective-permute-done.8.refs_1_
  71.2 3.8 %collective-permute-start.9 = (bf16[8,2048]{1,0:T(8,128)(2,1)S(1)}, bf16[8,2048]{1,0:T(8,128)(2,1)S(1)}, u32[]{:S(2)}, u32[]{:S(2)}) collective-permute-start(bf16[8,2048]{1,0:T(8,128)(2,1)S(1)} %slice.26), channel_id=1, source_target_pairs={{0,2},{1,15},{2,4},{3,1},{4,6},{5,3},{6,8},{7,5},{8,10},{9,7},{10,... | collective-permute-start | bytes 98312 | tf_op jit(solution)/shard_map/ppermute | solution.py:318
  75.0 3.9 %piece_states.8 = (f32[3,2,136,128]{3,2,1,0:T(8,128)S(1)}, f32[3,2,136,128]{3,2,1,0:T(8,128)S(1)}) custom-call(s32[3]{0:T(128)S(1)} %pad_add_fusion.m_ref, bf16[192,2048]{1,0:T(8,128)(2,1)S(1)} %collective-permute-done.2.refs_0_, bf16[208,2048]{1,0:T(8,128)(2,1)S(1)} %collective-permute-done.8.refs_1_, bf16[8,2048]{1,0:T(8,128)(2,1)S(1)} %pad.8.refs_1_.refs_2_, ...), custom_call_target="tpu_custom_call" | custom-call | flops 6723993600 | bytes 2101248 | tf_op jit(solution)/shard_map/piece_states/pallas_call | solution.py:129
  78.9 0.8 collective-permute-done.3.refs_0_
  79.7 0.4 collective-permute-done.9.refs_1_
  80.0 3.2 %piece_states.9 = (f32[3,2,136,128]{3,2,1,0:T(8,128)S(1)}, f32[3,2,136,128]{3,2,1,0:T(8,128)S(1)}) custom-call(s32[3]{0:T(128)S(1)} %pad_add_fusion.m_ref, bf16[192,2048]{1,0:T(8,128)(2,1)S(1)} %collective-permute-done.3.refs_0_, bf16[8,2048]{1,0:T(8,128)(2,1)S(1)} %collective-permute-done.9.refs_1_, bf16[8,2048]{1,0:T(8,128)(2,1)S(1)} %pad.8.refs_1_.refs_2_, ...), custom_call_target="tpu_custom_call" | custom-call | flops 3361996800 | bytes 2101248 | tf_op jit(solution)/shard_map/piece_states/pallas_call | solution.py:129
  83.2 4.3 %collective-permute-start.12 = (f32[3,2,136,128]{3,2,1,0:T(8,128)S(1)}, f32[3,2,136,128]{3,2,1,0:T(8,128)S(1)}, u32[]{:S(2)}, u32[]{:S(2)}) collective-permute-start(f32[3,2,136,128]{3,2,1,0:T(8,128)S(1)} %get-tuple-element.31), channel_id=1, source_target_pairs={{0,1},{1,0},{2,3},{3,2},{4,5},{5,4},{6,7},{7,6},{8,9},{9,8},{10,11... | collective-permute-start | bytes 1253384 | tf_op jit(solution)/shard_map/ppermute | solution.py:311
  87.5 1.4 %collective-permute-done.12.b_ref = f32[3,2,136,128]{3,2,1,0:T(8,128)S(1)} collective-permute-done((f32[3,2,136,128]{3,2,1,0:T(8,128)S(1)}, f32[3,2,136,128]{3,2,1,0:T(8,128)S(1)}, u32[]{:S(2)}, u32[]{:S(2)}) %collective-permute-start.12) | collective-permute-done | bytes 417824 | tf_op jit(solution)/shard_map/ppermute | solution.py:311
  88.9 0.8 packed.1
  89.7 22.4 %all_to_all.5.got_ref = bf16[32,16,128]{2,1,0:T(8,128)(2,1)S(1)} all-to-all(bf16[32,16,128]{2,1,0:T(8,128)(2,1)S(1)} %packed.1), channel_id=1, replica_groups=mesh['sp'=32,'y'=8,'c'=2] {'sp'}, dimensions={0} | all-to-all | bytes 262144 | tf_op jit(solution)/shard_map/all_to_all | solution.py:358
  112.1 1.6 %finished.1 = (bf16[2,2,2,128]{3,2,1,0:T(2,128)(2,1)}, bf16[2,2,2]{2,1,0:T(2,128)(2,1)}) custom-call(s32[3]{0:T(128)S(1)} %pad_add_fusion.m_ref, bf16[32,16,128]{2,1,0:T(8,128)(2,1)S(1)} %all_to_all.5.got_ref, f32[8,128]{1,0:T(8,128)S(1)} %get-tuple-element.33.fix_ref), custom_call_target="tpu_custom_call" | custom-call | tf_op jit(solution)/shard_map/finished/pallas_call | solution.py:287
  (33 shorter events, 0.2 us)
Async XLA Ops:
  0.6 16.0 %copy-start = (bf16[2048,128]{1,0:T(8,128)(2,1)S(1)}, bf16[2048,128]{1,0:T(8,128)(2,1)}, u32[]{:S(2)}) copy-start(bf16[2048,128]{1,0:T(8,128)(2,1)} %v_ref.2) | copy-start | bytes 1572868
  0.6 16.0 %copy-start.1 = (bf16[2048,128]{1,0:T(8,128)(2,1)S(1)}, bf16[2048,128]{1,0:T(8,128)(2,1)}, u32[]{:S(2)}) copy-start(bf16[2048,128]{1,0:T(8,128)(2,1)} %k_ref.2) | copy-start | bytes 1572868
  0.7 16.0 %copy-start.4 = (bf16[4,128]{1,0:T(4,128)(2,1)S(1)}, bf16[4,128]{1,0:T(4,128)(2,1)}, u32[]{:S(2)}) copy-start(bf16[4,128]{1,0:T(4,128)(2,1)} %cv_ref.1) | copy-start | bytes 3076
  0.7 16.0 %copy-start.5 = (bf16[4,128]{1,0:T(4,128)(2,1)S(1)}, bf16[4,128]{1,0:T(4,128)(2,1)}, u32[]{:S(2)}) copy-start(bf16[4,128]{1,0:T(4,128)(2,1)} %ck_ref.1) | copy-start | bytes 3076
  1.6 8.8 %collective-permute-start.4 = (bf16[8,2048]{1,0:T(8,128)(2,1)S(1)}, bf16[8,2048]{1,0:T(8,128)(2,1)S(1)}, u32[]{:S(2)}, u32[]{:S(2)}) collective-permute-start(bf16[8,2048]{1,0:T(8,128)(2,1)S(1)} %reshape.21), channel_id=1, source_target_pairs={{0,1},{1,2},{2,3},{3,4},{4,5},{5,6},{6,7},{7,8},{8,9},{9,10},{10,1... | collective-permute-start | bytes 98312 | tf_op jit(solution)/shard_map/ppermute | solution.py:324
  11.6 7.3 %copy-start.2 = (f32[2]{0:T(128)S(1)}, f32[2]{0:T(128)}, u32[]{:S(2)}) copy-start(f32[2]{0:T(128)} %r_ref.1) | copy-start | bytes 28
  11.7 7.3 %copy-start.3 = (f32[2]{0:T(128)S(1)}, f32[2]{0:T(128)}, u32[]{:S(2)}) copy-start(f32[2]{0:T(128)} %b_ref.1) | copy-start | bytes 28
  11.7 7.4 %collective-permute-start.5 = (bf16[200,2048]{1,0:T(8,128)(2,1)S(1)}, bf16[200,2048]{1,0:T(8,128)(2,1)S(1)}, u32[]{:S(2)}, u32[]{:S(2)}) collective-permute-start(bf16[200,2048]{1,0:T(8,128)(2,1)S(1)} %pad_maximum_fusion.1.refs_0_), channel_id=1, source_target_pairs={{0,1},{1,0},{2,3},{3,2},{4,5},{5,4},{6,7},{7,6},{8,9},{9,8},{10,11... | collective-permute-start | bytes 2457608 | tf_op jit(solution)/shard_map/ppermute | solution.py:311
  13.7 13.3 %collective-permute-start = (bf16[192,2048]{1,0:T(8,128)(2,1)}, bf16[192,2048]{1,0:T(8,128)(2,1)}, u32[]{:S(2)}, u32[]{:S(2)}) collective-permute-start(bf16[192,2048]{1,0:T(8,128)(2,1)} %bitcast.17), channel_id=1, source_target_pairs={{0,2},{1,15},{2,4},{3,1},{4,6},{5,3},{6,8},{7,5},{8,10},{9,7},{10,... | collective-permute-start | bytes 2359304 | tf_op jit(solution)/shard_map/ppermute | solution.py:318
  16.8 7.5 %copy-start.12 = (f32[2,1536,2]{1,2,0:T(2,128)S(1)}, f32[2,1536,2]{1,2,0:T(2,128)}, u32[]{:S(2)}) copy-start(f32[2,1536,2]{1,2,0:T(2,128)} %param.23) | copy-start | bytes 73732
  16.8 23.9 %copy-start.6 = (f32[2,2]{1,0:T(2,128)S(1)}, f32[2,2]{1,0:T(2,128)}, u32[]{:S(2)}) copy-start(f32[2,2]{1,0:T(2,128)} %n_ref.1) | copy-start | bytes 52
  16.9 23.9 %copy-start.7 = (bf16[2,128]{1,0:T(2,128)(2,1)S(1)}, bf16[2,128]{1,0:T(2,128)(2,1)}, u32[]{:S(2)}) copy-start(bf16[2,128]{1,0:T(2,128)(2,1)} %v_ref.3) | copy-start | bytes 1540
  16.9 23.9 %copy-start.8 = (bf16[2,128]{1,0:T(2,128)(2,1)S(1)}, bf16[2,128]{1,0:T(2,128)(2,1)}, u32[]{:S(2)}) copy-start(bf16[2,128]{1,0:T(2,128)(2,1)} %k_ref.3) | copy-start | bytes 1540
  16.9 23.9 %copy-start.9 = (bf16[2,128]{1,0:T(2,128)(2,1)S(1)}, bf16[2,128]{1,0:T(2,128)(2,1)}, u32[]{:S(2)}) copy-start(bf16[2,128]{1,0:T(2,128)(2,1)} %q_ref.1) | copy-start | bytes 1540
  16.9 23.9 %copy-start.10 = (bf16[2,128]{1,0:T(2,128)(2,1)S(1)}, bf16[2,128]{1,0:T(2,128)(2,1)}, u32[]{:S(2)}) copy-start(bf16[2,128]{1,0:T(2,128)(2,1)} %g_ref.1) | copy-start | bytes 1540
  16.9 23.9 %copy-start.11 = (bf16[128]{0:T(256)(128)(2,1)S(1)}, bf16[128]{0:T(256)(128)(2,1)}, u32[]{:S(2)}) copy-start(bf16[128]{0:T(256)(128)(2,1)} %param.29) | copy-start | bytes 772
  16.9 31.5 %collective-permute-start.10 = (bf16[2052,256]{1,0:T(8,128)(2,1)S(1)}, bf16[2052,256]{1,0:T(8,128)(2,1)}, u32[]{:S(2)}, u32[]{:S(2)}) collective-permute-start(bf16[2052,256]{1,0:T(8,128)(2,1)S(1)} %joined.1.refs_2_.refs_3_), channel_id=1, source_target_pairs={{0,1},{1,0},{2,3},{3,2},{4,5},{5,4},{6,7},{7,6},{8,9},{9,8},{10,11... | collective-permute-start | bytes 3151880 | tf_op jit(solution)/shard_map/ppermute | solution.py:311
  20.0 16.1 %collective-permute-start.6 = (bf16[208,2048]{1,0:T(8,128)(2,1)}, bf16[208,2048]{1,0:T(8,128)(2,1)S(1)}, u32[]{:S(2)}, u32[]{:S(2)}) collective-permute-start(bf16[208,2048]{1,0:T(8,128)(2,1)} %pad_maximum_fusion), channel_id=1, source_target_pairs={{0,2},{1,15},{2,4},{3,1},{4,6},{5,3},{6,8},{7,5},{8,10},{9,7},{10,... | collective-permute-start | bytes 2555912 | tf_op jit(solution)/shard_map/ppermute | solution.py:318
  24.4 17.1 %collective-permute-start.11 = (f32[2,2,1664]{2,1,0:T(2,128)S(1)}, f32[2,2,1664]{2,1,0:T(2,128)S(1)}, u32[]{:S(2)}, u32[]{:S(2)}) collective-permute-start(f32[2,2,1664]{2,1,0:T(2,128)S(1)} %pad_maximum_fusion.2), channel_id=1, source_target_pairs={{0,1},{1,0},{2,3},{3,2},{4,5},{5,4},{6,7},{7,6},{8,9},{9,8},{10,11... | collective-permute-start | bytes 79880 | tf_op jit(solution)/shard_map/ppermute | solution.py:311
  27.1 17.5 %collective-permute-start.1 = (bf16[192,2048]{1,0:T(8,128)(2,1)}, bf16[192,2048]{1,0:T(8,128)(2,1)}, u32[]{:S(2)}, u32[]{:S(2)}) collective-permute-start(bf16[192,2048]{1,0:T(8,128)(2,1)} %collective-permute-done.refs_0_), channel_id=1, source_target_pairs={{0,2},{1,15},{2,4},{3,1},{4,6},{5,3},{6,8},{7,5},{8,10},{9,7},{10,... | collective-permute-start | bytes 2359304 | tf_op jit(solution)/shard_map/ppermute | solution.py:318
  36.1 17.7 %collective-permute-start.7 = (bf16[208,2048]{1,0:T(8,128)(2,1)S(1)}, bf16[208,2048]{1,0:T(8,128)(2,1)}, u32[]{:S(2)}, u32[]{:S(2)}) collective-permute-start(bf16[208,2048]{1,0:T(8,128)(2,1)S(1)} %collective-permute-done.6.refs_1_), channel_id=1, source_target_pairs={{0,2},{1,15},{2,4},{3,1},{4,6},{5,3},{6,8},{7,5},{8,10},{9,7},{10,... | collective-permute-start | bytes 2555912 | tf_op jit(solution)/shard_map/ppermute | solution.py:318
  44.6 17.4 %collective-permute-start.2 = (bf16[192,2048]{1,0:T(8,128)(2,1)}, bf16[192,2048]{1,0:T(8,128)(2,1)S(1)}, u32[]{:S(2)}, u32[]{:S(2)}) collective-permute-start(bf16[192,2048]{1,0:T(8,128)(2,1)} %collective-permute-done.1.refs_0_), channel_id=1, source_target_pairs={{0,2},{1,15},{2,4},{3,1},{4,6},{5,3},{6,8},{7,5},{8,10},{9,7},{10,... | collective-permute-start | bytes 2359304 | tf_op jit(solution)/shard_map/ppermute | solution.py:318
  53.8 17.4 %collective-permute-start.8 = (bf16[208,2048]{1,0:T(8,128)(2,1)}, bf16[208,2048]{1,0:T(8,128)(2,1)S(1)}, u32[]{:S(2)}, u32[]{:S(2)}) collective-permute-start(bf16[208,2048]{1,0:T(8,128)(2,1)} %collective-permute-done.7.refs_1_), channel_id=1, source_target_pairs={{0,2},{1,15},{2,4},{3,1},{4,6},{5,3},{6,8},{7,5},{8,10},{9,7},{10,... | collective-permute-start | bytes 2555912 | tf_op jit(solution)/shard_map/ppermute | solution.py:318
  62.1 17.6 %collective-permute-start.3 = (bf16[192,2048]{1,0:T(8,128)(2,1)S(1)}, bf16[192,2048]{1,0:T(8,128)(2,1)S(1)}, u32[]{:S(2)}, u32[]{:S(2)}) collective-permute-start(bf16[192,2048]{1,0:T(8,128)(2,1)S(1)} %collective-permute-done.2.refs_0_), channel_id=1, source_target_pairs={{0,2},{1,15},{2,4},{3,1},{4,6},{5,3},{6,8},{7,5},{8,10},{9,7},{10,... | collective-permute-start | bytes 2359304 | tf_op jit(solution)/shard_map/ppermute | solution.py:318
  71.2 8.8 %collective-permute-start.9 = (bf16[8,2048]{1,0:T(8,128)(2,1)S(1)}, bf16[8,2048]{1,0:T(8,128)(2,1)S(1)}, u32[]{:S(2)}, u32[]{:S(2)}) collective-permute-start(bf16[8,2048]{1,0:T(8,128)(2,1)S(1)} %slice.26), channel_id=1, source_target_pairs={{0,2},{1,15},{2,4},{3,1},{4,6},{5,3},{6,8},{7,5},{8,10},{9,7},{10,... | collective-permute-start | bytes 98312 | tf_op jit(solution)/shard_map/ppermute | solution.py:318
  83.2 5.7 %collective-permute-start.12 = (f32[3,2,136,128]{3,2,1,0:T(8,128)S(1)}, f32[3,2,136,128]{3,2,1,0:T(8,128)S(1)}, u32[]{:S(2)}, u32[]{:S(2)}) collective-permute-start(f32[3,2,136,128]{3,2,1,0:T(8,128)S(1)} %get-tuple-element.31), channel_id=1, source_target_pairs={{0,1},{1,0},{2,3},{3,2},{4,5},{5,4},{6,7},{7,6},{8,9},{9,8},{10,11... | collective-permute-start | bytes 1253384 | tf_op jit(solution)/shard_map/ppermute | solution.py:311

commit v9 on v8

--- a/solution.py
+++ b/solution.py
@@ -34,23 +34,22 @@
     return jnp.maximum(v, 0.0) + jnp.log1p(jnp.exp(-jnp.abs(v)))
 
 
-def piece_states(meta, xs, halo, far, end, w_step, w, jump, rates, runs, rows, chips):
+def piece_states(meta, xs, halo, far, end, w_step, w, jump, rates, runs, groups, rows, chips):
     many, both = len(xs), 2 * rows
     depth = w[0].shape[0] - 4
     given = [] if runs is None else list(runs)
     xs = xs if halo is None else [*xs, halo]
-    held = len(xs)
+    held, wide = len(xs), len(groups)
 
     def body(m_ref, *refs):
         x_refs = list(refs[:held])
-        s_ref, wa_ref, wb_ref, j_ref, r_ref = refs[held : held + 5]
-        ins = refs[held + 5 : held + 5 + len(given)]
-        own_out, other_out, ext, full = refs[held + 5 + len(given) :]
+        s_ref, j_ref, r_ref, *w_refs = refs[held : held + 3 + wide]
+        ins = refs[held + 3 + wide : held + 3 + wide + len(given)]
+        *outs, ext, full = refs[held + 3 + wide + len(given) :]
         if held > many:
             full[:both, :] = x_refs[0][...]
             full[both:, :] = x_refs[1][...]
             x_refs = [full]
-        outs = (own_out, other_out)
         y, c = m_ref[0], m_ref[1]
         low = c == 0
         away = jnp.where(low, y - far, y + far)
@@ -58,7 +57,7 @@
         chip = jnp.where(away < 0, away + chips, jnp.where(away >= chips, away - chips, away))
         run = 2 if end else jnp.where(wrapped, 1, 0)
         place = (2 * chip + c, 2 * chip + 1 - c)
-        for g in range(2):
+        for g in range(wide):
             if given:
                 outs[g][...] = ins[g][...]
             else:
@@ -80,7 +79,7 @@
                 jnp.sum(jnp.where(lane < rows, 0.0, decay), axis=1, keepdims=True),
             ])
         total = [sum(v[s] for v in sums) for s in range(2)]
-        before = [own_out[run, s, 128:136, :] for s in range(2)]
+        before = [outs[0][run, s, 128:136, :] for s in range(2)]
         lead = [jnp.where(low, v[:, 0:1], 0.0) for v in before]
         lifts = []
         for n in range(many):
@@ -92,8 +91,8 @@
             weight = jnp.concatenate([weight, jnp.zeros((8, 256 - both), F32)], axis=1)
             lifts.append(jnp.transpose(weight))
 
-        taps = jnp.concatenate([r[depth : depth + 4, :] for r in (wa_ref, wb_ref)], axis=1).astype(F32)
-        for g, r in enumerate((wa_ref, wb_ref)):
+        taps = jnp.concatenate([r[depth : depth + 4, :] for r in w_refs], axis=1).astype(F32)
+        for g, r in enumerate(w_refs):
             cols = slice(256 * g, 256 * g + 256)
             p = [mm(v[...], r[:depth, :], ((1,), (0,))).astype(BF).astype(F32) for v in x_refs]
             for n in range(many):
@@ -102,36 +101,38 @@
                     ext[2 * n + s, 4:8, cols] = p[-1][base + 4 * s : base + 4 * s + 4, :]
                     ext[2 * n + s, 8 : 8 + rows, cols] = p[n][s * rows : (s + 1) * rows, :]
         for s in range(2):
-            states = [jnp.zeros((128, 128), F32)] * 2
+            states = [jnp.zeros((128, 128), F32)] * wide
             for n in range(many):
                 mixed = ext[2 * n + s, 5 : 5 + rows, :] * taps[0:1, :]
                 for k in range(1, 4):
                     mixed = mixed + ext[2 * n + s, 5 + k : 5 + k + rows, :] * taps[k : k + 1, :]
                 mixed = mixed / (1.0 + jnp.exp(-mixed))
                 lift = lifts[n][s * rows : (s + 1) * rows, :]
-                for g in range(2):
+                for g in range(wide):
+                    head = 2 * groups[g]
                     parts = [
-                        mixed[:, 256 * g + 64 * e : 256 * g + 64 * e + 64] * lift[:, 2 * g + e : 2 * g + e + 1]
+                        mixed[:, 256 * g + 64 * e : 256 * g + 64 * e + 64] * lift[:, head + e : head + e + 1]
                         for e in range(2)
                     ]
                     values = jnp.concatenate(parts, axis=1)
                     keys = mixed[:, 256 * g + 128 : 256 * g + 256]
                     states[g] = states[g] + product(values, keys)
             fade = jnp.where(low, 1.0, jnp.exp(total[s]))
-            for g in range(2):
+            for g in range(wide):
                 for e in range(2):
+                    head = 2 * groups[g] + e
                     part = slice(64 * e, 64 * e + 64)
                     old = outs[g][run, s, part, :]
-                    outs[g][run, s, part, :] = old * fade[2 * g + e : 2 * g + e + 1, :] + states[g][part, :]
+                    outs[g][run, s, part, :] = old * fade[head : head + 1, :] + states[g][part, :]
                 outs[g][run, s, 128:136, :] = before[s] + total[s]
 
     shape = (3, 2, 136, 128)
     return pl.pallas_call(
         body,
-        out_shape=[jax.ShapeDtypeStruct(shape, F32)] * 2,
-        in_specs=[SMEM] + [VMEM] * (held + 5 + len(given)),
-        out_specs=[VMEM] * 2,
-        scratch_shapes=[pltpu.VMEM((2 * many, rows + 8, 512), F32), pltpu.VMEM((both + 8, depth), BF)],
+        out_shape=[jax.ShapeDtypeStruct(shape, F32)] * wide,
+        in_specs=[SMEM] + [VMEM] * (held + 3 + wide + len(given)),
+        out_specs=[VMEM] * wide,
+        scratch_shapes=[pltpu.VMEM((2 * many, rows + 8, 256 * wide), F32), pltpu.VMEM((both + 8, depth), BF)],
         cost_estimate=pl.CostEstimate(
             flops=32 * sum(x.shape[0] for x in xs) * w[0].size,
             transcendentals=0,
@@ -139,7 +140,7 @@
         ),
         compiler_params=GRANT,
         name="piece_states",
-    )(meta, *xs, w_step, *w, jump, rates, *given)
+    )(meta, *xs, w_step, jump, rates, *w, *given)
 
 
 def joined(w_value, w_key, conv_value, conv_key):
@@ -324,8 +325,8 @@
     ends = lax.ppermute(ends, ("sp", "y", "c"), [(i, i + 1) for i in range(count - 1)])
     a = [x, onward(x)]
     first = jnp.concatenate([x, ends], axis=0)
-    b = [jnp.concatenate([swap(first), ends], axis=0)]
-    b.append(onward(b[0]))
+    b = [swap(first)]
+    b.append(jnp.concatenate([onward(b[0]), onward(ends)], axis=0))
 
     w_own = joined(w_value, w_key, conv_value, conv_key)
     w_both = w_own, swap(w_own)
@@ -340,8 +341,10 @@
     jump = jump[:, :, : tp_count * rows].reshape(2, 8, tp_count, rows).transpose(2, 1, 0, 3)
     jump = jump.reshape(tp_count, 8, 2 * rows)
 
-    def add(runs, xs, halo, far, end):
-        return piece_states(meta, xs, halo, far, end, w_steps, w_both, jump, rates, runs, rows, y_count)
+    def add(runs, xs, halo, far, end, groups=(0, 1)):
+        w = [w_both[g] for g in groups]
+        runs = runs and [runs[g] for g in groups]
+        return piece_states(meta, xs, halo, far, end, w_steps, w, jump, rates, runs, groups, rows, y_count)
 
     runs = add(None, [first], None, 0, False)
     for s in range(1, half):
@@ -353,8 +356,10 @@
     fixed, query = terms(step_bias, decay_rate, new_step, new_value, new_key, new_query, new_gate, read_gain)
     runs, fixed, query = lax.optimization_barrier((runs, fixed, query))
     last = onward(b[half - 1][2 * rows + 8 :])
-    own, other = add(runs, [a[half]], last, half, True)
-    sent = packed(meta, own, swap(other), query, sp_count, y_count)
+    (other,) = add(runs, [a[half]], last, half, True, (1,))
+    other = swap(other)
+    (own,) = add(runs, [a[half]], last, half, True, (0,))
+    sent = packed(meta, own, other, query, sp_count, y_count)
     got = lax.all_to_all(sent, "sp", 0, 0, tiled=True)
     return tuple(finished(meta, got, fixed))
 

time: 115 us -> 116 us (level)
  waiting for transfers between devices: 18.2 us -> 14 us
  starting transfers between devices: 44.5 us -> 47.2 us
  Pallas kernels: 22.1 us -> 24.1 us
  local copies, waits for them, and re-layouts: 2.24 us -> 3.44 us
    ppermute x8 -> x9, waiting for transfers between devices: 12.6 us -> 9.78 us  [onward(): return lax.ppermute(v, ('y', 'c'), pairs)]
    ppermute x8 -> x9, starting transfers between devices: 29.6 us -> 31.8 us  [onward(): return lax.ppermute(v, ('y', 'c'), pairs)]
    pallas_call x5 -> x6, Pallas kernels: 18.8 us -> 20.8 us  [piece_states(): pl.pallas_call(body, out_shape=[jax.ShapeDtypeStruct(shape, F32)] * wide,...]
    ppermute x4, waiting for transfers between devices: 1.37 us -> 0.01 us  [swap(): return lax.ppermute(v, 'c', [(0, 1), (1, 0)])]
    unnamed x26 -> x27, local copies, waits for them, and re-layouts: 0.07 us -> 1.27 us
  transfers between devices with their start and end apart: 13 -> 14, of which waited for: 9 -> 8; matrix products, arithmetic and copies ran while one was open for 3% -> 3% of each run, Pallas kernels for 14% -> 16%
where the time goes in v9:
time: 116 us; the launch traced here: 115 us
  starting transfers between devices  47.2 us (41%)
  Pallas kernels  24.1 us (21%)
  blocking collectives  23 us (20%)
  waiting for transfers between devices  14 us (12%)
  local copies, waits for them, and re-layouts  3.44 us (3%)
  other arithmetic  2.12 us (2%)
    ppermute x9, starting transfers between devices, onward(): return lax.ppermute(v, ('y', 'c'), pairs)  31.8 us
    all_to_all x1, blocking collectives, per_device(): got = lax.all_to_all(sent, 'sp', 0, 0, tiled=True)  23 us
    pallas_call x6, Pallas kernels, piece_states(): pl.pallas_call(body, out_shape=[jax.ShapeDtypeStruct(shape, F32)] * wide,...  20.8 us
    ppermute x4, starting transfers between devices, swap(): return lax.ppermute(v, 'c', [(0, 1), (1, 0)])  10.9 us
    ppermute x9, waiting for transfers between devices, onward(): return lax.ppermute(v, ('y', 'c'), pairs)  9.78 us
    ppermute x1, starting transfers between devices, per_device(): lax.ppermute(ends, ('sp', 'y', 'c'), [(i, i + 1) for i in range(count - 1)])  4.58 us
    ppermute x1, waiting for transfers between devices, per_device(): lax.ppermute(ends, ('sp', 'y', 'c'), [(i, i + 1) for i in range(count - 1)])  4.22 us
  transfers between devices with their start and end apart: 14, of which 8 were waited for; matrix products, arithmetic and copies ran while one was open for 3% of the time, Pallas kernels for 16%

profile of v9, /device:TPU:1, one launch (start us, length us, event | category | flops | bytes accessed | tf_op | source)
XLA Modules:
  0.0 115.0 jit_solution(11894480417291456295)
XLA Ops:
  0.7 0.9 slice.20
  1.7 4.6 %collective-permute-start.4 = (bf16[8,2048]{1,0:T(8,128)(2,1)S(1)}, bf16[8,2048]{1,0:T(8,128)(2,1)S(1)}, u32[]{:S(2)}, u32[]{:S(2)}) collective-permute-start(bf16[8,2048]{1,0:T(8,128)(2,1)S(1)} %reshape.21), channel_id=1, source_target_pairs={{0,1},{1,2},{2,3},{3,4},{4,5},{5,6},{6,7},{7,8},{8,9},{9,10},{10,1... | collective-permute-start | bytes 98312 | tf_op jit(solution)/shard_map/ppermute | solution.py:325
  6.3 4.2 %collective-permute-done.4 = bf16[8,2048]{1,0:T(8,128)(2,1)S(1)} collective-permute-done((bf16[8,2048]{1,0:T(8,128)(2,1)S(1)}, bf16[8,2048]{1,0:T(8,128)(2,1)S(1)}, u32[]{:S(2)}, u32[]{:S(2)}) %collective-permute-start.4) | collective-permute-done | bytes 32800 | tf_op jit(solution)/shard_map/ppermute | solution.py:325
  10.5 1.2 %pad_maximum_fusion.refs_0_ = bf16[200,2048]{1,0:T(8,128)(2,1)S(1)} fusion(bf16[8,2048]{1,0:T(8,128)(2,1)S(1)} %collective-permute-done.4, bf16[192,2048]{1,0:T(8,128)(2,1)} %bitcast.16), kind=kLoop, calls=%fused_computation | loop fusion | flops 1638400 | bytes 1638400 | tf_op jit(solution)/shard_map/concatenate | solution.py:327
  11.7 2.1 %collective-permute-start.5 = (bf16[200,2048]{1,0:T(8,128)(2,1)S(1)}, bf16[200,2048]{1,0:T(8,128)(2,1)}, u32[]{:S(2)}, u32[]{:S(2)}) collective-permute-start(bf16[200,2048]{1,0:T(8,128)(2,1)S(1)} %pad_maximum_fusion.refs_0_), channel_id=1, source_target_pairs={{0,1},{1,0},{2,3},{3,2},{4,5},{5,4},{6,7},{7,6},{8,9},{9,8},{10,11... | collective-permute-start | bytes 2457608 | tf_op jit(solution)/shard_map/ppermute | solution.py:312
  13.8 2.8 %collective-permute-start = (bf16[192,2048]{1,0:T(8,128)(2,1)}, bf16[192,2048]{1,0:T(8,128)(2,1)}, u32[]{:S(2)}, u32[]{:S(2)}) collective-permute-start(bf16[192,2048]{1,0:T(8,128)(2,1)} %bitcast.17), channel_id=1, source_target_pairs={{0,2},{1,15},{2,4},{3,1},{4,6},{5,3},{6,8},{7,5},{8,10},{9,7},{10,... | collective-permute-start | bytes 2359304 | tf_op jit(solution)/shard_map/ppermute | solution.py:319
  16.7 3.0 %collective-permute-start.6 = (bf16[200,2048]{1,0:T(8,128)(2,1)}, bf16[200,2048]{1,0:T(8,128)(2,1)}, u32[]{:S(2)}, u32[]{:S(2)}) collective-permute-start(bf16[200,2048]{1,0:T(8,128)(2,1)} %collective-permute-done.5), channel_id=1, source_target_pairs={{0,2},{1,15},{2,4},{3,1},{4,6},{5,3},{6,8},{7,5},{8,10},{9,7},{10,... | collective-permute-start | bytes 2457608 | tf_op jit(solution)/shard_map/ppermute | solution.py:319
  19.6 0.1 broadcast_in_dim.2
  19.7 1.9 %collective-permute-start.11 = (f32[2,2,1664]{2,1,0:T(2,128)S(1)}, f32[2,2,1664]{2,1,0:T(2,128)S(1)}, u32[]{:S(2)}, u32[]{:S(2)}) collective-permute-start(f32[2,2,1664]{2,1,0:T(2,128)S(1)} %pad_maximum_fusion.1), channel_id=1, source_target_pairs={{0,1},{1,0},{2,3},{3,2},{4,5},{5,4},{6,7},{7,6},{8,9},{9,8},{10,11... | collective-permute-start | bytes 79880 | tf_op jit(solution)/shard_map/ppermute | solution.py:312
  21.7 0.2 joined.1.refs_4_.refs_5_
  21.9 0.0 copy-start.6
  21.9 0.0 copy-start.7
  21.9 0.0 copy-start.8
  21.9 0.0 copy-start.9
  21.9 0.0 copy-start.10
  22.0 2.5 %collective-permute-start.12 = (bf16[2052,256]{1,0:T(8,128)(2,1)S(1)}, bf16[2052,256]{1,0:T(8,128)(2,1)}, u32[]{:S(2)}, u32[]{:S(2)}) collective-permute-start(bf16[2052,256]{1,0:T(8,128)(2,1)S(1)} %joined.1.refs_4_.refs_5_), channel_id=1, source_target_pairs={{0,1},{1,0},{2,3},{3,2},{4,5},{5,4},{6,7},{7,6},{8,9},{9,8},{10,11... | collective-permute-start | bytes 3151880 | tf_op jit(solution)/shard_map/ppermute | solution.py:312
  24.5 0.8 dynamic-slice_bitcast_fusion
  25.3 3.0 %collective-permute-start.7 = (bf16[8,2048]{1,0:T(8,128)(2,1)S(1)}, bf16[8,2048]{1,0:T(8,128)(2,1)S(1)}, u32[]{:S(2)}, u32[]{:S(2)}) collective-permute-start(bf16[8,2048]{1,0:T(8,128)(2,1)S(1)} %collective-permute-done.4), channel_id=1, source_target_pairs={{0,2},{1,15},{2,4},{3,1},{4,6},{5,3},{6,8},{7,5},{8,10},{9,7},{10,... | collective-permute-start | bytes 98312 | tf_op jit(solution)/shard_map/ppermute | solution.py:319
  28.3 4.2 %collective-permute-start.1 = (bf16[192,2048]{1,0:T(8,128)(2,1)}, bf16[192,2048]{1,0:T(8,128)(2,1)}, u32[]{:S(2)}, u32[]{:S(2)}) collective-permute-start(bf16[192,2048]{1,0:T(8,128)(2,1)} %collective-permute-done.refs_0_), channel_id=1, source_target_pairs={{0,2},{1,15},{2,4},{3,1},{4,6},{5,3},{6,8},{7,5},{8,10},{9,7},{10,... | collective-permute-start | bytes 2359304 | tf_op jit(solution)/shard_map/ppermute | solution.py:319
  32.5 3.4 %collective-permute-done.6 = bf16[200,2048]{1,0:T(8,128)(2,1)} collective-permute-done((bf16[200,2048]{1,0:T(8,128)(2,1)}, bf16[200,2048]{1,0:T(8,128)(2,1)}, u32[]{:S(2)}, u32[]{:S(2)}) %collective-permute-start.6) | collective-permute-done | bytes 819232 | tf_op jit(solution)/shard_map/ppermute | solution.py:319
  35.9 1.2 %constant_dynamic-update-slice_fusion.1 = bf16[208,2048]{1,0:T(8,128)(2,1)S(1)} fusion(bf16[200,2048]{1,0:T(8,128)(2,1)} %collective-permute-done.6), kind=kLoop, calls=%fused_computation.8 | loop fusion | bytes 1638400
  37.1 3.8 %collective-permute-start.8 = (bf16[208,2048]{1,0:T(8,128)(2,1)S(1)}, bf16[208,2048]{1,0:T(8,128)(2,1)}, u32[]{:S(2)}, u32[]{:S(2)}) collective-permute-start(bf16[208,2048]{1,0:T(8,128)(2,1)S(1)} %constant_dynamic-update-slice_fusion.refs_1_), channel_id=1, source_target_pairs={{0,2},{1,15},{2,4},{3,1},{4,6},{5,3},{6,8},{7,5},{8,10},{9,7},{10,... | collective-permute-start | bytes 2555912 | tf_op jit(solution)/shard_map/ppermute | solution.py:319
  40.9 0.8 maximum_select_fusion
  41.7 0.1 pad_add_fusion.m_ref
  41.8 0.6 terms.1
  42.5 0.1 reshape.22
  42.6 0.1 copy.17
  42.8 0.1 reshape.23.refs_2_.refs_3_
  42.9 1.8 %collective-permute-done.1.refs_0_ = bf16[192,2048]{1,0:T(8,128)(2,1)} collective-permute-done((bf16[192,2048]{1,0:T(8,128)(2,1)}, bf16[192,2048]{1,0:T(8,128)(2,1)}, u32[]{:S(2)}, u32[]{:S(2)}) %collective-permute-start.1) | collective-permute-done | bytes 786464 | tf_op jit(solution)/shard_map/ppermute | solution.py:319
  44.7 3.8 %collective-permute-start.2 = (bf16[192,2048]{1,0:T(8,128)(2,1)}, bf16[192,2048]{1,0:T(8,128)(2,1)S(1)}, u32[]{:S(2)}, u32[]{:S(2)}) collective-permute-start(bf16[192,2048]{1,0:T(8,128)(2,1)} %collective-permute-done.1.refs_0_), channel_id=1, source_target_pairs={{0,2},{1,15},{2,4},{3,1},{4,6},{5,3},{6,8},{7,5},{8,10},{9,7},{10,... | collective-permute-start | bytes 2359304 | tf_op jit(solution)/shard_map/ppermute | solution.py:319
  48.4 3.2 %piece_states.6 = (f32[3,2,136,128]{3,2,1,0:T(8,128)S(1)}, f32[3,2,136,128]{3,2,1,0:T(8,128)S(1)}) custom-call(s32[3]{0:T(128)S(1)} %pad_add_fusion.m_ref, bf16[200,2048]{1,0:T(8,128)(2,1)S(1)} %pad_maximum_fusion.refs_0_, bf16[8,2048]{1,0:T(8,128)(2,1)S(1)} %pad.8.refs_1_.refs_2_, f32[16,8,192]{2,1,0:T(8,128)S(1)} %reshape.23.refs_2_.refs_3_, ...), custom_call_target="tpu_custom_call" | custom-call | flops 3361996800 | bytes 2101248 | tf_op jit(solution)/shard_map/piece_states/pallas_call | solution.py:130
  51.7 2.1 %collective-permute-done.8.refs_1_ = bf16[208,2048]{1,0:T(8,128)(2,1)} collective-permute-done((bf16[208,2048]{1,0:T(8,128)(2,1)S(1)}, bf16[208,2048]{1,0:T(8,128)(2,1)}, u32[]{:S(2)}, u32[]{:S(2)}) %collective-permute-start.8) | collective-permute-done | bytes 852000 | tf_op jit(solution)/shard_map/ppermute | solution.py:319
  53.8 3.8 %collective-permute-start.9 = (bf16[208,2048]{1,0:T(8,128)(2,1)}, bf16[208,2048]{1,0:T(8,128)(2,1)S(1)}, u32[]{:S(2)}, u32[]{:S(2)}) collective-permute-start(bf16[208,2048]{1,0:T(8,128)(2,1)} %collective-permute-done.8.refs_1_), channel_id=1, source_target_pairs={{0,2},{1,15},{2,4},{3,1},{4,6},{5,3},{6,8},{7,5},{8,10},{9,7},{10,... | collective-permute-start | bytes 2555912 | tf_op jit(solution)/shard_map/ppermute | solution.py:319
  57.5 4.1 %piece_states.7 = (f32[3,2,136,128]{3,2,1,0:T(8,128)S(1)}, f32[3,2,136,128]{3,2,1,0:T(8,128)S(1)}) custom-call(s32[3]{0:T(128)S(1)} %pad_add_fusion.m_ref, bf16[192,2048]{1,0:T(8,128)(2,1)} %collective-permute-done.refs_0_, bf16[208,2048]{1,0:T(8,128)(2,1)S(1)} %constant_dynamic-update-slice_fusion.refs_1_, bf16[8,2048]{1,0:T(8,128)(2,1)S(1)} %pad.8.refs_1_.refs_2_, ...), custom_call_target="tpu_custom_call" | custom-call | flops 6723993600 | bytes 2101248 | tf_op jit(solution)/shard_map/piece_states/pallas_call | solution.py:130
  61.7 0.4 collective-permute-done.2.refs_0_
  62.1 3.8 %collective-permute-start.3 = (bf16[192,2048]{1,0:T(8,128)(2,1)S(1)}, bf16[192,2048]{1,0:T(8,128)(2,1)S(1)}, u32[]{:S(2)}, u32[]{:S(2)}) collective-permute-start(bf16[192,2048]{1,0:T(8,128)(2,1)S(1)} %collective-permute-done.2.refs_0_), channel_id=1, source_target_pairs={{0,2},{1,15},{2,4},{3,1},{4,6},{5,3},{6,8},{7,5},{8,10},{9,7},{10,... | collective-permute-start | bytes 2359304 | tf_op jit(solution)/shard_map/ppermute | solution.py:319
  65.9 4.4 %piece_states.8 = (f32[3,2,136,128]{3,2,1,0:T(8,128)S(1)}, f32[3,2,136,128]{3,2,1,0:T(8,128)S(1)}) custom-call(s32[3]{0:T(128)S(1)} %pad_add_fusion.m_ref, bf16[192,2048]{1,0:T(8,128)(2,1)} %collective-permute-done.1.refs_0_, bf16[208,2048]{1,0:T(8,128)(2,1)} %collective-permute-done.8.refs_1_, bf16[8,2048]{1,0:T(8,128)(2,1)S(1)} %pad.8.refs_1_.refs_2_, ...), custom_call_target="tpu_custom_call" | custom-call | flops 6723993600 | bytes 2101248 | tf_op jit(solution)/shard_map/piece_states/pallas_call | solution.py:130
  70.2 1.0 collective-permute-done.9.refs_1_
  71.2 3.8 %collective-permute-start.10 = (bf16[8,2048]{1,0:T(8,128)(2,1)S(1)}, bf16[8,2048]{1,0:T(8,128)(2,1)S(1)}, u32[]{:S(2)}, u32[]{:S(2)}) collective-permute-start(bf16[8,2048]{1,0:T(8,128)(2,1)S(1)} %slice.26), channel_id=1, source_target_pairs={{0,2},{1,15},{2,4},{3,1},{4,6},{5,3},{6,8},{7,5},{8,10},{9,7},{10,... | collective-permute-start | bytes 98312 | tf_op jit(solution)/shard_map/ppermute | solution.py:319
  75.0 3.9 %piece_states.9 = (f32[3,2,136,128]{3,2,1,0:T(8,128)S(1)}, f32[3,2,136,128]{3,2,1,0:T(8,128)S(1)}) custom-call(s32[3]{0:T(128)S(1)} %pad_add_fusion.m_ref, bf16[192,2048]{1,0:T(8,128)(2,1)S(1)} %collective-permute-done.2.refs_0_, bf16[208,2048]{1,0:T(8,128)(2,1)S(1)} %collective-permute-done.9.refs_1_, bf16[8,2048]{1,0:T(8,128)(2,1)S(1)} %pad.8.refs_1_.refs_2_, ...), custom_call_target="tpu_custom_call" | custom-call | flops 6723993600 | bytes 2101248 | tf_op jit(solution)/shard_map/piece_states/pallas_call | solution.py:130
  78.9 0.7 collective-permute-done.3.refs_0_
  79.7 0.4 collective-permute-done.10.refs_1_
  80.0 2.9 %piece_states.11 = f32[3,2,136,128]{3,2,1,0:T(8,128)S(1)} custom-call(s32[3]{0:T(128)S(1)} %pad_add_fusion.m_ref, bf16[192,2048]{1,0:T(8,128)(2,1)S(1)} %collective-permute-done.3.refs_0_, bf16[8,2048]{1,0:T(8,128)(2,1)S(1)} %collective-permute-done.10.refs_1_, bf16[8,2048]{1,0:T(8,128)(2,1)S(1)} %pad.8.refs_1_.refs_2_, ...), custom_call_target="tpu_custom_call" | custom-call | flops 3361996800 | bytes 2101248 | tf_op jit(solution)/shard_map/piece_states/pallas_call | solution.py:130
  82.9 4.3 %collective-permute-start.13 = (f32[3,2,136,128]{3,2,1,0:T(8,128)S(1)}, f32[3,2,136,128]{3,2,1,0:T(8,128)S(1)}, u32[]{:S(2)}, u32[]{:S(2)}) collective-permute-start(f32[3,2,136,128]{3,2,1,0:T(8,128)S(1)} %piece_states.11), channel_id=1, source_target_pairs={{0,1},{1,0},{2,3},{3,2},{4,5},{5,4},{6,7},{7,6},{8,9},{9,8},{10,11... | collective-permute-start | bytes 1253384 | tf_op jit(solution)/shard_map/ppermute | solution.py:312
  87.3 2.2 %piece_states.10.a_ref = f32[3,2,136,128]{3,2,1,0:T(8,128)S(1)} custom-call(s32[3]{0:T(128)S(1)} %pad_add_fusion.m_ref, bf16[192,2048]{1,0:T(8,128)(2,1)S(1)} %collective-permute-done.3.refs_0_, bf16[8,2048]{1,0:T(8,128)(2,1)S(1)} %collective-permute-done.10.refs_1_, bf16[8,2048]{1,0:T(8,128)(2,1)S(1)} %pad.8.refs_1_.refs_2_, ...), custom_call_target="tpu_custom_call" | custom-call | flops 3361996800 | bytes 2101248 | tf_op jit(solution)/shard_map/piece_states/pallas_call | solution.py:130
  89.5 0.8 packed.1
  90.4 23.0 %all_to_all.5.got_ref = bf16[32,16,128]{2,1,0:T(8,128)(2,1)S(1)} all-to-all(bf16[32,16,128]{2,1,0:T(8,128)(2,1)S(1)} %packed.1), channel_id=1, replica_groups=mesh['sp'=32,'y'=8,'c'=2] {'sp'}, dimensions={0} | all-to-all | bytes 262144 | tf_op jit(solution)/shard_map/all_to_all | solution.py:363
  113.3 1.6 %finished.1 = (bf16[2,2,2,128]{3,2,1,0:T(2,128)(2,1)}, bf16[2,2,2]{2,1,0:T(2,128)(2,1)}) custom-call(s32[3]{0:T(128)S(1)} %pad_add_fusion.m_ref, bf16[32,16,128]{2,1,0:T(8,128)(2,1)S(1)} %all_to_all.5.got_ref, f32[8,128]{1,0:T(8,128)S(1)} %get-tuple-element.29.fix_ref), custom_call_target="tpu_custom_call" | custom-call | tf_op jit(solution)/shard_map/finished/pallas_call | solution.py:288
  (37 shorter events, 0.2 us)
Async XLA Ops:
  0.6 16.0 %copy-start.3 = (f32[2]{0:T(128)S(1)}, f32[2]{0:T(128)}, u32[]{:S(2)}) copy-start(f32[2]{0:T(128)} %b_ref.1) | copy-start | bytes 28
  0.6 16.0 %copy-start.2 = (f32[2]{0:T(128)S(1)}, f32[2]{0:T(128)}, u32[]{:S(2)}) copy-start(f32[2]{0:T(128)} %r_ref.1) | copy-start | bytes 28
  0.7 19.1 %copy-start.12 = (f32[2,1536,2]{1,2,0:T(2,128)S(1)}, f32[2,1536,2]{1,2,0:T(2,128)}, u32[]{:S(2)}) copy-start(f32[2,1536,2]{1,2,0:T(2,128)} %param.23) | copy-start | bytes 73732
  0.7 21.0 %copy-start = (bf16[2048,128]{1,0:T(8,128)(2,1)S(1)}, bf16[2048,128]{1,0:T(8,128)(2,1)}, u32[]{:S(2)}) copy-start(bf16[2048,128]{1,0:T(8,128)(2,1)} %v_ref.2) | copy-start | bytes 1572868
  0.7 21.0 %copy-start.1 = (bf16[2048,128]{1,0:T(8,128)(2,1)S(1)}, bf16[2048,128]{1,0:T(8,128)(2,1)}, u32[]{:S(2)}) copy-start(bf16[2048,128]{1,0:T(8,128)(2,1)} %k_ref.2) | copy-start | bytes 1572868
  0.7 21.0 %copy-start.4 = (bf16[4,128]{1,0:T(4,128)(2,1)S(1)}, bf16[4,128]{1,0:T(4,128)(2,1)}, u32[]{:S(2)}) copy-start(bf16[4,128]{1,0:T(4,128)(2,1)} %cv_ref.1) | copy-start | bytes 3076
  0.7 21.0 %copy-start.5 = (bf16[4,128]{1,0:T(4,128)(2,1)S(1)}, bf16[4,128]{1,0:T(4,128)(2,1)}, u32[]{:S(2)}) copy-start(bf16[4,128]{1,0:T(4,128)(2,1)} %ck_ref.1) | copy-start | bytes 3076
  1.7 8.8 %collective-permute-start.4 = (bf16[8,2048]{1,0:T(8,128)(2,1)S(1)}, bf16[8,2048]{1,0:T(8,128)(2,1)S(1)}, u32[]{:S(2)}, u32[]{:S(2)}) collective-permute-start(bf16[8,2048]{1,0:T(8,128)(2,1)S(1)} %reshape.21), channel_id=1, source_target_pairs={{0,1},{1,2},{2,3},{3,4},{4,5},{5,6},{6,7},{7,8},{8,9},{9,10},{10,1... | collective-permute-start | bytes 98312 | tf_op jit(solution)/shard_map/ppermute | solution.py:325
  11.7 5.0 %collective-permute-start.5 = (bf16[200,2048]{1,0:T(8,128)(2,1)S(1)}, bf16[200,2048]{1,0:T(8,128)(2,1)}, u32[]{:S(2)}, u32[]{:S(2)}) collective-permute-start(bf16[200,2048]{1,0:T(8,128)(2,1)S(1)} %pad_maximum_fusion.refs_0_), channel_id=1, source_target_pairs={{0,1},{1,0},{2,3},{3,2},{4,5},{5,4},{6,7},{7,6},{8,9},{9,8},{10,11... | collective-permute-start | bytes 2457608 | tf_op jit(solution)/shard_map/ppermute | solution.py:312
  13.8 14.6 %collective-permute-start = (bf16[192,2048]{1,0:T(8,128)(2,1)}, bf16[192,2048]{1,0:T(8,128)(2,1)}, u32[]{:S(2)}, u32[]{:S(2)}) collective-permute-start(bf16[192,2048]{1,0:T(8,128)(2,1)} %bitcast.17), channel_id=1, source_target_pairs={{0,2},{1,15},{2,4},{3,1},{4,6},{5,3},{6,8},{7,5},{8,10},{9,7},{10,... | collective-permute-start | bytes 2359304 | tf_op jit(solution)/shard_map/ppermute | solution.py:319
  16.7 19.2 %collective-permute-start.6 = (bf16[200,2048]{1,0:T(8,128)(2,1)}, bf16[200,2048]{1,0:T(8,128)(2,1)}, u32[]{:S(2)}, u32[]{:S(2)}) collective-permute-start(bf16[200,2048]{1,0:T(8,128)(2,1)} %collective-permute-done.5), channel_id=1, source_target_pairs={{0,2},{1,15},{2,4},{3,1},{4,6},{5,3},{6,8},{7,5},{8,10},{9,7},{10,... | collective-permute-start | bytes 2457608 | tf_op jit(solution)/shard_map/ppermute | solution.py:319
  19.7 22.7 %collective-permute-start.11 = (f32[2,2,1664]{2,1,0:T(2,128)S(1)}, f32[2,2,1664]{2,1,0:T(2,128)S(1)}, u32[]{:S(2)}, u32[]{:S(2)}) collective-permute-start(f32[2,2,1664]{2,1,0:T(2,128)S(1)} %pad_maximum_fusion.1), channel_id=1, source_target_pairs={{0,1},{1,0},{2,3},{3,2},{4,5},{5,4},{6,7},{7,6},{8,9},{9,8},{10,11... | collective-permute-start | bytes 79880 | tf_op jit(solution)/shard_map/ppermute | solution.py:312
  21.9 19.9 %copy-start.6 = (f32[2,2]{1,0:T(2,128)S(1)}, f32[2,2]{1,0:T(2,128)}, u32[]{:S(2)}) copy-start(f32[2,2]{1,0:T(2,128)} %n_ref.1) | copy-start | bytes 52
  21.9 19.9 %copy-start.7 = (bf16[2,128]{1,0:T(2,128)(2,1)S(1)}, bf16[2,128]{1,0:T(2,128)(2,1)}, u32[]{:S(2)}) copy-start(bf16[2,128]{1,0:T(2,128)(2,1)} %v_ref.3) | copy-start | bytes 1540
  21.9 19.9 %copy-start.8 = (bf16[2,128]{1,0:T(2,128)(2,1)S(1)}, bf16[2,128]{1,0:T(2,128)(2,1)}, u32[]{:S(2)}) copy-start(bf16[2,128]{1,0:T(2,128)(2,1)} %k_ref.3) | copy-start | bytes 1540
  21.9 19.9 %copy-start.9 = (bf16[2,128]{1,0:T(2,128)(2,1)S(1)}, bf16[2,128]{1,0:T(2,128)(2,1)}, u32[]{:S(2)}) copy-start(bf16[2,128]{1,0:T(2,128)(2,1)} %q_ref.1) | copy-start | bytes 1540
  21.9 19.9 %copy-start.10 = (bf16[2,128]{1,0:T(2,128)(2,1)S(1)}, bf16[2,128]{1,0:T(2,128)(2,1)}, u32[]{:S(2)}) copy-start(bf16[2,128]{1,0:T(2,128)(2,1)} %g_ref.1) | copy-start | bytes 1540
  22.0 19.9 %copy-start.11 = (bf16[128]{0:T(256)(128)(2,1)S(1)}, bf16[128]{0:T(256)(128)(2,1)}, u32[]{:S(2)}) copy-start(bf16[128]{0:T(256)(128)(2,1)} %param.29) | copy-start | bytes 772
  22.0 26.4 %collective-permute-start.12 = (bf16[2052,256]{1,0:T(8,128)(2,1)S(1)}, bf16[2052,256]{1,0:T(8,128)(2,1)}, u32[]{:S(2)}, u32[]{:S(2)}) collective-permute-start(bf16[2052,256]{1,0:T(8,128)(2,1)S(1)} %joined.1.refs_4_.refs_5_), channel_id=1, source_target_pairs={{0,1},{1,0},{2,3},{3,2},{4,5},{5,4},{6,7},{7,6},{8,9},{9,8},{10,11... | collective-permute-start | bytes 3151880 | tf_op jit(solution)/shard_map/ppermute | solution.py:312
  25.3 11.7 %collective-permute-start.7 = (bf16[8,2048]{1,0:T(8,128)(2,1)S(1)}, bf16[8,2048]{1,0:T(8,128)(2,1)S(1)}, u32[]{:S(2)}, u32[]{:S(2)}) collective-permute-start(bf16[8,2048]{1,0:T(8,128)(2,1)S(1)} %collective-permute-done.4), channel_id=1, source_target_pairs={{0,2},{1,15},{2,4},{3,1},{4,6},{5,3},{6,8},{7,5},{8,10},{9,7},{10,... | collective-permute-start | bytes 98312 | tf_op jit(solution)/shard_map/ppermute | solution.py:319
  28.3 16.3 %collective-permute-start.1 = (bf16[192,2048]{1,0:T(8,128)(2,1)}, bf16[192,2048]{1,0:T(8,128)(2,1)}, u32[]{:S(2)}, u32[]{:S(2)}) collective-permute-start(bf16[192,2048]{1,0:T(8,128)(2,1)} %collective-permute-done.refs_0_), channel_id=1, source_target_pairs={{0,2},{1,15},{2,4},{3,1},{4,6},{5,3},{6,8},{7,5},{8,10},{9,7},{10,... | collective-permute-start | bytes 2359304 | tf_op jit(solution)/shard_map/ppermute | solution.py:319
  37.1 16.7 %collective-permute-start.8 = (bf16[208,2048]{1,0:T(8,128)(2,1)S(1)}, bf16[208,2048]{1,0:T(8,128)(2,1)}, u32[]{:S(2)}, u32[]{:S(2)}) collective-permute-start(bf16[208,2048]{1,0:T(8,128)(2,1)S(1)} %constant_dynamic-update-slice_fusion.refs_1_), channel_id=1, source_target_pairs={{0,2},{1,15},{2,4},{3,1},{4,6},{5,3},{6,8},{7,5},{8,10},{9,7},{10,... | collective-permute-start | bytes 2555912 | tf_op jit(solution)/shard_map/ppermute | solution.py:319
  44.7 17.4 %collective-permute-start.2 = (bf16[192,2048]{1,0:T(8,128)(2,1)}, bf16[192,2048]{1,0:T(8,128)(2,1)S(1)}, u32[]{:S(2)}, u32[]{:S(2)}) collective-permute-start(bf16[192,2048]{1,0:T(8,128)(2,1)} %collective-permute-done.1.refs_0_), channel_id=1, source_target_pairs={{0,2},{1,15},{2,4},{3,1},{4,6},{5,3},{6,8},{7,5},{8,10},{9,7},{10,... | collective-permute-start | bytes 2359304 | tf_op jit(solution)/shard_map/ppermute | solution.py:319
  53.8 17.4 %collective-permute-start.9 = (bf16[208,2048]{1,0:T(8,128)(2,1)}, bf16[208,2048]{1,0:T(8,128)(2,1)S(1)}, u32[]{:S(2)}, u32[]{:S(2)}) collective-permute-start(bf16[208,2048]{1,0:T(8,128)(2,1)} %collective-permute-done.8.refs_1_), channel_id=1, source_target_pairs={{0,2},{1,15},{2,4},{3,1},{4,6},{5,3},{6,8},{7,5},{8,10},{9,7},{10,... | collective-permute-start | bytes 2555912 | tf_op jit(solution)/shard_map/ppermute | solution.py:319
  62.1 17.6 %collective-permute-start.3 = (bf16[192,2048]{1,0:T(8,128)(2,1)S(1)}, bf16[192,2048]{1,0:T(8,128)(2,1)S(1)}, u32[]{:S(2)}, u32[]{:S(2)}) collective-permute-start(bf16[192,2048]{1,0:T(8,128)(2,1)S(1)} %collective-permute-done.2.refs_0_), channel_id=1, source_target_pairs={{0,2},{1,15},{2,4},{3,1},{4,6},{5,3},{6,8},{7,5},{8,10},{9,7},{10,... | collective-permute-start | bytes 2359304 | tf_op jit(solution)/shard_map/ppermute | solution.py:319
  71.2 8.8 %collective-permute-start.10 = (bf16[8,2048]{1,0:T(8,128)(2,1)S(1)}, bf16[8,2048]{1,0:T(8,128)(2,1)S(1)}, u32[]{:S(2)}, u32[]{:S(2)}) collective-permute-start(bf16[8,2048]{1,0:T(8,128)(2,1)S(1)} %slice.26), channel_id=1, source_target_pairs={{0,2},{1,15},{2,4},{3,1},{4,6},{5,3},{6,8},{7,5},{8,10},{9,7},{10,... | collective-permute-start | bytes 98312 | tf_op jit(solution)/shard_map/ppermute | solution.py:319
  82.9 6.6 %collective-permute-start.13 = (f32[3,2,136,128]{3,2,1,0:T(8,128)S(1)}, f32[3,2,136,128]{3,2,1,0:T(8,128)S(1)}, u32[]{:S(2)}, u32[]{:S(2)}) collective-permute-start(f32[3,2,136,128]{3,2,1,0:T(8,128)S(1)} %piece_states.11), channel_id=1, source_target_pairs={{0,1},{1,0},{2,3},{3,2},{4,5},{5,4},{6,7},{7,6},{8,9},{9,8},{10,11... | collective-permute-start | bytes 1253384 | tf_op jit(solution)/shard_map/ppermute | solution.py:312

commit v10 on v8

--- a/solution.py
+++ b/solution.py
@@ -159,6 +159,25 @@
         compiler_params=GRANT,
         name="joined",
     )(w_value, w_key, conv_value, conv_key)
+
+
+def stacked(*parts):
+    counts = [v.shape[0] for v in parts]
+
+    def body(*refs):
+        start = 0
+        for ref, count in zip(refs[:-1], counts):
+            refs[-1][start : start + count, :] = ref[...]
+            start += count
+
+    return pl.pallas_call(
+        body,
+        out_shape=jax.ShapeDtypeStruct((sum(counts), parts[0].shape[1]), parts[0].dtype),
+        in_specs=[VMEM] * len(parts),
+        out_specs=VMEM,
+        compiler_params=GRANT,
+        name="stacked",
+    )(*parts)
 
 
 def terms(step_bias, decay_rate, new_step, new_value, new_key, new_query, new_gate, read_gain):
@@ -324,11 +343,11 @@
     ends = lax.ppermute(ends, ("sp", "y", "c"), [(i, i + 1) for i in range(count - 1)])
     a = [x, onward(x)]
     first = jnp.concatenate([x, ends], axis=0)
-    b = [jnp.concatenate([swap(first), ends], axis=0)]
+    b = [stacked(swap(first), ends)]
     b.append(onward(b[0]))
 
     w_own = joined(w_value, w_key, conv_value, conv_key)
-    w_both = w_own, swap(w_own)
+    w_both = w_own, stacked(swap(w_own))
     pair = lax.dynamic_slice_in_dim(w_step.T, y * 2 * heads, 2 * heads, 0)
     pair = jnp.where(c == 0, pair, jnp.roll(pair, heads, axis=0))
     w_steps = jnp.pad(pair, ((0, 8 - 2 * heads), (0, 0)))

time: 115 us -> 114 us (level)
  waiting for transfers between devices: 18.2 us -> 20.7 us
  Pallas kernels: 22.1 us -> 19.7 us
    pallas_call x5, Pallas kernels: 18.8 us -> 16.3 us  [piece_states(): pl.pallas_call(body, out_shape=[jax.ShapeDtypeStruct(shape, F32)] * 2, in...]
    ppermute x8, waiting for transfers between devices: 12.6 us -> 15.1 us  [onward(): return lax.ppermute(v, ('y', 'c'), pairs)]
  transfers between devices with their start and end apart: 13 -> 13, of which waited for: 9 -> 10; matrix products, arithmetic and copies ran while one was open for 3% -> 2% of each run, Pallas kernels for 14% -> 13%
where the time goes in v10:
time: 114 us; the launch traced here: 113 us
  starting transfers between devices  44.9 us (39%)
  blocking collectives  22.4 us (20%)
  waiting for transfers between devices  20.7 us (18%)
  Pallas kernels  19.7 us (17%)
  local copies, waits for them, and re-layouts  2.25 us (2%)
  other arithmetic  2.12 us (2%)
  between operations  1.15 us (1%)
    ppermute x8, starting transfers between devices, onward(): return lax.ppermute(v, ('y', 'c'), pairs)  29.8 us
    all_to_all x1, blocking collectives, per_device(): got = lax.all_to_all(sent, 'sp', 0, 0, tiled=True)  22.4 us
    pallas_call x5, Pallas kernels, piece_states(): pl.pallas_call(body, out_shape=[jax.ShapeDtypeStruct(shape, F32)] * 2, in...  16.3 us
    ppermute x8, waiting for transfers between devices, onward(): return lax.ppermute(v, ('y', 'c'), pairs)  15.1 us
    ppermute x4, starting transfers between devices, swap(): return lax.ppermute(v, 'c', [(0, 1), (1, 0)])  10.5 us
    ppermute x1, starting transfers between devices, per_device(): lax.ppermute(ends, ('sp', 'y', 'c'), [(i, i + 1) for i in range(count - 1)])  4.58 us
    ppermute x1, waiting for transfers between devices, per_device(): lax.ppermute(ends, ('sp', 'y', 'c'), [(i, i + 1) for i in range(count - 1)])  4.22 us
  transfers between devices with their start and end apart: 13, of which 10 were waited for; matrix products, arithmetic and copies ran while one was open for 2% of the time, Pallas kernels for 13%

profile of v10, /device:TPU:1, one launch (start us, length us, event | category | flops | bytes accessed | tf_op | source)
XLA Modules:
  0.0 113.2 jit_solution(16749474351502112980)
XLA Ops:
  0.7 0.9 slice.20
  1.6 4.6 %collective-permute-start.4 = (bf16[8,2048]{1,0:T(8,128)(2,1)S(1)}, bf16[8,2048]{1,0:T(8,128)(2,1)S(1)}, u32[]{:S(2)}, u32[]{:S(2)}) collective-permute-start(bf16[8,2048]{1,0:T(8,128)(2,1)S(1)} %reshape.21), channel_id=1, source_target_pairs={{0,1},{1,2},{2,3},{3,4},{4,5},{5,6},{6,7},{7,8},{8,9},{9,10},{10,1... | collective-permute-start | bytes 98312 | tf_op jit(solution)/shard_map/ppermute | solution.py:343
  6.2 4.2 %collective-permute-done.4.refs_1_ = bf16[8,2048]{1,0:T(8,128)(2,1)S(1)} collective-permute-done((bf16[8,2048]{1,0:T(8,128)(2,1)S(1)}, bf16[8,2048]{1,0:T(8,128)(2,1)S(1)}, u32[]{:S(2)}, u32[]{:S(2)}) %collective-permute-start.4) | collective-permute-done | bytes 32800 | tf_op jit(solution)/shard_map/ppermute | solution.py:343
  10.5 1.2 %pad_maximum_fusion.refs_0_ = bf16[200,2048]{1,0:T(8,128)(2,1)S(1)} fusion(bf16[8,2048]{1,0:T(8,128)(2,1)S(1)} %collective-permute-done.4.refs_1_, bf16[192,2048]{1,0:T(8,128)(2,1)} %bitcast.16), kind=kLoop, calls=%fused_computation | loop fusion | flops 1638400 | bytes 1638400 | tf_op jit(solution)/shard_map/concatenate | solution.py:345
  11.7 0.0 copy-start.5
  11.7 2.2 %collective-permute-start.5 = (bf16[200,2048]{1,0:T(8,128)(2,1)S(1)}, bf16[200,2048]{1,0:T(8,128)(2,1)S(1)}, u32[]{:S(2)}, u32[]{:S(2)}) collective-permute-start(bf16[200,2048]{1,0:T(8,128)(2,1)S(1)} %pad_maximum_fusion.refs_0_), channel_id=1, source_target_pairs={{0,1},{1,0},{2,3},{3,2},{4,5},{5,4},{6,7},{7,6},{8,9},{9,8},{10,11... | collective-permute-start | bytes 2457608 | tf_op jit(solution)/shard_map/ppermute | solution.py:330
  13.9 2.8 %collective-permute-start = (bf16[192,2048]{1,0:T(8,128)(2,1)}, bf16[192,2048]{1,0:T(8,128)(2,1)}, u32[]{:S(2)}, u32[]{:S(2)}) collective-permute-start(bf16[192,2048]{1,0:T(8,128)(2,1)} %bitcast.17), channel_id=1, source_target_pairs={{0,2},{1,15},{2,4},{3,1},{4,6},{5,3},{6,8},{7,5},{8,10},{9,7},{10,... | collective-permute-start | bytes 2359304 | tf_op jit(solution)/shard_map/ppermute | solution.py:337
  16.8 0.2 joined.1.refs_2_.refs_3_
  17.0 0.0 copy-start.9
  17.0 0.0 copy-start.10
  17.1 0.0 copy-start.13
  17.1 2.1 %collective-permute-start.10 = (bf16[2052,256]{1,0:T(8,128)(2,1)S(1)}, bf16[2052,256]{1,0:T(8,128)(2,1)S(1)}, u32[]{:S(2)}, u32[]{:S(2)}) collective-permute-start(bf16[2052,256]{1,0:T(8,128)(2,1)S(1)} %joined.1.refs_2_.refs_3_), channel_id=1, source_target_pairs={{0,1},{1,0},{2,3},{3,2},{4,5},{5,4},{6,7},{7,6},{8,9},{9,8},{10,11... | collective-permute-start | bytes 3151880 | tf_op jit(solution)/shard_map/ppermute | solution.py:330
  19.2 0.1 stacked.2
  19.2 4.3 %collective-permute-start.6 = (bf16[208,2048]{1,0:T(8,128)(2,1)S(1)}, bf16[208,2048]{1,0:T(8,128)(2,1)}, u32[]{:S(2)}, u32[]{:S(2)}) collective-permute-start(bf16[208,2048]{1,0:T(8,128)(2,1)S(1)} %stacked.2), channel_id=1, source_target_pairs={{0,2},{1,15},{2,4},{3,1},{4,6},{5,3},{6,8},{7,5},{8,10},{9,7},{10,... | collective-permute-start | bytes 2555912 | tf_op jit(solution)/shard_map/ppermute | solution.py:337
  23.5 0.1 broadcast_in_dim.2
  23.6 1.9 %collective-permute-start.11 = (f32[2,2,1664]{2,1,0:T(2,128)S(1)}, f32[2,2,1664]{2,1,0:T(2,128)S(1)}, u32[]{:S(2)}, u32[]{:S(2)}) collective-permute-start(f32[2,2,1664]{2,1,0:T(2,128)S(1)} %pad_maximum_fusion.1), channel_id=1, source_target_pairs={{0,1},{1,0},{2,3},{3,2},{4,5},{5,4},{6,7},{7,6},{8,9},{9,8},{10,11... | collective-permute-start | bytes 79880 | tf_op jit(solution)/shard_map/ppermute | solution.py:330
  25.5 0.8 dynamic-slice_bitcast_fusion
  26.3 0.9 collective-permute-done.refs_0_
  27.2 3.8 %collective-permute-start.1 = (bf16[192,2048]{1,0:T(8,128)(2,1)}, bf16[192,2048]{1,0:T(8,128)(2,1)}, u32[]{:S(2)}, u32[]{:S(2)}) collective-permute-start(bf16[192,2048]{1,0:T(8,128)(2,1)} %collective-permute-done.refs_0_), channel_id=1, source_target_pairs={{0,2},{1,15},{2,4},{3,1},{4,6},{5,3},{6,8},{7,5},{8,10},{9,7},{10,... | collective-permute-start | bytes 2359304 | tf_op jit(solution)/shard_map/ppermute | solution.py:337
  31.0 5.3 %collective-permute-done.6.refs_1_ = bf16[208,2048]{1,0:T(8,128)(2,1)} collective-permute-done((bf16[208,2048]{1,0:T(8,128)(2,1)S(1)}, bf16[208,2048]{1,0:T(8,128)(2,1)}, u32[]{:S(2)}, u32[]{:S(2)}) %collective-permute-start.6) | collective-permute-done | bytes 852000 | tf_op jit(solution)/shard_map/ppermute | solution.py:337
  36.4 3.8 %collective-permute-start.7 = (bf16[208,2048]{1,0:T(8,128)(2,1)}, bf16[208,2048]{1,0:T(8,128)(2,1)}, u32[]{:S(2)}, u32[]{:S(2)}) collective-permute-start(bf16[208,2048]{1,0:T(8,128)(2,1)} %collective-permute-done.6.refs_1_), channel_id=1, source_target_pairs={{0,2},{1,15},{2,4},{3,1},{4,6},{5,3},{6,8},{7,5},{8,10},{9,7},{10,... | collective-permute-start | bytes 2555912 | tf_op jit(solution)/shard_map/ppermute | solution.py:337
  40.1 0.8 maximum_select_fusion
  40.9 0.1 pad_add_fusion.m_ref
  41.1 0.6 terms.1
  41.8 0.1 reshape.22
  41.9 0.1 copy.17
  42.0 0.1 reshape.23.refs_4_.refs_5_
  42.1 0.1 stacked.3.refs_3_.refs_4_
  42.2 2.6 %collective-permute-done.1.refs_0_ = bf16[192,2048]{1,0:T(8,128)(2,1)} collective-permute-done((bf16[192,2048]{1,0:T(8,128)(2,1)}, bf16[192,2048]{1,0:T(8,128)(2,1)}, u32[]{:S(2)}, u32[]{:S(2)}) %collective-permute-start.1) | collective-permute-done | bytes 786464 | tf_op jit(solution)/shard_map/ppermute | solution.py:337
  44.8 3.8 %collective-permute-start.2 = (bf16[192,2048]{1,0:T(8,128)(2,1)}, bf16[192,2048]{1,0:T(8,128)(2,1)S(1)}, u32[]{:S(2)}, u32[]{:S(2)}) collective-permute-start(bf16[192,2048]{1,0:T(8,128)(2,1)} %collective-permute-done.1.refs_0_), channel_id=1, source_target_pairs={{0,2},{1,15},{2,4},{3,1},{4,6},{5,3},{6,8},{7,5},{8,10},{9,7},{10,... | collective-permute-start | bytes 2359304 | tf_op jit(solution)/shard_map/ppermute | solution.py:337
  48.6 2.5 %piece_states.5 = (f32[3,2,136,128]{3,2,1,0:T(8,128)S(1)}, f32[3,2,136,128]{3,2,1,0:T(8,128)S(1)}) custom-call(s32[3]{0:T(128)S(1)} %pad_add_fusion.m_ref, bf16[200,2048]{1,0:T(8,128)(2,1)S(1)} %copy-done.1, bf16[8,2048]{1,0:T(8,128)(2,1)S(1)} %pad.8.refs_1_.refs_2_, bf16[2052,256]{1,0:T(8,128)(2,1)S(1)} %joined.1.refs_2_.refs_3_, ...), custom_call_target="tpu_custom_call" | custom-call | flops 3361996800 | bytes 2101248 | tf_op jit(solution)/shard_map/piece_states/pallas_call | solution.py:129
  51.1 2.8 %collective-permute-done.7.refs_1_ = bf16[208,2048]{1,0:T(8,128)(2,1)} collective-permute-done((bf16[208,2048]{1,0:T(8,128)(2,1)}, bf16[208,2048]{1,0:T(8,128)(2,1)}, u32[]{:S(2)}, u32[]{:S(2)}) %collective-permute-start.7) | collective-permute-done | bytes 852000 | tf_op jit(solution)/shard_map/ppermute | solution.py:337
  53.9 3.8 %collective-permute-start.8 = (bf16[208,2048]{1,0:T(8,128)(2,1)}, bf16[208,2048]{1,0:T(8,128)(2,1)S(1)}, u32[]{:S(2)}, u32[]{:S(2)}) collective-permute-start(bf16[208,2048]{1,0:T(8,128)(2,1)} %collective-permute-done.7.refs_1_), channel_id=1, source_target_pairs={{0,2},{1,15},{2,4},{3,1},{4,6},{5,3},{6,8},{7,5},{8,10},{9,7},{10,... | collective-permute-start | bytes 2555912 | tf_op jit(solution)/shard_map/ppermute | solution.py:337
  57.7 4.0 %piece_states.6 = (f32[3,2,136,128]{3,2,1,0:T(8,128)S(1)}, f32[3,2,136,128]{3,2,1,0:T(8,128)S(1)}) custom-call(s32[3]{0:T(128)S(1)} %pad_add_fusion.m_ref, bf16[192,2048]{1,0:T(8,128)(2,1)} %collective-permute-done.refs_0_, bf16[208,2048]{1,0:T(8,128)(2,1)} %collective-permute-done.6.refs_1_, bf16[8,2048]{1,0:T(8,128)(2,1)S(1)} %pad.8.refs_1_.refs_2_, ...), custom_call_target="tpu_custom_call" | custom-call | flops 6723993600 | bytes 2101248 | tf_op jit(solution)/shard_map/piece_states/pallas_call | solution.py:129
  61.7 0.5 collective-permute-done.2.refs_0_
  62.2 3.8 %collective-permute-start.3 = (bf16[192,2048]{1,0:T(8,128)(2,1)S(1)}, bf16[192,2048]{1,0:T(8,128)(2,1)S(1)}, u32[]{:S(2)}, u32[]{:S(2)}) collective-permute-start(bf16[192,2048]{1,0:T(8,128)(2,1)S(1)} %collective-permute-done.2.refs_0_), channel_id=1, source_target_pairs={{0,2},{1,15},{2,4},{3,1},{4,6},{5,3},{6,8},{7,5},{8,10},{9,7},{10,... | collective-permute-start | bytes 2359304 | tf_op jit(solution)/shard_map/ppermute | solution.py:337
  66.0 4.0 %piece_states.7 = (f32[3,2,136,128]{3,2,1,0:T(8,128)S(1)}, f32[3,2,136,128]{3,2,1,0:T(8,128)S(1)}) custom-call(s32[3]{0:T(128)S(1)} %pad_add_fusion.m_ref, bf16[192,2048]{1,0:T(8,128)(2,1)} %collective-permute-done.1.refs_0_, bf16[208,2048]{1,0:T(8,128)(2,1)} %collective-permute-done.7.refs_1_, bf16[8,2048]{1,0:T(8,128)(2,1)S(1)} %pad.8.refs_1_.refs_2_, ...), custom_call_target="tpu_custom_call" | custom-call | flops 6723993600 | bytes 2101248 | tf_op jit(solution)/shard_map/piece_states/pallas_call | solution.py:129
  70.1 1.3 %collective-permute-done.8.refs_1_ = bf16[208,2048]{1,0:T(8,128)(2,1)S(1)} collective-permute-done((bf16[208,2048]{1,0:T(8,128)(2,1)}, bf16[208,2048]{1,0:T(8,128)(2,1)S(1)}, u32[]{:S(2)}, u32[]{:S(2)}) %collective-permute-start.8) | collective-permute-done | bytes 852000 | tf_op jit(solution)/shard_map/ppermute | solution.py:337
  71.4 3.9 %collective-permute-start.9 = (bf16[8,2048]{1,0:T(8,128)(2,1)S(1)}, bf16[8,2048]{1,0:T(8,128)(2,1)S(1)}, u32[]{:S(2)}, u32[]{:S(2)}) collective-permute-start(bf16[8,2048]{1,0:T(8,128)(2,1)S(1)} %slice.26), channel_id=1, source_target_pairs={{0,2},{1,15},{2,4},{3,1},{4,6},{5,3},{6,8},{7,5},{8,10},{9,7},{10,... | collective-permute-start | bytes 98312 | tf_op jit(solution)/shard_map/ppermute | solution.py:337
  75.3 3.2 %piece_states.8 = (f32[3,2,136,128]{3,2,1,0:T(8,128)S(1)}, f32[3,2,136,128]{3,2,1,0:T(8,128)S(1)}) custom-call(s32[3]{0:T(128)S(1)} %pad_add_fusion.m_ref, bf16[192,2048]{1,0:T(8,128)(2,1)S(1)} %collective-permute-done.2.refs_0_, bf16[208,2048]{1,0:T(8,128)(2,1)S(1)} %collective-permute-done.8.refs_1_, bf16[8,2048]{1,0:T(8,128)(2,1)S(1)} %pad.8.refs_1_.refs_2_, ...), custom_call_target="tpu_custom_call" | custom-call | flops 6723993600 | bytes 2101248 | tf_op jit(solution)/shard_map/piece_states/pallas_call | solution.py:129
  78.5 1.3 %collective-permute-done.3.refs_0_ = bf16[192,2048]{1,0:T(8,128)(2,1)S(1)} collective-permute-done((bf16[192,2048]{1,0:T(8,128)(2,1)S(1)}, bf16[192,2048]{1,0:T(8,128)(2,1)S(1)}, u32[]{:S(2)}, u32[]{:S(2)}) %collective-permute-start.3) | collective-permute-done | bytes 786464 | tf_op jit(solution)/shard_map/ppermute | solution.py:337
  79.8 0.4 collective-permute-done.9.refs_1_
  80.1 2.5 %piece_states.9 = (f32[3,2,136,128]{3,2,1,0:T(8,128)S(1)}, f32[3,2,136,128]{3,2,1,0:T(8,128)S(1)}) custom-call(s32[3]{0:T(128)S(1)} %pad_add_fusion.m_ref, bf16[192,2048]{1,0:T(8,128)(2,1)S(1)} %collective-permute-done.3.refs_0_, bf16[8,2048]{1,0:T(8,128)(2,1)S(1)} %collective-permute-done.9.refs_1_, bf16[8,2048]{1,0:T(8,128)(2,1)S(1)} %pad.8.refs_1_.refs_2_, ...), custom_call_target="tpu_custom_call" | custom-call | flops 3361996800 | bytes 2101248 | tf_op jit(solution)/shard_map/piece_states/pallas_call | solution.py:129
  82.7 4.3 %collective-permute-start.12 = (f32[3,2,136,128]{3,2,1,0:T(8,128)S(1)}, f32[3,2,136,128]{3,2,1,0:T(8,128)S(1)}, u32[]{:S(2)}, u32[]{:S(2)}) collective-permute-start(f32[3,2,136,128]{3,2,1,0:T(8,128)S(1)} %get-tuple-element.31), channel_id=1, source_target_pairs={{0,1},{1,0},{2,3},{3,2},{4,5},{5,4},{6,7},{7,6},{8,9},{9,8},{10,11... | collective-permute-start | bytes 1253384 | tf_op jit(solution)/shard_map/ppermute | solution.py:330
  87.0 1.4 %collective-permute-done.12.b_ref = f32[3,2,136,128]{3,2,1,0:T(8,128)S(1)} collective-permute-done((f32[3,2,136,128]{3,2,1,0:T(8,128)S(1)}, f32[3,2,136,128]{3,2,1,0:T(8,128)S(1)}, u32[]{:S(2)}, u32[]{:S(2)}) %collective-permute-start.12) | collective-permute-done | bytes 417824 | tf_op jit(solution)/shard_map/ppermute | solution.py:330
  88.3 0.8 packed.1
  89.2 22.4 %all_to_all.5.got_ref = bf16[32,16,128]{2,1,0:T(8,128)(2,1)S(1)} all-to-all(bf16[32,16,128]{2,1,0:T(8,128)(2,1)S(1)} %packed.1), channel_id=1, replica_groups=mesh['sp'=32,'y'=8,'c'=2] {'sp'}, dimensions={0} | all-to-all | bytes 262144 | tf_op jit(solution)/shard_map/all_to_all | solution.py:377
  111.6 1.6 %finished.1 = (bf16[2,2,2,128]{3,2,1,0:T(2,128)(2,1)}, bf16[2,2,2]{2,1,0:T(2,128)(2,1)}) custom-call(s32[3]{0:T(128)S(1)} %pad_add_fusion.m_ref, bf16[32,16,128]{2,1,0:T(8,128)(2,1)S(1)} %all_to_all.5.got_ref, f32[8,128]{1,0:T(8,128)S(1)} %get-tuple-element.33.fix_ref), custom_call_target="tpu_custom_call" | custom-call | tf_op jit(solution)/shard_map/finished/pallas_call | solution.py:306
  (38 shorter events, 0.2 us)
Async XLA Ops:
  0.6 16.1 %copy-start.2 = (bf16[2048,128]{1,0:T(8,128)(2,1)S(1)}, bf16[2048,128]{1,0:T(8,128)(2,1)}, u32[]{:S(2)}) copy-start(bf16[2048,128]{1,0:T(8,128)(2,1)} %v_ref.2) | copy-start | bytes 1572868
  0.6 16.1 %copy-start.3 = (bf16[2048,128]{1,0:T(8,128)(2,1)S(1)}, bf16[2048,128]{1,0:T(8,128)(2,1)}, u32[]{:S(2)}) copy-start(bf16[2048,128]{1,0:T(8,128)(2,1)} %k_ref.2) | copy-start | bytes 1572868
  0.7 16.1 %copy-start.6 = (bf16[4,128]{1,0:T(4,128)(2,1)S(1)}, bf16[4,128]{1,0:T(4,128)(2,1)}, u32[]{:S(2)}) copy-start(bf16[4,128]{1,0:T(4,128)(2,1)} %cv_ref.1) | copy-start | bytes 3076
  0.7 16.1 %copy-start.7 = (bf16[4,128]{1,0:T(4,128)(2,1)S(1)}, bf16[4,128]{1,0:T(4,128)(2,1)}, u32[]{:S(2)}) copy-start(bf16[4,128]{1,0:T(4,128)(2,1)} %ck_ref.1) | copy-start | bytes 3076
  1.6 8.8 %collective-permute-start.4 = (bf16[8,2048]{1,0:T(8,128)(2,1)S(1)}, bf16[8,2048]{1,0:T(8,128)(2,1)S(1)}, u32[]{:S(2)}, u32[]{:S(2)}) collective-permute-start(bf16[8,2048]{1,0:T(8,128)(2,1)S(1)} %reshape.21), channel_id=1, source_target_pairs={{0,1},{1,2},{2,3},{3,4},{4,5},{5,6},{6,7},{7,8},{8,9},{9,10},{10,1... | collective-permute-start | bytes 98312 | tf_op jit(solution)/shard_map/ppermute | solution.py:343
  11.6 7.5 %copy-start = (bf16[200,2048]{1,0:T(8,128)(2,1)}, bf16[200,2048]{1,0:T(8,128)(2,1)S(1)}, u32[]{:S(2)}) copy-start(bf16[200,2048]{1,0:T(8,128)(2,1)S(1)} %pad_maximum_fusion.refs_0_) | copy-start | bytes 2457604
  11.7 7.5 %copy-start.4 = (f32[2]{0:T(128)S(1)}, f32[2]{0:T(128)}, u32[]{:S(2)}) copy-start(f32[2]{0:T(128)} %r_ref.1) | copy-start | bytes 28
  11.7 7.5 %copy-start.5 = (f32[2]{0:T(128)S(1)}, f32[2]{0:T(128)}, u32[]{:S(2)}) copy-start(f32[2]{0:T(128)} %b_ref.1) | copy-start | bytes 28
  11.7 7.5 %collective-permute-start.5 = (bf16[200,2048]{1,0:T(8,128)(2,1)S(1)}, bf16[200,2048]{1,0:T(8,128)(2,1)S(1)}, u32[]{:S(2)}, u32[]{:S(2)}) collective-permute-start(bf16[200,2048]{1,0:T(8,128)(2,1)S(1)} %pad_maximum_fusion.refs_0_), channel_id=1, source_target_pairs={{0,1},{1,0},{2,3},{3,2},{4,5},{5,4},{6,7},{7,6},{8,9},{9,8},{10,11... | collective-permute-start | bytes 2457608 | tf_op jit(solution)/shard_map/ppermute | solution.py:330
  13.9 13.3 %collective-permute-start = (bf16[192,2048]{1,0:T(8,128)(2,1)}, bf16[192,2048]{1,0:T(8,128)(2,1)}, u32[]{:S(2)}, u32[]{:S(2)}) collective-permute-start(bf16[192,2048]{1,0:T(8,128)(2,1)} %bitcast.17), channel_id=1, source_target_pairs={{0,2},{1,15},{2,4},{3,1},{4,6},{5,3},{6,8},{7,5},{8,10},{9,7},{10,... | collective-permute-start | bytes 2359304 | tf_op jit(solution)/shard_map/ppermute | solution.py:337
  17.0 6.6 %copy-start.14 = (f32[2,1536,2]{1,2,0:T(2,128)S(1)}, f32[2,1536,2]{1,2,0:T(2,128)}, u32[]{:S(2)}) copy-start(f32[2,1536,2]{1,2,0:T(2,128)} %param.23) | copy-start | bytes 73732
  17.0 24.0 %copy-start.8 = (f32[2,2]{1,0:T(2,128)S(1)}, f32[2,2]{1,0:T(2,128)}, u32[]{:S(2)}) copy-start(f32[2,2]{1,0:T(2,128)} %n_ref.1) | copy-start | bytes 52
  17.0 24.0 %copy-start.9 = (bf16[2,128]{1,0:T(2,128)(2,1)S(1)}, bf16[2,128]{1,0:T(2,128)(2,1)}, u32[]{:S(2)}) copy-start(bf16[2,128]{1,0:T(2,128)(2,1)} %v_ref.3) | copy-start | bytes 1540
  17.0 24.0 %copy-start.10 = (bf16[2,128]{1,0:T(2,128)(2,1)S(1)}, bf16[2,128]{1,0:T(2,128)(2,1)}, u32[]{:S(2)}) copy-start(bf16[2,128]{1,0:T(2,128)(2,1)} %k_ref.3) | copy-start | bytes 1540
  17.0 24.0 %copy-start.11 = (bf16[2,128]{1,0:T(2,128)(2,1)S(1)}, bf16[2,128]{1,0:T(2,128)(2,1)}, u32[]{:S(2)}) copy-start(bf16[2,128]{1,0:T(2,128)(2,1)} %q_ref.1) | copy-start | bytes 1540
  17.0 24.0 %copy-start.12 = (bf16[2,128]{1,0:T(2,128)(2,1)S(1)}, bf16[2,128]{1,0:T(2,128)(2,1)}, u32[]{:S(2)}) copy-start(bf16[2,128]{1,0:T(2,128)(2,1)} %g_ref.1) | copy-start | bytes 1540
  17.1 24.0 %copy-start.13 = (bf16[128]{0:T(256)(128)(2,1)S(1)}, bf16[128]{0:T(256)(128)(2,1)}, u32[]{:S(2)}) copy-start(bf16[128]{0:T(256)(128)(2,1)} %param.29) | copy-start | bytes 772
  17.1 25.1 %collective-permute-start.10 = (bf16[2052,256]{1,0:T(8,128)(2,1)S(1)}, bf16[2052,256]{1,0:T(8,128)(2,1)S(1)}, u32[]{:S(2)}, u32[]{:S(2)}) collective-permute-start(bf16[2052,256]{1,0:T(8,128)(2,1)S(1)} %joined.1.refs_2_.refs_3_), channel_id=1, source_target_pairs={{0,1},{1,0},{2,3},{3,2},{4,5},{5,4},{6,7},{7,6},{8,9},{9,8},{10,11... | collective-permute-start | bytes 3151880 | tf_op jit(solution)/shard_map/ppermute | solution.py:330
  19.2 17.1 %collective-permute-start.6 = (bf16[208,2048]{1,0:T(8,128)(2,1)S(1)}, bf16[208,2048]{1,0:T(8,128)(2,1)}, u32[]{:S(2)}, u32[]{:S(2)}) collective-permute-start(bf16[208,2048]{1,0:T(8,128)(2,1)S(1)} %stacked.2), channel_id=1, source_target_pairs={{0,2},{1,15},{2,4},{3,1},{4,6},{5,3},{6,8},{7,5},{8,10},{9,7},{10,... | collective-permute-start | bytes 2555912 | tf_op jit(solution)/shard_map/ppermute | solution.py:337
  23.6 18.1 %collective-permute-start.11 = (f32[2,2,1664]{2,1,0:T(2,128)S(1)}, f32[2,2,1664]{2,1,0:T(2,128)S(1)}, u32[]{:S(2)}, u32[]{:S(2)}) collective-permute-start(f32[2,2,1664]{2,1,0:T(2,128)S(1)} %pad_maximum_fusion.1), channel_id=1, source_target_pairs={{0,1},{1,0},{2,3},{3,2},{4,5},{5,4},{6,7},{7,6},{8,9},{9,8},{10,11... | collective-permute-start | bytes 79880 | tf_op jit(solution)/shard_map/ppermute | solution.py:330
  27.2 17.6 %collective-permute-start.1 = (bf16[192,2048]{1,0:T(8,128)(2,1)}, bf16[192,2048]{1,0:T(8,128)(2,1)}, u32[]{:S(2)}, u32[]{:S(2)}) collective-permute-start(bf16[192,2048]{1,0:T(8,128)(2,1)} %collective-permute-done.refs_0_), channel_id=1, source_target_pairs={{0,2},{1,15},{2,4},{3,1},{4,6},{5,3},{6,8},{7,5},{8,10},{9,7},{10,... | collective-permute-start | bytes 2359304 | tf_op jit(solution)/shard_map/ppermute | solution.py:337
  36.4 17.6 %collective-permute-start.7 = (bf16[208,2048]{1,0:T(8,128)(2,1)}, bf16[208,2048]{1,0:T(8,128)(2,1)}, u32[]{:S(2)}, u32[]{:S(2)}) collective-permute-start(bf16[208,2048]{1,0:T(8,128)(2,1)} %collective-permute-done.6.refs_1_), channel_id=1, source_target_pairs={{0,2},{1,15},{2,4},{3,1},{4,6},{5,3},{6,8},{7,5},{8,10},{9,7},{10,... | collective-permute-start | bytes 2555912 | tf_op jit(solution)/shard_map/ppermute | solution.py:337
  42.1 6.4 %copy-start.1 = (bf16[200,2048]{1,0:T(8,128)(2,1)S(1)}, bf16[200,2048]{1,0:T(8,128)(2,1)}, u32[]{:S(2)}) copy-start(bf16[200,2048]{1,0:T(8,128)(2,1)} %copy-done) | copy-start | bytes 2457604
  44.8 17.4 %collective-permute-start.2 = (bf16[192,2048]{1,0:T(8,128)(2,1)}, bf16[192,2048]{1,0:T(8,128)(2,1)S(1)}, u32[]{:S(2)}, u32[]{:S(2)}) collective-permute-start(bf16[192,2048]{1,0:T(8,128)(2,1)} %collective-permute-done.1.refs_0_), channel_id=1, source_target_pairs={{0,2},{1,15},{2,4},{3,1},{4,6},{5,3},{6,8},{7,5},{8,10},{9,7},{10,... | collective-permute-start | bytes 2359304 | tf_op jit(solution)/shard_map/ppermute | solution.py:337
  53.9 17.4 %collective-permute-start.8 = (bf16[208,2048]{1,0:T(8,128)(2,1)}, bf16[208,2048]{1,0:T(8,128)(2,1)S(1)}, u32[]{:S(2)}, u32[]{:S(2)}) collective-permute-start(bf16[208,2048]{1,0:T(8,128)(2,1)} %collective-permute-done.7.refs_1_), channel_id=1, source_target_pairs={{0,2},{1,15},{2,4},{3,1},{4,6},{5,3},{6,8},{7,5},{8,10},{9,7},{10,... | collective-permute-start | bytes 2555912 | tf_op jit(solution)/shard_map/ppermute | solution.py:337
  62.2 17.6 %collective-permute-start.3 = (bf16[192,2048]{1,0:T(8,128)(2,1)S(1)}, bf16[192,2048]{1,0:T(8,128)(2,1)S(1)}, u32[]{:S(2)}, u32[]{:S(2)}) collective-permute-start(bf16[192,2048]{1,0:T(8,128)(2,1)S(1)} %collective-permute-done.2.refs_0_), channel_id=1, source_target_pairs={{0,2},{1,15},{2,4},{3,1},{4,6},{5,3},{6,8},{7,5},{8,10},{9,7},{10,... | collective-permute-start | bytes 2359304 | tf_op jit(solution)/shard_map/ppermute | solution.py:337
  71.4 8.8 %collective-permute-start.9 = (bf16[8,2048]{1,0:T(8,128)(2,1)S(1)}, bf16[8,2048]{1,0:T(8,128)(2,1)S(1)}, u32[]{:S(2)}, u32[]{:S(2)}) collective-permute-start(bf16[8,2048]{1,0:T(8,128)(2,1)S(1)} %slice.26), channel_id=1, source_target_pairs={{0,2},{1,15},{2,4},{3,1},{4,6},{5,3},{6,8},{7,5},{8,10},{9,7},{10,... | collective-permute-start | bytes 98312 | tf_op jit(solution)/shard_map/ppermute | solution.py:337
  82.7 5.7 %collective-permute-start.12 = (f32[3,2,136,128]{3,2,1,0:T(8,128)S(1)}, f32[3,2,136,128]{3,2,1,0:T(8,128)S(1)}, u32[]{:S(2)}, u32[]{:S(2)}) collective-permute-start(f32[3,2,136,128]{3,2,1,0:T(8,128)S(1)} %get-tuple-element.31), channel_id=1, source_target_pairs={{0,1},{1,0},{2,3},{3,2},{4,5},{5,4},{6,7},{7,6},{8,9},{9,8},{10,11... | collective-permute-start | bytes 1253384 | tf_op jit(solution)/shard_map/ppermute | solution.py:330
